TPU v7x, 256 devices: a whole 4x4x8 slice. The times are simulated.
256 devices in a mesh: sp: 32 (over z, y), tp: 8 (over x, core).
Axes of the slice: x: 4, y: 4, z: 8, core: 2. Of those that a mesh axis runs over, the one named last changes fastest.
Arguments:
- latent: bfloat16 [8192, 2048], P(('sp', 'tp')), may hold values from -6 to 6
- log_decay: float32 [8192, 8], P('sp', 'tp'), may hold values from -2 to 0
- context: bfloat16 [512, 2048], P('sp'), may hold values from -6 to 6
- condition: bfloat16 [2, 2048], replicated, may hold values from -6 to 6
- w_modulate: bfloat16 [2048, 6144], P('sp', 'tp'), may hold values from -1 to 1
- norm_gain: bfloat16 [2048], replicated, may hold values from 0.099609375 to 1.8984375
- w_query: bfloat16 [2048, 2048], P(None, 'tp'), may hold values from -0.125 to 0.125
- w_key: bfloat16 [2048, 2048], P(None, 'tp'), may hold values from -0.125 to 0.125
- w_value: bfloat16 [2048, 4096], P(None, 'tp'), may hold values from -0.125 to 0.125
- w_gate: bfloat16 [2048, 4096], P(None, 'tp'), may hold values from -0.125 to 0.125
- group_gain: bfloat16 [4096], P('tp'), may hold values from 0.099609375 to 1.8984375
- w_output: bfloat16 [4096, 2048], P('tp'), may hold values from -0.125 to 0.125
Outputs:
- updated: bfloat16 [8192, 2048], P(('sp', 'tp'))
All inputs are finite; a program needn't handle non-finite values.
Results may differ from a plain program's by a relative error of at most 0.014.
Values may be sent and summed in bfloat16 or wider, within the bound.
No kernel may reach another device: no remote copies, remote signals or barrier semaphores. Data moves between devices by JAX's collectives and lax.ppermute only.
A program may use at most 128 MiB of HBM per device.

v0:
```python
import jax
import jax.numpy as jnp
from jax import lax
from jax.sharding import Mesh
from jax.sharding import PartitionSpec as P

DK = 256
DV = 512
BLOCK = 128
GRID_W = 64
CTX_LIFT = 4
SP = ("sp_0", "sp_1")
SP_TP = ("sp_0", "sp_1", "tp")


epsilon = 1e-06
rotary_base = 10000.0


def from_everyone(array, axis):
    size = lax.axis_size(axis)
    return lax.all_to_all(
        jnp.broadcast_to(array[None], (size, *array.shape)), axis, 0, 0, tiled=True
    )


def of_everyone(array, axis):
    everything = from_everyone(array, axis)
    return jnp.sum(everything, axis=0)


def in_order(tiles, dim):
    tiles = jnp.moveaxis(tiles, 0, dim)
    shape = tiles.shape
    return tiles.reshape(*shape[:dim], shape[dim] * shape[dim + 1], *shape[dim + 2 :])


def gather_directly(array, axis, dim):
    tiles = from_everyone(array, axis)
    return in_order(tiles, dim)


def rows_for(lines, size):
    spare = -len(lines) % size
    return jnp.pad(lines, [(0, spare)] + [(0, 0)] * (lines.ndim - 1))


def sum_in_order(tiles, axes, order):
    inside = tiles.shape[1:]
    tiles = tiles.reshape(*(lax.axis_size(a) for a in axes), *inside)
    tiles = jnp.moveaxis(tiles, order, range(len(axes))).reshape(-1, *inside)
    for k in order:
        tiles = lax.psum_scatter(tiles, axes[k], scatter_dimension=0, tiled=True)
    return tiles[0]


def stacked_from(array, axes, order):
    tiles = array
    for k in order:
        tiles = lax.all_gather(tiles, axes[k])
    done = order[::-1]
    back = [done.index(k) for k in range(len(axes))]
    tiles = tiles.transpose(*back, *range(len(axes), tiles.ndim))
    return tiles.reshape(-1, *array.shape)


def sum_in_two_steps(array, axes, order):
    size, lines = (lax.axis_size(axes), array.reshape(-1, *array.shape[1:][-1:]))
    tiles = rows_for(lines, size).reshape(size, -1, *lines.shape[1:])
    own = sum_in_order(tiles, axes, order)
    whole = stacked_from(own, axes, order[::-1]).reshape(-1, *lines.shape[1:])
    return whole[: len(lines)].reshape(array.shape)


def nothing_yet(array, identity):
    return jax.tree.map(
        lambda a, e: jnp.broadcast_to(jnp.asarray(e, a.dtype), a.shape), array, identity
    )


def entering_2(array, axes, combine, identity, reverse):
    before = start = nothing_yet(array, identity)
    subtotal = array
    for axis in reversed(axes):
        size, here = (lax.axis_size(axis), lax.axis_index(axis))
        pieces = jax.tree.map(lambda part: lax.all_gather(part, axis), subtotal)
        inside, subtotal = (start, start)
        for k in reversed(range(size)) if reverse else range(size):
            passed = k > here if reverse else k < here
            subtotal = combine(subtotal, jax.tree.map(lambda part: part[k], pieces))
            inside = jax.tree.map(lambda new, old: jnp.where(passed, new, old), subtotal, inside)
        before = combine(inside, before)
    return before


def cut_along(array, dim, size):
    shape = array.shape
    tiles = array.reshape(*shape[:dim], size, shape[dim] // size, *shape[dim + 1 :])
    return jnp.moveaxis(tiles, dim, 0)


def summed_on_arrival(array, axis, dim):
    size = lax.axis_size(axis)
    tiles = lax.all_to_all(cut_along(array, dim, size), axis, 0, 0, tiled=True)
    return jnp.sum(tiles.astype(jnp.float32), axis=0)


def modulate_rows(row_block, norm_gain, shift_vec, scale_vec):
    wide = row_block.astype(jnp.float32)
    normal = wide * lax.rsqrt(jnp.mean(wide * wide, axis=-1, keepdims=True) + epsilon)
    return (normal * norm_gain.astype(jnp.float32) * (1.0 + scale_vec) + shift_vec).astype(
        jnp.bfloat16
    )


def rotate(projected, positions):
    pairs = DK // 4
    inverse = rotary_base ** (-jnp.arange(pairs, dtype=jnp.float32) / pairs)
    grid_row = (positions // GRID_W).astype(jnp.float32)
    grid_column = (positions % GRID_W).astype(jnp.float32)
    angles = jnp.concatenate([grid_row[:, None] * inverse, grid_column[:, None] * inverse], axis=-1)
    cosine = jnp.cos(angles)[:, None, :]
    sine_part = jnp.sin(angles)[:, None, :]
    paired = projected.reshape(projected.shape[0], -1, DK // 2, 2)
    even_part = paired[..., 0]
    odd_part = paired[..., 1]
    turned = jnp.stack(
        [even_part * cosine - odd_part * sine_part, even_part * sine_part + odd_part * cosine],
        axis=-1,
    )
    return turned.reshape(projected.shape)


def context_terms(normal_rows, w_key, w_value):
    head_count = w_key.shape[1] // DK
    key_part = (
        jnp.dot(normal_rows, w_key, preferred_element_type=jnp.float32) * DK ** (-0.5)
    ).astype(jnp.bfloat16)
    value_part = jnp.dot(normal_rows, w_value, preferred_element_type=jnp.float32).astype(
        jnp.bfloat16
    )
    return jnp.einsum(
        "jhd,jhv->hdv",
        key_part.reshape(-1, head_count, DK),
        value_part.reshape(-1, head_count, DV),
        preferred_element_type=jnp.float32,
    )


def block_pass(queries, key_rows, value_rows, decays):
    block_count = queries.shape[0] // BLOCK
    head_count = queries.shape[1]
    query_blocks = queries.reshape(block_count, BLOCK, head_count, DK)
    key_blocks = key_rows.reshape(block_count, BLOCK, head_count, DK)
    value_blocks = value_rows.reshape(block_count, BLOCK, head_count, DV)
    cumulative = jnp.cumsum(decays.reshape(block_count, BLOCK, head_count), axis=1)
    by_head = jnp.swapaxes(cumulative, 1, 2)
    within = jnp.arange(BLOCK, dtype=jnp.int32)
    lower_mask = within[:, None] >= within[None, :]
    log_gaps = by_head[:, :, :, None] - by_head[:, :, None, :]
    weights = jnp.where(lower_mask, jnp.exp(jnp.where(lower_mask, log_gaps, 0.0)), 0.0)
    scores = jnp.einsum(
        "nihd,njhd->nhij", query_blocks, key_blocks, preferred_element_type=jnp.float32
    )
    weighted = (scores * weights).astype(jnp.bfloat16)
    inside = jnp.einsum(
        "nhij,njhv->nihv", weighted, value_blocks, preferred_element_type=jnp.float32
    )
    totals = cumulative[:, -1, :]
    decayed = (
        key_blocks.astype(jnp.float32) * jnp.exp(totals[:, None, :] - cumulative)[..., None]
    ).astype(jnp.bfloat16)
    updates = jnp.einsum(
        "njhd,njhv->nhdv", decayed, value_blocks, preferred_element_type=jnp.float32
    )
    return (query_blocks, cumulative, inside, totals, updates)


def fold_blocks(totals, updates):

    def fold_advance(carried, element):
        log_total, states = carried
        block_total, block_update = element
        return (
            (log_total + block_total, jnp.exp(block_total)[:, None, None] * states + block_update),
            None,
        )

    initial = (jnp.zeros(totals.shape[1:], jnp.float32), jnp.zeros(updates.shape[1:], jnp.float32))
    result, unused = lax.scan(fold_advance, initial, (totals, updates))
    return result


def link_states(earlier, later):
    return (earlier[0] + later[0], jnp.exp(later[0])[:, None, None] * earlier[1] + later[1])


def finish_pass(query_blocks, cumulative, inside, totals, updates, entry):

    def finish_advance(states, element):
        block_total, block_update = element
        return (jnp.exp(block_total)[:, None, None] * states + block_update, states)

    unused, entering = lax.scan(finish_advance, entry, (totals, updates))
    carried_in = jnp.exp(cumulative)[..., None] * jnp.einsum(
        "nihd,nhdv->nihv",
        query_blocks,
        entering.astype(jnp.bfloat16),
        preferred_element_type=jnp.float32,
    )
    combined = inside + carried_in
    return combined.reshape(-1, combined.shape[2], combined.shape[3])


def enter_state(prefix, context_state):
    return jnp.exp(prefix[0])[:, None, None] * context_state + prefix[1]


def per_device(
    latent,
    log_decay,
    context,
    condition,
    w_modulate,
    norm_gain,
    w_query,
    w_key,
    w_value,
    w_gate,
    group_gain,
    w_output,
):
    head_devices = lax.axis_size("tp")
    seq_index = lax.axis_index(SP)
    model_width = latent.shape[1]
    head_count = w_query.shape[1] // DK
    activated = jax.nn.silu(condition.astype(jnp.float32)).astype(jnp.bfloat16)
    input_rows = w_modulate.shape[0]
    own_inputs = lax.dynamic_slice_in_dim(activated, seq_index * input_rows, input_rows, 1)
    partial_mod = jnp.dot(own_inputs, w_modulate, preferred_element_type=jnp.float32)
    summed = of_everyone(partial_mod, SP)
    modulation = gather_directly(summed, "tp", 1)
    latent_shift = modulation[0, :model_width]
    latent_scale = modulation[0, model_width : 2 * model_width]
    latent_gate = modulation[0, 2 * model_width :]
    context_shift = modulation[1, :model_width]
    context_scale = modulation[1, model_width : 2 * model_width]
    normed = modulate_rows(latent, norm_gain, latent_shift, latent_scale)
    row_base = seq_index * (latent.shape[0] * head_devices)
    key_width = w_query.shape[1]
    value_width = w_value.shape[1]
    shard_rows = gather_directly(normed, "tp", 0)
    positions = row_base + jnp.arange(shard_rows.shape[0], dtype=jnp.int32)
    query_part = rotate(jnp.dot(shard_rows, w_query, preferred_element_type=jnp.float32), positions)
    key_part = rotate(
        jnp.dot(shard_rows, w_key, preferred_element_type=jnp.float32), positions
    ) * DK ** (-0.5)
    value_part = jnp.dot(shard_rows, w_value, preferred_element_type=jnp.float32)
    gate_part = jnp.dot(shard_rows, w_gate, preferred_element_type=jnp.float32)
    projected = jnp.concatenate([query_part, key_part, value_part, gate_part], axis=1).astype(
        jnp.bfloat16
    )
    row_total = projected.shape[0]
    query_rows = projected[:, :key_width].reshape(row_total, head_count, DK)
    key_rows = projected[:, key_width : 2 * key_width].reshape(row_total, head_count, DK)
    value_rows = projected[:, 2 * key_width : 2 * key_width + value_width].reshape(
        row_total, head_count, DV
    )
    gate_rows = projected[:, 2 * key_width + value_width :]
    empty_state = jnp.zeros((head_count, DK, DV), jnp.float32)
    own_terms = context_terms(
        modulate_rows(context, norm_gain, context_shift, context_scale), w_key, w_value
    )
    context_sum = sum_in_two_steps(own_terms, SP, (0, 1))
    context_state = context_sum * float(CTX_LIFT)
    forward_parts = block_pass(query_rows, key_rows, value_rows, log_decay)
    backward_parts = block_pass(
        jnp.flip(query_rows, 0),
        jnp.flip(key_rows, 0),
        jnp.flip(value_rows, 0),
        jnp.flip(log_decay, 0),
    )
    identity = (jnp.zeros((head_count,), jnp.float32), empty_state)
    earlier_blocks = entering_2(
        fold_blocks(forward_parts[3], forward_parts[4]), SP, link_states, identity, False
    )
    later_blocks = entering_2(
        fold_blocks(backward_parts[3], backward_parts[4]), SP, link_states, identity, True
    )
    forward = finish_pass(*forward_parts, enter_state(earlier_blocks, context_state))
    backward = jnp.flip(finish_pass(*backward_parts, enter_state(later_blocks, context_state)), 0)
    mixed_heads = forward + backward
    average = jnp.mean(mixed_heads, axis=-1, keepdims=True)
    variance = jnp.mean(jnp.square(mixed_heads - average), axis=-1, keepdims=True)
    normal_heads = ((mixed_heads - average) * lax.rsqrt(variance + epsilon)).reshape(
        row_total, head_count * DV
    )
    attended = (
        jax.nn.silu(gate_rows.astype(jnp.float32)) * normal_heads * group_gain.astype(jnp.float32)
    ).astype(jnp.bfloat16)
    projected_sum = summed_on_arrival(
        jnp.dot(attended, w_output, preferred_element_type=jnp.float32).astype(jnp.bfloat16),
        "tp",
        0,
    )
    return (latent.astype(jnp.float32) + latent_gate * projected_sum).astype(jnp.bfloat16)


def solution(mesh):
    torus = Mesh(mesh.devices.reshape(8, 4, mesh.shape["tp"]), ("sp_0", "sp_1", "tp"))
    in_specs = (
        P(SP_TP, None),
        P(SP, "tp"),
        P(SP, None),
        P(),
        P(SP, "tp"),
        P(),
        P(None, "tp"),
        P(None, "tp"),
        P(None, "tp"),
        P(None, "tp"),
        P("tp"),
        P("tp", None),
    )
    out_specs = P(SP_TP, None)
    return jax.shard_map(
        per_device, mesh=torus, in_specs=in_specs, out_specs=out_specs, check_vma=False
    )
```

profile of v0, /device:TPU:1, one launch (start us, length us, event | category | flops | bytes accessed | tf_op | source)
XLA Modules:
  0.0 336.2 jit_solution(12697696626924543084)
XLA Ops:
  10.1 12.0 %all-to-all-start = ((f32[32,2,768]{2,1,0:T(2,128)}), f32[32,2,768]{2,1,0:T(2,128)S(1)}, u32[]{:S(2)}, u32[]{:S(2)}) async-start(f32[32,2,768]{2,1,0:T(2,128)} %broadcast_in_dim.30), calls=%async_computation | async-start | bytes 393216 | tf_op jit(solution)/shard_map/all_to_all | solution.py:22
  26.0 6.1 %all-to-all-done = f32[32,2,768]{2,1,0:T(2,128)S(1)} async-done(((f32[32,2,768]{2,1,0:T(2,128)}), f32[32,2,768]{2,1,0:T(2,128)S(1)}, u32[]{:S(2)}, u32[]{:S(2)}) %all-to-all-start) | async-done | bytes 196640 | tf_op jit(solution)/shard_map/all_to_all | solution.py:22
  32.8 6.9 %all-to-all-start.1 = ((f32[8,2,768]{2,1,0:T(2,128)}), f32[8,2,768]{2,1,0:T(2,128)S(1)}, u32[]{:S(2)}, u32[]{:S(2)}) async-start(f32[8,2,768]{2,1,0:T(2,128)} %broadcast_in_dim.31), calls=%async_computation.1 | async-start | bytes 98304 | tf_op jit(solution)/shard_map/all_to_all | solution.py:22
  40.4 4.1 %all-to-all-done.1 = f32[8,2,768]{2,1,0:T(2,128)S(1)} async-done(((f32[8,2,768]{2,1,0:T(2,128)}), f32[8,2,768]{2,1,0:T(2,128)S(1)}, u32[]{:S(2)}, u32[]{:S(2)}) %all-to-all-start.1) | async-done | bytes 49184 | tf_op jit(solution)/shard_map/all_to_all | solution.py:22
  46.7 4.9 %all-to-all-start.2 = ((bf16[8,32,2048]{2,1,0:T(8,128)(2,1)}), bf16[8,32,2048]{2,1,0:T(8,128)(2,1)}, u32[]{:S(2)}, u32[]{:S(2)}) async-start(bf16[8,32,2048]{2,1,0:T(8,128)(2,1)} %broadcast_in_dim.32), calls=%async_computation.2 | async-start | bytes 2097152 | tf_op jit(solution)/shard_map/all_to_all | solution.py:22
  51.6 1.4 copy.92
  53.0 2.5 reshape.1227
  55.5 2.3 copy.89
  57.8 2.5 reshape.1225
  60.9 3.1 fusion.12
  64.1 2.6 all-to-all-done.2
  66.7 2.1 convolution_bitcast_fusion.6
  68.8 2.0 convolution_bitcast_fusion.7
  72.4 2.6 convolution_convert_fusion.1
  76.0 6.3 %while.52 = (s32[]{:T(128)}, f32[1]{0:T(128)}, f32[1,256,512]{2,1,0:T(8,128)}, f32[2,1]{0,1:T(1,128)S(1)}, f32[2,1,256,512]{3,2,1,0:T(8,128)S(1)}, /*index=5*/s32[]{:T(128)}, s32[]{:T(128)}) while((s32[]{:T(128)}, f32[1]{0:T(128)}, f32[1,256,512]{2,1,0:T(8,128)}, f32[2,1]{0,1:T(1,128)S(1)}, f32[2,1,256,512]{3,2,1,0:T(8,128)S(1)}, ...), condition=%wide.region_7.8_spmd.clone, body=%wide.region_6.7_spmd.clone.sunk | while | flops 393220 | bytes 1572991 | solution.py:190
  79.8 1.9 bitcast_add_fusion.12
  84.7 3.2 reverse.9
  87.9 1.5 reverse.11
  90.4 2.1 convolution_bitcast_fusion
  92.5 9.1 %while.53 = (s32[]{:T(128)}, f32[1]{0:T(128)}, f32[1,256,512]{2,1,0:T(8,128)}, f32[2,1]{0,1:T(1,128)}, f32[2,1,256,512]{3,2,1,0:T(8,128)}, /*index=5*/s32[]{:T(128)}, s32[]{:T(128)}) while((s32[]{:T(128)}, f32[1]{0:T(128)}, f32[1,256,512]{2,1,0:T(8,128)}, f32[2,1]{0,1:T(1,128)}, f32[2,1,256,512]{3,2,1,0:T(8,128)}, ...), condition=%wide.region_12.13_spmd.clone, body=%wide.region_11.12_spmd.clone.sunk | while | flops 393220 | bytes 1572991 | solution.py:190
  94.4 1.9 bitcast_add_fusion.13
  98.8 2.1 bitcast_add_fusion.13
  101.7 1.3 dynamic-slice
  104.4 7.1 %all-reduce.5 = (f32[4]{0:T(128)S(1)}, f32[4]{0:T(128)S(1)}) all-reduce(f32[4]{0:T(128)S(1)} %dynamic-update-slice.2, f32[4]{0:T(128)S(1)} %dynamic-update-slice), channel_id=6, replica_groups=mesh['sp_0'=8,'sp_1'=4,'tp'=8] {'sp_1'}, use_global_device_ids=true, to_apply=%add.2 | all-reduce | flops 8 | bytes 64
  115.0 2.5 fusion.24
  118.3 1.3 slice_add_fusion.26
  122.2 21.9 %all-gather.18.cloned.1.call-done = f32[4,256,512]{2,1,0:T(8,128)} async-done(((f32[1,256,512]{2,1,0:T(8,128)}), f32[4,256,512]{2,1,0:T(8,128)}) %all-gather.18.cloned.1.call-update) | async-done | bytes 2097168 | tf_op jit(solution)/shard_map/all_gather | solution.py:86
  144.2 2.5 fusion.18
  147.5 1.3 slice_add_fusion.29
  148.7 1.4 dynamic-update-slice.1
  150.1 1.4 dynamic-update-slice.3
  152.1 14.1 %all-reduce.4 = (f32[8]{0:T(128)S(1)}, f32[8]{0:T(128)S(1)}) all-reduce(f32[8]{0:T(128)S(1)} %dynamic-update-slice.3, f32[8]{0:T(128)S(1)} %dynamic-update-slice.1), channel_id=7, replica_groups=mesh['sp_0'=8,'sp_1'=4,'tp'=8] {'sp_0'}, use_global_device_ids=true, to_apply=%add.3 | all-reduce | flops 16 | bytes 128
  198.0 10.4 %all_gather.53 = f32[4,8,512]{2,1,0:T(8,128)S(1)} all-gather(f32[1,8,512]{2,1,0:T(8,128)} %reduce-scatter.5.cloned.1.call-done), channel_id=1, replica_groups=mesh['sp_0'=8,'sp_1'=4,'tp'=8] {'sp_1'}, dimensions={0}, use_global_device_ids=true | all-gather | bytes 81920 | tf_op jit(solution)/shard_map/all_gather | solution.py:60
  208.4 23.4 %all-gather = f32[32,8,512]{2,1,0:T(8,128)S(1)} all-gather(f32[4,8,512]{2,1,0:T(8,128)S(1)} %all_gather.53), channel_id=2, replica_groups=mesh['sp_0'=8,'sp_1'=4,'tp'=8] {'sp_0'}, dimensions={0}, use_global_device_ids=true | all-gather | bytes 589824 | tf_op jit(solution)/shard_map/all_gather | solution.py:60
  231.8 3.7 %fusion.23 = f32[1,256,512]{2,1,0:T(8,128)S(1)} fusion(f32[8,1,256,512]{3,2,1,0:T(8,128)} %all-gather.12.cloned.1.call-done, f32[32,8,512]{2,1,0:T(8,128)S(1)} %all-gather, f32[4,256,512]{2,1,0:T(8,128)} %all-gather.16.cloned.1.call-done, f32[]{:T(128)} %bitcast.48, f32[]{:T(128)} %bitcast.57, f32[]{:T(128)} %bitcast.49, f32[]{:T(128)} %bitcast.59, ...), kind=kLoop, calls=%fused_computation.64 | loop fusion | flops 4980736 | bytes 7340100 | tf_op jit(solution)/shard_map/add | solution.py:216
  236.3 6.7 %while.50 = (s32[]{:T(128)}, f32[1,256,512]{2,1,0:T(8,128)S(1)}, bf16[2,1,256,512]{3,2,1,0:T(8,128)(2,1)}, f32[2,1]{0,1:T(1,128)S(1)}, f32[2,1,256,512]{3,2,1,0:T(8,128)}, /*index=5*/s32[]{:T(128)}) while((s32[]{:T(128)}, f32[1,256,512]{2,1,0:T(8,128)S(1)}, bf16[2,1,256,512]{3,2,1,0:T(8,128)(2,1)}, f32[2,1]{0,1:T(1,128)S(1)}, ...), condition=%wide.region_9.10_spmd, body=%wide.region_8.9_spmd.sunk | while | flops 262146 | bytes 2622041 | solution.py:204
  237.7 1.9 bitcast_add_fusion.10
  241.0 2.0 bitcast_add_fusion.10
  243.0 41.9 %all-gather.14.cloned.1.call-done = f32[8,1,256,512]{3,2,1,0:T(8,128)} async-done(((f32[1,1,256,512]{3,2,1,0:T(8,128)}), f32[8,1,256,512]{3,2,1,0:T(8,128)}) %all-gather.14.cloned.1.call-update) | async-done | bytes 4194320 | tf_op jit(solution)/shard_map/all_gather | solution.py:86
  285.0 3.7 %fusion.17 = f32[1,256,512]{2,1,0:T(8,128)S(1)} fusion(f32[8,1,256,512]{3,2,1,0:T(8,128)} %all-gather.14.cloned.1.call-done, f32[32,8,512]{2,1,0:T(8,128)S(1)} %all-gather, f32[4,256,512]{2,1,0:T(8,128)} %all-gather.18.cloned.1.call-done, f32[]{:T(128)} %bitcast.90, f32[]{:T(128)} %bitcast.99, f32[]{:T(128)} %bitcast.91, f32[]{:T(128)} %bitcast.101, ...), kind=kLoop, calls=%fused_computation.46 | loop fusion | flops 4980736 | bytes 7340100 | tf_op jit(solution)/shard_map/add | solution.py:216
  289.4 6.5 %while.51 = (s32[]{:T(128)}, f32[1,256,512]{2,1,0:T(8,128)S(1)}, bf16[2,1,256,512]{3,2,1,0:T(8,128)(2,1)}, f32[2,1]{0,1:T(1,128)S(1)}, f32[2,1,256,512]{3,2,1,0:T(8,128)}, /*index=5*/s32[]{:T(128)}) while((s32[]{:T(128)}, f32[1,256,512]{2,1,0:T(8,128)S(1)}, bf16[2,1,256,512]{3,2,1,0:T(8,128)(2,1)}, f32[2,1]{0,1:T(1,128)S(1)}, ...), condition=%wide.region_14.15_spmd, body=%wide.region_13.14_spmd.sunk | while | flops 262146 | bytes 2622041 | solution.py:204
  290.8 1.9 bitcast_add_fusion.11
  294.1 1.9 bitcast_add_fusion.11
  296.0 2.1 fusion.3
  298.1 3.4 %rev.14 = f32[256,1,512]{2,0,1:T(8,128)S(1)} reverse(f32[256,1,512]{2,0,1:T(8,128)} %bitcast.255), dimensions={0} | reverse | bytes 1048576 | tf_op jit(solution)/shard_map/jit(_flip)/rev | solution.py:291
  301.6 1.3 fusion.1
  303.3 4.3 %convolution_convert_fusion = bf16[256,2048]{1,0:T(8,128)(2,1)} fusion(bf16[512,2048]{1,0:T(8,128)(2,1)S(1)} %copy-done, bf16[256,2048]{1,0:T(8,128)(2,1)} %bitcast.12, bf16[2048,512]{1,0:T(8,128)(2,1)} %param.29, f32[256,1,512]{2,0,1:T(8,128)S(1)} %get-tuple-element.302, f32[512]{0:T(512)S(1)} %copy-done.22, f32[256]{0:T(256)S(1)} %add_rsqrt_fusion, ...), kind=kOutput, calls=%fused_computation.12 | convolution fusion | flops 1075707904 | bytes 6819840 | tf_op jit(solution)/shard_map/dot_general | solution.py:302
  307.6 20.2 %all_to_all.20 = bf16[8,32,2048]{2,1,0:T(8,128)(2,1)S(1)} all-to-all(bf16[8,32,2048]{2,1,0:T(8,128)(2,1)} %bitcast.261), channel_id=1, replica_groups=mesh['sp_0'=8,'sp_1'=4,'tp'=8] {'tp'}, dimensions={0} | all-to-all | bytes 2097152 | tf_op jit(solution)/shard_map/all_to_all | solution.py:104
  (156 shorter events, 38.3 us)
Async XLA Ops:
  7.4 295.9 %copy-start = (bf16[512,2048]{1,0:T(8,128)(2,1)S(1)}, bf16[512,2048]{1,0:T(8,128)(2,1)}, u32[]{:S(2)}) copy-start(bf16[512,2048]{1,0:T(8,128)(2,1)} %param.31) | copy-start | bytes 6291460
  10.1 22.0 %all-to-all-start = ((f32[32,2,768]{2,1,0:T(2,128)}), f32[32,2,768]{2,1,0:T(2,128)S(1)}, u32[]{:S(2)}, u32[]{:S(2)}) async-start(f32[32,2,768]{2,1,0:T(2,128)} %broadcast_in_dim.30), calls=%async_computation | async-start | bytes 393216 | tf_op jit(solution)/shard_map/all_to_all | solution.py:22
  24.3 27.3 %copy-start.2 = (bf16[2048,256]{1,0:T(8,128)(2,1)S(1)}, bf16[2048,256]{1,0:T(8,128)(2,1)}, u32[]{:S(2)}) copy-start(bf16[2048,256]{1,0:T(8,128)(2,1)} %param.27) | copy-start | bytes 3145732
  32.8 11.7 %all-to-all-start.1 = ((f32[8,2,768]{2,1,0:T(2,128)}), f32[8,2,768]{2,1,0:T(2,128)S(1)}, u32[]{:S(2)}, u32[]{:S(2)}) async-start(f32[8,2,768]{2,1,0:T(2,128)} %broadcast_in_dim.31), calls=%async_computation.1 | async-start | bytes 98304 | tf_op jit(solution)/shard_map/all_to_all | solution.py:22
  46.7 20.0 %all-to-all-start.2 = ((bf16[8,32,2048]{2,1,0:T(8,128)(2,1)}), bf16[8,32,2048]{2,1,0:T(8,128)(2,1)}, u32[]{:S(2)}, u32[]{:S(2)}) async-start(bf16[8,32,2048]{2,1,0:T(8,128)(2,1)} %broadcast_in_dim.32), calls=%async_computation.2 | async-start | bytes 2097152 | tf_op jit(solution)/shard_map/all_to_all | solution.py:22
  51.5 63.4 %reduce-scatter.3.cloned.1.call-start = ((), (), s32[]{:S(2)}) async-start(), calls=%async_computation.6 | async-start | bytes 589824 | tf_op jit(solution)/shard_map/reduce_scatter | solution.py:53
  55.5 4.9 %copy-start.16 = (bf16[16,2048]{1,0:T(8,128)(2,1)S(1)}, bf16[16,2048]{1,0:T(8,128)(2,1)}, u32[]{:S(2)}) copy-start(bf16[16,2048]{1,0:T(8,128)(2,1)} %param.22) | copy-start | bytes 196612
  60.8 5.9 %copy-start.14 = (bf16[128,2,2048]{2,1,0:T(2,128)(2,1)S(1)}, bf16[128,2,2048]{2,1,0:T(2,128)(2,1)}, u32[]{:S(2)}) copy-start(bf16[128,2,2048]{2,1,0:T(2,128)(2,1)} %reshape.1227) | copy-start | bytes 3145732
  64.0 51.0 %all-gather.16.cloned.1.call-start = ((), (), s32[]{:S(2)}) async-start(), calls=%async_computation.10 | async-start | bytes 2621440 | tf_op jit(solution)/shard_map/all_gather | solution.py:86
  66.6 2.1 copy-start.15
  72.3 2.8 copy-start.12
  75.0 0.7 copy-start.3
  76.0 6.4 %copy-start.21 = (f32[256,1]{0,1:T(1,128)S(1)}, f32[256,1]{0,1:T(1,128)}, u32[]{:S(2)}) copy-start(f32[256,1]{0,1:T(1,128)} %param.21) | copy-start | bytes 3076
  82.3 0.6 copy-start.24
  82.3 10.2 %copy-start.1 = (f32[2,1,256,512]{3,2,1,0:T(8,128)}, f32[2,1,256,512]{3,2,1,0:T(8,128)S(1)}, u32[]{:S(2)}) copy-start(f32[2,1,256,512]{3,2,1,0:T(8,128)S(1)} %get-tuple-element.560) | copy-start | bytes 3145732
  82.4 61.8 %all-gather.18.cloned.1.call-start = ((), (), s32[]{:S(2)}) async-start(), calls=%async_computation.11 | async-start | bytes 2621440 | tf_op jit(solution)/shard_map/all_gather | solution.py:86
  83.5 0.5 copy-start.26
  101.6 96.4 %reduce-scatter.5.cloned.1.call-start = ((), (), s32[]{:S(2)}) async-start(), calls=%async_computation.7 | async-start | bytes 81920 | tf_op jit(solution)/shard_map/reduce_scatter | solution.py:53
  115.0 116.8 %all-gather.12.cloned.1.call-start = ((), (), s32[]{:S(2)}) async-start(), calls=%async_computation.8 | async-start | bytes 4718592 | tf_op jit(solution)/shard_map/all_gather | solution.py:86
  117.6 29.2 %copy-start.28 = (u32[256]{0:T(256)S(1)}, u32[256]{0:T(256)}, u32[]{:S(2)}) copy-start(u32[256]{0:T(256)} %constant.148) | copy-start | bytes 3076
  117.6 33.9 %copy-start.23 = (bf16[512]{0:T(512)(128)(2,1)S(1)}, bf16[512]{0:T(512)(128)(2,1)}, u32[]{:S(2)}) copy-start(bf16[512]{0:T(512)(128)(2,1)} %param.30) | copy-start | bytes 3076
  117.6 55.1 %copy-start.17 = (bf16[256,1,128,1]{0,2,3,1:T(8,128)(2,1)S(1)}, bf16[256,1,128,1]{0,2,3,1:T(8,128)(2,1)}, u32[]{:S(2)}) copy-start(bf16[256,1,128,1]{0,2,3,1:T(8,128)(2,1)} %get-tuple-element.307) | copy-start | bytes 196612
  117.6 55.1 %copy-start.18 = (bf16[256,1,128,1]{0,2,3,1:T(8,128)(2,1)S(1)}, bf16[256,1,128,1]{0,2,3,1:T(8,128)(2,1)}, u32[]{:S(2)}) copy-start(bf16[256,1,128,1]{0,2,3,1:T(8,128)(2,1)} %get-tuple-element.308) | copy-start | bytes 196612
  117.6 167.3 %all-gather.14.cloned.1.call-start = ((), (), s32[]{:S(2)}) async-start(), calls=%async_computation.9 | async-start | bytes 4718592 | tf_op jit(solution)/shard_map/all_gather | solution.py:86
  146.7 50.1 %copy-start.4 = (bf16[256,512]{1,0:T(8,128)(2,1)S(1)}, bf16[256,512]{1,0:T(8,128)(2,1)}, u32[]{:S(2)}) copy-start(bf16[256,512]{1,0:T(8,128)(2,1)} %copy-done.3) | copy-start | bytes 786436
  146.7 50.1 %copy-start.13 = (bf16[2,128,256]{1,0,2:T(2,128)(2,1)S(1)}, bf16[2,128,256]{1,0,2:T(2,128)(2,1)}, u32[]{:S(2)}) copy-start(bf16[2,128,256]{1,0,2:T(2,128)(2,1)} %copy-done.12) | copy-start | bytes 393220
  184.2 47.6 %copy-start.8 = (bf16[2,128,256]{2,1,0:T(8,128)(2,1)}, bf16[2,128,256]{2,1,0:T(8,128)(2,1)S(1)}, u32[]{:S(2)}) copy-start(bf16[2,128,256]{2,1,0:T(8,128)(2,1)S(1)} %copy.95) | copy-start | bytes 393220
  195.7 36.1 %copy-start.10 = (bf16[256,256]{1,0:T(8,128)(2,1)}, bf16[256,256]{1,0:T(8,128)(2,1)S(1)}, u32[]{:S(2)}) copy-start(bf16[256,256]{1,0:T(8,128)(2,1)S(1)} %copy.113) | copy-start | bytes 393220
  231.8 4.5 %copy-start.25 = (f32[2,1]{0,1:T(1,128)S(1)}, f32[2,1]{0,1:T(1,128)}, u32[]{:S(2)}) copy-start(f32[2,1]{0,1:T(1,128)} %copy-done.24) | copy-start | bytes 28
  285.0 4.5 %copy-start.27 = (f32[2,1]{0,1:T(1,128)S(1)}, f32[2,1]{0,1:T(1,128)}, u32[]{:S(2)}) copy-start(f32[2,1]{0,1:T(1,128)} %get-tuple-element.585) | copy-start | bytes 28
  289.4 6.5 %copy-start.6 = (f32[2,1,512,128]{2,3,0,1:T(8,128)S(1)}, f32[2,1,512,128]{2,3,0,1:T(8,128)}, u32[]{:S(2)}) copy-start(f32[2,1,512,128]{2,3,0,1:T(8,128)} %convolution_bitcast_fusion.3) | copy-start | bytes 1572868
  289.4 6.5 %copy-start.11 = (bf16[256,256]{1,0:T(8,128)(2,1)S(1)}, bf16[256,256]{1,0:T(8,128)(2,1)}, u32[]{:S(2)}) copy-start(bf16[256,256]{1,0:T(8,128)(2,1)} %copy-done.10) | copy-start | bytes 393220
  289.4 6.5 %copy-start.20 = (f32[2,128]{1,0:T(2,128)S(1)}, f32[2,128]{1,0:T(2,128)}, u32[]{:S(2)}) copy-start(f32[2,128]{1,0:T(2,128)} %get-tuple-element.316) | copy-start | bytes 3076
  295.9 5.6 %copy-start.5 = (f32[2,1,512,128]{2,3,0,1:T(8,128)S(1)}, f32[2,1,512,128]{2,3,0,1:T(8,128)}, u32[]{:S(2)}) copy-start(f32[2,1,512,128]{2,3,0,1:T(8,128)} %convolution_bitcast_fusion.5) | copy-start | bytes 1572868
  295.9 5.6 %copy-start.9 = (bf16[2,128,256]{2,1,0:T(8,128)(2,1)S(1)}, bf16[2,128,256]{2,1,0:T(8,128)(2,1)}, u32[]{:S(2)}) copy-start(bf16[2,128,256]{2,1,0:T(8,128)(2,1)} %copy-done.8) | copy-start | bytes 393220
  295.9 5.6 %copy-start.19 = (f32[2,128]{1,0:T(2,128)S(1)}, f32[2,128]{1,0:T(2,128)}, u32[]{:S(2)}) copy-start(f32[2,128]{1,0:T(2,128)} %get-tuple-element.314) | copy-start | bytes 3076
  301.6 1.7 copy-start.22
  307.6 20.4 %copy-start.7 = (bf16[32,2048]{1,0:T(8,128)(2,1)S(1)}, bf16[32,2048]{1,0:T(8,128)(2,1)}, u32[]{:S(2)}) copy-start(bf16[32,2048]{1,0:T(8,128)(2,1)} %param.20) | copy-start | bytes 393220
Sparse Core Ops, SparseCore 0:
  64.1 28.0 reduce-scatter.2
Sparse Core Ops, SparseCore 1:
  82.5 26.6 all-gather.15
  110.8 33.3 all-gather.17
  146.5 21.1 reduce-scatter.4
  169.5 59.3 all-gather.11
  230.7 54.2 all-gather.13
where the time goes:
time: 339 us; the launch traced here: 336 us
  waiting for transfers between devices  76.8 us (23%)
  blocking collectives  75.1 us (22%)
  between operations  48.1 us (14%)
  local copies, waits for them, and re-layouts  42.8 us (13%)
  other arithmetic  40.6 us (12%)
  starting transfers between devices  24 us (7%)
  matrix products  23.6 us (7%)
  loops' own time  5.1 us (2%)
    all_gather x4, waiting for transfers between devices, entering_2(): pieces = jax.tree.map(lambda part: lax.all_gather(part, axis), subtotal)  63.9 us
    all_gather x2, blocking collectives, stacked_from(): tiles = lax.all_gather(tiles, axes[k])  33.8 us
    all_to_all x3, starting transfers between devices, from_everyone(): lax.all_to_all(jnp.broadcast_to(array[None], (size, *array.shape)), axis,...  23.8 us
    unnamed x2, blocking collectives  21.1 us
    all_to_all x1, blocking collectives, summed_on_arrival(): tiles = lax.all_to_all(cut_along(array, dim, size), axis, 0, 0, tiled=True)  20.2 us
    another operation x13, local copies, waits for them, and re-layouts  13.4 us
    all_to_all x3, waiting for transfers between devices, from_everyone(): lax.all_to_all(jnp.broadcast_to(array[None], (size, *array.shape)), axis,...  12.8 us
    unnamed x68, local copies, waits for them, and re-layouts  7.76 us
  transfers between devices with their start and end apart: 9, of which 5 were waited for; matrix products, arithmetic and copies ran while one was open for 23% of the time, Pallas kernels for 0%

commit v1 on v0

v1 whole, which is shorter than its diff:
```python
import jax
import jax.numpy as jnp
from jax import lax
from jax.experimental import pallas as pl
from jax.experimental.pallas import tpu as pltpu
from jax.sharding import Mesh
from jax.sharding import PartitionSpec as P

DK = 256
DV = 512
GRID_W = 64
CTX_LIFT = 4
SP = ("z", "y")
TP = ("x", "c")
ALL = ("z", "y", "x", "c")
f32 = jnp.float32
bf16 = jnp.bfloat16

epsilon = 1e-06
rotary_base = 10000.0
MIB = 1024 * 1024


def from_everyone(array, axis):
    size = lax.axis_size(axis)
    return lax.all_to_all(
        jnp.broadcast_to(array[None], (size, *array.shape)), axis, 0, 0, tiled=True
    )


def kernel_call(body, outs, vmem, flops, *args):
    moved = sum(a.size * a.dtype.itemsize for a in args)
    return pl.pallas_call(
        body,
        out_shape=outs,
        compiler_params=pltpu.CompilerParams(vmem_limit_bytes=vmem * MIB),
        cost_estimate=pl.CostEstimate(flops=flops, bytes_accessed=moved, transcendentals=0),
    )(*args)


def dot(a, b):
    return jnp.dot(a, b, preferred_element_type=f32)


def dot_t(a, b):
    return lax.dot_general(a, b, (((1,), (1,)), ((), ())), preferred_element_type=f32)


def turn(u, tab_ref):
    lanes = lax.broadcasted_iota(jnp.int32, u.shape, 1)
    swapped = jnp.where(lanes % 2 == 0, pltpu.roll(u, DK - 1, 1), pltpu.roll(u, 1, 1))
    return u * tab_ref[:, :DK] + swapped * tab_ref[:, DK:]


def keys_kernel(
    own_ref, other_ref, ctx_ref, mod_ref, gain_ref, wk_ref, wv_ref, tab_ref, col_ref,
    send_ref, normed_ref, k_ref, v_ref,
):
    width = own_ref.shape[1]
    gain = gain_ref[...].astype(f32)
    tp = mod_ref.shape[0]

    def modulated(rows, which):
        line = jnp.concatenate([mod_ref[t, which : which + 1, :] for t in range(tp)], axis=1)
        shift, scale = line[:, :width], line[:, width : 2 * width]
        wide = rows.astype(f32)
        normal = wide * lax.rsqrt(jnp.mean(wide * wide, axis=-1, keepdims=True) + epsilon)
        return (normal * gain * (1.0 + scale) + shift).astype(bf16)

    half = own_ref.shape[0]
    rows = 2 * half
    normed_ref[0:half, :] = modulated(own_ref[...], 0)
    normed_ref[half:rows, :] = modulated(other_ref[...], 0)
    normed_ref[rows:, :] = modulated(ctx_ref[...], 1)
    keys = dot(normed_ref[...], wk_ref[...])
    values = dot(normed_ref[...], wv_ref[...]).astype(bf16)
    key_rows = (turn(keys[:rows], tab_ref) * DK ** (-0.5)).astype(bf16)
    ctx_keys = (keys[rows:] * DK ** (-0.5)).astype(bf16)
    k_ref[...] = key_rows
    v_ref[...] = values[:rows]
    wide = key_rows.astype(f32)
    ahead = (wide * jnp.exp(col_ref[:, 0:1])).astype(bf16)
    behind = (wide * jnp.exp(col_ref[:, 1:2])).astype(bf16)
    turned = values.T
    send_ref[:, 0:DK] = dot(turned[:, :rows], ahead).astype(bf16)
    send_ref[:, DK : 2 * DK] = dot(turned[:, :rows], behind).astype(bf16)
    send_ref[:, 2 * DK :] = dot(turned[:, rows:], ctx_keys).astype(bf16)


def inside_kernel(
    normed_ref, k_ref, v_ref, wq_ref, wg_ref, tab_ref, col_ref, line_ref, q_ref, g_ref, y_ref
):
    rows = k_ref.shape[0]
    queries = turn(dot(normed_ref[0:rows, :], wq_ref[...]), tab_ref).astype(bf16)
    q_ref[...] = queries
    g_ref[...] = dot(normed_ref[0:rows, :], wg_ref[...]).astype(bf16)
    scores = dot_t(queries, k_ref[...])
    here, there = col_ref[:, 4:5], line_ref[2:3, :]
    gaps = jnp.where(
        here >= there,
        col_ref[:, 2:3] - line_ref[0:1, :],
        line_ref[1:2, :] - col_ref[:, 1:2],
    )
    weights = jnp.exp(gaps) * jnp.where(here == there, 2.0, 1.0)
    y_ref[...] = dot((scores * weights).astype(bf16), v_ref[...])


def scan_kernel(parts_ref, decay_ref, out_ref):
    count = parts_ref.shape[0]
    lift = jnp.zeros((parts_ref.shape[1], DK), f32)
    for r in range(count):
        lift = lift + parts_ref[r, :, 2 * DK :].astype(f32)
    ahead = behind = lift * float(CTX_LIFT)
    for r in range(count):
        s = count - 1 - r
        out_ref[r, :, 0:DK] = ahead.astype(bf16)
        out_ref[s, :, DK:] = behind.astype(bf16)
        ahead = decay_ref[r : r + 1, :] * ahead + parts_ref[r, :, 0:DK].astype(f32)
        behind = decay_ref[s : s + 1, :] * behind + parts_ref[s, :, DK : 2 * DK].astype(f32)


def output_kernel(y_ref, q_ref, g_ref, states_ref, col_ref, gain_ref, wo_ref, out_ref):
    queries = q_ref[...]
    mixed = (
        y_ref[...]
        + jnp.exp(col_ref[:, 2:3]) * dot_t(queries, states_ref[:, 0:DK])
        + jnp.exp(col_ref[:, 3:4]) * dot_t(queries, states_ref[:, DK:])
    )
    average = jnp.mean(mixed, axis=-1, keepdims=True)
    centred = mixed - average
    variance = jnp.mean(centred * centred, axis=-1, keepdims=True)
    gates = g_ref[...].astype(f32)
    attended = (
        gates * jax.nn.sigmoid(gates) * (centred * lax.rsqrt(variance + epsilon))
        * gain_ref[...].astype(f32)
    ).astype(bf16)
    out_ref[...] = dot(attended, wo_ref[...]).astype(bf16)


def shaped(*shape, dtype=bf16):
    return jax.ShapeDtypeStruct(shape, dtype)


def per_device(
    latent,
    log_decay,
    context,
    condition,
    w_modulate,
    norm_gain,
    w_query,
    w_key,
    w_value,
    w_gate,
    group_gain,
    w_output,
):
    seq_index = lax.axis_index(SP)
    core = lax.axis_index("c")
    lines, width = latent.shape
    x_size = lax.axis_size("x")
    half = lines * x_size
    rows = 2 * half
    swap = [(0, 1), (1, 0)]

    own_rows = from_everyone(latent, "x").reshape(half, width)
    other_rows = lax.ppermute(own_rows, "c", swap)

    activated = jax.nn.silu(condition.astype(f32)).astype(bf16)
    input_rows = w_modulate.shape[0]
    own_inputs = lax.dynamic_slice_in_dim(activated, seq_index * input_rows, input_rows, 1)
    partial_mod = jnp.dot(own_inputs, w_modulate, preferred_element_type=f32)
    total = jnp.sum(log_decay)
    packed = jnp.concatenate(
        [partial_mod, jnp.broadcast_to(total[None, None], (1, partial_mod.shape[1]))], axis=0
    )
    pieces = from_everyone(packed, SP)
    modulation = from_everyone(jnp.sum(pieces[:, :2], axis=0), TP)
    decays = jnp.exp(pieces[:, 2, :DK])

    local = jnp.arange(rows, dtype=jnp.int32)
    grid_row = (local // lines) % x_size
    grid_column = ((local // half + core) % 2) * lines + local % lines
    here = grid_row * GRID_W + grid_column
    slots = jnp.arange(rows, dtype=jnp.int32)
    flat = log_decay[:, 0]
    upto = jnp.sum(jnp.where(slots[None, :] <= here[:, None], flat[None, :], 0.0), axis=1)
    before = jnp.sum(jnp.where(slots[None, :] < here[:, None], flat[None, :], 0.0), axis=1)
    place = here.astype(f32)
    col = jnp.stack([total - upto, before, upto, total - before, place], axis=1)
    line = jnp.stack([upto, before, place], axis=0)

    pairs = DK // 4
    inverse = rotary_base ** (-jnp.arange(pairs, dtype=f32) / pairs)
    inverse = jnp.repeat(inverse, 2)
    first_row = seq_index * (rows // GRID_W)
    angles = jnp.concatenate(
        [
            (first_row + grid_row).astype(f32)[:, None] * inverse,
            grid_column.astype(f32)[:, None] * inverse,
        ],
        axis=1,
    )
    sign = jnp.where(jnp.arange(DK) % 2 == 0, -1.0, 1.0)
    table = jnp.concatenate([jnp.cos(angles), jnp.sin(angles) * sign], axis=1)

    ctx = context.shape[0]
    send, normed, key_rows, value_rows = kernel_call(
        keys_kernel,
        (shaped(DV, 3 * DK), shaped(rows + ctx, width), shaped(rows, DK), shaped(rows, DV)),
        32,
        2 * (rows + ctx) * width * (DK + DV),
        own_rows,
        other_rows,
        context,
        modulation,
        norm_gain[None],
        w_key,
        w_value,
        table,
        col,
    )
    count = lax.axis_size(SP)
    parts = lax.all_to_all(send.reshape(count, DV // count, 3 * DK), SP, 0, 0, tiled=True)
    queries, gates, inside = kernel_call(
        inside_kernel,
        (shaped(rows, DK), shaped(rows, DV), shaped(rows, DV, dtype=f32)),
        32,
        2 * rows * width * (DK + DV),
        normed,
        key_rows,
        value_rows,
        w_query,
        w_gate,
        table,
        col,
        line,
    )
    entering = kernel_call(
        scan_kernel, shaped(count, DV // count, 2 * DK), 16, 10 * parts.size, parts, decays
    )
    states = lax.all_to_all(entering, SP, 0, 0, tiled=True).reshape(DV, 2 * DK)
    partial = kernel_call(
        output_kernel,
        shaped(rows, width),
        32,
        2 * rows * DV * width,
        inside,
        queries,
        gates,
        states,
        col,
        group_gain[None],
        w_output,
    )
    crossed = lax.ppermute(partial[half:], "c", swap)
    paired = (partial[:half].astype(f32) + crossed.astype(f32)).astype(bf16)
    tiles = lax.all_to_all(paired.reshape(x_size, lines, width), "x", 0, 0, tiled=True)
    projected = jnp.sum(tiles.astype(f32), axis=0)
    gate = modulation[:, 0].reshape(-1)[2 * width :]
    return (latent.astype(f32) + gate * projected).astype(bf16)


def solution(mesh):
    torus = Mesh(mesh.devices.reshape(8, 4, 4, 2), ALL)
    in_specs = (
        P(ALL, None),
        P(SP, TP),
        P(SP, None),
        P(),
        P(SP, TP),
        P(),
        P(None, TP),
        P(None, TP),
        P(None, TP),
        P(None, TP),
        P(TP),
        P(TP, None),
    )
    return jax.shard_map(
        per_device, mesh=torus, in_specs=in_specs, out_specs=P(ALL, None), check_vma=False
    )
```

time: 339 us -> 136 us (0.40)
  blocking collectives: 75.1 us -> 0 us
  between operations: 48.1 us -> 0.3 us
  other arithmetic: 40.6 us -> 7.96 us
  waiting for transfers between devices: 76.8 us -> 52.5 us
  matrix products: 23.6 us -> 0.2 us
  starting transfers between devices: 24 us -> 44.5 us
  local copies, waits for them, and re-layouts: 42.8 us -> 22.9 us
  Pallas kernels: 0 us -> 6.38 us
  loops' own time: 5.1 us -> 0 us
    all_gather x4 -> x0, waiting for transfers between devices: 63.9 us -> none  [entering_2(): pieces = jax.tree.map(lambda part: lax.all_gather(part, axis), subtotal)]
    all_to_all x0 -> x3, waiting for transfers between devices: none -> 36.4 us  [the longest x1 20.1 us: per_device(): lax.all_to_all(send.reshape(count, DV // count, 3 * DK), SP, 0, 0, tiled=...]
    all_gather x2 -> x0, blocking collectives: 33.8 us -> none  [stacked_from(): tiles = lax.all_gather(tiles, axes[k])]
    add x15 -> x1, other arithmetic: 30.1 us -> 0.01 us  [per_device(): here = grid_row * GRID_W + grid_column]
    dot_general x13 -> x1, matrix products: 23.6 us -> 0.2 us  [per_device(): partial_mod = jnp.dot(own_inputs, w_modulate, preferred_element_type=f32)]
    unnamed x2 -> x0, blocking collectives: 21.1 us -> none
    all_to_all x1 -> x0, blocking collectives: 20.2 us -> none  [summed_on_arrival(): tiles = lax.all_to_all(cut_along(array, dim, size), axis, 0, 0, tiled=True)]
    all_to_all x0 -> x3, starting transfers between devices: none -> 13.4 us  [the longest x1 5.81 us: per_device(): states = lax.all_to_all(entering, SP, 0, 0, tiled=True).reshape(DV, 2 * DK)]
  transfers between devices with their start and end apart: 9 -> 8, of which waited for: 5 -> 7; matrix products, arithmetic and copies ran while one was open for 23% -> 8% of each run, Pallas kernels for 0% -> 1%
where the time goes in v1:
time: 136 us; the launch traced here: 135 us
  waiting for transfers between devices  52.5 us (39%)
  starting transfers between devices  44.5 us (33%)
  local copies, waits for them, and re-layouts  22.9 us (17%)
  other arithmetic  7.96 us (6%)
  Pallas kernels  6.38 us (5%)
    all_to_all x3, starting transfers between devices, from_everyone(): lax.all_to_all(jnp.broadcast_to(array[None], (size, *array.shape)), axis,...  24.7 us
    all_to_all x1, waiting for transfers between devices, per_device(): lax.all_to_all(send.reshape(count, DV // count, 3 * DK), SP, 0, 0, tiled=...  20.1 us
    unnamed x56, local copies, waits for them, and re-layouts  16.4 us
    all_to_all x3, waiting for transfers between devices, from_everyone(): lax.all_to_all(jnp.broadcast_to(array[None], (size, *array.shape)), axis,...  14.5 us
    all_to_all x1, waiting for transfers between devices, per_device(): lax.all_to_all(paired.reshape(x_size, lines, width), 'x', 0, 0, tiled=True)  9.13 us
    all_to_all x1, waiting for transfers between devices, per_device(): states = lax.all_to_all(entering, SP, 0, 0, tiled=True).reshape(DV, 2 * DK)  7.2 us
    pallas_call x4, Pallas kernels, kernel_call(): pl.pallas_call(body, out_shape=outs, compiler_params=pltpu.CompilerParams...  6.38 us
    all_to_all x1, starting transfers between devices, per_device(): states = lax.all_to_all(entering, SP, 0, 0, tiled=True).reshape(DV, 2 * DK)  5.81 us
  transfers between devices with their start and end apart: 8, of which 7 were waited for; matrix products, arithmetic and copies ran while one was open for 8% of the time, Pallas kernels for 1%

profile of v1, /device:TPU:1, one launch (start us, length us, event | category | flops | bytes accessed | tf_op | source)
XLA Modules:
  0.0 134.7 jit_solution(6907437131154370518)
XLA Ops:
  0.0 1.8 %broadcast_in_dim.69 = bf16[4,32,2048]{2,1,0:T(8,128)(2,1)} broadcast(bf16[32,2048]{1,0:T(8,128)(2,1)} %param.12), dimensions={1,2} | broadcast | bytes 655360 | tf_op jit(solution)/shard_map/broadcast_in_dim | solution.py:27
  1.8 4.8 %all-to-all-start.2 = ((bf16[4,32,2048]{2,1,0:T(8,128)(2,1)}), bf16[4,32,2048]{2,1,0:T(8,128)(2,1)S(1)}, u32[]{:S(2)}, u32[]{:S(2)}) async-start(bf16[4,32,2048]{2,1,0:T(8,128)(2,1)} %broadcast_in_dim.69), calls=%async_computation.2 | async-start | bytes 1048576 | tf_op jit(solution)/shard_map/all_to_all | solution.py:26
  6.6 0.9 convert_element_type.58
  8.7 0.6 concatenate.9
  9.4 1.6 %fusion = (f32[256,256]{1,0:T(8,128)S(1)}, f32[256,256]{1,0:T(8,128)}) fusion(f32[256,128]{1,0:T(8,128)S(1)} %get-tuple-element.24, f32[256,128]{1,0:T(8,128)S(1)} %get-tuple-element.23, f32[256]{0:T(256)S(1)} %compare_select_fusion.12), kind=kLoop, calls=%fused_computation.10 | loop fusion | flops 131072 | bytes 787456 | tf_op jit(solution)/shard_map/cos | solution.py:205
  11.0 3.1 %all-to-all-done.2 = bf16[4,32,2048]{2,1,0:T(8,128)(2,1)S(1)} async-done(((bf16[4,32,2048]{2,1,0:T(8,128)(2,1)}), bf16[4,32,2048]{2,1,0:T(8,128)(2,1)S(1)}, u32[]{:S(2)}, u32[]{:S(2)}) %all-to-all-start.2) | async-done | bytes 524320 | tf_op jit(solution)/shard_map/all_to_all | solution.py:26
  14.1 0.8 broadcast_in_dim.67
  14.9 12.2 %all-to-all-start = ((f32[32,3,768]{2,1,0:T(4,128)}), f32[32,3,768]{2,1,0:T(4,128)}, u32[]{:S(2)}, u32[]{:S(2)}) async-start(f32[32,3,768]{2,1,0:T(4,128)} %broadcast_in_dim.67), calls=%async_computation | async-start | bytes 786432 | tf_op jit(solution)/shard_map/all_to_all | solution.py:26
  27.1 1.0 pad_maximum_fusion.tab_ref
  28.1 2.5 %collective-permute-start = (bf16[128,2048]{1,0:T(8,128)(2,1)S(1)}, bf16[128,2048]{1,0:T(8,128)(2,1)}, u32[]{:S(2)}, u32[]{:S(2)}) collective-permute-start(bf16[128,2048]{1,0:T(8,128)(2,1)S(1)} %bitcast.13), channel_id=1, source_target_pairs={{0,1},{1,0},{2,3},{3,2},{4,5},{5,4},{6,7},{7,6},{8,9},{9,8},{10,11... | collective-permute-start | bytes 1572872 | tf_op jit(solution)/shard_map/ppermute | solution.py:167
  30.8 0.7 broadcast_subtract_fusion
  31.5 7.4 %all-to-all-done = f32[32,3,768]{2,1,0:T(4,128)} async-done(((f32[32,3,768]{2,1,0:T(4,128)}), f32[32,3,768]{2,1,0:T(4,128)}, u32[]{:S(2)}, u32[]{:S(2)}) %all-to-all-start) | async-done | bytes 294944 | tf_op jit(solution)/shard_map/all_to_all | solution.py:26
  38.9 1.1 slice_reduce_fusion
  40.0 0.6 broadcast_in_dim.68
  40.6 7.7 %all-to-all-start.1 = ((f32[8,2,768]{2,1,0:T(2,128)}), f32[8,2,768]{2,1,0:T(2,128)S(1)}, u32[]{:S(2)}, u32[]{:S(2)}) async-start(f32[8,2,768]{2,1,0:T(2,128)} %broadcast_in_dim.68), calls=%async_computation.1 | async-start | bytes 98304 | tf_op jit(solution)/shard_map/all_to_all | solution.py:26
  49.1 4.0 %all-to-all-done.1.mod_ref = f32[8,2,768]{2,1,0:T(2,128)S(1)} async-done(((f32[8,2,768]{2,1,0:T(2,128)}), f32[8,2,768]{2,1,0:T(2,128)S(1)}, u32[]{:S(2)}, u32[]{:S(2)}) %all-to-all-start.1) | async-done | bytes 49184 | tf_op jit(solution)/shard_map/all_to_all | solution.py:26
  53.1 1.2 copy-done.6
  54.3 0.8 copy-done.17
  55.2 0.7 copy-done.18
  55.9 3.1 %shard_map.118 = (bf16[512,768]{1,0:T(8,128)(2,1)S(1)}, bf16[272,2048]{1,0:T(8,128)(2,1)S(1)}, bf16[256,256]{1,0:T(8,128)(2,1)S(1)}, bf16[256,512]{1,0:T(8,128)(2,1)S(1)}) custom-call(bf16[128,2048]{1,0:T(8,128)(2,1)S(1)} %bitcast.14, bf16[128,2048]{1,0:T(8,128)(2,1)} %collective-permute-done.other_ref, bf16[16,2048]{1,0:T(8,128)(2,1)S(1)} %copy-done.17, ...), custom_call_target="tpu_custom_call" | custom-call | flops 855638016 | bytes 4842496 | tf_op jit(solution)/shard_map/pallas_call | solution.py:33
  59.0 1.0 copy-done.4
  59.9 0.9 copy-done.8
  60.8 0.7 copy-done.11
  61.5 4.1 %all-to-all-start.3 = ((bf16[32,16,768]{2,1,0:T(8,128)(2,1)}), bf16[32,16,768]{2,1,0:T(8,128)(2,1)S(1)}, u32[]{:S(2)}, u32[]{:S(2)}) async-start(bf16[32,16,768]{2,1,0:T(8,128)(2,1)} %bitcast.16), calls=%async_computation.3 | async-start | bytes 1572864 | tf_op jit(solution)/shard_map/all_to_all | solution.py:224
  65.7 0.9 slice.27
  66.6 20.1 %all-to-all-done.3.parts_ref = bf16[32,16,768]{2,1,0:T(8,128)(2,1)S(1)} async-done(((bf16[32,16,768]{2,1,0:T(8,128)(2,1)}), bf16[32,16,768]{2,1,0:T(8,128)(2,1)S(1)}, u32[]{:S(2)}, u32[]{:S(2)}) %all-to-all-start.3) | async-done | bytes 786464 | tf_op jit(solution)/shard_map/all_to_all | solution.py:224
  86.7 1.0 shard_map.120
  87.7 5.8 %all-to-all-start.4 = ((bf16[32,16,512]{2,1,0:T(8,128)(2,1)}), bf16[32,16,512]{2,1,0:T(8,128)(2,1)S(1)}, u32[]{:S(2)}, u32[]{:S(2)}) async-start(bf16[32,16,512]{2,1,0:T(8,128)(2,1)} %shard_map.120), calls=%async_computation.4 | async-start | bytes 1048576 | tf_op jit(solution)/shard_map/all_to_all | solution.py:242
  94.2 1.6 %copy-done.2 = bf16[2048,512]{1,0:T(8,128)(2,1)S(1)} copy-done((bf16[2048,512]{1,0:T(8,128)(2,1)S(1)}, bf16[2048,512]{1,0:T(8,128)(2,1)}, u32[]{:S(2)}) %copy-start.2) | copy-done | bytes 2097176
  95.8 1.2 copy-done.7
  97.0 0.9 copy-done.12
  97.9 1.1 shard_map.119
  99.1 0.8 copy-done.9
  99.9 0.7 copy-done.13
  100.6 0.7 copy-done.15
  101.2 7.2 %all-to-all-done.4 = bf16[32,16,512]{2,1,0:T(8,128)(2,1)S(1)} async-done(((bf16[32,16,512]{2,1,0:T(8,128)(2,1)}), bf16[32,16,512]{2,1,0:T(8,128)(2,1)S(1)}, u32[]{:S(2)}, u32[]{:S(2)}) %all-to-all-start.4) | async-done | bytes 524320 | tf_op jit(solution)/shard_map/all_to_all | solution.py:242
  108.4 1.6 %copy-done.3 = bf16[512,2048]{1,0:T(8,128)(2,1)S(1)} copy-done((bf16[512,2048]{1,0:T(8,128)(2,1)S(1)}, bf16[512,2048]{1,0:T(8,128)(2,1)}, u32[]{:S(2)}) %copy-start.3) | copy-done | bytes 2097176
  110.0 1.0 copy-done.10
  111.1 0.9 copy-done.14
  112.0 0.9 copy-done.16
  112.9 0.7 copy-done.19
  113.6 1.2 shard_map.121
  114.9 4.0 %collective-permute-start.1 = (bf16[128,2048]{1,0:T(8,128)(2,1)S(1)}, bf16[128,2048]{1,0:T(8,128)(2,1)S(1)}, u32[]{:S(2)}, u32[]{:S(2)}) collective-permute-start(bf16[128,2048]{1,0:T(8,128)(2,1)S(1)} %slice.29), channel_id=1, source_target_pairs={{0,1},{1,0},{2,3},{3,2},{4,5},{5,4},{6,7},{7,6},{8,9},{9,8},{10,11... | collective-permute-start | bytes 1572872 | tf_op jit(solution)/shard_map/ppermute | solution.py:256
  118.8 1.5 %collective-permute-done.1 = bf16[128,2048]{1,0:T(8,128)(2,1)S(1)} collective-permute-done((bf16[128,2048]{1,0:T(8,128)(2,1)S(1)}, bf16[128,2048]{1,0:T(8,128)(2,1)S(1)}, u32[]{:S(2)}, u32[]{:S(2)}) %collective-permute-start.1) | collective-permute-done | bytes 524320 | tf_op jit(solution)/shard_map/ppermute | solution.py:256
  120.4 0.9 add_convert_fusion
  121.3 3.5 %all-to-all-start.5 = ((bf16[4,32,2048]{2,1,0:T(8,128)(2,1)}), bf16[4,32,2048]{2,1,0:T(8,128)(2,1)S(1)}, u32[]{:S(2)}, u32[]{:S(2)}) async-start(bf16[4,32,2048]{2,1,0:T(8,128)(2,1)} %bitcast.10), calls=%async_computation.5 | async-start | bytes 1048576 | tf_op jit(solution)/shard_map/all_to_all | solution.py:258
  124.8 9.1 %all-to-all-done.5 = bf16[4,32,2048]{2,1,0:T(8,128)(2,1)S(1)} async-done(((bf16[4,32,2048]{2,1,0:T(8,128)(2,1)}), bf16[4,32,2048]{2,1,0:T(8,128)(2,1)S(1)}, u32[]{:S(2)}, u32[]{:S(2)}) %all-to-all-start.5) | async-done | bytes 524320 | tf_op jit(solution)/shard_map/all_to_all | solution.py:258
  134.0 0.7 add_convert_fusion.1
  (62 shorter events, 3.1 us)
Async XLA Ops:
  0.0 7.9 %copy-start = (bf16[64,768]{1,0:T(8,128)(2,1)S(1)}, bf16[64,768]{1,0:T(8,128)(2,1)}, u32[]{:S(2)}) copy-start(bf16[64,768]{1,0:T(8,128)(2,1)} %param.16) | copy-start | bytes 294916
  0.0 8.1 %copy-start.26 = (f32[256,1]{0,1:T(1,128)S(1)}, f32[256,1]{0,1:T(1,128)}, u32[]{:S(2)}) copy-start(f32[256,1]{0,1:T(1,128)} %param.13) | copy-start | bytes 3076
  1.8 12.3 %all-to-all-start.2 = ((bf16[4,32,2048]{2,1,0:T(8,128)(2,1)}), bf16[4,32,2048]{2,1,0:T(8,128)(2,1)S(1)}, u32[]{:S(2)}, u32[]{:S(2)}) async-start(bf16[4,32,2048]{2,1,0:T(8,128)(2,1)} %broadcast_in_dim.69), calls=%async_computation.2 | async-start | bytes 1048576 | tf_op jit(solution)/shard_map/all_to_all | solution.py:26
  6.6 41.7 %copy-start.25 = (bf16[2048]{0:T(1024)(128)(2,1)S(1)}, bf16[2048]{0:T(1024)(128)(2,1)}, u32[]{:S(2)}) copy-start(bf16[2048]{0:T(1024)(128)(2,1)} %param.17) | copy-start | bytes 12292
  6.6 46.5 %copy-start.1 = (bf16[2048,512]{1,0:T(8,128)(2,1)S(1)}, bf16[2048,512]{1,0:T(8,128)(2,1)}, u32[]{:S(2)}) copy-start(bf16[2048,512]{1,0:T(8,128)(2,1)} %wv_ref.1) | copy-start | bytes 6291460
  14.9 24.0 %all-to-all-start = ((f32[32,3,768]{2,1,0:T(4,128)}), f32[32,3,768]{2,1,0:T(4,128)}, u32[]{:S(2)}, u32[]{:S(2)}) async-start(f32[32,3,768]{2,1,0:T(4,128)} %broadcast_in_dim.67), calls=%async_computation | async-start | bytes 786432 | tf_op jit(solution)/shard_map/all_to_all | solution.py:26
  28.1 25.0 %collective-permute-start = (bf16[128,2048]{1,0:T(8,128)(2,1)S(1)}, bf16[128,2048]{1,0:T(8,128)(2,1)}, u32[]{:S(2)}, u32[]{:S(2)}) collective-permute-start(bf16[128,2048]{1,0:T(8,128)(2,1)S(1)} %bitcast.13), channel_id=1, source_target_pairs={{0,1},{1,0},{2,3},{3,2},{4,5},{5,4},{6,7},{7,6},{8,9},{9,8},{10,11... | collective-permute-start | bytes 1572872 | tf_op jit(solution)/shard_map/ppermute | solution.py:167
  30.8 18.1 %copy-start.21 = (f32[256]{0:T(256)}, f32[256]{0:T(256)S(1)}, u32[]{:S(2)}) copy-start(f32[256]{0:T(256)S(1)} %get-tuple-element.19) | copy-start | bytes 3076
  30.8 18.1 %copy-start.23 = (f32[256]{0:T(256)}, f32[256]{0:T(256)S(1)}, u32[]{:S(2)}) copy-start(f32[256]{0:T(256)S(1)} %get-tuple-element.20) | copy-start | bytes 3076
  40.6 12.5 %all-to-all-start.1 = ((f32[8,2,768]{2,1,0:T(2,128)}), f32[8,2,768]{2,1,0:T(2,128)S(1)}, u32[]{:S(2)}, u32[]{:S(2)}) async-start(f32[8,2,768]{2,1,0:T(2,128)} %broadcast_in_dim.68), calls=%async_computation.1 | async-start | bytes 98304 | tf_op jit(solution)/shard_map/all_to_all | solution.py:26
  53.1 1.2 copy-start.6
  54.3 0.8 copy-start.17
  55.2 0.7 copy-start.18
  58.9 1.0 copy-start.4
  59.9 0.9 copy-start.8
  60.8 0.7 copy-start.11
  61.5 32.0 %copy-start.27 = (bf16[512]{0:T(512)(128)(2,1)S(1)}, bf16[512]{0:T(512)(128)(2,1)}, u32[]{:S(2)}) copy-start(bf16[512]{0:T(512)(128)(2,1)} %param.22) | copy-start | bytes 3076
  61.5 32.6 %copy-start.22 = (f32[256]{0:T(256)S(1)}, f32[256]{0:T(256)}, u32[]{:S(2)}) copy-start(f32[256]{0:T(256)} %copy-done.21) | copy-start | bytes 3076
  61.5 32.6 %copy-start.24 = (f32[256]{0:T(256)S(1)}, f32[256]{0:T(256)}, u32[]{:S(2)}) copy-start(f32[256]{0:T(256)} %copy-done.23) | copy-start | bytes 3076
  61.5 32.6 %copy-start.5 = (bf16[272,2048]{1,0:T(8,128)(2,1)S(1)}, bf16[272,2048]{1,0:T(8,128)(2,1)}, u32[]{:S(2)}) copy-start(bf16[272,2048]{1,0:T(8,128)(2,1)} %copy-done.4) | copy-start | bytes 3342340
  61.5 25.2 %all-to-all-start.3 = ((bf16[32,16,768]{2,1,0:T(8,128)(2,1)}), bf16[32,16,768]{2,1,0:T(8,128)(2,1)S(1)}, u32[]{:S(2)}, u32[]{:S(2)}) async-start(bf16[32,16,768]{2,1,0:T(8,128)(2,1)} %bitcast.16), calls=%async_computation.3 | async-start | bytes 1572864 | tf_op jit(solution)/shard_map/all_to_all | solution.py:224
  87.7 20.8 %all-to-all-start.4 = ((bf16[32,16,512]{2,1,0:T(8,128)(2,1)}), bf16[32,16,512]{2,1,0:T(8,128)(2,1)S(1)}, u32[]{:S(2)}, u32[]{:S(2)}) async-start(bf16[32,16,512]{2,1,0:T(8,128)(2,1)} %shard_map.120), calls=%async_computation.4 | async-start | bytes 1048576 | tf_op jit(solution)/shard_map/all_to_all | solution.py:242
  94.2 1.6 %copy-start.2 = (bf16[2048,512]{1,0:T(8,128)(2,1)S(1)}, bf16[2048,512]{1,0:T(8,128)(2,1)}, u32[]{:S(2)}) copy-start(bf16[2048,512]{1,0:T(8,128)(2,1)} %wg_ref.1) | copy-start | bytes 6291460
  95.8 1.2 copy-start.7
  97.0 0.9 copy-start.12
  99.1 0.8 copy-start.9
  99.9 0.7 copy-start.13
  100.6 0.7 copy-start.15
  108.4 1.6 %copy-start.3 = (bf16[512,2048]{1,0:T(8,128)(2,1)S(1)}, bf16[512,2048]{1,0:T(8,128)(2,1)}, u32[]{:S(2)}) copy-start(bf16[512,2048]{1,0:T(8,128)(2,1)} %wo_ref.1) | copy-start | bytes 6291460
  110.0 1.0 copy-start.10
  111.1 0.9 copy-start.14
  112.0 0.9 copy-start.16
  112.9 0.7 copy-start.19
  114.8 19.2 %copy-start.20 = (bf16[32,2048]{1,0:T(8,128)(2,1)S(1)}, bf16[32,2048]{1,0:T(8,128)(2,1)}, u32[]{:S(2)}) copy-start(bf16[32,2048]{1,0:T(8,128)(2,1)} %param.12) | copy-start | bytes 393220
  114.9 5.5 %collective-permute-start.1 = (bf16[128,2048]{1,0:T(8,128)(2,1)S(1)}, bf16[128,2048]{1,0:T(8,128)(2,1)S(1)}, u32[]{:S(2)}, u32[]{:S(2)}) collective-permute-start(bf16[128,2048]{1,0:T(8,128)(2,1)S(1)} %slice.29), channel_id=1, source_target_pairs={{0,1},{1,0},{2,3},{3,2},{4,5},{5,4},{6,7},{7,6},{8,9},{9,8},{10,11... | collective-permute-start | bytes 1572872 | tf_op jit(solution)/shard_map/ppermute | solution.py:256
  121.3 12.6 %all-to-all-start.5 = ((bf16[4,32,2048]{2,1,0:T(8,128)(2,1)}), bf16[4,32,2048]{2,1,0:T(8,128)(2,1)S(1)}, u32[]{:S(2)}, u32[]{:S(2)}) async-start(bf16[4,32,2048]{2,1,0:T(8,128)(2,1)} %bitcast.10), calls=%async_computation.5 | async-start | bytes 1048576 | tf_op jit(solution)/shard_map/all_to_all | solution.py:258

commit v2 on v1

v2 whole, which is shorter than its diff:
```python
import jax
import jax.numpy as jnp
from jax import lax
from jax.experimental import pallas as pl
from jax.experimental.pallas import tpu as pltpu
from jax.sharding import Mesh
from jax.sharding import PartitionSpec as P

DK = 256
DV = 512
GRID_W = 64
CTX_LIFT = 4
SP = ("z", "y")
TP = ("x", "c")
ALL = ("z", "y", "x", "c")
f32 = jnp.float32
bf16 = jnp.bfloat16

epsilon = 1e-06
rotary_base = 10000.0
MIB = 1024 * 1024


def kernel_call(body, outs, ins, scratch, vmem, flops, *args):
    spaces = {"h": pltpu.MemorySpace.HBM, "v": pltpu.MemorySpace.VMEM}
    moved = sum(a.size * a.dtype.itemsize for a in args)
    args = [
        pltpu.with_memory_space_constraint(a, pltpu.HBM) if k == "h" else a
        for k, a in zip(ins, args)
    ]
    return pl.pallas_call(
        body,
        out_shape=tuple(pltpu.HBM(a.shape, a.dtype) if k == "h" else a for k, a in outs),
        in_specs=[pl.BlockSpec(memory_space=spaces[k]) for k in ins],
        out_specs=tuple(pl.BlockSpec(memory_space=spaces[k]) for k, _ in outs),
        scratch_shapes=scratch,
        compiler_params=pltpu.CompilerParams(vmem_limit_bytes=vmem * MIB),
        cost_estimate=pl.CostEstimate(flops=flops, bytes_accessed=moved, transcendentals=0),
    )(*args)


def started(source, target, sems, slot):
    copy = pltpu.make_async_copy(source, target, sems.at[slot])
    copy.start()
    return copy


def dot(a, b):
    return jnp.dot(a, b, preferred_element_type=f32)


def dot_t(a, b):
    return lax.dot_general(a, b, (((1,), (1,)), ((), ())), preferred_element_type=f32)


def turn(u, tab_ref):
    lanes = lax.broadcasted_iota(jnp.int32, u.shape, 1)
    swapped = jnp.where(lanes % 2 == 0, pltpu.roll(u, DK - 1, 1), pltpu.roll(u, 1, 1))
    return u * tab_ref[:, :DK] + swapped * tab_ref[:, DK:]


def prepare_kernel(inputs_ref, weights_ref, decay_ref, out_ref):
    inputs = inputs_ref[...].astype(f32)
    activated = (inputs / (1.0 + jnp.exp(-inputs))).astype(bf16)
    part = dot(activated, weights_ref[...])
    total = jnp.sum(decay_ref[...], axis=0, keepdims=True)
    packed = jnp.concatenate([part, jnp.broadcast_to(total, (1, part.shape[1]))], axis=0)
    for r in range(out_ref.shape[0]):
        out_ref[r] = packed


def gather_kernel(pieces_ref, out_ref, decay_ref):
    summed = pieces_ref[0, 0:2, :]
    for r in range(1, pieces_ref.shape[0]):
        summed = summed + pieces_ref[r, 0:2, :]
    for t in range(out_ref.shape[0]):
        out_ref[t] = summed
    for r in range(pieces_ref.shape[0]):
        decay_ref[r : r + 1, :] = jnp.exp(pieces_ref[r, 2:3, 0:DK])


def keys_kernel(*refs):
    pieces, refs = refs[:8], refs[8:]
    (
        near_hbm, far_hbm, tab_hbm, wk_hbm, mod_ref, gain_ref, wv_ref, col_ref, line_ref,
        send_hbm, normed_hbm, k_hbm, v_hbm,
        raw_ref, ctx_ref, tab_ref, wk_ref, normed_ref, k_ref, v_ref, send_ref, sems,
    ) = refs
    lines, width = pieces[0].shape
    half = 4 * lines
    rows = 2 * half
    near = near_hbm.shape[0]
    raws = [
        started(piece, raw_ref.at[i * lines : (i + 1) * lines], sems, 10 + i)
        for i, piece in enumerate(pieces)
    ]
    loads = [
        started(near_hbm, ctx_ref.at[0:near], sems, 2),
        started(far_hbm, ctx_ref.at[near:], sems, 3),
        started(tab_hbm, tab_ref, sems, 4),
        started(wk_hbm, wk_ref, sems, 9),
    ]
    gain = gain_ref[...].astype(f32)
    tp = mod_ref.shape[0]

    def modulated(values, which):
        line = jnp.concatenate([mod_ref[t, which : which + 1, :] for t in range(tp)], axis=1)
        shift, scale = line[:, :width], line[:, width : 2 * width]
        wide = values.astype(f32)
        normal = wide * lax.rsqrt(jnp.mean(wide * wide, axis=-1, keepdims=True) + epsilon)
        return (normal * gain * (1.0 + scale) + shift).astype(bf16)

    for part in range(2):
        own = slice(part * half, (part + 1) * half)
        for copy in raws[part * 4 : part * 4 + 4]:
            copy.wait()
        normed_ref[own, :] = modulated(raw_ref[own, :], 0)
    stores = [started(normed_ref.at[0:rows], normed_hbm, sems, 5)]
    loads[0].wait()
    loads[1].wait()
    normed_ref[rows:, :] = modulated(ctx_ref[...], 1)
    values = dot(normed_ref[...], wv_ref[...]).astype(bf16)
    loads[2].wait()
    loads[3].wait()
    keys = dot(normed_ref[...], wk_ref[...])
    key_rows = (turn(keys[:rows], tab_ref) * DK ** (-0.5)).astype(bf16)
    ctx_keys = (keys[rows:] * DK ** (-0.5)).astype(bf16)
    k_ref[...] = key_rows
    v_ref[...] = values[:rows]
    stores.append(started(k_ref, k_hbm, sems, 6))
    stores.append(started(v_ref, v_hbm, sems, 7))
    wide = key_rows.astype(f32)
    ahead = (wide * jnp.exp(col_ref[:, 0:1])).astype(bf16)
    behind = (wide * jnp.exp(col_ref[:, 1:2])).astype(bf16)
    turned = values.T
    send_ref[:, 0:DK] = dot(turned[:, :rows], ahead).astype(bf16)
    send_ref[:, DK : 2 * DK] = dot(turned[:, :rows], behind).astype(bf16)
    odd = line_ref[3:4, 0 : DK // 2] > 0.5
    own_keys = jnp.where(
        odd, ctx_keys[:, DK // 2 :].astype(f32), ctx_keys[:, : DK // 2].astype(f32)
    ).astype(bf16)
    send_ref[:, 2 * DK :] = dot(turned[:, rows:], own_keys).astype(bf16)
    stores.append(started(send_ref, send_hbm, sems, 8))
    for copy in stores:
        copy.wait()


def inside_kernel(
    normed_hbm, k_hbm, v_hbm, wq_hbm, wg_hbm, tab_hbm, col_ref, line_ref,
    q_hbm, g_hbm, y_hbm,
    normed_ref, k_ref, v_ref, wq_ref, wg_ref, tab_ref, q_ref, g_ref, y_ref, sems,
):
    pairs = [
        (normed_hbm, normed_ref), (wq_hbm, wq_ref), (tab_hbm, tab_ref), (k_hbm, k_ref),
        (v_hbm, v_ref), (wg_hbm, wg_ref),
    ]
    loads = [started(a, b, sems, i) for i, (a, b) in enumerate(pairs)]
    for copy in loads[:4]:
        copy.wait()
    queries = turn(dot(normed_ref[...], wq_ref[...]), tab_ref).astype(bf16)
    q_ref[...] = queries
    stores = [started(q_ref, q_hbm, sems, 6)]
    scores = dot_t(queries, k_ref[...])
    here, there = col_ref[:, 4:5], line_ref[2:3, :]
    gaps = jnp.where(
        here >= there,
        col_ref[:, 2:3] - line_ref[0:1, :],
        line_ref[1:2, :] - col_ref[:, 1:2],
    )
    weights = jnp.exp(gaps) * jnp.where(here == there, 2.0, 1.0)
    loads[4].wait()
    y_ref[...] = dot((scores * weights).astype(bf16), v_ref[...])
    stores.append(started(y_ref, y_hbm, sems, 7))
    loads[5].wait()
    g_ref[...] = dot(normed_ref[...], wg_ref[...]).astype(bf16)
    stores.append(started(g_ref, g_hbm, sems, 8))
    for copy in stores:
        copy.wait()


def scan_kernel(parts_ref, decay_ref, out_ref):
    count = parts_ref.shape[0]
    lifts = []
    for parity in range(2):
        lift = parts_ref[parity, :, 2 * DK :].astype(f32)
        for r in range(parity + 2, count, 2):
            lift = lift + parts_ref[r, :, 2 * DK :].astype(f32)
        lifts.append(lift)
    ahead = behind = jnp.concatenate(lifts, axis=1) * float(CTX_LIFT)
    for r in range(count):
        s = count - 1 - r
        out_ref[r, :, 0:DK] = ahead.astype(bf16)
        out_ref[s, :, DK:] = behind.astype(bf16)
        ahead = decay_ref[r : r + 1, :] * ahead + parts_ref[r, :, 0:DK].astype(f32)
        behind = decay_ref[s : s + 1, :] * behind + parts_ref[s, :, DK : 2 * DK].astype(f32)


def output_kernel(
    q_hbm, y_hbm, g_hbm, states_ref, col_ref, gain_ref, wo_ref,
    out_hbm,
    q_ref, y_ref, g_ref, out_ref, sems,
):
    pairs = [(q_hbm, q_ref), (y_hbm, y_ref), (g_hbm, g_ref)]
    loads = [started(a, b, sems, i) for i, (a, b) in enumerate(pairs)]
    for copy in loads:
        copy.wait()
    queries = q_ref[...]
    mixed = (
        y_ref[...]
        + jnp.exp(col_ref[:, 2:3]) * dot_t(queries, states_ref[:, 0:DK])
        + jnp.exp(col_ref[:, 3:4]) * dot_t(queries, states_ref[:, DK:])
    )
    average = jnp.mean(mixed, axis=-1, keepdims=True)
    centred = mixed - average
    variance = jnp.mean(centred * centred, axis=-1, keepdims=True)
    gates = g_ref[...].astype(f32)
    attended = (
        gates * jax.nn.sigmoid(gates) * (centred * lax.rsqrt(variance + epsilon))
        * gain_ref[...].astype(f32)
    ).astype(bf16)
    half = out_hbm.shape[0] // 2
    stores = []
    for part in (1, 0):
        own = slice(part * half, (part + 1) * half)
        out_ref[own, :] = dot(attended[own], wo_ref[...]).astype(bf16)
        stores.append(started(out_ref.at[own], out_hbm.at[own], sems, 3 + part))
    for copy in stores:
        copy.wait()


def ring(size, step):
    return [(i, (i + step) % size) for i in range(size)]


def shaped(*shape, dtype=bf16):
    return jax.ShapeDtypeStruct(shape, dtype)


def per_device(
    latent,
    log_decay,
    context,
    condition,
    w_modulate,
    norm_gain,
    w_query,
    w_key,
    w_value,
    w_gate,
    group_gain,
    w_output,
):
    seq_index = lax.axis_index(SP)
    core = lax.axis_index("c")
    lines, width = latent.shape
    x_size = lax.axis_size("x")
    half = lines * x_size
    rows = 2 * half
    swap = [(0, 1), (1, 0)]

    input_rows, columns = w_modulate.shape
    own_inputs = lax.dynamic_slice_in_dim(condition, seq_index * input_rows, input_rows, 1)
    count, tp = lax.axis_size(SP), lax.axis_size(TP)
    (packed,) = kernel_call(
        prepare_kernel,
        [("v", shaped(count, 3, columns, dtype=f32))],
        "vvv",
        [],
        4,
        1000000,
        own_inputs,
        w_modulate,
        log_decay,
    )
    pieces = lax.all_to_all(packed, SP, 0, 0, tiled=True)
    spread, decays = kernel_call(
        gather_kernel,
        [("v", shaped(tp, 2, columns, dtype=f32)), ("v", shaped(count, DK, dtype=f32))],
        "v",
        [],
        4,
        1000000,
        pieces,
    )
    modulation = lax.all_to_all(spread, TP, 0, 0, tiled=True)

    later, spare_decay, place_index, _ = lax.optimization_barrier(
        (latent, log_decay, jnp.stack([seq_index, core, lax.axis_index("y") % 2, lax.axis_index("x")]), packed)
    )
    own_rows = [later] + [lax.ppermute(later, "x", ring(x_size, d)) for d in range(1, x_size)]
    other_rows = [lax.ppermute(piece, "c", swap) for piece in own_rows]
    far = lax.ppermute(context, "y", [(0, 1), (1, 0), (2, 3), (3, 2)])
    total = jnp.sum(spare_decay)

    local = jnp.arange(rows, dtype=jnp.int32)
    grid_row = (place_index[3] - local // lines) % x_size
    grid_column = ((local // half + place_index[1]) % 2) * lines + local % lines
    here = grid_row * GRID_W + grid_column
    slots = jnp.arange(rows, dtype=jnp.int32)
    flat = spare_decay[:, 0]
    upto = jnp.sum(jnp.where(slots[None, :] <= here[:, None], flat[None, :], 0.0), axis=1)
    before = jnp.sum(jnp.where(slots[None, :] < here[:, None], flat[None, :], 0.0), axis=1)
    place = here.astype(f32)
    col = jnp.stack([total - upto, before, upto, total - before, place], axis=1)
    odd = jnp.full((rows,), place_index[2], f32)
    line = jnp.stack([upto, before, place, odd], axis=0)

    pairs = DK // 4
    inverse = rotary_base ** (-jnp.arange(pairs, dtype=f32) / pairs)
    inverse = jnp.repeat(inverse, 2)
    first_row = place_index[0] * (rows // GRID_W)
    angles = jnp.concatenate(
        [
            (first_row + grid_row).astype(f32)[:, None] * inverse,
            grid_column.astype(f32)[:, None] * inverse,
        ],
        axis=1,
    )
    sign = jnp.where(jnp.arange(DK) % 2 == 0, -1.0, 1.0)
    table = jnp.concatenate([jnp.cos(angles), jnp.sin(angles) * sign], axis=1)

    ctx = 2 * context.shape[0]
    lanes = 2 * DK + DK // 2
    sems = pltpu.SemaphoreType.DMA
    send, normed, key_rows, value_rows = kernel_call(
        keys_kernel,
        [
            ("h", shaped(DV, lanes)),
            ("h", shaped(rows, width)),
            ("h", shaped(rows, DK)),
            ("h", shaped(rows, DV)),
        ],
        "hhhhhhhh" + "hhhhvvvvv",
        [
            pltpu.VMEM((rows, width), bf16),
            pltpu.VMEM((ctx, width), bf16),
            pltpu.VMEM((rows, 2 * DK), f32),
            pltpu.VMEM((width, DK), bf16),
            pltpu.VMEM((rows + ctx, width), bf16),
            pltpu.VMEM((rows, DK), bf16),
            pltpu.VMEM((rows, DV), bf16),
            pltpu.VMEM((DV, lanes), bf16),
            sems((18,)),
        ],
        32,
        2 * (rows + ctx) * width * (DK + DV),
        *own_rows,
        *other_rows,
        context,
        far,
        table,
        w_key,
        modulation,
        norm_gain[None],
        w_value,
        col,
        line,
    )
    parts = lax.all_to_all(send.reshape(count, DV // count, lanes), SP, 0, 0, tiled=True)
    queries, gates, inside = kernel_call(
        inside_kernel,
        [
            ("h", shaped(rows, DK)),
            ("h", shaped(rows, DV)),
            ("h", shaped(rows, DV, dtype=f32)),
        ],
        "hhhhhhvv",
        [
            pltpu.VMEM((rows, width), bf16),
            pltpu.VMEM((rows, DK), bf16),
            pltpu.VMEM((rows, DV), bf16),
            pltpu.VMEM((width, DK), bf16),
            pltpu.VMEM((width, DV), bf16),
            pltpu.VMEM((rows, 2 * DK), f32),
            pltpu.VMEM((rows, DK), bf16),
            pltpu.VMEM((rows, DV), bf16),
            pltpu.VMEM((rows, DV), f32),
            sems((9,)),
        ],
        32,
        2 * rows * width * (DK + DV),
        normed,
        key_rows,
        value_rows,
        w_query,
        w_gate,
        table,
        col,
        line,
    )
    (entering,) = kernel_call(
        scan_kernel,
        [("v", shaped(count, DV // count, 2 * DK))],
        "vv",
        [],
        16,
        10 * parts.size,
        parts,
        decays,
    )
    states = lax.all_to_all(entering, SP, 0, 0, tiled=True).reshape(DV, 2 * DK)
    (partial,) = kernel_call(
        output_kernel,
        [("h", shaped(rows, width))],
        "hhhvvvv",
        [
            pltpu.VMEM((rows, DK), bf16),
            pltpu.VMEM((rows, DV), f32),
            pltpu.VMEM((rows, DV), bf16),
            pltpu.VMEM((rows, width), bf16),
            sems((5,)),
        ],
        32,
        2 * rows * DV * width,
        queries,
        inside,
        gates,
        states,
        col,
        group_gain[None],
        w_output,
    )
    crossed = lax.ppermute(partial[half:], "c", swap)
    paired = (partial[:half].astype(f32) + crossed.astype(f32)).astype(bf16)
    tiles = paired.reshape(x_size, lines, width)
    projected = tiles[0].astype(f32)
    for d in range(1, x_size):
        arrived = lax.ppermute(tiles[d], "x", ring(x_size, -d))
        projected = projected + arrived.astype(f32)
    gate = modulation[:, 0].reshape(-1)[2 * width :]
    return (latent.astype(f32) + gate * projected).astype(bf16)


def solution(mesh):
    torus = Mesh(mesh.devices.reshape(8, 4, 4, 2), ALL)
    in_specs = (
        P(ALL, None),
        P(SP, TP),
        P(SP, None),
        P(),
        P(SP, TP),
        P(),
        P(None, TP),
        P(None, TP),
        P(None, TP),
        P(None, TP),
        P(TP),
        P(TP, None),
    )
    return jax.shard_map(
        per_device, mesh=torus, in_specs=in_specs, out_specs=P(ALL, None), check_vma=False
    )
```

time: 136 us -> 120 us (0.88)
  waiting for transfers between devices: 52.5 us -> 22.5 us
  blocking collectives: 0 us -> 24.9 us
  local copies, waits for them, and re-layouts: 22.9 us -> 4.09 us
  Pallas kernels: 6.38 us -> 15.4 us
  starting transfers between devices: 44.5 us -> 39.2 us
  other arithmetic: 7.96 us -> 11.7 us
    all_to_all x5 -> x2, waiting for transfers between devices: 43.7 us -> 4.24 us  [the longest x1 3.31 us: per_device(): modulation = lax.all_to_all(spread, TP, 0, 0, tiled=True)]
    all_to_all x0 -> x1, blocking collectives: none -> 24.9 us  [per_device(): lax.all_to_all(send.reshape(count, DV // count, lanes), SP, 0, 0, tiled=T...]
    all_to_all x5 -> x2, starting transfers between devices: 32.3 us -> 16.3 us  [the longest x1 11.2 us: per_device(): pieces = lax.all_to_all(packed, SP, 0, 0, tiled=True)]
    unnamed x56 -> x27, local copies, waits for them, and re-layouts: 16.4 us -> 1.77 us
    ppermute x1 -> x11, starting transfers between devices: 2.47 us -> 13.4 us  [the longest x3 5.65 us: per_device(): lax.ppermute(later, 'x', ring(x_size, d))]
    pallas_call x4 -> x6, Pallas kernels: 6.38 us -> 15.4 us  [kernel_call(): pl.pallas_call(body, out_shape=tuple((pltpu.HBM(a.shape, a.dtype) if k ==...]
    ppermute x1 -> x11, waiting for transfers between devices: 0.01 us -> 6.3 us  [the longest x3 6.28 us: per_device(): arrived = lax.ppermute(tiles[d], 'x', ring(x_size, -d))]
    broadcast_in_dim x3 -> x0, local copies, waits for them, and re-layouts: 3.23 us -> none  [from_everyone(): jnp.broadcast_to(array[None], (size, *array.shape))]
  transfers between devices with their start and end apart: 8 -> 15, of which waited for: 7 -> 6; matrix products, arithmetic and copies ran while one was open for 8% -> 9% of each run, Pallas kernels for 1% -> 4%
where the time goes in v2:
time: 120 us; the launch traced here: 119 us
  starting transfers between devices  39.2 us (33%)
  blocking collectives  24.9 us (21%)
  waiting for transfers between devices  22.5 us (19%)
  Pallas kernels  15.4 us (13%)
  other arithmetic  11.7 us (10%)
  local copies, waits for them, and re-layouts  4.09 us (3%)
  between operations  1.6 us (1%)
    all_to_all x1, blocking collectives, per_device(): lax.all_to_all(send.reshape(count, DV // count, lanes), SP, 0, 0, tiled=T...  24.9 us
    pallas_call x6, Pallas kernels, kernel_call(): pl.pallas_call(body, out_shape=tuple((pltpu.HBM(a.shape, a.dtype) if k ==...  15.4 us
    all_to_all x1, starting transfers between devices, per_device(): pieces = lax.all_to_all(packed, SP, 0, 0, tiled=True)  11.2 us
    all_to_all x1, waiting for transfers between devices, per_device(): states = lax.all_to_all(entering, SP, 0, 0, tiled=True).reshape(DV, 2 * DK)  10.4 us
    ppermute x3, waiting for transfers between devices, per_device(): arrived = lax.ppermute(tiles[d], 'x', ring(x_size, -d))  6.28 us
    all_to_all x1, starting transfers between devices, per_device(): states = lax.all_to_all(entering, SP, 0, 0, tiled=True).reshape(DV, 2 * DK)  5.67 us
    ppermute x3, starting transfers between devices, per_device(): lax.ppermute(later, 'x', ring(x_size, d))  5.65 us
    all_to_all x1, starting transfers between devices, per_device(): modulation = lax.all_to_all(spread, TP, 0, 0, tiled=True)  5.14 us
  transfers between devices with their start and end apart: 15, of which 6 were waited for; matrix products, arithmetic and copies ran while one was open for 9% of the time, Pallas kernels for 4%

profile of v2, /device:TPU:1, one launch (start us, length us, event | category | flops | bytes accessed | tf_op | source)
XLA Modules:
  0.0 119.4 jit_solution(1736861576165686320)
XLA Ops:
  0.0 0.8 copy.23.decay_ref
  0.8 0.1 constant_dynamic-slice_fusion.inputs_ref
  0.9 0.9 copy-done.3
  1.8 0.9 shard_map.118
  2.8 2.0 %collective-permute-start = (bf16[32,2048]{1,0:T(8,128)(2,1)}, bf16[32,2048]{1,0:T(8,128)(2,1)S(1)}, u32[]{:S(2)}, u32[]{:S(2)}) collective-permute-start(bf16[32,2048]{1,0:T(8,128)(2,1)} %refs_0_), channel_id=1, source_target_pairs={{0,2},{2,4},{4,6},{6,0},{1,3},{3,5},{5,7},{7,1},{8,10},{10,12},{12... | collective-permute-start | bytes 393224 | tf_op jit(solution)/shard_map/ppermute | solution.py:290
  4.9 2.5 %collective-permute-start.1 = (bf16[32,2048]{1,0:T(8,128)(2,1)}, bf16[32,2048]{1,0:T(8,128)(2,1)S(1)}, u32[]{:S(2)}, u32[]{:S(2)}) collective-permute-start(bf16[32,2048]{1,0:T(8,128)(2,1)} %refs_0_), channel_id=1, source_target_pairs={{0,4},{2,6},{4,0},{6,2},{1,5},{3,7},{5,1},{7,3},{8,12},{10,14},{12... | collective-permute-start | bytes 393224 | tf_op jit(solution)/shard_map/ppermute | solution.py:290
  7.3 1.2 collective-permute-start.2
  8.5 1.5 %collective-permute-start.3 = (bf16[32,2048]{1,0:T(8,128)(2,1)}, bf16[32,2048]{1,0:T(8,128)(2,1)S(1)}, u32[]{:S(2)}, u32[]{:S(2)}) collective-permute-start(bf16[32,2048]{1,0:T(8,128)(2,1)} %refs_0_), channel_id=1, source_target_pairs={{0,1},{1,0},{2,3},{3,2},{4,5},{5,4},{6,7},{7,6},{8,9},{9,8},{10,11... | collective-permute-start | bytes 393224 | tf_op jit(solution)/shard_map/ppermute | solution.py:291
  10.0 11.2 %all-to-all-start = ((f32[32,3,768]{2,1,0:T(4,128)}), f32[32,3,768]{2,1,0:T(4,128)S(1)}, u32[]{:S(2)}, u32[]{:S(2)}) async-start(f32[32,3,768]{2,1,0:T(4,128)} %shard_map.118), calls=%async_computation | async-start | bytes 786432 | tf_op jit(solution)/shard_map/all_to_all | solution.py:275
  21.2 1.3 %collective-permute-start.7 = (bf16[16,2048]{1,0:T(8,128)(2,1)}, bf16[16,2048]{1,0:T(8,128)(2,1)S(1)}, u32[]{:S(2)}, u32[]{:S(2)}) collective-permute-start(bf16[16,2048]{1,0:T(8,128)(2,1)} %refs_8_.1), channel_id=1, source_target_pairs={{0,8},{8,0},{16,24},{24,16},{1,9},{9,1},{17,25},{25,17},{2,10},{10... | collective-permute-start | bytes 196616 | tf_op jit(solution)/shard_map/ppermute | solution.py:292
  22.5 0.6 fusion.30
  23.1 0.6 fusion.28
  23.7 1.2 %fusion.26 = f32[1,256]{1,0:T(1,128)S(1)} fusion(s32[]{:T(128)} %bitcast.7, s32[]{:T(128)} %bitcast.6), kind=kLoop, calls=%fused_computation.82 | loop fusion | flops 12032 | bytes 1032 | tf_op jit(solution)/shard_map/convert_element_type | solution.py:303
  25.5 1.2 %multiply_add_fusion = (s32[256]{0:T(256)S(1)}, f32[256]{0:T(256)S(1)}) fusion(s32[]{:T(128)} %bitcast.7, s32[]{:T(128)} %bitcast.6, s32[]{:T(128)} %bitcast.5), kind=kLoop, calls=%fused_computation.84 | loop fusion | flops 12288 | bytes 2060 | tf_op jit(solution)/shard_map/add | solution.py:298
  27.5 0.1 mul.123
  27.6 1.3 %reduce_sum.29 = f32[]{:T(128)} reduce(f32[256,1]{0,1:T(1,128)} %param.13, f32[]{:T(128)} %constant.132.clone.1), dimensions={0,1}, to_apply=%region_0.1 | reduce | flops 255 | bytes 1032 | tf_op jit(solution)/shard_map/reduce_sum | solution.py:293
  28.9 0.9 select_reduce_fusion
  29.9 0.1 broadcast_multiply_fusion.1
  30.0 0.9 fusion
  31.0 0.6 broadcast_subtract_fusion
  31.7 0.7 broadcast_subtract_fusion.1
  32.4 0.9 collective-permute-start.4
  33.3 0.1 collective-permute-start.5
  33.4 0.4 collective-permute-start.6
  33.8 0.9 pad_maximum_fusion.refs_10_.tab_hbm
  34.7 0.9 all-to-all-done.pieces_ref
  35.6 0.7 shard_map.119
  36.3 5.1 %all-to-all-start.1 = ((f32[8,2,768]{2,1,0:T(2,128)}), f32[8,2,768]{2,1,0:T(2,128)S(1)}, u32[]{:S(2)}, u32[]{:S(2)}) async-start(f32[8,2,768]{2,1,0:T(2,128)} %get-tuple-element.17), calls=%async_computation.1 | async-start | bytes 98304 | tf_op jit(solution)/shard_map/all_to_all | solution.py:285
  41.4 1.2 %fusion.23 = f32[256,1]{0,1:T(1,128)S(1)} fusion(s32[]{:T(128)} %bitcast.7, s32[]{:T(128)} %bitcast.6), kind=kLoop, calls=%fused_computation.79 | loop fusion | flops 12032 | bytes 1032 | tf_op jit(solution)/shard_map/convert_element_type | solution.py:303
  42.7 0.1 copy.24.refs_15_.col_ref
  42.9 3.3 %all-to-all-done.1.refs_12_ = f32[8,2,768]{2,1,0:T(2,128)S(1)} async-done(((f32[8,2,768]{2,1,0:T(2,128)}), f32[8,2,768]{2,1,0:T(2,128)S(1)}, u32[]{:S(2)}, u32[]{:S(2)}) %all-to-all-start.1) | async-done | bytes 49184 | tf_op jit(solution)/shard_map/all_to_all | solution.py:285
  46.3 5.1 %shard_map.120 = (bf16[512,640]{1,0:T(8,128)(2,1)}, bf16[256,2048]{1,0:T(8,128)(2,1)}, bf16[256,256]{1,0:T(8,128)(2,1)}, bf16[256,512]{1,0:T(8,128)(2,1)}) custom-call(bf16[32,2048]{1,0:T(8,128)(2,1)} %refs_0_, bf16[32,2048]{1,0:T(8,128)(2,1)} %copy-done.5, bf16[32,2048]{1,0:T(8,128)(2,1)} %copy-done.6, bf16[32,2048]{1,0:T(8,128)(2,1)} %copy-done.7, ...), custom_call_target="tpu_custom_call" | custom-call | flops 905969664 | bytes 4912128 | tf_op jit(solution)/shard_map/pallas_call | solution.py:31
  51.4 24.9 %all_to_all.20.parts_ref = bf16[32,16,640]{2,1,0:T(8,128)(2,1)S(1)} all-to-all(bf16[32,16,640]{2,1,0:T(8,128)(2,1)} %bitcast.17), channel_id=1, replica_groups=mesh['z'=8,'y'=4,'x'=4,'c'=2] {'z','y'}, dimensions={0} | all-to-all | bytes 1310720 | tf_op jit(solution)/shard_map/all_to_all | solution.py:359
  76.3 0.9 shard_map.122
  77.3 5.7 %all-to-all-start.3 = ((bf16[32,16,512]{2,1,0:T(8,128)(2,1)}), bf16[32,16,512]{2,1,0:T(8,128)(2,1)S(1)}, u32[]{:S(2)}, u32[]{:S(2)}) async-start(bf16[32,16,512]{2,1,0:T(8,128)(2,1)} %shard_map.122), calls=%async_computation.3 | async-start | bytes 1048576 | tf_op jit(solution)/shard_map/all_to_all | solution.py:401
  83.0 4.5 %shard_map.121 = (bf16[256,256]{1,0:T(8,128)(2,1)}, bf16[256,512]{1,0:T(8,128)(2,1)}, f32[256,512]{1,0:T(8,128)}) custom-call(bf16[256,2048]{1,0:T(8,128)(2,1)} %get-tuple-element.21.normed_hbm, bf16[256,256]{1,0:T(8,128)(2,1)} %get-tuple-element.22.k_hbm, bf16[256,512]{1,0:T(8,128)(2,1)} %get-tuple-element.23.v_hbm, bf16[2048,256]{1,0:T(8,128)(2,1)} %wq_hbm.1, ...), custom_call_target="tpu_custom_call" | custom-call | flops 805306368 | bytes 5121024 | tf_op jit(solution)/shard_map/pallas_call | solution.py:31
  87.5 10.4 %all-to-all-done.3 = bf16[32,16,512]{2,1,0:T(8,128)(2,1)S(1)} async-done(((bf16[32,16,512]{2,1,0:T(8,128)(2,1)}), bf16[32,16,512]{2,1,0:T(8,128)(2,1)S(1)}, u32[]{:S(2)}, u32[]{:S(2)}) %all-to-all-start.3) | async-done | bytes 524320 | tf_op jit(solution)/shard_map/all_to_all | solution.py:401
  97.9 3.3 %shard_map.123 = bf16[256,2048]{1,0:T(8,128)(2,1)} custom-call(bf16[256,256]{1,0:T(8,128)(2,1)} %get-tuple-element.24.q_hbm, f32[256,512]{1,0:T(8,128)} %get-tuple-element.25.y_hbm, bf16[256,512]{1,0:T(8,128)(2,1)} %get-tuple-element.26.g_hbm, bf16[512,512]{1,0:T(8,128)(2,1)S(1)} %bitcast.16, f32[256,5]{1,0:T(8,128)S(1)} %copy.24.refs_15_.col_ref, ...), custom_call_target="tpu_custom_call" | custom-call | flops 536870912 | bytes 3545088 | tf_op jit(solution)/shard_map/pallas_call | solution.py:31
  101.2 1.1 slice.55
  102.3 3.8 %collective-permute-start.8 = (bf16[128,2048]{1,0:T(8,128)(2,1)S(1)}, bf16[128,2048]{1,0:T(8,128)(2,1)S(1)}, u32[]{:S(2)}, u32[]{:S(2)}) collective-permute-start(bf16[128,2048]{1,0:T(8,128)(2,1)S(1)} %slice.55), channel_id=1, source_target_pairs={{0,1},{1,0},{2,3},{3,2},{4,5},{5,4},{6,7},{7,6},{8,9},{9,8},{10,11... | collective-permute-start | bytes 1572872 | tf_op jit(solution)/shard_map/ppermute | solution.py:423
  106.1 1.5 %collective-permute-done.8 = bf16[128,2048]{1,0:T(8,128)(2,1)S(1)} collective-permute-done((bf16[128,2048]{1,0:T(8,128)(2,1)S(1)}, bf16[128,2048]{1,0:T(8,128)(2,1)S(1)}, u32[]{:S(2)}, u32[]{:S(2)}) %collective-permute-start.8) | collective-permute-done | bytes 524320 | tf_op jit(solution)/shard_map/ppermute | solution.py:423
  107.6 1.2 add_convert_fusion
  108.9 0.8 collective-permute-start.10
  109.7 0.7 collective-permute-start.11
  110.4 2.0 %collective-permute-start.9 = (bf16[32,2048]{1,0:T(8,128)(2,1)S(1)}, bf16[32,2048]{1,0:T(8,128)(2,1)S(1)}, u32[]{:S(2)}, u32[]{:S(2)}) collective-permute-start(bf16[32,2048]{1,0:T(8,128)(2,1)S(1)} %get-tuple-element.31), channel_id=1, source_target_pairs={{0,6},{2,0},{4,2},{6,4},{1,7},{3,1},{5,3},{7,5},{8,14},{10,8},{12,... | collective-permute-start | bytes 393224 | tf_op jit(solution)/shard_map/ppermute | solution.py:428
  112.4 2.7 %collective-permute-done.10 = bf16[32,2048]{1,0:T(8,128)(2,1)S(1)} collective-permute-done((bf16[32,2048]{1,0:T(8,128)(2,1)S(1)}, bf16[32,2048]{1,0:T(8,128)(2,1)S(1)}, u32[]{:S(2)}, u32[]{:S(2)}) %collective-permute-start.10) | collective-permute-done | bytes 131104 | tf_op jit(solution)/shard_map/ppermute | solution.py:428
  115.1 3.5 %collective-permute-done.11 = bf16[32,2048]{1,0:T(8,128)(2,1)S(1)} collective-permute-done((bf16[32,2048]{1,0:T(8,128)(2,1)S(1)}, bf16[32,2048]{1,0:T(8,128)(2,1)S(1)}, u32[]{:S(2)}, u32[]{:S(2)}) %collective-permute-start.11) | collective-permute-done | bytes 131104 | tf_op jit(solution)/shard_map/ppermute | solution.py:428
  118.7 0.8 add_convert_fusion.1
  (46 shorter events, 0.5 us)
Async XLA Ops:
  0.0 0.8 copy-start
  0.9 0.9 copy-start.3
  1.8 41.0 %copy-start.11 = (bf16[2048]{0:T(1024)(128)(2,1)S(1)}, bf16[2048]{0:T(1024)(128)(2,1)}, u32[]{:S(2)}) copy-start(bf16[2048]{0:T(1024)(128)(2,1)} %param.17) | copy-start | bytes 12292
  1.8 44.5 %copy-start.1 = (bf16[2048,512]{1,0:T(8,128)(2,1)S(1)}, bf16[2048,512]{1,0:T(8,128)(2,1)}, u32[]{:S(2)}) copy-start(bf16[2048,512]{1,0:T(8,128)(2,1)} %refs_14_.1) | copy-start | bytes 6291460
  2.8 29.5 %collective-permute-start = (bf16[32,2048]{1,0:T(8,128)(2,1)}, bf16[32,2048]{1,0:T(8,128)(2,1)S(1)}, u32[]{:S(2)}, u32[]{:S(2)}) collective-permute-start(bf16[32,2048]{1,0:T(8,128)(2,1)} %refs_0_), channel_id=1, source_target_pairs={{0,2},{2,4},{4,6},{6,0},{1,3},{3,5},{5,7},{7,1},{8,10},{10,12},{12... | collective-permute-start | bytes 393224 | tf_op jit(solution)/shard_map/ppermute | solution.py:290
  4.9 28.4 %collective-permute-start.1 = (bf16[32,2048]{1,0:T(8,128)(2,1)}, bf16[32,2048]{1,0:T(8,128)(2,1)S(1)}, u32[]{:S(2)}, u32[]{:S(2)}) collective-permute-start(bf16[32,2048]{1,0:T(8,128)(2,1)} %refs_0_), channel_id=1, source_target_pairs={{0,4},{2,6},{4,0},{6,2},{1,5},{3,7},{5,1},{7,3},{8,12},{10,14},{12... | collective-permute-start | bytes 393224 | tf_op jit(solution)/shard_map/ppermute | solution.py:290
  7.3 26.1 %collective-permute-start.2 = (bf16[32,2048]{1,0:T(8,128)(2,1)}, bf16[32,2048]{1,0:T(8,128)(2,1)S(1)}, u32[]{:S(2)}, u32[]{:S(2)}) collective-permute-start(bf16[32,2048]{1,0:T(8,128)(2,1)} %refs_0_), channel_id=1, source_target_pairs={{0,6},{2,0},{4,2},{6,4},{1,7},{3,1},{5,3},{7,5},{8,14},{10,8},{12,... | collective-permute-start | bytes 393224 | tf_op jit(solution)/shard_map/ppermute | solution.py:290
  8.5 34.4 %collective-permute-start.3 = (bf16[32,2048]{1,0:T(8,128)(2,1)}, bf16[32,2048]{1,0:T(8,128)(2,1)S(1)}, u32[]{:S(2)}, u32[]{:S(2)}) collective-permute-start(bf16[32,2048]{1,0:T(8,128)(2,1)} %refs_0_), channel_id=1, source_target_pairs={{0,1},{1,0},{2,3},{3,2},{4,5},{5,4},{6,7},{7,6},{8,9},{9,8},{10,11... | collective-permute-start | bytes 393224 | tf_op jit(solution)/shard_map/ppermute | solution.py:291
  10.0 25.6 %all-to-all-start = ((f32[32,3,768]{2,1,0:T(4,128)}), f32[32,3,768]{2,1,0:T(4,128)S(1)}, u32[]{:S(2)}, u32[]{:S(2)}) async-start(f32[32,3,768]{2,1,0:T(4,128)} %shard_map.118), calls=%async_computation | async-start | bytes 786432 | tf_op jit(solution)/shard_map/all_to_all | solution.py:275
  21.2 21.7 %collective-permute-start.7 = (bf16[16,2048]{1,0:T(8,128)(2,1)}, bf16[16,2048]{1,0:T(8,128)(2,1)S(1)}, u32[]{:S(2)}, u32[]{:S(2)}) collective-permute-start(bf16[16,2048]{1,0:T(8,128)(2,1)} %refs_8_.1), channel_id=1, source_target_pairs={{0,8},{8,0},{16,24},{24,16},{1,9},{9,1},{17,25},{25,17},{2,10},{10... | collective-permute-start | bytes 196616 | tf_op jit(solution)/shard_map/ppermute | solution.py:292
  32.4 13.9 %copy-start.5 = (bf16[32,2048]{1,0:T(8,128)(2,1)}, bf16[32,2048]{1,0:T(8,128)(2,1)S(1)}, u32[]{:S(2)}) copy-start(bf16[32,2048]{1,0:T(8,128)(2,1)S(1)} %collective-permute-done.refs_1_) | copy-start | bytes 393220
  32.4 10.5 %collective-permute-start.4 = (bf16[32,2048]{1,0:T(8,128)(2,1)S(1)}, bf16[32,2048]{1,0:T(8,128)(2,1)S(1)}, u32[]{:S(2)}, u32[]{:S(2)}) collective-permute-start(bf16[32,2048]{1,0:T(8,128)(2,1)S(1)} %collective-permute-done.refs_1_), channel_id=1, source_target_pairs={{0,1},{1,0},{2,3},{3,2},{4,5},{5,4},{6,7},{7,6},{8,9},{9,8},{10,11... | collective-permute-start | bytes 393224 | tf_op jit(solution)/shard_map/ppermute | solution.py:291
  33.3 12.9 %copy-start.6 = (bf16[32,2048]{1,0:T(8,128)(2,1)}, bf16[32,2048]{1,0:T(8,128)(2,1)S(1)}, u32[]{:S(2)}) copy-start(bf16[32,2048]{1,0:T(8,128)(2,1)S(1)} %collective-permute-done.1.refs_2_) | copy-start | bytes 393220
  33.3 9.6 %collective-permute-start.5 = (bf16[32,2048]{1,0:T(8,128)(2,1)S(1)}, bf16[32,2048]{1,0:T(8,128)(2,1)}, u32[]{:S(2)}, u32[]{:S(2)}) collective-permute-start(bf16[32,2048]{1,0:T(8,128)(2,1)S(1)} %collective-permute-done.1.refs_2_), channel_id=1, source_target_pairs={{0,1},{1,0},{2,3},{3,2},{4,5},{5,4},{6,7},{7,6},{8,9},{9,8},{10,11... | collective-permute-start | bytes 393224 | tf_op jit(solution)/shard_map/ppermute | solution.py:291
  33.4 12.8 %copy-start.7 = (bf16[32,2048]{1,0:T(8,128)(2,1)}, bf16[32,2048]{1,0:T(8,128)(2,1)S(1)}, u32[]{:S(2)}) copy-start(bf16[32,2048]{1,0:T(8,128)(2,1)S(1)} %collective-permute-done.2.refs_3_) | copy-start | bytes 393220
  33.4 9.5 %collective-permute-start.6 = (bf16[32,2048]{1,0:T(8,128)(2,1)S(1)}, bf16[32,2048]{1,0:T(8,128)(2,1)}, u32[]{:S(2)}, u32[]{:S(2)}) collective-permute-start(bf16[32,2048]{1,0:T(8,128)(2,1)S(1)} %collective-permute-done.2.refs_3_), channel_id=1, source_target_pairs={{0,1},{1,0},{2,3},{3,2},{4,5},{5,4},{6,7},{7,6},{8,9},{9,8},{10,11... | collective-permute-start | bytes 393224 | tf_op jit(solution)/shard_map/ppermute | solution.py:291
  36.3 9.9 %all-to-all-start.1 = ((f32[8,2,768]{2,1,0:T(2,128)}), f32[8,2,768]{2,1,0:T(2,128)S(1)}, u32[]{:S(2)}, u32[]{:S(2)}) async-start(f32[8,2,768]{2,1,0:T(2,128)} %get-tuple-element.17), calls=%async_computation.1 | async-start | bytes 98304 | tf_op jit(solution)/shard_map/all_to_all | solution.py:285
  42.9 3.4 %copy-start.10 = (bf16[16,2048]{1,0:T(8,128)(2,1)}, bf16[16,2048]{1,0:T(8,128)(2,1)S(1)}, u32[]{:S(2)}) copy-start(bf16[16,2048]{1,0:T(8,128)(2,1)S(1)} %collective-permute-done.7.refs_9_) | copy-start | bytes 196612
  42.9 3.4 %copy-start.8 = (bf16[32,2048]{1,0:T(8,128)(2,1)}, bf16[32,2048]{1,0:T(8,128)(2,1)S(1)}, u32[]{:S(2)}) copy-start(bf16[32,2048]{1,0:T(8,128)(2,1)S(1)} %collective-permute-done.3.refs_4_) | copy-start | bytes 393220
  42.9 3.4 %copy-start.9 = (bf16[32,2048]{1,0:T(8,128)(2,1)}, bf16[32,2048]{1,0:T(8,128)(2,1)S(1)}, u32[]{:S(2)}) copy-start(bf16[32,2048]{1,0:T(8,128)(2,1)S(1)} %collective-permute-done.4.refs_5_) | copy-start | bytes 393220
  51.4 31.5 %copy-start.12 = (bf16[512]{0:T(512)(128)(2,1)S(1)}, bf16[512]{0:T(512)(128)(2,1)}, u32[]{:S(2)}) copy-start(bf16[512]{0:T(512)(128)(2,1)} %param.22) | copy-start | bytes 3076
  77.3 20.6 %all-to-all-start.3 = ((bf16[32,16,512]{2,1,0:T(8,128)(2,1)}), bf16[32,16,512]{2,1,0:T(8,128)(2,1)S(1)}, u32[]{:S(2)}, u32[]{:S(2)}) async-start(bf16[32,16,512]{2,1,0:T(8,128)(2,1)} %shard_map.122), calls=%async_computation.3 | async-start | bytes 1048576 | tf_op jit(solution)/shard_map/all_to_all | solution.py:401
  83.0 14.9 %copy-start.2 = (bf16[512,2048]{1,0:T(8,128)(2,1)S(1)}, bf16[512,2048]{1,0:T(8,128)(2,1)}, u32[]{:S(2)}) copy-start(bf16[512,2048]{1,0:T(8,128)(2,1)} %wo_ref.1) | copy-start | bytes 6291460
  101.2 17.5 %copy-start.4 = (bf16[32,2048]{1,0:T(8,128)(2,1)S(1)}, bf16[32,2048]{1,0:T(8,128)(2,1)}, u32[]{:S(2)}) copy-start(bf16[32,2048]{1,0:T(8,128)(2,1)} %refs_0_) | copy-start | bytes 393220
  102.3 5.3 %collective-permute-start.8 = (bf16[128,2048]{1,0:T(8,128)(2,1)S(1)}, bf16[128,2048]{1,0:T(8,128)(2,1)S(1)}, u32[]{:S(2)}, u32[]{:S(2)}) collective-permute-start(bf16[128,2048]{1,0:T(8,128)(2,1)S(1)} %slice.55), channel_id=1, source_target_pairs={{0,1},{1,0},{2,3},{3,2},{4,5},{5,4},{6,7},{7,6},{8,9},{9,8},{10,11... | collective-permute-start | bytes 1572872 | tf_op jit(solution)/shard_map/ppermute | solution.py:423
  108.9 6.3 %collective-permute-start.10 = (bf16[32,2048]{1,0:T(8,128)(2,1)S(1)}, bf16[32,2048]{1,0:T(8,128)(2,1)S(1)}, u32[]{:S(2)}, u32[]{:S(2)}) collective-permute-start(bf16[32,2048]{1,0:T(8,128)(2,1)S(1)} %get-tuple-element.33), channel_id=1, source_target_pairs={{0,4},{2,6},{4,0},{6,2},{1,5},{3,7},{5,1},{7,3},{8,12},{10,14},{12... | collective-permute-start | bytes 393224 | tf_op jit(solution)/shard_map/ppermute | solution.py:428
  109.7 9.0 %collective-permute-start.11 = (bf16[32,2048]{1,0:T(8,128)(2,1)S(1)}, bf16[32,2048]{1,0:T(8,128)(2,1)S(1)}, u32[]{:S(2)}, u32[]{:S(2)}) collective-permute-start(bf16[32,2048]{1,0:T(8,128)(2,1)S(1)} %get-tuple-element.32), channel_id=1, source_target_pairs={{0,2},{2,4},{4,6},{6,0},{1,3},{3,5},{5,7},{7,1},{8,10},{10,12},{12... | collective-permute-start | bytes 393224 | tf_op jit(solution)/shard_map/ppermute | solution.py:428
  110.4 8.3 %collective-permute-start.9 = (bf16[32,2048]{1,0:T(8,128)(2,1)S(1)}, bf16[32,2048]{1,0:T(8,128)(2,1)S(1)}, u32[]{:S(2)}, u32[]{:S(2)}) collective-permute-start(bf16[32,2048]{1,0:T(8,128)(2,1)S(1)} %get-tuple-element.31), channel_id=1, source_target_pairs={{0,6},{2,0},{4,2},{6,4},{1,7},{3,1},{5,3},{7,5},{8,14},{10,8},{12,... | collective-permute-start | bytes 393224 | tf_op jit(solution)/shard_map/ppermute | solution.py:428

commit v3 on v2

v3 whole, which is shorter than its diff:
```python
import functools

import jax
import jax.numpy as jnp
import numpy as np
from jax import lax
from jax.experimental import pallas as pl
from jax.experimental.pallas import tpu as pltpu
from jax.sharding import Mesh
from jax.sharding import PartitionSpec as P

DK = 256
DV = 512
GRID_W = 64
CTX_LIFT = 4
SP = ("z", "y")
TP = ("x", "c")
ALL = ("z", "y", "x", "c")
f32 = jnp.float32
bf16 = jnp.bfloat16

epsilon = 1e-06
rotary_base = 10000.0
MIB = 1024 * 1024


def kernel_call(body, outs, ins, scratch, vmem, flops, *args):
    spaces = {"h": pltpu.MemorySpace.HBM, "v": pltpu.MemorySpace.VMEM}
    moved = sum(a.size * a.dtype.itemsize for a in args)
    args = [
        pltpu.with_memory_space_constraint(a, pltpu.HBM) if k == "h" else a
        for k, a in zip(ins, args)
    ]
    return pl.pallas_call(
        body,
        out_shape=tuple(pltpu.HBM(a.shape, a.dtype) if k == "h" else a for k, a in outs),
        in_specs=[pl.BlockSpec(memory_space=spaces[k]) for k in ins],
        out_specs=tuple(pl.BlockSpec(memory_space=spaces[k]) for k, _ in outs),
        scratch_shapes=scratch,
        compiler_params=pltpu.CompilerParams(vmem_limit_bytes=vmem * MIB),
        cost_estimate=pl.CostEstimate(flops=flops, bytes_accessed=moved, transcendentals=0),
    )(*args)


def started(source, target, sems, slot):
    copy = pltpu.make_async_copy(source, target, sems.at[slot])
    copy.start()
    return copy


def dot(a, b):
    return jnp.dot(a, b, preferred_element_type=f32)


def dot_t(a, b):
    return lax.dot_general(a, b, (((1,), (1,)), ((), ())), preferred_element_type=f32)


def turn(u, tab_ref):
    lanes = lax.broadcasted_iota(jnp.int32, u.shape, 1)
    swapped = jnp.where(lanes % 2 == 0, pltpu.roll(u, DK - 1, 1), pltpu.roll(u, 1, 1))
    return u * tab_ref[:, :DK] + swapped * tab_ref[:, DK:]


def prepare_kernel(
    weights_hbm, condition_hbm, decay_hbm, out_ref, weights_ref, condition_ref, decay_ref, sems
):
    loads = [
        started(condition_hbm, condition_ref, sems, 0),
        started(decay_hbm, decay_ref, sems, 1),
        started(weights_hbm, weights_ref, sems, 2),
    ]
    size, width = weights_hbm.shape[0], condition_hbm.shape[1]
    seq = lax.axis_index("z") * lax.axis_size("y") + lax.axis_index("y")
    loads[0].wait()
    values = condition_ref[...].astype(f32)
    values = jnp.concatenate([values] * 4, axis=0)
    inputs = pltpu.roll(values, (width - seq * size) % width, 1)[0:2, 0:size]
    activated = (inputs / (1.0 + jnp.exp(-inputs))).astype(bf16)
    loads[1].wait()
    total = jnp.sum(decay_ref[...], axis=1, keepdims=True)
    loads[2].wait()
    part = dot(activated, weights_ref[...])
    packed = jnp.concatenate([part, jnp.broadcast_to(total, (1, part.shape[1]))], axis=0)
    for r in range(out_ref.shape[0]):
        out_ref[r] = packed


def rotary_tables(count):
    pairs = DK // 4
    exponents = -np.arange(pairs, dtype=np.float32) / np.float32(pairs)
    inverse = np.repeat(np.float32(rotary_base) ** exponents, 2).astype(np.float32)
    angles = np.arange(count, dtype=np.float32)[:, None] * inverse
    sign = np.where(np.arange(DK // 2) % 2 == 0, -1.0, 1.0).astype(np.float32)
    return np.concatenate([np.cos(angles), np.sin(angles) * sign], axis=1)


def tables_kernel(
    lines, chips, decay_hbm, row_hbm, column_hbm, col_ref, line_ref, tab_hbm,
    decay_ref, row_ref, column_ref, tab_ref, sems,
):
    loads = [
        started(row_hbm, row_ref, sems, 1),
        started(column_hbm, column_ref, sems, 2),
        started(decay_hbm, decay_ref, sems, 3),
    ]
    rows = 2 * chips * lines
    seq = lax.axis_index("z") * lax.axis_size("y") + lax.axis_index("y")
    chip, core = lax.axis_index("x"), lax.axis_index("c")
    pair = DK // 2
    loads[0].wait()
    loads[1].wait()
    for h in range(2):
        column = pl.multiple_of(((h + core) % 2) * lines, lines)
        for d in range(chips):
            own = slice((h * chips + d) * lines, (h * chips + d + 1) * lines)
            row = seq * chips + (chip - d + chips) % chips
            for k in range(2):
                part = slice(k * pair, (k + 1) * pair)
                tab_ref[own, k * DK : k * DK + pair] = jnp.broadcast_to(
                    row_ref[row, :, part], (lines, pair)
                )
                tab_ref[own, k * DK + pair : (k + 1) * DK] = column_ref[
                    pl.ds(column, lines), part
                ]
    store = started(tab_ref, tab_hbm, sems, 0)

    def position(local):
        origin = (chip - (local // lines) % chips + chips) % chips
        return origin * GRID_W + ((local // (chips * lines) + core) % 2) * lines + local % lines

    down = lax.broadcasted_iota(jnp.int32, (rows, rows), 0)
    across = lax.broadcasted_iota(jnp.int32, (rows, rows), 1)
    place_col = position(lax.broadcasted_iota(jnp.int32, (rows, 1), 0))
    place_line = position(lax.broadcasted_iota(jnp.int32, (1, rows), 1))
    loads[2].wait()
    flat = decay_ref[...]
    total = jnp.sum(flat, axis=1, keepdims=True)
    flat_col = jnp.sum(jnp.where(down == across, flat, 0.0), axis=1, keepdims=True)
    upto = jnp.sum(jnp.where(across <= place_col, flat, 0.0), axis=1, keepdims=True)
    before = jnp.sum(jnp.where(across < place_col, flat, 0.0), axis=1, keepdims=True)
    col_ref[:, 0:1] = total - upto
    col_ref[:, 1:2] = before
    col_ref[:, 2:3] = upto
    col_ref[:, 3:4] = total - before
    col_ref[:, 4:5] = place_col.astype(f32)
    line_ref[0:1, :] = jnp.sum(jnp.where(down <= place_line, flat_col, 0.0), axis=0, keepdims=True)
    line_ref[1:2, :] = jnp.sum(jnp.where(down < place_line, flat_col, 0.0), axis=0, keepdims=True)
    line_ref[2:3, :] = place_line.astype(f32)
    odd = lax.axis_index("y") % 2
    line_ref[3:4, :] = jnp.full((1, rows), odd, jnp.int32).astype(f32)
    store.wait()


def gather_kernel(pieces_ref, out_ref, decay_ref):
    summed = pieces_ref[0, 0:2, :]
    for r in range(1, pieces_ref.shape[0]):
        summed = summed + pieces_ref[r, 0:2, :]
    for t in range(out_ref.shape[0]):
        out_ref[t] = summed
    for r in range(pieces_ref.shape[0]):
        decay_ref[r : r + 1, :] = jnp.exp(pieces_ref[r, 2:3, 0:DK])


def keys_kernel(*refs):
    pieces, refs = refs[:8], refs[8:]
    (
        near_hbm, far_ref, tab_hbm, wk_hbm, wv_hbm, mod_ref, gain_ref, col_ref, line_ref,
        send_hbm, normed_hbm, k_hbm, v_hbm,
        own_ref, near_ref, tab_ref, wk_ref, wv_ref, normed_ref, k_ref, v_ref, send_ref, sems,
    ) = refs
    lines, width = pieces[0].shape
    rows = 8 * lines
    near = near_ref.shape[0]
    own = [started(pieces[0], own_ref, sems, 7), started(near_hbm, near_ref, sems, 8)]
    loads = [
        started(wv_hbm, wv_ref, sems, 0),
        started(wk_hbm, wk_ref, sems, 1),
        started(tab_hbm, tab_ref, sems, 2),
    ]
    gain = gain_ref[...].astype(f32)
    tp = mod_ref.shape[0]

    def modulated(values, which):
        line = jnp.concatenate([mod_ref[t, which : which + 1, :] for t in range(tp)], axis=1)
        shift, scale = line[:, :width], line[:, width : 2 * width]
        wide = values.astype(f32)
        normal = wide * lax.rsqrt(jnp.mean(wide * wide, axis=-1, keepdims=True) + epsilon)
        return (normal * gain * (1.0 + scale) + shift).astype(bf16)

    for i, piece in enumerate(pieces[1:]):
        normed_ref[(i + 1) * lines : (i + 2) * lines, :] = modulated(piece[...], 0)
    normed_ref[rows + near :, :] = modulated(far_ref[...], 1)
    for copy in own:
        copy.wait()
    normed_ref[0:lines, :] = modulated(own_ref[...], 0)
    normed_ref[rows : rows + near, :] = modulated(near_ref[...], 1)
    loads[0].wait()
    values = dot(normed_ref[...], wv_ref[...]).astype(bf16)
    loads[1].wait()
    keys = dot(normed_ref[...], wk_ref[...])
    loads[2].wait()
    key_rows = (turn(keys[:rows], tab_ref) * DK ** (-0.5)).astype(bf16)
    ctx_keys = (keys[rows:] * DK ** (-0.5)).astype(bf16)
    k_ref[...] = key_rows
    v_ref[...] = values[:rows]
    wide = key_rows.astype(f32)
    ahead = (wide * jnp.exp(col_ref[:, 0:1])).astype(bf16)
    behind = (wide * jnp.exp(col_ref[:, 1:2])).astype(bf16)
    turned = values.T
    send_ref[:, 0:DK] = dot(turned[:, :rows], ahead).astype(bf16)
    send_ref[:, DK : 2 * DK] = dot(turned[:, :rows], behind).astype(bf16)
    odd = line_ref[3:4, 0 : DK // 2] > 0.5
    own_keys = jnp.where(
        odd, ctx_keys[:, DK // 2 :].astype(f32), ctx_keys[:, : DK // 2].astype(f32)
    ).astype(bf16)
    send_ref[:, 2 * DK :] = dot(turned[:, rows:], own_keys).astype(bf16)
    stores = [
        started(send_ref, send_hbm, sems, 3),
        started(normed_ref.at[0:rows], normed_hbm, sems, 4),
        started(k_ref, k_hbm, sems, 5),
        started(v_ref, v_hbm, sems, 6),
    ]
    for copy in stores:
        copy.wait()


def inside_kernel(
    normed_hbm, k_hbm, v_hbm, wq_hbm, wg_hbm, tab_hbm, col_ref, line_ref,
    q_ref, g_hbm, y_hbm,
    normed_ref, k_ref, v_ref, wq_ref, wg_ref, tab_ref, g_ref, y_ref, sems,
):
    pairs = [
        (normed_hbm, normed_ref), (wq_hbm, wq_ref), (tab_hbm, tab_ref), (k_hbm, k_ref),
        (v_hbm, v_ref), (wg_hbm, wg_ref),
    ]
    loads = [started(a, b, sems, i) for i, (a, b) in enumerate(pairs)]
    for copy in loads[:4]:
        copy.wait()
    queries = turn(dot(normed_ref[...], wq_ref[...]), tab_ref).astype(bf16)
    q_ref[...] = queries
    scores = dot_t(queries, k_ref[...])
    here, there = col_ref[:, 4:5], line_ref[2:3, :]
    gaps = jnp.where(
        here >= there,
        col_ref[:, 2:3] - line_ref[0:1, :],
        line_ref[1:2, :] - col_ref[:, 1:2],
    )
    weights = jnp.exp(gaps) * jnp.where(here == there, 2.0, 1.0)
    loads[4].wait()
    y_ref[...] = dot((scores * weights).astype(bf16), v_ref[...])
    stores = [started(y_ref, y_hbm, sems, 7)]
    loads[5].wait()
    g_ref[...] = dot(normed_ref[...], wg_ref[...]).astype(bf16)
    stores.append(started(g_ref, g_hbm, sems, 8))
    for copy in stores:
        copy.wait()


def scan_kernel(parts_ref, decay_ref, out_ref):
    count = parts_ref.shape[0]
    lifts = []
    for parity in range(2):
        lift = parts_ref[parity, :, 2 * DK :].astype(f32)
        for r in range(parity + 2, count, 2):
            lift = lift + parts_ref[r, :, 2 * DK :].astype(f32)
        lifts.append(lift)
    ahead = behind = jnp.concatenate(lifts, axis=1) * float(CTX_LIFT)
    for r in range(count):
        s = count - 1 - r
        out_ref[r, :, 0:DK] = ahead.astype(bf16)
        out_ref[s, :, DK:] = behind.astype(bf16)
        ahead = decay_ref[r : r + 1, :] * ahead + parts_ref[r, :, 0:DK].astype(f32)
        behind = decay_ref[s : s + 1, :] * behind + parts_ref[s, :, DK : 2 * DK].astype(f32)


def output_kernel(
    part, y_hbm, g_hbm, q_ref, states_ref, col_ref, gain_ref, wo_ref, out_ref, y_ref, g_ref, sems
):
    half = out_ref.shape[0]
    own = slice(part * half, (part + 1) * half)
    loads = [started(y_hbm.at[own], y_ref, sems, 0), started(g_hbm.at[own], g_ref, sems, 1)]
    queries = q_ref[own, :]
    mixed = jnp.exp(col_ref[own, 2:3]) * dot_t(queries, states_ref[:, 0:DK]) + jnp.exp(
        col_ref[own, 3:4]
    ) * dot_t(queries, states_ref[:, DK:])
    loads[0].wait()
    mixed = mixed + y_ref[...]
    average = jnp.mean(mixed, axis=-1, keepdims=True)
    centred = mixed - average
    variance = jnp.mean(centred * centred, axis=-1, keepdims=True)
    loads[1].wait()
    gates = g_ref[...].astype(f32)
    attended = (
        gates * jax.nn.sigmoid(gates) * (centred * lax.rsqrt(variance + epsilon))
        * gain_ref[...].astype(f32)
    ).astype(bf16)
    out_ref[...] = dot(attended, wo_ref[...]).astype(bf16)


def pair_kernel(own_ref, crossed_ref, *out_refs):
    lines = out_refs[0].shape[0]
    for d, out_ref in enumerate(out_refs):
        own = slice(d * lines, (d + 1) * lines)
        out_ref[...] = (own_ref[own, :].astype(f32) + crossed_ref[own, :].astype(f32)).astype(bf16)


def ring(size, step):
    return [(i, (i + step) % size) for i in range(size)]


def shaped(*shape, dtype=bf16):
    return jax.ShapeDtypeStruct(shape, dtype)


def per_device(
    latent,
    log_decay,
    context,
    condition,
    w_modulate,
    norm_gain,
    w_query,
    w_key,
    w_value,
    w_gate,
    group_gain,
    w_output,
):
    lines, width = latent.shape
    x_size = lax.axis_size("x")
    half = lines * x_size
    rows = 2 * half
    swap = [(0, 1), (1, 0)]

    columns = w_modulate.shape[1]
    sems = pltpu.SemaphoreType.DMA
    count, tp = lax.axis_size(SP), lax.axis_size(TP)
    (packed,) = kernel_call(
        prepare_kernel,
        [("v", shaped(count, 3, columns, dtype=f32))],
        "hhh",
        [
            pltpu.VMEM(w_modulate.shape, bf16),
            pltpu.VMEM(condition.shape, bf16),
            pltpu.VMEM((1, rows), f32),
            sems((3,)),
        ],
        4,
        1000000,
        w_modulate,
        condition,
        log_decay.T,
    )
    pieces = lax.all_to_all(packed, SP, 0, 0, tiled=True)
    spread, decays = kernel_call(
        gather_kernel,
        [("v", shaped(tp, 2, columns, dtype=f32)), ("v", shaped(count, DK, dtype=f32))],
        "v",
        [],
        4,
        1000000,
        pieces,
    )
    modulation = lax.all_to_all(spread, TP, 0, 0, tiled=True)

    later, near, later_decay, _ = lax.optimization_barrier((latent, context, log_decay.T, packed))
    own_rows = [later] + [lax.ppermute(later, "x", ring(x_size, d)) for d in range(1, x_size)]
    other_rows = [lax.ppermute(piece, "c", swap) for piece in own_rows]
    far = lax.ppermute(near, "y", [(0, 1), (1, 0), (2, 3), (3, 2)])
    seq_rows = count * rows // GRID_W
    col, line, table = kernel_call(
        functools.partial(tables_kernel, lines, x_size),
        [
            ("v", shaped(rows, 8, dtype=f32)),
            ("v", shaped(4, rows, dtype=f32)),
            ("h", shaped(rows, 2 * DK, dtype=f32)),
        ],
        "hhh",
        [
            pltpu.VMEM((1, rows), f32),
            pltpu.VMEM((seq_rows, 1, DK), f32),
            pltpu.VMEM((GRID_W, DK), f32),
            pltpu.VMEM((rows, 2 * DK), f32),
            sems((4,)),
        ],
        8,
        1000000,
        later_decay,
        jnp.asarray(rotary_tables(seq_rows))[:, None],
        jnp.asarray(rotary_tables(GRID_W)),
    )

    ctx = 2 * context.shape[0]
    lanes = 2 * DK + DK // 2
    send, normed, key_rows, value_rows = kernel_call(
        keys_kernel,
        [
            ("h", shaped(DV, lanes)),
            ("h", shaped(rows, width)),
            ("h", shaped(rows, DK)),
            ("h", shaped(rows, DV)),
        ],
        "hvvvvvvv" + "hvhhhvvvv",
        [
            pltpu.VMEM((lines, width), bf16),
            pltpu.VMEM(context.shape, bf16),
            pltpu.VMEM((rows, 2 * DK), f32),
            pltpu.VMEM((width, DK), bf16),
            pltpu.VMEM((width, DV), bf16),
            pltpu.VMEM((rows + ctx, width), bf16),
            pltpu.VMEM((rows, DK), bf16),
            pltpu.VMEM((rows, DV), bf16),
            pltpu.VMEM((DV, lanes), bf16),
            sems((9,)),
        ],
        32,
        2 * (rows + ctx) * width * (DK + DV),
        *own_rows,
        *other_rows,
        near,
        far,
        table,
        w_key,
        w_value,
        modulation,
        norm_gain[None],
        col,
        line,
    )
    parts = lax.all_to_all(send.reshape(count, DV // count, lanes), SP, 0, 0, tiled=True)
    queries, gates, inside = kernel_call(
        inside_kernel,
        [
            ("v", shaped(rows, DK)),
            ("h", shaped(rows, DV)),
            ("h", shaped(rows, DV, dtype=f32)),
        ],
        "hhhhhhvv",
        [
            pltpu.VMEM((rows, width), bf16),
            pltpu.VMEM((rows, DK), bf16),
            pltpu.VMEM((rows, DV), bf16),
            pltpu.VMEM((width, DK), bf16),
            pltpu.VMEM((width, DV), bf16),
            pltpu.VMEM((rows, 2 * DK), f32),
            pltpu.VMEM((rows, DV), bf16),
            pltpu.VMEM((rows, DV), f32),
            sems((9,)),
        ],
        32,
        2 * rows * width * (DK + DV),
        normed,
        key_rows,
        value_rows,
        w_query,
        w_gate,
        table,
        col,
        line,
    )
    (entering,) = kernel_call(
        scan_kernel,
        [("v", shaped(count, DV // count, 2 * DK))],
        "vv",
        [],
        16,
        10 * parts.size,
        parts,
        decays,
    )
    states = lax.all_to_all(entering, SP, 0, 0, tiled=True).reshape(DV, 2 * DK)
    partials = []
    for part in (1, 0):
        (partial,) = kernel_call(
            functools.partial(output_kernel, part),
            [("v", shaped(half, width))],
            "hhvvvvv",
            [pltpu.VMEM((half, DV), f32), pltpu.VMEM((half, DV), bf16), sems((2,))],
            32,
            2 * half * DV * width,
            inside,
            gates,
            queries,
            states,
            col,
            group_gain[None],
            w_output,
        )
        partials.append(partial)
    crossed = lax.ppermute(partials[0], "c", swap)
    tiles = kernel_call(
        pair_kernel,
        [("v", shaped(lines, width))] * x_size,
        "vv",
        [],
        8,
        half * width,
        partials[1],
        crossed,
    )
    projected = tiles[0].astype(f32)
    for d in (2, 1, 3):
        arrived = lax.ppermute(tiles[d], "x", ring(x_size, -d))
        projected = projected + arrived.astype(f32)
    gate = modulation[:, 0].reshape(-1)[2 * width :]
    return (latent.astype(f32) + gate * projected).astype(bf16)


def solution(mesh):
    torus = Mesh(mesh.devices.reshape(8, 4, 4, 2), ALL)
    in_specs = (
        P(ALL, None),
        P(SP, TP),
        P(SP, None),
        P(),
        P(SP, TP),
        P(),
        P(None, TP),
        P(None, TP),
        P(None, TP),
        P(None, TP),
        P(TP),
        P(TP, None),
    )
    return jax.shard_map(
        per_device, mesh=torus, in_specs=in_specs, out_specs=P(ALL, None), check_vma=False
    )
```

time: 120 us -> 109 us (0.908)
  other arithmetic: 11.7 us -> 0.75 us
  Pallas kernels: 15.4 us -> 18.9 us
  local copies, waits for them, and re-layouts: 4.09 us -> 0.74 us
  starting transfers between devices: 39.2 us -> 41.5 us
  between operations: 1.6 us -> 0.18 us
    convert_element_type x4 -> x0, other arithmetic: 4.17 us -> none  [the longest x2 2.43 us: per_device(): place = here.astype(f32)]
    pallas_call x6 -> x9, Pallas kernels: 15.4 us -> 18.9 us  [kernel_call(): pl.pallas_call(body, out_shape=tuple((pltpu.HBM(a.shape, a.dtype) if k ==...]
    reduce_sum x2 -> x0, other arithmetic: 2.2 us -> none  [the longest x1 1.29 us: per_device(): total = jnp.sum(spare_decay)]
    ppermute x4, starting transfers between devices: 2.96 us -> 4.77 us  [per_device(): other_rows = [lax.ppermute(piece, 'c', swap) for piece in own_rows]]
    slice x3 -> x0, local copies, waits for them, and re-layouts: 1.75 us -> none  [the longest x1 1.11 us: per_device(): crossed = lax.ppermute(partial[half:], 'c', swap)]
    unnamed x27 -> x6, local copies, waits for them, and re-layouts: 1.77 us -> 0.02 us
    all_to_all x1, starting transfers between devices: 5.14 us -> 6.72 us  [per_device(): modulation = lax.all_to_all(spread, TP, 0, 0, tiled=True)]
    ppermute x3, waiting for transfers between devices: 0.01 us -> 1.54 us  [per_device(): lax.ppermute(later, 'x', ring(x_size, d))]
  transfers between devices with their start and end apart: 15 -> 15, of which waited for: 6 -> 6; matrix products, arithmetic and copies ran while one was open for 9% -> 1% of each run, Pallas kernels for 4% -> 8%
where the time goes in v3:
time: 109 us
  starting transfers between devices  41.5 us (38%)
  blocking collectives  23.8 us (22%)
  waiting for transfers between devices  22.9 us (21%)
  Pallas kernels  18.9 us (17%)
    all_to_all x1, blocking collectives, per_device(): lax.all_to_all(send.reshape(count, DV // count, lanes), SP, 0, 0, tiled=T...  23.8 us
    pallas_call x9, Pallas kernels, kernel_call(): pl.pallas_call(body, out_shape=tuple((pltpu.HBM(a.shape, a.dtype) if k ==...  18.9 us
    all_to_all x1, starting transfers between devices, per_device(): pieces = lax.all_to_all(packed, SP, 0, 0, tiled=True)  12 us
    all_to_all x1, waiting for transfers between devices, per_device(): states = lax.all_to_all(entering, SP, 0, 0, tiled=True).reshape(DV, 2 * DK)  10.6 us
    ppermute x3, waiting for transfers between devices, per_device(): arrived = lax.ppermute(tiles[d], 'x', ring(x_size, -d))  7.28 us
    all_to_all x1, starting transfers between devices, per_device(): modulation = lax.all_to_all(spread, TP, 0, 0, tiled=True)  6.72 us
    all_to_all x1, starting transfers between devices, per_device(): states = lax.all_to_all(entering, SP, 0, 0, tiled=True).reshape(DV, 2 * DK)  5.49 us
    ppermute x3, starting transfers between devices, per_device(): lax.ppermute(later, 'x', ring(x_size, d))  4.89 us
  transfers between devices with their start and end apart: 15, of which 6 were waited for; matrix products, arithmetic and copies ran while one was open for 1% of the time, Pallas kernels for 8%

profile of v3, /device:TPU:1, one launch (start us, length us, event | category | flops | bytes accessed | tf_op | source)
XLA Modules:
  0.0 108.7 jit_solution(16868101336147032024)
XLA Ops:
  0.0 1.8 %shard_map.136 = f32[32,3,768]{2,1,0:T(4,128)} custom-call(bf16[64,768]{1,0:T(8,128)(2,1)} %weights_hbm.1, bf16[2,2048]{1,0:T(2,128)(2,1)} %condition_hbm.1, f32[1,256]{1,0:T(1,128)} %bitcast.8), custom_call_target="tpu_custom_call" | custom-call | flops 1000000 | bytes 107520 | tf_op jit(solution)/shard_map/pallas_call | solution.py:34
  1.8 12.0 %all-to-all-start = ((f32[32,3,768]{2,1,0:T(4,128)}), f32[32,3,768]{2,1,0:T(4,128)S(1)}, u32[]{:S(2)}, u32[]{:S(2)}) async-start(f32[32,3,768]{2,1,0:T(4,128)} %shard_map.136), calls=%async_computation | async-start | bytes 786432 | tf_op jit(solution)/shard_map/all_to_all | solution.py:355
  13.9 1.3 %collective-permute-start = (bf16[32,2048]{1,0:T(8,128)(2,1)}, bf16[32,2048]{1,0:T(8,128)(2,1)S(1)}, u32[]{:S(2)}, u32[]{:S(2)}) collective-permute-start(bf16[32,2048]{1,0:T(8,128)(2,1)} %refs_0_), channel_id=1, source_target_pairs={{0,2},{2,4},{4,6},{6,0},{1,3},{3,5},{5,7},{7,1},{8,10},{10,12},{12... | collective-permute-start | bytes 393224 | tf_op jit(solution)/shard_map/ppermute | solution.py:368
  15.2 2.5 %collective-permute-start.1 = (bf16[32,2048]{1,0:T(8,128)(2,1)}, bf16[32,2048]{1,0:T(8,128)(2,1)S(1)}, u32[]{:S(2)}, u32[]{:S(2)}) collective-permute-start(bf16[32,2048]{1,0:T(8,128)(2,1)} %refs_0_), channel_id=1, source_target_pairs={{0,4},{2,6},{4,0},{6,2},{1,5},{3,7},{5,1},{7,3},{8,12},{10,14},{12... | collective-permute-start | bytes 393224 | tf_op jit(solution)/shard_map/ppermute | solution.py:368
  17.6 1.2 %collective-permute-start.2 = (bf16[32,2048]{1,0:T(8,128)(2,1)}, bf16[32,2048]{1,0:T(8,128)(2,1)S(1)}, u32[]{:S(2)}, u32[]{:S(2)}) collective-permute-start(bf16[32,2048]{1,0:T(8,128)(2,1)} %refs_0_), channel_id=1, source_target_pairs={{0,6},{2,0},{4,2},{6,4},{1,7},{3,1},{5,3},{7,5},{8,14},{10,8},{12,... | collective-permute-start | bytes 393224 | tf_op jit(solution)/shard_map/ppermute | solution.py:368
  18.8 1.8 %collective-permute-start.3 = (bf16[32,2048]{1,0:T(8,128)(2,1)}, bf16[32,2048]{1,0:T(8,128)(2,1)S(1)}, u32[]{:S(2)}, u32[]{:S(2)}) collective-permute-start(bf16[32,2048]{1,0:T(8,128)(2,1)} %refs_0_), channel_id=1, source_target_pairs={{0,1},{1,0},{2,3},{3,2},{4,5},{5,4},{6,7},{7,6},{8,9},{9,8},{10,11... | collective-permute-start | bytes 393224 | tf_op jit(solution)/shard_map/ppermute | solution.py:369
  20.6 0.0 collective-permute-done.refs_1_
  20.6 1.2 %collective-permute-start.4 = (bf16[32,2048]{1,0:T(8,128)(2,1)S(1)}, bf16[32,2048]{1,0:T(8,128)(2,1)S(1)}, u32[]{:S(2)}, u32[]{:S(2)}) collective-permute-start(bf16[32,2048]{1,0:T(8,128)(2,1)S(1)} %collective-permute-done.refs_1_), channel_id=1, source_target_pairs={{0,1},{1,0},{2,3},{3,2},{4,5},{5,4},{6,7},{7,6},{8,9},{9,8},{10,11... | collective-permute-start | bytes 393224 | tf_op jit(solution)/shard_map/ppermute | solution.py:369
  21.7 1.5 %collective-permute-done.1.refs_2_ = bf16[32,2048]{1,0:T(8,128)(2,1)S(1)} collective-permute-done((bf16[32,2048]{1,0:T(8,128)(2,1)}, bf16[32,2048]{1,0:T(8,128)(2,1)S(1)}, u32[]{:S(2)}, u32[]{:S(2)}) %collective-permute-start.1) | collective-permute-done | bytes 131104 | tf_op jit(solution)/shard_map/ppermute | solution.py:368
  23.3 1.8 %collective-permute-start.5 = (bf16[32,2048]{1,0:T(8,128)(2,1)S(1)}, bf16[32,2048]{1,0:T(8,128)(2,1)S(1)}, u32[]{:S(2)}, u32[]{:S(2)}) collective-permute-start(bf16[32,2048]{1,0:T(8,128)(2,1)S(1)} %collective-permute-done.1.refs_2_), channel_id=1, source_target_pairs={{0,1},{1,0},{2,3},{3,2},{4,5},{5,4},{6,7},{7,6},{8,9},{9,8},{10,11... | collective-permute-start | bytes 393224 | tf_op jit(solution)/shard_map/ppermute | solution.py:369
  25.1 0.0 collective-permute-done.2.refs_3_
  25.1 0.0 collective-permute-start.6
  25.1 1.3 %collective-permute-start.7 = (bf16[16,2048]{1,0:T(8,128)(2,1)}, bf16[16,2048]{1,0:T(8,128)(2,1)S(1)}, u32[]{:S(2)}, u32[]{:S(2)}) collective-permute-start(bf16[16,2048]{1,0:T(8,128)(2,1)} %refs_8_), channel_id=1, source_target_pairs={{0,8},{8,0},{16,24},{24,16},{1,9},{9,1},{17,25},{25,17},{2,10},{10... | collective-permute-start | bytes 196616 | tf_op jit(solution)/shard_map/ppermute | solution.py:370
  26.4 1.3 %all-to-all-done.pieces_ref = f32[32,3,768]{2,1,0:T(4,128)S(1)} async-done(((f32[32,3,768]{2,1,0:T(4,128)}), f32[32,3,768]{2,1,0:T(4,128)S(1)}, u32[]{:S(2)}, u32[]{:S(2)}) %all-to-all-start) | async-done | bytes 294944 | tf_op jit(solution)/shard_map/all_to_all | solution.py:355
  27.7 0.7 shard_map.137
  28.4 6.7 %all-to-all-start.1 = ((f32[8,2,768]{2,1,0:T(2,128)}), f32[8,2,768]{2,1,0:T(2,128)S(1)}, u32[]{:S(2)}, u32[]{:S(2)}) async-start(f32[8,2,768]{2,1,0:T(2,128)} %get-tuple-element.24), calls=%async_computation.1 | async-start | bytes 98304 | tf_op jit(solution)/shard_map/all_to_all | solution.py:365
  35.1 0.7 broadcast_in_dim.12.refs_14_
  35.8 1.9 %shard_map.138 = (f32[256,8]{1,0:T(8,128)S(1)}, f32[4,256]{1,0:T(4,128)S(1)}, f32[256,512]{1,0:T(8,128)}) custom-call(f32[1,256]{1,0:T(1,128)} %bitcast.9, f32[128,1,256]{2,1,0:T(1,128)} %constant.9.row_hbm, f32[64,256]{1,0:T(8,128)} %constant.5.clone.column_hbm), custom_call_target="tpu_custom_call" | custom-call | flops 1000000 | bytes 197632 | tf_op jit(solution)/shard_map/pallas_call | solution.py:34
  37.7 0.0 collective-permute-done.7.refs_9_
  37.7 0.0 collective-permute-done.3.refs_4_
  37.7 0.0 collective-permute-done.4.refs_5_
  37.7 0.0 collective-permute-done.5.refs_6_
  37.7 0.0 collective-permute-done.6.refs_7_
  37.7 2.2 %all-to-all-done.1.refs_13_ = f32[8,2,768]{2,1,0:T(2,128)S(1)} async-done(((f32[8,2,768]{2,1,0:T(2,128)}), f32[8,2,768]{2,1,0:T(2,128)S(1)}, u32[]{:S(2)}, u32[]{:S(2)}) %all-to-all-start.1) | async-done | bytes 49184 | tf_op jit(solution)/shard_map/all_to_all | solution.py:365
  39.9 5.4 %shard_map.139 = (bf16[512,640]{1,0:T(8,128)(2,1)}, bf16[256,2048]{1,0:T(8,128)(2,1)}, bf16[256,256]{1,0:T(8,128)(2,1)}, bf16[256,512]{1,0:T(8,128)(2,1)}) custom-call(bf16[32,2048]{1,0:T(8,128)(2,1)} %refs_0_, bf16[32,2048]{1,0:T(8,128)(2,1)S(1)} %collective-permute-done.refs_1_, bf16[32,2048]{1,0:T(8,128)(2,1)S(1)} %collective-permute-done.1.refs_2_, ...), custom_call_target="tpu_custom_call" | custom-call | flops 905969664 | bytes 4915200 | tf_op jit(solution)/shard_map/pallas_call | solution.py:34
  45.3 0.0 copy-start.2
  45.4 23.8 %all_to_all.20.parts_ref = bf16[32,16,640]{2,1,0:T(8,128)(2,1)S(1)} all-to-all(bf16[32,16,640]{2,1,0:T(8,128)(2,1)} %bitcast.6), channel_id=1, replica_groups=mesh['z'=8,'y'=4,'x'=4,'c'=2] {'z','y'}, dimensions={0} | all-to-all | bytes 1310720 | tf_op jit(solution)/shard_map/all_to_all | solution.py:431
  69.1 0.9 shard_map.141
  70.1 5.5 %all-to-all-start.3 = ((bf16[32,16,512]{2,1,0:T(8,128)(2,1)}), bf16[32,16,512]{2,1,0:T(8,128)(2,1)S(1)}, u32[]{:S(2)}, u32[]{:S(2)}) async-start(bf16[32,16,512]{2,1,0:T(8,128)(2,1)} %shard_map.141), calls=%async_computation.3 | async-start | bytes 1048576 | tf_op jit(solution)/shard_map/all_to_all | solution.py:472
  75.6 0.0 copy-done.2
  75.6 0.0 copy-start
  75.6 4.5 %shard_map.140 = (bf16[256,256]{1,0:T(8,128)(2,1)S(1)}, bf16[256,512]{1,0:T(8,128)(2,1)}, f32[256,512]{1,0:T(8,128)}) custom-call(bf16[256,2048]{1,0:T(8,128)(2,1)} %get-tuple-element.31.normed_hbm, bf16[256,256]{1,0:T(8,128)(2,1)} %get-tuple-element.32.k_hbm, bf16[256,512]{1,0:T(8,128)(2,1)} %get-tuple-element.33.v_hbm, bf16[2048,256]{1,0:T(8,128)(2,1)} %wq_hbm.1, ...), custom_call_target="tpu_custom_call" | custom-call | flops 805306368 | bytes 5124096 | tf_op jit(solution)/shard_map/pallas_call | solution.py:34
  80.1 10.6 %all-to-all-done.3 = bf16[32,16,512]{2,1,0:T(8,128)(2,1)S(1)} async-done(((bf16[32,16,512]{2,1,0:T(8,128)(2,1)}), bf16[32,16,512]{2,1,0:T(8,128)(2,1)S(1)}, u32[]{:S(2)}, u32[]{:S(2)}) %all-to-all-start.3) | async-done | bytes 524320 | tf_op jit(solution)/shard_map/all_to_all | solution.py:472
  90.7 0.0 copy-done
  90.7 1.7 %shard_map.143 = bf16[128,2048]{1,0:T(8,128)(2,1)S(1)} custom-call(f32[256,512]{1,0:T(8,128)} %get-tuple-element.34.y_hbm, bf16[256,512]{1,0:T(8,128)(2,1)} %get-tuple-element.35.g_hbm, bf16[256,256]{1,0:T(8,128)(2,1)S(1)} %get-tuple-element.36.q_ref, bf16[512,512]{1,0:T(8,128)(2,1)S(1)} %bitcast.4, f32[256,8]{1,0:T(8,128)S(1)} %get-tuple-element.29.refs_15_.col_ref, ...), custom_call_target="tpu_custom_call" | custom-call | flops 268435456 | bytes 3548160 | tf_op jit(solution)/shard_map/pallas_call | solution.py:34
  92.4 0.0 copy-start.1
  92.4 4.0 %collective-permute-start.8 = (bf16[128,2048]{1,0:T(8,128)(2,1)S(1)}, bf16[128,2048]{1,0:T(8,128)(2,1)S(1)}, u32[]{:S(2)}, u32[]{:S(2)}) collective-permute-start(bf16[128,2048]{1,0:T(8,128)(2,1)S(1)} %shard_map.143), channel_id=1, source_target_pairs={{0,1},{1,0},{2,3},{3,2},{4,5},{5,4},{6,7},{7,6},{8,9},{9,8},{10,11... | collective-permute-start | bytes 1572872 | tf_op jit(solution)/shard_map/ppermute | solution.py:491
  96.4 1.7 %shard_map.142.own_ref = bf16[128,2048]{1,0:T(8,128)(2,1)S(1)} custom-call(f32[256,512]{1,0:T(8,128)} %get-tuple-element.34.y_hbm, bf16[256,512]{1,0:T(8,128)(2,1)} %get-tuple-element.35.g_hbm, bf16[256,256]{1,0:T(8,128)(2,1)S(1)} %get-tuple-element.36.q_ref, bf16[512,512]{1,0:T(8,128)(2,1)S(1)} %bitcast.5, f32[256,8]{1,0:T(8,128)S(1)} %get-tuple-element.29.refs_15_.col_ref, ...), custom_call_target="tpu_custom_call" | custom-call | flops 268435456 | bytes 3548160 | tf_op jit(solution)/shard_map/pallas_call | solution.py:34
  98.1 0.0 collective-permute-done.8.crossed_ref
  98.2 0.1 shard_map.144
  98.3 1.0 collective-permute-start.10
  99.3 0.6 collective-permute-start.11
  99.8 0.8 collective-permute-start.9
  100.6 2.6 %collective-permute-done.10 = bf16[32,2048]{1,0:T(8,128)(2,1)S(1)} collective-permute-done((bf16[32,2048]{1,0:T(8,128)(2,1)S(1)}, bf16[32,2048]{1,0:T(8,128)(2,1)S(1)}, u32[]{:S(2)}, u32[]{:S(2)}) %collective-permute-start.10) | collective-permute-done | bytes 131104 | tf_op jit(solution)/shard_map/ppermute | solution.py:504
  103.3 4.6 %collective-permute-done.11 = bf16[32,2048]{1,0:T(8,128)(2,1)S(1)} collective-permute-done((bf16[32,2048]{1,0:T(8,128)(2,1)S(1)}, bf16[32,2048]{1,0:T(8,128)(2,1)S(1)}, u32[]{:S(2)}, u32[]{:S(2)}) %collective-permute-start.11) | collective-permute-done | bytes 131104 | tf_op jit(solution)/shard_map/ppermute | solution.py:504
  107.9 0.0 collective-permute-done.9
  107.9 0.0 copy-done.1
  107.9 0.8 add_convert_fusion
  (3 shorter events, 0.0 us)
Async XLA Ops:
  1.8 25.9 %all-to-all-start = ((f32[32,3,768]{2,1,0:T(4,128)}), f32[32,3,768]{2,1,0:T(4,128)S(1)}, u32[]{:S(2)}, u32[]{:S(2)}) async-start(f32[32,3,768]{2,1,0:T(4,128)} %shard_map.136), calls=%async_computation | async-start | bytes 786432 | tf_op jit(solution)/shard_map/all_to_all | solution.py:355
  13.9 6.7 %collective-permute-start = (bf16[32,2048]{1,0:T(8,128)(2,1)}, bf16[32,2048]{1,0:T(8,128)(2,1)S(1)}, u32[]{:S(2)}, u32[]{:S(2)}) collective-permute-start(bf16[32,2048]{1,0:T(8,128)(2,1)} %refs_0_), channel_id=1, source_target_pairs={{0,2},{2,4},{4,6},{6,0},{1,3},{3,5},{5,7},{7,1},{8,10},{10,12},{12... | collective-permute-start | bytes 393224 | tf_op jit(solution)/shard_map/ppermute | solution.py:368
  15.2 8.1 %collective-permute-start.1 = (bf16[32,2048]{1,0:T(8,128)(2,1)}, bf16[32,2048]{1,0:T(8,128)(2,1)S(1)}, u32[]{:S(2)}, u32[]{:S(2)}) collective-permute-start(bf16[32,2048]{1,0:T(8,128)(2,1)} %refs_0_), channel_id=1, source_target_pairs={{0,4},{2,6},{4,0},{6,2},{1,5},{3,7},{5,1},{7,3},{8,12},{10,14},{12... | collective-permute-start | bytes 393224 | tf_op jit(solution)/shard_map/ppermute | solution.py:368
  17.6 7.5 %collective-permute-start.2 = (bf16[32,2048]{1,0:T(8,128)(2,1)}, bf16[32,2048]{1,0:T(8,128)(2,1)S(1)}, u32[]{:S(2)}, u32[]{:S(2)}) collective-permute-start(bf16[32,2048]{1,0:T(8,128)(2,1)} %refs_0_), channel_id=1, source_target_pairs={{0,6},{2,0},{4,2},{6,4},{1,7},{3,1},{5,3},{7,5},{8,14},{10,8},{12,... | collective-permute-start | bytes 393224 | tf_op jit(solution)/shard_map/ppermute | solution.py:368
  18.8 18.9 %collective-permute-start.3 = (bf16[32,2048]{1,0:T(8,128)(2,1)}, bf16[32,2048]{1,0:T(8,128)(2,1)S(1)}, u32[]{:S(2)}, u32[]{:S(2)}) collective-permute-start(bf16[32,2048]{1,0:T(8,128)(2,1)} %refs_0_), channel_id=1, source_target_pairs={{0,1},{1,0},{2,3},{3,2},{4,5},{5,4},{6,7},{7,6},{8,9},{9,8},{10,11... | collective-permute-start | bytes 393224 | tf_op jit(solution)/shard_map/ppermute | solution.py:369
  20.6 17.1 %collective-permute-start.4 = (bf16[32,2048]{1,0:T(8,128)(2,1)S(1)}, bf16[32,2048]{1,0:T(8,128)(2,1)S(1)}, u32[]{:S(2)}, u32[]{:S(2)}) collective-permute-start(bf16[32,2048]{1,0:T(8,128)(2,1)S(1)} %collective-permute-done.refs_1_), channel_id=1, source_target_pairs={{0,1},{1,0},{2,3},{3,2},{4,5},{5,4},{6,7},{7,6},{8,9},{9,8},{10,11... | collective-permute-start | bytes 393224 | tf_op jit(solution)/shard_map/ppermute | solution.py:369
  23.3 14.4 %collective-permute-start.5 = (bf16[32,2048]{1,0:T(8,128)(2,1)S(1)}, bf16[32,2048]{1,0:T(8,128)(2,1)S(1)}, u32[]{:S(2)}, u32[]{:S(2)}) collective-permute-start(bf16[32,2048]{1,0:T(8,128)(2,1)S(1)} %collective-permute-done.1.refs_2_), channel_id=1, source_target_pairs={{0,1},{1,0},{2,3},{3,2},{4,5},{5,4},{6,7},{7,6},{8,9},{9,8},{10,11... | collective-permute-start | bytes 393224 | tf_op jit(solution)/shard_map/ppermute | solution.py:369
  25.1 12.6 %collective-permute-start.6 = (bf16[32,2048]{1,0:T(8,128)(2,1)S(1)}, bf16[32,2048]{1,0:T(8,128)(2,1)S(1)}, u32[]{:S(2)}, u32[]{:S(2)}) collective-permute-start(bf16[32,2048]{1,0:T(8,128)(2,1)S(1)} %collective-permute-done.2.refs_3_), channel_id=1, source_target_pairs={{0,1},{1,0},{2,3},{3,2},{4,5},{5,4},{6,7},{7,6},{8,9},{9,8},{10,11... | collective-permute-start | bytes 393224 | tf_op jit(solution)/shard_map/ppermute | solution.py:369
  25.1 12.6 %collective-permute-start.7 = (bf16[16,2048]{1,0:T(8,128)(2,1)}, bf16[16,2048]{1,0:T(8,128)(2,1)S(1)}, u32[]{:S(2)}, u32[]{:S(2)}) collective-permute-start(bf16[16,2048]{1,0:T(8,128)(2,1)} %refs_8_), channel_id=1, source_target_pairs={{0,8},{8,0},{16,24},{24,16},{1,9},{9,1},{17,25},{25,17},{2,10},{10... | collective-permute-start | bytes 196616 | tf_op jit(solution)/shard_map/ppermute | solution.py:370
  28.4 11.5 %all-to-all-start.1 = ((f32[8,2,768]{2,1,0:T(2,128)}), f32[8,2,768]{2,1,0:T(2,128)S(1)}, u32[]{:S(2)}, u32[]{:S(2)}) async-start(f32[8,2,768]{2,1,0:T(2,128)} %get-tuple-element.24), calls=%async_computation.1 | async-start | bytes 98304 | tf_op jit(solution)/shard_map/all_to_all | solution.py:365
  45.3 30.2 %copy-start.2 = (bf16[512]{0:T(512)(128)(2,1)S(1)}, bf16[512]{0:T(512)(128)(2,1)}, u32[]{:S(2)}) copy-start(bf16[512]{0:T(512)(128)(2,1)} %param.24) | copy-start | bytes 3076
  70.1 20.6 %all-to-all-start.3 = ((bf16[32,16,512]{2,1,0:T(8,128)(2,1)}), bf16[32,16,512]{2,1,0:T(8,128)(2,1)S(1)}, u32[]{:S(2)}, u32[]{:S(2)}) async-start(bf16[32,16,512]{2,1,0:T(8,128)(2,1)} %shard_map.141), calls=%async_computation.3 | async-start | bytes 1048576 | tf_op jit(solution)/shard_map/all_to_all | solution.py:472
  75.6 15.1 %copy-start = (bf16[512,2048]{1,0:T(8,128)(2,1)S(1)}, bf16[512,2048]{1,0:T(8,128)(2,1)}, u32[]{:S(2)}) copy-start(bf16[512,2048]{1,0:T(8,128)(2,1)} %wo_ref.3) | copy-start | bytes 6291460
  92.4 15.5 %copy-start.1 = (bf16[32,2048]{1,0:T(8,128)(2,1)S(1)}, bf16[32,2048]{1,0:T(8,128)(2,1)}, u32[]{:S(2)}) copy-start(bf16[32,2048]{1,0:T(8,128)(2,1)} %refs_0_) | copy-start | bytes 393220
  92.4 5.7 %collective-permute-start.8 = (bf16[128,2048]{1,0:T(8,128)(2,1)S(1)}, bf16[128,2048]{1,0:T(8,128)(2,1)S(1)}, u32[]{:S(2)}, u32[]{:S(2)}) collective-permute-start(bf16[128,2048]{1,0:T(8,128)(2,1)S(1)} %shard_map.143), channel_id=1, source_target_pairs={{0,1},{1,0},{2,3},{3,2},{4,5},{5,4},{6,7},{7,6},{8,9},{9,8},{10,11... | collective-permute-start | bytes 1572872 | tf_op jit(solution)/shard_map/ppermute | solution.py:491
  98.3 5.0 %collective-permute-start.10 = (bf16[32,2048]{1,0:T(8,128)(2,1)S(1)}, bf16[32,2048]{1,0:T(8,128)(2,1)S(1)}, u32[]{:S(2)}, u32[]{:S(2)}) collective-permute-start(bf16[32,2048]{1,0:T(8,128)(2,1)S(1)} %get-tuple-element.41), channel_id=1, source_target_pairs={{0,6},{2,0},{4,2},{6,4},{1,7},{3,1},{5,3},{7,5},{8,14},{10,8},{12,... | collective-permute-start | bytes 393224 | tf_op jit(solution)/shard_map/ppermute | solution.py:504
  99.3 8.7 %collective-permute-start.11 = (bf16[32,2048]{1,0:T(8,128)(2,1)S(1)}, bf16[32,2048]{1,0:T(8,128)(2,1)S(1)}, u32[]{:S(2)}, u32[]{:S(2)}) collective-permute-start(bf16[32,2048]{1,0:T(8,128)(2,1)S(1)} %get-tuple-element.42), channel_id=1, source_target_pairs={{0,2},{2,4},{4,6},{6,0},{1,3},{3,5},{5,7},{7,1},{8,10},{10,12},{12... | collective-permute-start | bytes 393224 | tf_op jit(solution)/shard_map/ppermute | solution.py:504
  99.8 8.1 %collective-permute-start.9 = (bf16[32,2048]{1,0:T(8,128)(2,1)S(1)}, bf16[32,2048]{1,0:T(8,128)(2,1)S(1)}, u32[]{:S(2)}, u32[]{:S(2)}) collective-permute-start(bf16[32,2048]{1,0:T(8,128)(2,1)S(1)} %get-tuple-element.40), channel_id=1, source_target_pairs={{0,4},{2,6},{4,0},{6,2},{1,5},{3,7},{5,1},{7,3},{8,12},{10,14},{12... | collective-permute-start | bytes 393224 | tf_op jit(solution)/shard_map/ppermute | solution.py:504

commit v4 on v3

--- a/solution.py
+++ b/solution.py
@@ -14,6 +14,7 @@
 GRID_W = 64
 CTX_LIFT = 4
 SP = ("z", "y")
+YZ = ("y", "z")
 TP = ("x", "c")
 ALL = ("z", "y", "x", "c")
 f32 = jnp.float32
@@ -56,10 +57,18 @@
     return lax.dot_general(a, b, (((1,), (1,)), ((), ())), preferred_element_type=f32)
 
 
-def turn(u, tab_ref):
+def turn(u, row_ref, column_ref):
     lanes = lax.broadcasted_iota(jnp.int32, u.shape, 1)
     swapped = jnp.where(lanes % 2 == 0, pltpu.roll(u, DK - 1, 1), pltpu.roll(u, 1, 1))
-    return u * tab_ref[:, :DK] + swapped * tab_ref[:, DK:]
+    chips, lines, pair = row_ref.shape[0], column_ref.shape[0] // 2, DK // 2
+    turned = []
+    for i in range(2 * chips):
+        own, half, d = slice(i * lines, (i + 1) * lines), i // chips, i % chips
+        column = column_ref[half * lines : (half + 1) * lines, :]
+        low = u[own, :pair] * row_ref[d, :, :pair] + swapped[own, :pair] * row_ref[d, :, pair:]
+        high = u[own, pair:] * column[:, :pair] + swapped[own, pair:] * column[:, pair:]
+        turned.append(jnp.concatenate([low, high], axis=1))
+    return jnp.concatenate(turned, axis=0)
 
 
 def prepare_kernel(
@@ -81,7 +90,10 @@
     total = jnp.sum(decay_ref[...], axis=1, keepdims=True)
     loads[2].wait()
     part = dot(activated, weights_ref[...])
-    packed = jnp.concatenate([part, jnp.broadcast_to(total, (1, part.shape[1]))], axis=0)
+    cuts = part.shape[1] // 128
+    packed = [part[i : i + 1, k * 128 : (k + 1) * 128] for i in range(2) for k in range(cuts)]
+    spare = out_ref.shape[1] - len(packed)
+    packed = jnp.concatenate(packed + [jnp.broadcast_to(total, (spare, 128))], axis=0)
     for r in range(out_ref.shape[0]):
         out_ref[r] = packed
 
@@ -96,34 +108,22 @@
 
 
 def tables_kernel(
-    lines, chips, decay_hbm, row_hbm, column_hbm, col_ref, line_ref, tab_hbm,
-    decay_ref, row_ref, column_ref, tab_ref, sems,
+    lines, chips, decay_hbm, row_hbm, column_hbm,
+    col_ref, line_ref, row_ref, column_ref,
+    decay_ref, sems,
 ):
-    loads = [
-        started(row_hbm, row_ref, sems, 1),
-        started(column_hbm, column_ref, sems, 2),
-        started(decay_hbm, decay_ref, sems, 3),
-    ]
     rows = 2 * chips * lines
     seq = lax.axis_index("z") * lax.axis_size("y") + lax.axis_index("y")
     chip, core = lax.axis_index("x"), lax.axis_index("c")
-    pair = DK // 2
-    loads[0].wait()
-    loads[1].wait()
+    started(decay_hbm, decay_ref, sems, 0).wait()
+    loads = []
     for h in range(2):
         column = pl.multiple_of(((h + core) % 2) * lines, lines)
-        for d in range(chips):
-            own = slice((h * chips + d) * lines, (h * chips + d + 1) * lines)
-            row = seq * chips + (chip - d + chips) % chips
-            for k in range(2):
-                part = slice(k * pair, (k + 1) * pair)
-                tab_ref[own, k * DK : k * DK + pair] = jnp.broadcast_to(
-                    row_ref[row, :, part], (lines, pair)
-                )
-                tab_ref[own, k * DK + pair : (k + 1) * DK] = column_ref[
-                    pl.ds(column, lines), part
-                ]
-    store = started(tab_ref, tab_hbm, sems, 0)
+        target = column_ref.at[h * lines : (h + 1) * lines]
+        loads.append(started(column_hbm.at[pl.ds(column, lines)], target, sems, 1 + h))
+    for d in range(chips):
+        row = seq * chips + (chip - d + chips) % chips
+        loads.append(started(row_hbm.at[row], row_ref.at[d], sems, 3 + d))
 
     def position(local):
         origin = (chip - (local // lines) % chips + chips) % chips
@@ -133,7 +133,6 @@
     across = lax.broadcasted_iota(jnp.int32, (rows, rows), 1)
     place_col = position(lax.broadcasted_iota(jnp.int32, (rows, 1), 0))
     place_line = position(lax.broadcasted_iota(jnp.int32, (1, rows), 1))
-    loads[2].wait()
     flat = decay_ref[...]
     total = jnp.sum(flat, axis=1, keepdims=True)
     flat_col = jnp.sum(jnp.where(down == across, flat, 0.0), axis=1, keepdims=True)
@@ -149,25 +148,33 @@
     line_ref[2:3, :] = place_line.astype(f32)
     odd = lax.axis_index("y") % 2
     line_ref[3:4, :] = jnp.full((1, rows), odd, jnp.int32).astype(f32)
-    store.wait()
+    for copy in loads:
+        copy.wait()
 
 
 def gather_kernel(pieces_ref, out_ref, decay_ref):
-    summed = pieces_ref[0, 0:2, :]
+    cuts = out_ref.shape[2] // 128
+    summed = pieces_ref[0]
     for r in range(1, pieces_ref.shape[0]):
-        summed = summed + pieces_ref[r, 0:2, :]
+        summed = summed + pieces_ref[r]
+    rows = [
+        jnp.concatenate([summed[i * cuts + k : i * cuts + k + 1, :] for k in range(cuts)], axis=1)
+        for i in range(2)
+    ]
     for t in range(out_ref.shape[0]):
-        out_ref[t] = summed
+        out_ref[t] = jnp.concatenate(rows, axis=0)
     for r in range(pieces_ref.shape[0]):
-        decay_ref[r : r + 1, :] = jnp.exp(pieces_ref[r, 2:3, 0:DK])
+        decay = jnp.exp(pieces_ref[r, 2 * cuts : 2 * cuts + 1, :])
+        decay_ref[r : r + 1, :] = jnp.concatenate([decay, decay], axis=1)
 
 
 def keys_kernel(*refs):
     pieces, refs = refs[:8], refs[8:]
     (
-        near_hbm, far_ref, tab_hbm, wk_hbm, wv_hbm, mod_ref, gain_ref, col_ref, line_ref,
-        send_hbm, normed_hbm, k_hbm, v_hbm,
-        own_ref, near_ref, tab_ref, wk_ref, wv_ref, normed_ref, k_ref, v_ref, send_ref, sems,
+        near_hbm, wk_hbm, wv_hbm, far_ref, mod_ref, gain_ref, col_ref, line_ref, row_ref,
+        column_ref,
+        send_ref, normed_hbm, k_hbm, v_hbm,
+        own_ref, near_ref, wk_ref, wv_ref, normed_ref, k_ref, v_ref, sems,
     ) = refs
     lines, width = pieces[0].shape
     rows = 8 * lines
@@ -176,7 +183,6 @@
     loads = [
         started(wv_hbm, wv_ref, sems, 0),
         started(wk_hbm, wk_ref, sems, 1),
-        started(tab_hbm, tab_ref, sems, 2),
     ]
     gain = gain_ref[...].astype(f32)
     tp = mod_ref.shape[0]
@@ -195,15 +201,17 @@
         copy.wait()
     normed_ref[0:lines, :] = modulated(own_ref[...], 0)
     normed_ref[rows : rows + near, :] = modulated(near_ref[...], 1)
+    stores = [started(normed_ref.at[0:rows], normed_hbm, sems, 2)]
     loads[0].wait()
     values = dot(normed_ref[...], wv_ref[...]).astype(bf16)
+    v_ref[...] = values[:rows]
+    stores.append(started(v_ref, v_hbm, sems, 3))
     loads[1].wait()
     keys = dot(normed_ref[...], wk_ref[...])
-    loads[2].wait()
-    key_rows = (turn(keys[:rows], tab_ref) * DK ** (-0.5)).astype(bf16)
+    key_rows = (turn(keys[:rows], row_ref, column_ref) * DK ** (-0.5)).astype(bf16)
     ctx_keys = (keys[rows:] * DK ** (-0.5)).astype(bf16)
     k_ref[...] = key_rows
-    v_ref[...] = values[:rows]
+    stores.append(started(k_ref, k_hbm, sems, 4))
     wide = key_rows.astype(f32)
     ahead = (wide * jnp.exp(col_ref[:, 0:1])).astype(bf16)
     behind = (wide * jnp.exp(col_ref[:, 1:2])).astype(bf16)
@@ -215,29 +223,23 @@
         odd, ctx_keys[:, DK // 2 :].astype(f32), ctx_keys[:, : DK // 2].astype(f32)
     ).astype(bf16)
     send_ref[:, 2 * DK :] = dot(turned[:, rows:], own_keys).astype(bf16)
-    stores = [
-        started(send_ref, send_hbm, sems, 3),
-        started(normed_ref.at[0:rows], normed_hbm, sems, 4),
-        started(k_ref, k_hbm, sems, 5),
-        started(v_ref, v_hbm, sems, 6),
-    ]
     for copy in stores:
         copy.wait()
 
 
 def inside_kernel(
-    normed_hbm, k_hbm, v_hbm, wq_hbm, wg_hbm, tab_hbm, col_ref, line_ref,
+    normed_hbm, k_hbm, v_hbm, wq_hbm, wg_hbm, col_ref, line_ref, row_ref, column_ref,
     q_ref, g_hbm, y_hbm,
-    normed_ref, k_ref, v_ref, wq_ref, wg_ref, tab_ref, g_ref, y_ref, sems,
+    normed_ref, k_ref, v_ref, wq_ref, wg_ref, g_ref, y_ref, sems,
 ):
     pairs = [
-        (normed_hbm, normed_ref), (wq_hbm, wq_ref), (tab_hbm, tab_ref), (k_hbm, k_ref),
-        (v_hbm, v_ref), (wg_hbm, wg_ref),
+        (normed_hbm, normed_ref), (wq_hbm, wq_ref), (k_hbm, k_ref), (v_hbm, v_ref),
+        (wg_hbm, wg_ref),
     ]
     loads = [started(a, b, sems, i) for i, (a, b) in enumerate(pairs)]
-    for copy in loads[:4]:
+    for copy in loads[:3]:
         copy.wait()
-    queries = turn(dot(normed_ref[...], wq_ref[...]), tab_ref).astype(bf16)
+    queries = turn(dot(normed_ref[...], wq_ref[...]), row_ref, column_ref).astype(bf16)
     q_ref[...] = queries
     scores = dot_t(queries, k_ref[...])
     here, there = col_ref[:, 4:5], line_ref[2:3, :]
@@ -247,10 +249,10 @@
         line_ref[1:2, :] - col_ref[:, 1:2],
     )
     weights = jnp.exp(gaps) * jnp.where(here == there, 2.0, 1.0)
-    loads[4].wait()
+    loads[3].wait()
     y_ref[...] = dot((scores * weights).astype(bf16), v_ref[...])
     stores = [started(y_ref, y_hbm, sems, 7)]
-    loads[5].wait()
+    loads[4].wait()
     g_ref[...] = dot(normed_ref[...], wg_ref[...]).astype(bf16)
     stores.append(started(g_ref, g_hbm, sems, 8))
     for copy in stores:
@@ -258,20 +260,24 @@
 
 
 def scan_kernel(parts_ref, decay_ref, out_ref):
-    count = parts_ref.shape[0]
+    count, z_size = parts_ref.shape[0], lax.axis_size("z")
+    y_size = count // z_size
+    spot = [(r % y_size) * z_size + r // y_size for r in range(count)]
     lifts = []
     for parity in range(2):
-        lift = parts_ref[parity, :, 2 * DK :].astype(f32)
+        lift = parts_ref[spot[parity], :, 2 * DK :].astype(f32)
         for r in range(parity + 2, count, 2):
-            lift = lift + parts_ref[r, :, 2 * DK :].astype(f32)
+            lift = lift + parts_ref[spot[r], :, 2 * DK :].astype(f32)
         lifts.append(lift)
     ahead = behind = jnp.concatenate(lifts, axis=1) * float(CTX_LIFT)
     for r in range(count):
         s = count - 1 - r
-        out_ref[r, :, 0:DK] = ahead.astype(bf16)
-        out_ref[s, :, DK:] = behind.astype(bf16)
-        ahead = decay_ref[r : r + 1, :] * ahead + parts_ref[r, :, 0:DK].astype(f32)
-        behind = decay_ref[s : s + 1, :] * behind + parts_ref[s, :, DK : 2 * DK].astype(f32)
+        out_ref[spot[r], :, 0:DK] = ahead.astype(bf16)
+        out_ref[spot[s], :, DK:] = behind.astype(bf16)
+        ahead = decay_ref[r : r + 1, :] * ahead + parts_ref[spot[r], :, 0:DK].astype(f32)
+        behind = (
+            decay_ref[s : s + 1, :] * behind + parts_ref[spot[s], :, DK : 2 * DK].astype(f32)
+        )
 
 
 def output_kernel(
@@ -338,7 +344,7 @@
     count, tp = lax.axis_size(SP), lax.axis_size(TP)
     (packed,) = kernel_call(
         prepare_kernel,
-        [("v", shaped(count, 3, columns, dtype=f32))],
+        [("v", shaped(count, 16, 128, dtype=f32))],
         "hhh",
         [
             pltpu.VMEM(w_modulate.shape, bf16),
@@ -369,21 +375,16 @@
     other_rows = [lax.ppermute(piece, "c", swap) for piece in own_rows]
     far = lax.ppermute(near, "y", [(0, 1), (1, 0), (2, 3), (3, 2)])
     seq_rows = count * rows // GRID_W
-    col, line, table = kernel_call(
+    col, line, row_table, column_table = kernel_call(
         functools.partial(tables_kernel, lines, x_size),
         [
             ("v", shaped(rows, 8, dtype=f32)),
             ("v", shaped(4, rows, dtype=f32)),
-            ("h", shaped(rows, 2 * DK, dtype=f32)),
+            ("v", shaped(x_size, 1, DK, dtype=f32)),
+            ("v", shaped(2 * lines, DK, dtype=f32)),
         ],
         "hhh",
-        [
-            pltpu.VMEM((1, rows), f32),
-            pltpu.VMEM((seq_rows, 1, DK), f32),
-            pltpu.VMEM((GRID_W, DK), f32),
-            pltpu.VMEM((rows, 2 * DK), f32),
-            sems((4,)),
-        ],
+        [pltpu.VMEM((1, rows), f32), sems((3 + x_size,))],
         8,
         1000000,
         later_decay,
@@ -396,22 +397,20 @@
     send, normed, key_rows, value_rows = kernel_call(
         keys_kernel,
         [
-            ("h", shaped(DV, lanes)),
+            ("v", shaped(DV, lanes)),
             ("h", shaped(rows, width)),
             ("h", shaped(rows, DK)),
             ("h", shaped(rows, DV)),
         ],
-        "hvvvvvvv" + "hvhhhvvvv",
+        "hvvvvvvv" + "hhhvvvvvvv",
         [
             pltpu.VMEM((lines, width), bf16),
             pltpu.VMEM(context.shape, bf16),
-            pltpu.VMEM((rows, 2 * DK), f32),
             pltpu.VMEM((width, DK), bf16),
             pltpu.VMEM((width, DV), bf16),
             pltpu.VMEM((rows + ctx, width), bf16),
             pltpu.VMEM((rows, DK), bf16),
             pltpu.VMEM((rows, DV), bf16),
-            pltpu.VMEM((DV, lanes), bf16),
             sems((9,)),
         ],
         32,
@@ -419,16 +418,17 @@
         *own_rows,
         *other_rows,
         near,
-        far,
-        table,
         w_key,
         w_value,
+        far,
         modulation,
         norm_gain[None],
         col,
         line,
-    )
-    parts = lax.all_to_all(send.reshape(count, DV // count, lanes), SP, 0, 0, tiled=True)
+        row_table,
+        column_table,
+    )
+    parts = lax.all_to_all(send.reshape(count, DV // count, lanes), YZ, 0, 0, tiled=True)
     queries, gates, inside = kernel_call(
         inside_kernel,
         [
@@ -436,14 +436,13 @@
             ("h", shaped(rows, DV)),
             ("h", shaped(rows, DV, dtype=f32)),
         ],
-        "hhhhhhvv",
+        "hhhhhvvvv",
         [
             pltpu.VMEM((rows, width), bf16),
             pltpu.VMEM((rows, DK), bf16),
             pltpu.VMEM((rows, DV), bf16),
             pltpu.VMEM((width, DK), bf16),
             pltpu.VMEM((width, DV), bf16),
-            pltpu.VMEM((rows, 2 * DK), f32),
             pltpu.VMEM((rows, DV), bf16),
             pltpu.VMEM((rows, DV), f32),
             sems((9,)),
@@ -455,9 +454,10 @@
         value_rows,
         w_query,
         w_gate,
-        table,
         col,
         line,
+        row_table,
+        column_table,
     )
     (entering,) = kernel_call(
         scan_kernel,
@@ -469,7 +469,7 @@
         parts,
         decays,
     )
-    states = lax.all_to_all(entering, SP, 0, 0, tiled=True).reshape(DV, 2 * DK)
+    states = lax.all_to_all(entering, YZ, 0, 0, tiled=True).reshape(DV, 2 * DK)
     partials = []
     for part in (1, 0):
         (partial,) = kernel_call(

time: 109 us -> 108 us (level)
  waiting for transfers between devices: 22.9 us -> 20.7 us
  Pallas kernels: 18.9 us -> 17.3 us
  starting transfers between devices: 41.5 us -> 42.9 us
    all_to_all x1, starting transfers between devices: 5.49 us -> 7.73 us  [per_device(): states = lax.all_to_all(entering, YZ, 0, 0, tiled=True).reshape(DV, 2 * DK)]
    pallas_call x9, Pallas kernels: 18.9 us -> 17.3 us  [kernel_call(): pl.pallas_call(body, out_shape=tuple((pltpu.HBM(a.shape, a.dtype) if k ==...]
    all_to_all x1, waiting for transfers between devices: 1.32 us -> 0.01 us  [per_device(): pieces = lax.all_to_all(packed, SP, 0, 0, tiled=True)]
    all_to_all x1, starting transfers between devices: 6.72 us -> 5.56 us  [per_device(): modulation = lax.all_to_all(spread, TP, 0, 0, tiled=True)]
  transfers between devices with their start and end apart: 15 -> 15, of which waited for: 6 -> 5; matrix products, arithmetic and copies ran while one was open for 1% -> 1% of each run, Pallas kernels for 8% -> 8%
where the time goes in v4:
time: 108 us; the launch traced here: 107 us
  starting transfers between devices  42.9 us (40%)
  blocking collectives  24.3 us (22%)
  waiting for transfers between devices  20.7 us (19%)
  Pallas kernels  17.3 us (16%)
    all_to_all x1, blocking collectives, per_device(): lax.all_to_all(send.reshape(count, DV // count, lanes), YZ, 0, 0, tiled=T...  24.3 us
    pallas_call x9, Pallas kernels, kernel_call(): pl.pallas_call(body, out_shape=tuple((pltpu.HBM(a.shape, a.dtype) if k ==...  17.3 us
    all_to_all x1, starting transfers between devices, per_device(): pieces = lax.all_to_all(packed, SP, 0, 0, tiled=True)  12 us
    all_to_all x1, waiting for transfers between devices, per_device(): states = lax.all_to_all(entering, YZ, 0, 0, tiled=True).reshape(DV, 2 * DK)  9.6 us
    all_to_all x1, starting transfers between devices, per_device(): states = lax.all_to_all(entering, YZ, 0, 0, tiled=True).reshape(DV, 2 * DK)  7.73 us
    ppermute x3, waiting for transfers between devices, per_device(): arrived = lax.ppermute(tiles[d], 'x', ring(x_size, -d))  7.28 us
    all_to_all x1, starting transfers between devices, per_device(): modulation = lax.all_to_all(spread, TP, 0, 0, tiled=True)  5.56 us
    ppermute x3, starting transfers between devices, per_device(): lax.ppermute(later, 'x', ring(x_size, d))  4.89 us
  transfers between devices with their start and end apart: 15, of which 5 were waited for; matrix products, arithmetic and copies ran while one was open for 1% of the time, Pallas kernels for 8%

profile of v4, /device:TPU:1, one launch (start us, length us, event | category | flops | bytes accessed | tf_op | source)
XLA Modules:
  0.0 106.9 jit_solution(4728749531321301325)
XLA Ops:
  0.0 1.8 %shard_map.136 = f32[32,16,128]{2,1,0:T(8,128)} custom-call(bf16[64,768]{1,0:T(8,128)(2,1)} %weights_hbm.1, bf16[2,2048]{1,0:T(2,128)(2,1)} %condition_hbm.1, f32[1,256]{1,0:T(1,128)} %bitcast.8), custom_call_target="tpu_custom_call" | custom-call | flops 1000000 | bytes 107520 | tf_op jit(solution)/shard_map/pallas_call | solution.py:35
  1.8 12.0 %all-to-all-start = ((f32[32,16,128]{2,1,0:T(8,128)}), f32[32,16,128]{2,1,0:T(8,128)S(1)}, u32[]{:S(2)}, u32[]{:S(2)}) async-start(f32[32,16,128]{2,1,0:T(8,128)} %shard_map.136), calls=%async_computation | async-start | bytes 524288 | tf_op jit(solution)/shard_map/all_to_all | solution.py:361
  13.9 1.3 %collective-permute-start = (bf16[32,2048]{1,0:T(8,128)(2,1)}, bf16[32,2048]{1,0:T(8,128)(2,1)S(1)}, u32[]{:S(2)}, u32[]{:S(2)}) collective-permute-start(bf16[32,2048]{1,0:T(8,128)(2,1)} %refs_0_), channel_id=1, source_target_pairs={{0,2},{2,4},{4,6},{6,0},{1,3},{3,5},{5,7},{7,1},{8,10},{10,12},{12... | collective-permute-start | bytes 393224 | tf_op jit(solution)/shard_map/ppermute | solution.py:374
  15.1 2.5 %collective-permute-start.1 = (bf16[32,2048]{1,0:T(8,128)(2,1)}, bf16[32,2048]{1,0:T(8,128)(2,1)S(1)}, u32[]{:S(2)}, u32[]{:S(2)}) collective-permute-start(bf16[32,2048]{1,0:T(8,128)(2,1)} %refs_0_), channel_id=1, source_target_pairs={{0,4},{2,6},{4,0},{6,2},{1,5},{3,7},{5,1},{7,3},{8,12},{10,14},{12... | collective-permute-start | bytes 393224 | tf_op jit(solution)/shard_map/ppermute | solution.py:374
  17.6 1.2 %collective-permute-start.2 = (bf16[32,2048]{1,0:T(8,128)(2,1)}, bf16[32,2048]{1,0:T(8,128)(2,1)S(1)}, u32[]{:S(2)}, u32[]{:S(2)}) collective-permute-start(bf16[32,2048]{1,0:T(8,128)(2,1)} %refs_0_), channel_id=1, source_target_pairs={{0,6},{2,0},{4,2},{6,4},{1,7},{3,1},{5,3},{7,5},{8,14},{10,8},{12,... | collective-permute-start | bytes 393224 | tf_op jit(solution)/shard_map/ppermute | solution.py:374
  18.7 1.8 %collective-permute-start.3 = (bf16[32,2048]{1,0:T(8,128)(2,1)}, bf16[32,2048]{1,0:T(8,128)(2,1)S(1)}, u32[]{:S(2)}, u32[]{:S(2)}) collective-permute-start(bf16[32,2048]{1,0:T(8,128)(2,1)} %refs_0_), channel_id=1, source_target_pairs={{0,1},{1,0},{2,3},{3,2},{4,5},{5,4},{6,7},{7,6},{8,9},{9,8},{10,11... | collective-permute-start | bytes 393224 | tf_op jit(solution)/shard_map/ppermute | solution.py:375
  20.5 0.0 collective-permute-done.refs_1_
  20.5 1.2 %collective-permute-start.4 = (bf16[32,2048]{1,0:T(8,128)(2,1)S(1)}, bf16[32,2048]{1,0:T(8,128)(2,1)S(1)}, u32[]{:S(2)}, u32[]{:S(2)}) collective-permute-start(bf16[32,2048]{1,0:T(8,128)(2,1)S(1)} %collective-permute-done.refs_1_), channel_id=1, source_target_pairs={{0,1},{1,0},{2,3},{3,2},{4,5},{5,4},{6,7},{7,6},{8,9},{9,8},{10,11... | collective-permute-start | bytes 393224 | tf_op jit(solution)/shard_map/ppermute | solution.py:375
  21.7 1.5 %collective-permute-done.1.refs_2_ = bf16[32,2048]{1,0:T(8,128)(2,1)S(1)} collective-permute-done((bf16[32,2048]{1,0:T(8,128)(2,1)}, bf16[32,2048]{1,0:T(8,128)(2,1)S(1)}, u32[]{:S(2)}, u32[]{:S(2)}) %collective-permute-start.1) | collective-permute-done | bytes 131104 | tf_op jit(solution)/shard_map/ppermute | solution.py:374
  23.2 1.8 %collective-permute-start.5 = (bf16[32,2048]{1,0:T(8,128)(2,1)S(1)}, bf16[32,2048]{1,0:T(8,128)(2,1)S(1)}, u32[]{:S(2)}, u32[]{:S(2)}) collective-permute-start(bf16[32,2048]{1,0:T(8,128)(2,1)S(1)} %collective-permute-done.1.refs_2_), channel_id=1, source_target_pairs={{0,1},{1,0},{2,3},{3,2},{4,5},{5,4},{6,7},{7,6},{8,9},{9,8},{10,11... | collective-permute-start | bytes 393224 | tf_op jit(solution)/shard_map/ppermute | solution.py:375
  25.1 0.0 collective-permute-done.2.refs_3_
  25.1 0.0 collective-permute-start.6
  25.1 1.3 %collective-permute-start.7 = (bf16[16,2048]{1,0:T(8,128)(2,1)}, bf16[16,2048]{1,0:T(8,128)(2,1)S(1)}, u32[]{:S(2)}, u32[]{:S(2)}) collective-permute-start(bf16[16,2048]{1,0:T(8,128)(2,1)} %refs_8_), channel_id=1, source_target_pairs={{0,8},{8,0},{16,24},{24,16},{1,9},{9,1},{17,25},{25,17},{2,10},{10... | collective-permute-start | bytes 196616 | tf_op jit(solution)/shard_map/ppermute | solution.py:376
  26.3 0.0 all-to-all-done.pieces_ref
  26.4 0.7 shard_map.137
  27.0 5.6 %all-to-all-start.1 = ((f32[8,2,768]{2,1,0:T(2,128)}), f32[8,2,768]{2,1,0:T(2,128)S(1)}, u32[]{:S(2)}, u32[]{:S(2)}) async-start(f32[8,2,768]{2,1,0:T(2,128)} %get-tuple-element.25), calls=%async_computation.1 | async-start | bytes 98304 | tf_op jit(solution)/shard_map/all_to_all | solution.py:371
  32.6 0.7 broadcast_in_dim.11.refs_13_
  33.3 1.8 %shard_map.138 = (f32[256,8]{1,0:T(8,128)S(1)}, f32[4,256]{1,0:T(4,128)S(1)}, f32[4,1,256]{2,1,0:T(1,128)S(1)}, f32[64,256]{1,0:T(8,128)S(1)}) custom-call(f32[1,256]{1,0:T(1,128)} %bitcast.9, f32[128,1,256]{2,1,0:T(1,128)} %constant.9.row_hbm, f32[64,256]{1,0:T(8,128)} %constant.5.clone.column_hbm), custom_call_target="tpu_custom_call" | custom-call | flops 1000000 | bytes 197632 | tf_op jit(solution)/shard_map/pallas_call | solution.py:35
  35.0 0.0 collective-permute-done.7.refs_11_
  35.0 0.0 collective-permute-done.3.refs_4_
  35.1 0.0 collective-permute-done.4.refs_5_
  35.1 0.0 collective-permute-done.5.refs_6_
  35.1 0.0 collective-permute-done.6.refs_7_
  35.1 2.3 %all-to-all-done.1.refs_12_ = f32[8,2,768]{2,1,0:T(2,128)S(1)} async-done(((f32[8,2,768]{2,1,0:T(2,128)}), f32[8,2,768]{2,1,0:T(2,128)S(1)}, u32[]{:S(2)}, u32[]{:S(2)}) %all-to-all-start.1) | async-done | bytes 49184 | tf_op jit(solution)/shard_map/all_to_all | solution.py:371
  37.4 4.2 %shard_map.139 = (bf16[512,640]{1,0:T(8,128)(2,1)S(1)}, bf16[256,2048]{1,0:T(8,128)(2,1)}, bf16[256,256]{1,0:T(8,128)(2,1)}, bf16[256,512]{1,0:T(8,128)(2,1)}) custom-call(bf16[32,2048]{1,0:T(8,128)(2,1)} %refs_0_, bf16[32,2048]{1,0:T(8,128)(2,1)S(1)} %collective-permute-done.refs_1_, bf16[32,2048]{1,0:T(8,128)(2,1)S(1)} %collective-permute-done.1.refs_2_, ...), custom_call_target="tpu_custom_call" | custom-call | flops 905969664 | bytes 4460544 | tf_op jit(solution)/shard_map/pallas_call | solution.py:35
  41.6 0.0 copy-start.2
  41.6 24.3 %all_to_all.20.parts_ref = bf16[32,16,640]{2,1,0:T(8,128)(2,1)S(1)} all-to-all(bf16[32,16,640]{2,1,0:T(8,128)(2,1)S(1)} %bitcast.6), channel_id=1, replica_groups=mesh['z'=8,'y'=4,'x'=4,'c'=2] {'y','z'}, dimensions={0} | all-to-all | bytes 1310720 | tf_op jit(solution)/shard_map/all_to_all | solution.py:431
  65.9 0.9 shard_map.141
  66.8 7.7 %all-to-all-start.3 = ((bf16[32,16,512]{2,1,0:T(8,128)(2,1)}), bf16[32,16,512]{2,1,0:T(8,128)(2,1)S(1)}, u32[]{:S(2)}, u32[]{:S(2)}) async-start(bf16[32,16,512]{2,1,0:T(8,128)(2,1)} %shard_map.141), calls=%async_computation.3 | async-start | bytes 1048576 | tf_op jit(solution)/shard_map/all_to_all | solution.py:472
  74.5 0.0 copy-done.2
  74.5 0.0 copy-start
  74.6 4.3 %shard_map.140 = (bf16[256,256]{1,0:T(8,128)(2,1)S(1)}, bf16[256,512]{1,0:T(8,128)(2,1)}, f32[256,512]{1,0:T(8,128)}) custom-call(bf16[256,2048]{1,0:T(8,128)(2,1)} %get-tuple-element.33.normed_hbm, bf16[256,256]{1,0:T(8,128)(2,1)} %get-tuple-element.34.k_hbm, bf16[256,512]{1,0:T(8,128)(2,1)} %get-tuple-element.35.v_hbm, bf16[2048,256]{1,0:T(8,128)(2,1)} %wq_hbm.1, ...), custom_call_target="tpu_custom_call" | custom-call | flops 805306368 | bytes 4669440 | tf_op jit(solution)/shard_map/pallas_call | solution.py:35
  78.9 9.6 %all-to-all-done.3 = bf16[32,16,512]{2,1,0:T(8,128)(2,1)S(1)} async-done(((bf16[32,16,512]{2,1,0:T(8,128)(2,1)}), bf16[32,16,512]{2,1,0:T(8,128)(2,1)S(1)}, u32[]{:S(2)}, u32[]{:S(2)}) %all-to-all-start.3) | async-done | bytes 524320 | tf_op jit(solution)/shard_map/all_to_all | solution.py:472
  88.5 0.0 copy-done
  88.5 1.7 %shard_map.143 = bf16[128,2048]{1,0:T(8,128)(2,1)S(1)} custom-call(f32[256,512]{1,0:T(8,128)} %get-tuple-element.36.y_hbm, bf16[256,512]{1,0:T(8,128)(2,1)} %get-tuple-element.37.g_hbm, bf16[256,256]{1,0:T(8,128)(2,1)S(1)} %get-tuple-element.38.q_ref, bf16[512,512]{1,0:T(8,128)(2,1)S(1)} %bitcast.4, f32[256,8]{1,0:T(8,128)S(1)} %get-tuple-element.29.refs_14_.col_ref, ...), custom_call_target="tpu_custom_call" | custom-call | flops 268435456 | bytes 3548160 | tf_op jit(solution)/shard_map/pallas_call | solution.py:35
  90.3 0.0 copy-start.1
  90.3 4.3 %collective-permute-start.8 = (bf16[128,2048]{1,0:T(8,128)(2,1)S(1)}, bf16[128,2048]{1,0:T(8,128)(2,1)S(1)}, u32[]{:S(2)}, u32[]{:S(2)}) collective-permute-start(bf16[128,2048]{1,0:T(8,128)(2,1)S(1)} %shard_map.143), channel_id=1, source_target_pairs={{0,1},{1,0},{2,3},{3,2},{4,5},{5,4},{6,7},{7,6},{8,9},{9,8},{10,11... | collective-permute-start | bytes 1572872 | tf_op jit(solution)/shard_map/ppermute | solution.py:491
  94.6 1.7 %shard_map.142.own_ref = bf16[128,2048]{1,0:T(8,128)(2,1)S(1)} custom-call(f32[256,512]{1,0:T(8,128)} %get-tuple-element.36.y_hbm, bf16[256,512]{1,0:T(8,128)(2,1)} %get-tuple-element.37.g_hbm, bf16[256,256]{1,0:T(8,128)(2,1)S(1)} %get-tuple-element.38.q_ref, bf16[512,512]{1,0:T(8,128)(2,1)S(1)} %bitcast.5, f32[256,8]{1,0:T(8,128)S(1)} %get-tuple-element.29.refs_14_.col_ref, ...), custom_call_target="tpu_custom_call" | custom-call | flops 268435456 | bytes 3548160 | tf_op jit(solution)/shard_map/pallas_call | solution.py:35
  96.4 0.0 collective-permute-done.8.crossed_ref
  96.4 0.1 shard_map.144
  96.5 1.0 collective-permute-start.10
  97.5 0.6 collective-permute-start.11
  98.1 0.8 collective-permute-start.9
  98.9 2.7 %collective-permute-done.10 = bf16[32,2048]{1,0:T(8,128)(2,1)S(1)} collective-permute-done((bf16[32,2048]{1,0:T(8,128)(2,1)S(1)}, bf16[32,2048]{1,0:T(8,128)(2,1)S(1)}, u32[]{:S(2)}, u32[]{:S(2)}) %collective-permute-start.10) | collective-permute-done | bytes 131104 | tf_op jit(solution)/shard_map/ppermute | solution.py:504
  101.5 4.6 %collective-permute-done.11 = bf16[32,2048]{1,0:T(8,128)(2,1)S(1)} collective-permute-done((bf16[32,2048]{1,0:T(8,128)(2,1)S(1)}, bf16[32,2048]{1,0:T(8,128)(2,1)S(1)}, u32[]{:S(2)}, u32[]{:S(2)}) %collective-permute-start.11) | collective-permute-done | bytes 131104 | tf_op jit(solution)/shard_map/ppermute | solution.py:504
  106.1 0.0 collective-permute-done.9
  106.1 0.0 copy-done.1
  106.1 0.8 add_convert_fusion
  (3 shorter events, 0.0 us)
Async XLA Ops:
  1.8 24.5 %all-to-all-start = ((f32[32,16,128]{2,1,0:T(8,128)}), f32[32,16,128]{2,1,0:T(8,128)S(1)}, u32[]{:S(2)}, u32[]{:S(2)}) async-start(f32[32,16,128]{2,1,0:T(8,128)} %shard_map.136), calls=%async_computation | async-start | bytes 524288 | tf_op jit(solution)/shard_map/all_to_all | solution.py:361
  13.9 6.7 %collective-permute-start = (bf16[32,2048]{1,0:T(8,128)(2,1)}, bf16[32,2048]{1,0:T(8,128)(2,1)S(1)}, u32[]{:S(2)}, u32[]{:S(2)}) collective-permute-start(bf16[32,2048]{1,0:T(8,128)(2,1)} %refs_0_), channel_id=1, source_target_pairs={{0,2},{2,4},{4,6},{6,0},{1,3},{3,5},{5,7},{7,1},{8,10},{10,12},{12... | collective-permute-start | bytes 393224 | tf_op jit(solution)/shard_map/ppermute | solution.py:374
  15.1 8.1 %collective-permute-start.1 = (bf16[32,2048]{1,0:T(8,128)(2,1)}, bf16[32,2048]{1,0:T(8,128)(2,1)S(1)}, u32[]{:S(2)}, u32[]{:S(2)}) collective-permute-start(bf16[32,2048]{1,0:T(8,128)(2,1)} %refs_0_), channel_id=1, source_target_pairs={{0,4},{2,6},{4,0},{6,2},{1,5},{3,7},{5,1},{7,3},{8,12},{10,14},{12... | collective-permute-start | bytes 393224 | tf_op jit(solution)/shard_map/ppermute | solution.py:374
  17.6 7.5 %collective-permute-start.2 = (bf16[32,2048]{1,0:T(8,128)(2,1)}, bf16[32,2048]{1,0:T(8,128)(2,1)S(1)}, u32[]{:S(2)}, u32[]{:S(2)}) collective-permute-start(bf16[32,2048]{1,0:T(8,128)(2,1)} %refs_0_), channel_id=1, source_target_pairs={{0,6},{2,0},{4,2},{6,4},{1,7},{3,1},{5,3},{7,5},{8,14},{10,8},{12,... | collective-permute-start | bytes 393224 | tf_op jit(solution)/shard_map/ppermute | solution.py:374
  18.7 16.3 %collective-permute-start.3 = (bf16[32,2048]{1,0:T(8,128)(2,1)}, bf16[32,2048]{1,0:T(8,128)(2,1)S(1)}, u32[]{:S(2)}, u32[]{:S(2)}) collective-permute-start(bf16[32,2048]{1,0:T(8,128)(2,1)} %refs_0_), channel_id=1, source_target_pairs={{0,1},{1,0},{2,3},{3,2},{4,5},{5,4},{6,7},{7,6},{8,9},{9,8},{10,11... | collective-permute-start | bytes 393224 | tf_op jit(solution)/shard_map/ppermute | solution.py:375
  20.5 14.5 %collective-permute-start.4 = (bf16[32,2048]{1,0:T(8,128)(2,1)S(1)}, bf16[32,2048]{1,0:T(8,128)(2,1)S(1)}, u32[]{:S(2)}, u32[]{:S(2)}) collective-permute-start(bf16[32,2048]{1,0:T(8,128)(2,1)S(1)} %collective-permute-done.refs_1_), channel_id=1, source_target_pairs={{0,1},{1,0},{2,3},{3,2},{4,5},{5,4},{6,7},{7,6},{8,9},{9,8},{10,11... | collective-permute-start | bytes 393224 | tf_op jit(solution)/shard_map/ppermute | solution.py:375
  23.2 11.8 %collective-permute-start.5 = (bf16[32,2048]{1,0:T(8,128)(2,1)S(1)}, bf16[32,2048]{1,0:T(8,128)(2,1)S(1)}, u32[]{:S(2)}, u32[]{:S(2)}) collective-permute-start(bf16[32,2048]{1,0:T(8,128)(2,1)S(1)} %collective-permute-done.1.refs_2_), channel_id=1, source_target_pairs={{0,1},{1,0},{2,3},{3,2},{4,5},{5,4},{6,7},{7,6},{8,9},{9,8},{10,11... | collective-permute-start | bytes 393224 | tf_op jit(solution)/shard_map/ppermute | solution.py:375
  25.1 10.0 %collective-permute-start.6 = (bf16[32,2048]{1,0:T(8,128)(2,1)S(1)}, bf16[32,2048]{1,0:T(8,128)(2,1)S(1)}, u32[]{:S(2)}, u32[]{:S(2)}) collective-permute-start(bf16[32,2048]{1,0:T(8,128)(2,1)S(1)} %collective-permute-done.2.refs_3_), channel_id=1, source_target_pairs={{0,1},{1,0},{2,3},{3,2},{4,5},{5,4},{6,7},{7,6},{8,9},{9,8},{10,11... | collective-permute-start | bytes 393224 | tf_op jit(solution)/shard_map/ppermute | solution.py:375
  25.1 10.0 %collective-permute-start.7 = (bf16[16,2048]{1,0:T(8,128)(2,1)}, bf16[16,2048]{1,0:T(8,128)(2,1)S(1)}, u32[]{:S(2)}, u32[]{:S(2)}) collective-permute-start(bf16[16,2048]{1,0:T(8,128)(2,1)} %refs_8_), channel_id=1, source_target_pairs={{0,8},{8,0},{16,24},{24,16},{1,9},{9,1},{17,25},{25,17},{2,10},{10... | collective-permute-start | bytes 196616 | tf_op jit(solution)/shard_map/ppermute | solution.py:376
  27.0 10.3 %all-to-all-start.1 = ((f32[8,2,768]{2,1,0:T(2,128)}), f32[8,2,768]{2,1,0:T(2,128)S(1)}, u32[]{:S(2)}, u32[]{:S(2)}) async-start(f32[8,2,768]{2,1,0:T(2,128)} %get-tuple-element.25), calls=%async_computation.1 | async-start | bytes 98304 | tf_op jit(solution)/shard_map/all_to_all | solution.py:371
  41.6 33.0 %copy-start.2 = (bf16[512]{0:T(512)(128)(2,1)S(1)}, bf16[512]{0:T(512)(128)(2,1)}, u32[]{:S(2)}) copy-start(bf16[512]{0:T(512)(128)(2,1)} %param.24) | copy-start | bytes 3076
  66.8 21.7 %all-to-all-start.3 = ((bf16[32,16,512]{2,1,0:T(8,128)(2,1)}), bf16[32,16,512]{2,1,0:T(8,128)(2,1)S(1)}, u32[]{:S(2)}, u32[]{:S(2)}) async-start(bf16[32,16,512]{2,1,0:T(8,128)(2,1)} %shard_map.141), calls=%async_computation.3 | async-start | bytes 1048576 | tf_op jit(solution)/shard_map/all_to_all | solution.py:472
  74.5 14.0 %copy-start = (bf16[512,2048]{1,0:T(8,128)(2,1)S(1)}, bf16[512,2048]{1,0:T(8,128)(2,1)}, u32[]{:S(2)}) copy-start(bf16[512,2048]{1,0:T(8,128)(2,1)} %wo_ref.3) | copy-start | bytes 6291460
  90.3 15.9 %copy-start.1 = (bf16[32,2048]{1,0:T(8,128)(2,1)S(1)}, bf16[32,2048]{1,0:T(8,128)(2,1)}, u32[]{:S(2)}) copy-start(bf16[32,2048]{1,0:T(8,128)(2,1)} %refs_0_) | copy-start | bytes 393220
  90.3 6.1 %collective-permute-start.8 = (bf16[128,2048]{1,0:T(8,128)(2,1)S(1)}, bf16[128,2048]{1,0:T(8,128)(2,1)S(1)}, u32[]{:S(2)}, u32[]{:S(2)}) collective-permute-start(bf16[128,2048]{1,0:T(8,128)(2,1)S(1)} %shard_map.143), channel_id=1, source_target_pairs={{0,1},{1,0},{2,3},{3,2},{4,5},{5,4},{6,7},{7,6},{8,9},{9,8},{10,11... | collective-permute-start | bytes 1572872 | tf_op jit(solution)/shard_map/ppermute | solution.py:491
  96.5 5.0 %collective-permute-start.10 = (bf16[32,2048]{1,0:T(8,128)(2,1)S(1)}, bf16[32,2048]{1,0:T(8,128)(2,1)S(1)}, u32[]{:S(2)}, u32[]{:S(2)}) collective-permute-start(bf16[32,2048]{1,0:T(8,128)(2,1)S(1)} %get-tuple-element.43), channel_id=1, source_target_pairs={{0,6},{2,0},{4,2},{6,4},{1,7},{3,1},{5,3},{7,5},{8,14},{10,8},{12,... | collective-permute-start | bytes 393224 | tf_op jit(solution)/shard_map/ppermute | solution.py:504
  97.5 8.6 %collective-permute-start.11 = (bf16[32,2048]{1,0:T(8,128)(2,1)S(1)}, bf16[32,2048]{1,0:T(8,128)(2,1)S(1)}, u32[]{:S(2)}, u32[]{:S(2)}) collective-permute-start(bf16[32,2048]{1,0:T(8,128)(2,1)S(1)} %get-tuple-element.44), channel_id=1, source_target_pairs={{0,2},{2,4},{4,6},{6,0},{1,3},{3,5},{5,7},{7,1},{8,10},{10,12},{12... | collective-permute-start | bytes 393224 | tf_op jit(solution)/shard_map/ppermute | solution.py:504
  98.1 8.1 %collective-permute-start.9 = (bf16[32,2048]{1,0:T(8,128)(2,1)S(1)}, bf16[32,2048]{1,0:T(8,128)(2,1)S(1)}, u32[]{:S(2)}, u32[]{:S(2)}) collective-permute-start(bf16[32,2048]{1,0:T(8,128)(2,1)S(1)} %get-tuple-element.42), channel_id=1, source_target_pairs={{0,4},{2,6},{4,0},{6,2},{1,5},{3,7},{5,1},{7,3},{8,12},{10,14},{12... | collective-permute-start | bytes 393224 | tf_op jit(solution)/shard_map/ppermute | solution.py:504

commit v5 on v4

--- a/solution.py
+++ b/solution.py
@@ -47,6 +47,11 @@
     copy = pltpu.make_async_copy(source, target, sems.at[slot])
     copy.start()
     return copy
+
+
+def flat_gain(gain_ref):
+    wide = gain_ref[...].astype(f32)
+    return jnp.concatenate([wide[i : i + 1, :] for i in range(wide.shape[0])], axis=1)
 
 
 def dot(a, b):
@@ -92,8 +97,12 @@
     part = dot(activated, weights_ref[...])
     cuts = part.shape[1] // 128
     packed = [part[i : i + 1, k * 128 : (k + 1) * 128] for i in range(2) for k in range(cuts)]
-    spare = out_ref.shape[1] - len(packed)
-    packed = jnp.concatenate(packed + [jnp.broadcast_to(total, (spare, 128))], axis=0)
+    rest = total
+    while len(packed) < out_ref.shape[1]:
+        term = rest.astype(bf16).astype(f32)
+        packed.append(jnp.broadcast_to(term, (1, 128)))
+        rest = rest - term
+    packed = jnp.concatenate(packed, axis=0).astype(bf16)
     for r in range(out_ref.shape[0]):
         out_ref[r] = packed
 
@@ -154,37 +163,38 @@
 
 def gather_kernel(pieces_ref, out_ref, decay_ref):
     cuts = out_ref.shape[2] // 128
-    summed = pieces_ref[0]
-    for r in range(1, pieces_ref.shape[0]):
-        summed = summed + pieces_ref[r]
+    pieces = [pieces_ref[r].astype(f32) for r in range(pieces_ref.shape[0])]
+    summed = functools.reduce(jnp.add, pieces)
     rows = [
         jnp.concatenate([summed[i * cuts + k : i * cuts + k + 1, :] for k in range(cuts)], axis=1)
         for i in range(2)
     ]
     for t in range(out_ref.shape[0]):
         out_ref[t] = jnp.concatenate(rows, axis=0)
-    for r in range(pieces_ref.shape[0]):
-        decay = jnp.exp(pieces_ref[r, 2 * cuts : 2 * cuts + 1, :])
+    for r, piece in enumerate(pieces):
+        decay = jnp.exp(jnp.sum(piece[2 * cuts :, :], axis=0, keepdims=True))
         decay_ref[r : r + 1, :] = jnp.concatenate([decay, decay], axis=1)
 
 
 def keys_kernel(*refs):
     pieces, refs = refs[:8], refs[8:]
     (
-        near_hbm, wk_hbm, wv_hbm, far_ref, mod_ref, gain_ref, col_ref, line_ref, row_ref,
+        near_hbm, wk_hbm, wv_hbm, gain_hbm, far_ref, mod_ref, col_ref, line_ref, row_ref,
         column_ref,
-        send_ref, normed_hbm, k_hbm, v_hbm,
-        own_ref, near_ref, wk_ref, wv_ref, normed_ref, k_ref, v_ref, sems,
+        send_ref, normed_hbm, k_ref, v_ref,
+        own_ref, near_ref, gain_ref, wk_ref, wv_ref, normed_ref, sems,
     ) = refs
     lines, width = pieces[0].shape
     rows = 8 * lines
     near = near_ref.shape[0]
+    load_gain = started(gain_hbm, gain_ref, sems, 5)
     own = [started(pieces[0], own_ref, sems, 7), started(near_hbm, near_ref, sems, 8)]
     loads = [
-        started(wv_hbm, wv_ref, sems, 0),
-        started(wk_hbm, wk_ref, sems, 1),
+        started(wk_hbm, wk_ref, sems, 0),
+        started(wv_hbm, wv_ref, sems, 1),
     ]
-    gain = gain_ref[...].astype(f32)
+    load_gain.wait()
+    gain = flat_gain(gain_ref)
     tp = mod_ref.shape[0]
 
     def modulated(values, which):
@@ -203,15 +213,13 @@
     normed_ref[rows : rows + near, :] = modulated(near_ref[...], 1)
     stores = [started(normed_ref.at[0:rows], normed_hbm, sems, 2)]
     loads[0].wait()
+    keys = dot(normed_ref[...], wk_ref[...])
+    loads[1].wait()
     values = dot(normed_ref[...], wv_ref[...]).astype(bf16)
     v_ref[...] = values[:rows]
-    stores.append(started(v_ref, v_hbm, sems, 3))
-    loads[1].wait()
-    keys = dot(normed_ref[...], wk_ref[...])
     key_rows = (turn(keys[:rows], row_ref, column_ref) * DK ** (-0.5)).astype(bf16)
     ctx_keys = (keys[rows:] * DK ** (-0.5)).astype(bf16)
     k_ref[...] = key_rows
-    stores.append(started(k_ref, k_hbm, sems, 4))
     wide = key_rows.astype(f32)
     ahead = (wide * jnp.exp(col_ref[:, 0:1])).astype(bf16)
     behind = (wide * jnp.exp(col_ref[:, 1:2])).astype(bf16)
@@ -228,16 +236,13 @@
 
 
 def inside_kernel(
-    normed_hbm, k_hbm, v_hbm, wq_hbm, wg_hbm, col_ref, line_ref, row_ref, column_ref,
+    normed_hbm, wq_hbm, wg_hbm, k_ref, v_ref, col_ref, line_ref, row_ref, column_ref,
     q_ref, g_hbm, y_hbm,
-    normed_ref, k_ref, v_ref, wq_ref, wg_ref, g_ref, y_ref, sems,
+    normed_ref, wq_ref, wg_ref, g_ref, y_ref, sems,
 ):
-    pairs = [
-        (normed_hbm, normed_ref), (wq_hbm, wq_ref), (k_hbm, k_ref), (v_hbm, v_ref),
-        (wg_hbm, wg_ref),
-    ]
+    pairs = [(normed_hbm, normed_ref), (wq_hbm, wq_ref), (wg_hbm, wg_ref)]
     loads = [started(a, b, sems, i) for i, (a, b) in enumerate(pairs)]
-    for copy in loads[:3]:
+    for copy in loads[:2]:
         copy.wait()
     queries = turn(dot(normed_ref[...], wq_ref[...]), row_ref, column_ref).astype(bf16)
     q_ref[...] = queries
@@ -249,12 +254,11 @@
         line_ref[1:2, :] - col_ref[:, 1:2],
     )
     weights = jnp.exp(gaps) * jnp.where(here == there, 2.0, 1.0)
-    loads[3].wait()
     y_ref[...] = dot((scores * weights).astype(bf16), v_ref[...])
-    stores = [started(y_ref, y_hbm, sems, 7)]
-    loads[4].wait()
+    stores = [started(y_ref, y_hbm, sems, 3)]
+    loads[2].wait()
     g_ref[...] = dot(normed_ref[...], wg_ref[...]).astype(bf16)
-    stores.append(started(g_ref, g_hbm, sems, 8))
+    stores.append(started(g_ref, g_hbm, sems, 4))
     for copy in stores:
         copy.wait()
 
@@ -299,7 +303,7 @@
     gates = g_ref[...].astype(f32)
     attended = (
         gates * jax.nn.sigmoid(gates) * (centred * lax.rsqrt(variance + epsilon))
-        * gain_ref[...].astype(f32)
+        * flat_gain(gain_ref)
     ).astype(bf16)
     out_ref[...] = dot(attended, wo_ref[...]).astype(bf16)
 
@@ -344,7 +348,7 @@
     count, tp = lax.axis_size(SP), lax.axis_size(TP)
     (packed,) = kernel_call(
         prepare_kernel,
-        [("v", shaped(count, 16, 128, dtype=f32))],
+        [("v", shaped(count, 16, 128))],
         "hhh",
         [
             pltpu.VMEM(w_modulate.shape, bf16),
@@ -399,18 +403,17 @@
         [
             ("v", shaped(DV, lanes)),
             ("h", shaped(rows, width)),
-            ("h", shaped(rows, DK)),
-            ("h", shaped(rows, DV)),
+            ("v", shaped(rows, DK)),
+            ("v", shaped(rows, DV)),
         ],
-        "hvvvvvvv" + "hhhvvvvvvv",
+        "hvvvvvvv" + "hhhhvvvvvv",
         [
             pltpu.VMEM((lines, width), bf16),
             pltpu.VMEM(context.shape, bf16),
+            pltpu.VMEM((width // 128, 128), bf16),
             pltpu.VMEM((width, DK), bf16),
             pltpu.VMEM((width, DV), bf16),
             pltpu.VMEM((rows + ctx, width), bf16),
-            pltpu.VMEM((rows, DK), bf16),
-            pltpu.VMEM((rows, DV), bf16),
             sems((9,)),
         ],
         32,
@@ -420,9 +423,9 @@
         near,
         w_key,
         w_value,
+        norm_gain.reshape(-1, 128),
         far,
         modulation,
-        norm_gain[None],
         col,
         line,
         row_table,
@@ -436,24 +439,22 @@
             ("h", shaped(rows, DV)),
             ("h", shaped(rows, DV, dtype=f32)),
         ],
-        "hhhhhvvvv",
+        "hhhvvvvvv",
         [
             pltpu.VMEM((rows, width), bf16),
-            pltpu.VMEM((rows, DK), bf16),
-            pltpu.VMEM((rows, DV), bf16),
             pltpu.VMEM((width, DK), bf16),
             pltpu.VMEM((width, DV), bf16),
             pltpu.VMEM((rows, DV), bf16),
             pltpu.VMEM((rows, DV), f32),
-            sems((9,)),
+            sems((5,)),
         ],
         32,
         2 * rows * width * (DK + DV),
         normed,
+        w_query,
+        w_gate,
         key_rows,
         value_rows,
-        w_query,
-        w_gate,
         col,
         line,
         row_table,
@@ -484,7 +485,7 @@
             queries,
             states,
             col,
-            group_gain[None],
+            group_gain.reshape(-1, 128),
             w_output,
         )
         partials.append(partial)

time: 108 us -> 107 us (level)
  starting transfers between devices: 42.9 us -> 41.5 us
  blocking collectives: 24.3 us -> 25.6 us
    all_to_all x1, blocking collectives: 24.3 us -> 25.6 us  [per_device(): lax.all_to_all(send.reshape(count, DV // count, lanes), YZ, 0, 0, tiled=T...]
    all_to_all x1, starting transfers between devices: 5.56 us -> 4.2 us  [per_device(): modulation = lax.all_to_all(spread, TP, 0, 0, tiled=True)]
  transfers between devices with their start and end apart: 15 -> 15, of which waited for: 5 -> 5; matrix products, arithmetic and copies ran while one was open for 1% -> 0% of each run, Pallas kernels for 8% -> 8%
where the time goes in v5:
time: 107 us; the launch traced here: 106 us
  starting transfers between devices  41.5 us (39%)
  blocking collectives  25.6 us (24%)
  waiting for transfers between devices  21.5 us (20%)
  Pallas kernels  16.6 us (16%)
    all_to_all x1, blocking collectives, per_device(): lax.all_to_all(send.reshape(count, DV // count, lanes), YZ, 0, 0, tiled=T...  25.6 us
    pallas_call x9, Pallas kernels, kernel_call(): pl.pallas_call(body, out_shape=tuple((pltpu.HBM(a.shape, a.dtype) if k ==...  16.6 us
    all_to_all x1, starting transfers between devices, per_device(): pieces = lax.all_to_all(packed, SP, 0, 0, tiled=True)  12 us
    all_to_all x1, waiting for transfers between devices, per_device(): states = lax.all_to_all(entering, YZ, 0, 0, tiled=True).reshape(DV, 2 * DK)  9.71 us
    all_to_all x1, starting transfers between devices, per_device(): states = lax.all_to_all(entering, YZ, 0, 0, tiled=True).reshape(DV, 2 * DK)  7.73 us
    ppermute x3, waiting for transfers between devices, per_device(): arrived = lax.ppermute(tiles[d], 'x', ring(x_size, -d))  7.28 us
    ppermute x3, starting transfers between devices, per_device(): lax.ppermute(later, 'x', ring(x_size, d))  4.89 us
    ppermute x4, starting transfers between devices, per_device(): other_rows = [lax.ppermute(piece, 'c', swap) for piece in own_rows]  4.77 us
  transfers between devices with their start and end apart: 15, of which 5 were waited for; matrix products, arithmetic and copies ran while one was open for 0% of the time, Pallas kernels for 8%

profile of v5, /device:TPU:1, one launch (start us, length us, event | category | flops | bytes accessed | tf_op | source)
XLA Modules:
  0.0 106.2 jit_solution(17500316672954666236)
XLA Ops:
  0.0 1.7 %shard_map.136 = bf16[32,16,128]{2,1,0:T(8,128)(2,1)} custom-call(bf16[64,768]{1,0:T(8,128)(2,1)} %weights_hbm.1, bf16[2,2048]{1,0:T(2,128)(2,1)} %condition_hbm.1, f32[1,256]{1,0:T(1,128)} %bitcast.12), custom_call_target="tpu_custom_call" | custom-call | flops 1000000 | bytes 107520 | tf_op jit(solution)/shard_map/pallas_call | solution.py:35
  1.8 12.0 %all-to-all-start = ((bf16[32,16,128]{2,1,0:T(8,128)(2,1)}), bf16[32,16,128]{2,1,0:T(8,128)(2,1)S(1)}, u32[]{:S(2)}, u32[]{:S(2)}) async-start(bf16[32,16,128]{2,1,0:T(8,128)(2,1)} %shard_map.136), calls=%async_computation | async-start | bytes 262144 | tf_op jit(solution)/shard_map/all_to_all | solution.py:365
  13.8 1.3 %collective-permute-start = (bf16[32,2048]{1,0:T(8,128)(2,1)}, bf16[32,2048]{1,0:T(8,128)(2,1)S(1)}, u32[]{:S(2)}, u32[]{:S(2)}) collective-permute-start(bf16[32,2048]{1,0:T(8,128)(2,1)} %refs_0_), channel_id=1, source_target_pairs={{0,2},{2,4},{4,6},{6,0},{1,3},{3,5},{5,7},{7,1},{8,10},{10,12},{12... | collective-permute-start | bytes 393224 | tf_op jit(solution)/shard_map/ppermute | solution.py:378
  15.1 2.5 %collective-permute-start.1 = (bf16[32,2048]{1,0:T(8,128)(2,1)}, bf16[32,2048]{1,0:T(8,128)(2,1)S(1)}, u32[]{:S(2)}, u32[]{:S(2)}) collective-permute-start(bf16[32,2048]{1,0:T(8,128)(2,1)} %refs_0_), channel_id=1, source_target_pairs={{0,4},{2,6},{4,0},{6,2},{1,5},{3,7},{5,1},{7,3},{8,12},{10,14},{12... | collective-permute-start | bytes 393224 | tf_op jit(solution)/shard_map/ppermute | solution.py:378
  17.5 1.2 %collective-permute-start.2 = (bf16[32,2048]{1,0:T(8,128)(2,1)}, bf16[32,2048]{1,0:T(8,128)(2,1)S(1)}, u32[]{:S(2)}, u32[]{:S(2)}) collective-permute-start(bf16[32,2048]{1,0:T(8,128)(2,1)} %refs_0_), channel_id=1, source_target_pairs={{0,6},{2,0},{4,2},{6,4},{1,7},{3,1},{5,3},{7,5},{8,14},{10,8},{12,... | collective-permute-start | bytes 393224 | tf_op jit(solution)/shard_map/ppermute | solution.py:378
  18.7 1.8 %collective-permute-start.3 = (bf16[32,2048]{1,0:T(8,128)(2,1)}, bf16[32,2048]{1,0:T(8,128)(2,1)S(1)}, u32[]{:S(2)}, u32[]{:S(2)}) collective-permute-start(bf16[32,2048]{1,0:T(8,128)(2,1)} %refs_0_), channel_id=1, source_target_pairs={{0,1},{1,0},{2,3},{3,2},{4,5},{5,4},{6,7},{7,6},{8,9},{9,8},{10,11... | collective-permute-start | bytes 393224 | tf_op jit(solution)/shard_map/ppermute | solution.py:379
  20.5 0.0 collective-permute-done.refs_1_
  20.5 1.2 %collective-permute-start.4 = (bf16[32,2048]{1,0:T(8,128)(2,1)S(1)}, bf16[32,2048]{1,0:T(8,128)(2,1)S(1)}, u32[]{:S(2)}, u32[]{:S(2)}) collective-permute-start(bf16[32,2048]{1,0:T(8,128)(2,1)S(1)} %collective-permute-done.refs_1_), channel_id=1, source_target_pairs={{0,1},{1,0},{2,3},{3,2},{4,5},{5,4},{6,7},{7,6},{8,9},{9,8},{10,11... | collective-permute-start | bytes 393224 | tf_op jit(solution)/shard_map/ppermute | solution.py:379
  21.7 1.5 %collective-permute-done.1.refs_2_ = bf16[32,2048]{1,0:T(8,128)(2,1)S(1)} collective-permute-done((bf16[32,2048]{1,0:T(8,128)(2,1)}, bf16[32,2048]{1,0:T(8,128)(2,1)S(1)}, u32[]{:S(2)}, u32[]{:S(2)}) %collective-permute-start.1) | collective-permute-done | bytes 131104 | tf_op jit(solution)/shard_map/ppermute | solution.py:378
  23.2 1.8 %collective-permute-start.5 = (bf16[32,2048]{1,0:T(8,128)(2,1)S(1)}, bf16[32,2048]{1,0:T(8,128)(2,1)S(1)}, u32[]{:S(2)}, u32[]{:S(2)}) collective-permute-start(bf16[32,2048]{1,0:T(8,128)(2,1)S(1)} %collective-permute-done.1.refs_2_), channel_id=1, source_target_pairs={{0,1},{1,0},{2,3},{3,2},{4,5},{5,4},{6,7},{7,6},{8,9},{9,8},{10,11... | collective-permute-start | bytes 393224 | tf_op jit(solution)/shard_map/ppermute | solution.py:379
  25.0 0.0 collective-permute-done.2.refs_3_
  25.0 0.0 collective-permute-start.6
  25.0 1.3 %collective-permute-start.7 = (bf16[16,2048]{1,0:T(8,128)(2,1)}, bf16[16,2048]{1,0:T(8,128)(2,1)S(1)}, u32[]{:S(2)}, u32[]{:S(2)}) collective-permute-start(bf16[16,2048]{1,0:T(8,128)(2,1)} %refs_8_), channel_id=1, source_target_pairs={{0,8},{8,0},{16,24},{24,16},{1,9},{9,1},{17,25},{25,17},{2,10},{10... | collective-permute-start | bytes 196616 | tf_op jit(solution)/shard_map/ppermute | solution.py:380
  26.3 0.0 all-to-all-done.pieces_ref
  26.3 0.7 shard_map.137
  27.0 4.2 %all-to-all-start.1 = ((f32[8,2,768]{2,1,0:T(2,128)}), f32[8,2,768]{2,1,0:T(2,128)S(1)}, u32[]{:S(2)}, u32[]{:S(2)}) async-start(f32[8,2,768]{2,1,0:T(2,128)} %get-tuple-element.25), calls=%async_computation.1 | async-start | bytes 98304 | tf_op jit(solution)/shard_map/all_to_all | solution.py:375
  31.2 1.8 %shard_map.138 = (f32[256,8]{1,0:T(8,128)S(1)}, f32[4,256]{1,0:T(4,128)S(1)}, f32[4,1,256]{2,1,0:T(1,128)S(1)}, f32[64,256]{1,0:T(8,128)S(1)}) custom-call(f32[1,256]{1,0:T(1,128)} %bitcast.13, f32[128,1,256]{2,1,0:T(1,128)} %constant.9.row_hbm, f32[64,256]{1,0:T(8,128)} %constant.5.clone.column_hbm), custom_call_target="tpu_custom_call" | custom-call | flops 1000000 | bytes 197632 | tf_op jit(solution)/shard_map/pallas_call | solution.py:35
  32.9 0.0 collective-permute-done.7.refs_12_
  32.9 0.0 collective-permute-done.3.refs_4_
  33.0 0.0 collective-permute-done.4.refs_5_
  33.0 0.0 collective-permute-done.5.refs_6_
  33.0 0.0 collective-permute-done.6.refs_7_
  33.0 3.0 %all-to-all-done.1.refs_13_ = f32[8,2,768]{2,1,0:T(2,128)S(1)} async-done(((f32[8,2,768]{2,1,0:T(2,128)}), f32[8,2,768]{2,1,0:T(2,128)S(1)}, u32[]{:S(2)}, u32[]{:S(2)}) %all-to-all-start.1) | async-done | bytes 49184 | tf_op jit(solution)/shard_map/all_to_all | solution.py:375
  36.0 3.6 %shard_map.139 = (bf16[512,640]{1,0:T(8,128)(2,1)S(1)}, bf16[256,2048]{1,0:T(8,128)(2,1)}, bf16[256,256]{1,0:T(8,128)(2,1)S(1)}, bf16[256,512]{1,0:T(8,128)(2,1)S(1)}) custom-call(bf16[32,2048]{1,0:T(8,128)(2,1)} %refs_0_, bf16[32,2048]{1,0:T(8,128)(2,1)S(1)} %collective-permute-done.refs_1_, bf16[32,2048]{1,0:T(8,128)(2,1)S(1)} %collective-permute-done.1.refs_2_, ...), custom_call_target="tpu_custom_call" | custom-call | flops 905969664 | bytes 4460544 | tf_op jit(solution)/shard_map/pallas_call | solution.py:35
  39.5 25.6 %all_to_all.20.parts_ref = bf16[32,16,640]{2,1,0:T(8,128)(2,1)S(1)} all-to-all(bf16[32,16,640]{2,1,0:T(8,128)(2,1)S(1)} %bitcast.8), channel_id=1, replica_groups=mesh['z'=8,'y'=4,'x'=4,'c'=2] {'y','z'}, dimensions={0} | all-to-all | bytes 1310720 | tf_op jit(solution)/shard_map/all_to_all | solution.py:434
  65.2 0.9 shard_map.141
  66.1 7.7 %all-to-all-start.3 = ((bf16[32,16,512]{2,1,0:T(8,128)(2,1)}), bf16[32,16,512]{2,1,0:T(8,128)(2,1)S(1)}, u32[]{:S(2)}, u32[]{:S(2)}) async-start(bf16[32,16,512]{2,1,0:T(8,128)(2,1)} %shard_map.141), calls=%async_computation.3 | async-start | bytes 1048576 | tf_op jit(solution)/shard_map/all_to_all | solution.py:473
  73.9 0.0 copy-start
  73.9 0.0 copy-start.1
  73.9 4.2 %shard_map.140 = (bf16[256,256]{1,0:T(8,128)(2,1)S(1)}, bf16[256,512]{1,0:T(8,128)(2,1)}, f32[256,512]{1,0:T(8,128)}) custom-call(bf16[256,2048]{1,0:T(8,128)(2,1)} %get-tuple-element.33.normed_hbm, bf16[2048,256]{1,0:T(8,128)(2,1)} %wq_hbm.1, bf16[2048,512]{1,0:T(8,128)(2,1)} %wg_hbm.1, bf16[256,256]{1,0:T(8,128)(2,1)S(1)} %get-tuple-element.34.k_ref, ...), custom_call_target="tpu_custom_call" | custom-call | flops 805306368 | bytes 4669440 | tf_op jit(solution)/shard_map/pallas_call | solution.py:35
  78.1 9.7 %all-to-all-done.3 = bf16[32,16,512]{2,1,0:T(8,128)(2,1)S(1)} async-done(((bf16[32,16,512]{2,1,0:T(8,128)(2,1)}), bf16[32,16,512]{2,1,0:T(8,128)(2,1)S(1)}, u32[]{:S(2)}, u32[]{:S(2)}) %all-to-all-start.3) | async-done | bytes 524320 | tf_op jit(solution)/shard_map/all_to_all | solution.py:473
  87.9 0.0 copy-done
  87.9 0.0 copy-done.1
  87.9 1.7 %shard_map.143 = bf16[128,2048]{1,0:T(8,128)(2,1)S(1)} custom-call(f32[256,512]{1,0:T(8,128)} %get-tuple-element.36.y_hbm, bf16[256,512]{1,0:T(8,128)(2,1)} %get-tuple-element.37.g_hbm, bf16[256,256]{1,0:T(8,128)(2,1)S(1)} %get-tuple-element.38.q_ref, bf16[512,512]{1,0:T(8,128)(2,1)S(1)} %bitcast.6, f32[256,8]{1,0:T(8,128)S(1)} %get-tuple-element.29.refs_14_.col_ref, ...), custom_call_target="tpu_custom_call" | custom-call | flops 268435456 | bytes 3548160 | tf_op jit(solution)/shard_map/pallas_call | solution.py:35
  89.6 0.0 copy-start.2
  89.6 4.3 %collective-permute-start.8 = (bf16[128,2048]{1,0:T(8,128)(2,1)S(1)}, bf16[128,2048]{1,0:T(8,128)(2,1)S(1)}, u32[]{:S(2)}, u32[]{:S(2)}) collective-permute-start(bf16[128,2048]{1,0:T(8,128)(2,1)S(1)} %shard_map.143), channel_id=1, source_target_pairs={{0,1},{1,0},{2,3},{3,2},{4,5},{5,4},{6,7},{7,6},{8,9},{9,8},{10,11... | collective-permute-start | bytes 1572872 | tf_op jit(solution)/shard_map/ppermute | solution.py:492
  94.0 1.7 %shard_map.142.own_ref = bf16[128,2048]{1,0:T(8,128)(2,1)S(1)} custom-call(f32[256,512]{1,0:T(8,128)} %get-tuple-element.36.y_hbm, bf16[256,512]{1,0:T(8,128)(2,1)} %get-tuple-element.37.g_hbm, bf16[256,256]{1,0:T(8,128)(2,1)S(1)} %get-tuple-element.38.q_ref, bf16[512,512]{1,0:T(8,128)(2,1)S(1)} %bitcast.7, f32[256,8]{1,0:T(8,128)S(1)} %get-tuple-element.29.refs_14_.col_ref, ...), custom_call_target="tpu_custom_call" | custom-call | flops 268435456 | bytes 3548160 | tf_op jit(solution)/shard_map/pallas_call | solution.py:35
  95.7 0.0 collective-permute-done.8.crossed_ref
  95.7 0.1 shard_map.144
  95.9 1.0 collective-permute-start.10
  96.8 0.6 collective-permute-start.11
  97.4 0.8 collective-permute-start.9
  98.2 2.7 %collective-permute-done.10 = bf16[32,2048]{1,0:T(8,128)(2,1)S(1)} collective-permute-done((bf16[32,2048]{1,0:T(8,128)(2,1)S(1)}, bf16[32,2048]{1,0:T(8,128)(2,1)S(1)}, u32[]{:S(2)}, u32[]{:S(2)}) %collective-permute-start.10) | collective-permute-done | bytes 131104 | tf_op jit(solution)/shard_map/ppermute | solution.py:505
  100.8 4.6 %collective-permute-done.11 = bf16[32,2048]{1,0:T(8,128)(2,1)S(1)} collective-permute-done((bf16[32,2048]{1,0:T(8,128)(2,1)S(1)}, bf16[32,2048]{1,0:T(8,128)(2,1)S(1)}, u32[]{:S(2)}, u32[]{:S(2)}) %collective-permute-start.11) | collective-permute-done | bytes 131104 | tf_op jit(solution)/shard_map/ppermute | solution.py:505
  105.5 0.0 collective-permute-done.9
  105.5 0.0 copy-done.2
  105.5 0.8 add_convert_fusion
  (2 shorter events, 0.0 us)
Async XLA Ops:
  1.8 24.5 %all-to-all-start = ((bf16[32,16,128]{2,1,0:T(8,128)(2,1)}), bf16[32,16,128]{2,1,0:T(8,128)(2,1)S(1)}, u32[]{:S(2)}, u32[]{:S(2)}) async-start(bf16[32,16,128]{2,1,0:T(8,128)(2,1)} %shard_map.136), calls=%async_computation | async-start | bytes 262144 | tf_op jit(solution)/shard_map/all_to_all | solution.py:365
  13.8 6.7 %collective-permute-start = (bf16[32,2048]{1,0:T(8,128)(2,1)}, bf16[32,2048]{1,0:T(8,128)(2,1)S(1)}, u32[]{:S(2)}, u32[]{:S(2)}) collective-permute-start(bf16[32,2048]{1,0:T(8,128)(2,1)} %refs_0_), channel_id=1, source_target_pairs={{0,2},{2,4},{4,6},{6,0},{1,3},{3,5},{5,7},{7,1},{8,10},{10,12},{12... | collective-permute-start | bytes 393224 | tf_op jit(solution)/shard_map/ppermute | solution.py:378
  15.1 8.1 %collective-permute-start.1 = (bf16[32,2048]{1,0:T(8,128)(2,1)}, bf16[32,2048]{1,0:T(8,128)(2,1)S(1)}, u32[]{:S(2)}, u32[]{:S(2)}) collective-permute-start(bf16[32,2048]{1,0:T(8,128)(2,1)} %refs_0_), channel_id=1, source_target_pairs={{0,4},{2,6},{4,0},{6,2},{1,5},{3,7},{5,1},{7,3},{8,12},{10,14},{12... | collective-permute-start | bytes 393224 | tf_op jit(solution)/shard_map/ppermute | solution.py:378
  17.5 7.5 %collective-permute-start.2 = (bf16[32,2048]{1,0:T(8,128)(2,1)}, bf16[32,2048]{1,0:T(8,128)(2,1)S(1)}, u32[]{:S(2)}, u32[]{:S(2)}) collective-permute-start(bf16[32,2048]{1,0:T(8,128)(2,1)} %refs_0_), channel_id=1, source_target_pairs={{0,6},{2,0},{4,2},{6,4},{1,7},{3,1},{5,3},{7,5},{8,14},{10,8},{12,... | collective-permute-start | bytes 393224 | tf_op jit(solution)/shard_map/ppermute | solution.py:378
  18.7 14.3 %collective-permute-start.3 = (bf16[32,2048]{1,0:T(8,128)(2,1)}, bf16[32,2048]{1,0:T(8,128)(2,1)S(1)}, u32[]{:S(2)}, u32[]{:S(2)}) collective-permute-start(bf16[32,2048]{1,0:T(8,128)(2,1)} %refs_0_), channel_id=1, source_target_pairs={{0,1},{1,0},{2,3},{3,2},{4,5},{5,4},{6,7},{7,6},{8,9},{9,8},{10,11... | collective-permute-start | bytes 393224 | tf_op jit(solution)/shard_map/ppermute | solution.py:379
  20.5 12.5 %collective-permute-start.4 = (bf16[32,2048]{1,0:T(8,128)(2,1)S(1)}, bf16[32,2048]{1,0:T(8,128)(2,1)S(1)}, u32[]{:S(2)}, u32[]{:S(2)}) collective-permute-start(bf16[32,2048]{1,0:T(8,128)(2,1)S(1)} %collective-permute-done.refs_1_), channel_id=1, source_target_pairs={{0,1},{1,0},{2,3},{3,2},{4,5},{5,4},{6,7},{7,6},{8,9},{9,8},{10,11... | collective-permute-start | bytes 393224 | tf_op jit(solution)/shard_map/ppermute | solution.py:379
  23.2 9.8 %collective-permute-start.5 = (bf16[32,2048]{1,0:T(8,128)(2,1)S(1)}, bf16[32,2048]{1,0:T(8,128)(2,1)S(1)}, u32[]{:S(2)}, u32[]{:S(2)}) collective-permute-start(bf16[32,2048]{1,0:T(8,128)(2,1)S(1)} %collective-permute-done.1.refs_2_), channel_id=1, source_target_pairs={{0,1},{1,0},{2,3},{3,2},{4,5},{5,4},{6,7},{7,6},{8,9},{9,8},{10,11... | collective-permute-start | bytes 393224 | tf_op jit(solution)/shard_map/ppermute | solution.py:379
  25.0 8.0 %collective-permute-start.6 = (bf16[32,2048]{1,0:T(8,128)(2,1)S(1)}, bf16[32,2048]{1,0:T(8,128)(2,1)S(1)}, u32[]{:S(2)}, u32[]{:S(2)}) collective-permute-start(bf16[32,2048]{1,0:T(8,128)(2,1)S(1)} %collective-permute-done.2.refs_3_), channel_id=1, source_target_pairs={{0,1},{1,0},{2,3},{3,2},{4,5},{5,4},{6,7},{7,6},{8,9},{9,8},{10,11... | collective-permute-start | bytes 393224 | tf_op jit(solution)/shard_map/ppermute | solution.py:379
  25.0 7.9 %collective-permute-start.7 = (bf16[16,2048]{1,0:T(8,128)(2,1)}, bf16[16,2048]{1,0:T(8,128)(2,1)S(1)}, u32[]{:S(2)}, u32[]{:S(2)}) collective-permute-start(bf16[16,2048]{1,0:T(8,128)(2,1)} %refs_8_), channel_id=1, source_target_pairs={{0,8},{8,0},{16,24},{24,16},{1,9},{9,1},{17,25},{25,17},{2,10},{10... | collective-permute-start | bytes 196616 | tf_op jit(solution)/shard_map/ppermute | solution.py:380
  27.0 9.0 %all-to-all-start.1 = ((f32[8,2,768]{2,1,0:T(2,128)}), f32[8,2,768]{2,1,0:T(2,128)S(1)}, u32[]{:S(2)}, u32[]{:S(2)}) async-start(f32[8,2,768]{2,1,0:T(2,128)} %get-tuple-element.25), calls=%async_computation.1 | async-start | bytes 98304 | tf_op jit(solution)/shard_map/all_to_all | solution.py:375
  66.1 21.7 %all-to-all-start.3 = ((bf16[32,16,512]{2,1,0:T(8,128)(2,1)}), bf16[32,16,512]{2,1,0:T(8,128)(2,1)S(1)}, u32[]{:S(2)}, u32[]{:S(2)}) async-start(bf16[32,16,512]{2,1,0:T(8,128)(2,1)} %shard_map.141), calls=%async_computation.3 | async-start | bytes 1048576 | tf_op jit(solution)/shard_map/all_to_all | solution.py:473
  73.9 14.0 %copy-start = (bf16[512,2048]{1,0:T(8,128)(2,1)S(1)}, bf16[512,2048]{1,0:T(8,128)(2,1)}, u32[]{:S(2)}) copy-start(bf16[512,2048]{1,0:T(8,128)(2,1)} %wo_ref.3) | copy-start | bytes 6291460
  73.9 14.0 %copy-start.1 = (bf16[512]{0:T(512)(128)(2,1)S(1)}, bf16[512]{0:T(512)(128)(2,1)}, u32[]{:S(2)}) copy-start(bf16[512]{0:T(512)(128)(2,1)} %param.24) | copy-start | bytes 3076
  89.6 15.9 %copy-start.2 = (bf16[32,2048]{1,0:T(8,128)(2,1)S(1)}, bf16[32,2048]{1,0:T(8,128)(2,1)}, u32[]{:S(2)}) copy-start(bf16[32,2048]{1,0:T(8,128)(2,1)} %refs_0_) | copy-start | bytes 393220
  89.6 6.1 %collective-permute-start.8 = (bf16[128,2048]{1,0:T(8,128)(2,1)S(1)}, bf16[128,2048]{1,0:T(8,128)(2,1)S(1)}, u32[]{:S(2)}, u32[]{:S(2)}) collective-permute-start(bf16[128,2048]{1,0:T(8,128)(2,1)S(1)} %shard_map.143), channel_id=1, source_target_pairs={{0,1},{1,0},{2,3},{3,2},{4,5},{5,4},{6,7},{7,6},{8,9},{9,8},{10,11... | collective-permute-start | bytes 1572872 | tf_op jit(solution)/shard_map/ppermute | solution.py:492
  95.9 5.0 %collective-permute-start.10 = (bf16[32,2048]{1,0:T(8,128)(2,1)S(1)}, bf16[32,2048]{1,0:T(8,128)(2,1)S(1)}, u32[]{:S(2)}, u32[]{:S(2)}) collective-permute-start(bf16[32,2048]{1,0:T(8,128)(2,1)S(1)} %get-tuple-element.43), channel_id=1, source_target_pairs={{0,6},{2,0},{4,2},{6,4},{1,7},{3,1},{5,3},{7,5},{8,14},{10,8},{12,... | collective-permute-start | bytes 393224 | tf_op jit(solution)/shard_map/ppermute | solution.py:505
  96.8 8.6 %collective-permute-start.11 = (bf16[32,2048]{1,0:T(8,128)(2,1)S(1)}, bf16[32,2048]{1,0:T(8,128)(2,1)S(1)}, u32[]{:S(2)}, u32[]{:S(2)}) collective-permute-start(bf16[32,2048]{1,0:T(8,128)(2,1)S(1)} %get-tuple-element.44), channel_id=1, source_target_pairs={{0,2},{2,4},{4,6},{6,0},{1,3},{3,5},{5,7},{7,1},{8,10},{10,12},{12... | collective-permute-start | bytes 393224 | tf_op jit(solution)/shard_map/ppermute | solution.py:505
  97.4 8.1 %collective-permute-start.9 = (bf16[32,2048]{1,0:T(8,128)(2,1)S(1)}, bf16[32,2048]{1,0:T(8,128)(2,1)S(1)}, u32[]{:S(2)}, u32[]{:S(2)}) collective-permute-start(bf16[32,2048]{1,0:T(8,128)(2,1)S(1)} %get-tuple-element.42), channel_id=1, source_target_pairs={{0,4},{2,6},{4,0},{6,2},{1,5},{3,7},{5,1},{7,3},{8,12},{10,14},{12... | collective-permute-start | bytes 393224 | tf_op jit(solution)/shard_map/ppermute | solution.py:505

commit v6 on v5

--- a/solution.py
+++ b/solution.py
@@ -77,15 +77,26 @@
 
 
 def prepare_kernel(
-    weights_hbm, condition_hbm, decay_hbm, out_ref, weights_ref, condition_ref, decay_ref, sems
+    lines, weights_hbm, condition_hbm, decay_hbm, row_hbm, column_hbm,
+    out_ref, decay_ref, row_ref, column_ref,
+    weights_ref, condition_ref, sems,
 ):
+    size, width = weights_hbm.shape[0], condition_hbm.shape[1]
+    seq = lax.axis_index("z") * lax.axis_size("y") + lax.axis_index("y")
+    chip, core = lax.axis_index("x"), lax.axis_index("c")
+    chips = row_ref.shape[0]
     loads = [
         started(condition_hbm, condition_ref, sems, 0),
         started(decay_hbm, decay_ref, sems, 1),
         started(weights_hbm, weights_ref, sems, 2),
     ]
-    size, width = weights_hbm.shape[0], condition_hbm.shape[1]
-    seq = lax.axis_index("z") * lax.axis_size("y") + lax.axis_index("y")
+    for h in range(2):
+        column = pl.multiple_of(((h + core) % 2) * lines, lines)
+        target = column_ref.at[h * lines : (h + 1) * lines]
+        loads.append(started(column_hbm.at[pl.ds(column, lines)], target, sems, 3 + h))
+    for d in range(chips):
+        row = seq * chips + (chip - d + chips) % chips
+        loads.append(started(row_hbm.at[row], row_ref.at[d], sems, 5 + d))
     loads[0].wait()
     values = condition_ref[...].astype(f32)
     values = jnp.concatenate([values] * 4, axis=0)
@@ -105,6 +116,8 @@
     packed = jnp.concatenate(packed, axis=0).astype(bf16)
     for r in range(out_ref.shape[0]):
         out_ref[r] = packed
+    for copy in loads[3:]:
+        copy.wait()
 
 
 def rotary_tables(count):
@@ -116,23 +129,9 @@
     return np.concatenate([np.cos(angles), np.sin(angles) * sign], axis=1)
 
 
-def tables_kernel(
-    lines, chips, decay_hbm, row_hbm, column_hbm,
-    col_ref, line_ref, row_ref, column_ref,
-    decay_ref, sems,
-):
+def tables_kernel(lines, chips, decay_ref, col_ref, line_ref):
     rows = 2 * chips * lines
-    seq = lax.axis_index("z") * lax.axis_size("y") + lax.axis_index("y")
     chip, core = lax.axis_index("x"), lax.axis_index("c")
-    started(decay_hbm, decay_ref, sems, 0).wait()
-    loads = []
-    for h in range(2):
-        column = pl.multiple_of(((h + core) % 2) * lines, lines)
-        target = column_ref.at[h * lines : (h + 1) * lines]
-        loads.append(started(column_hbm.at[pl.ds(column, lines)], target, sems, 1 + h))
-    for d in range(chips):
-        row = seq * chips + (chip - d + chips) % chips
-        loads.append(started(row_hbm.at[row], row_ref.at[d], sems, 3 + d))
 
     def position(local):
         origin = (chip - (local // lines) % chips + chips) % chips
@@ -157,8 +156,6 @@
     line_ref[2:3, :] = place_line.astype(f32)
     odd = lax.axis_index("y") % 2
     line_ref[3:4, :] = jnp.full((1, rows), odd, jnp.int32).astype(f32)
-    for copy in loads:
-        copy.wait()
 
 
 def gather_kernel(pieces_ref, out_ref, decay_ref):
@@ -189,10 +186,7 @@
     near = near_ref.shape[0]
     load_gain = started(gain_hbm, gain_ref, sems, 5)
     own = [started(pieces[0], own_ref, sems, 7), started(near_hbm, near_ref, sems, 8)]
-    loads = [
-        started(wk_hbm, wk_ref, sems, 0),
-        started(wv_hbm, wv_ref, sems, 1),
-    ]
+    loads = [started(wk_hbm, wk_ref, sems, 0), started(wv_hbm, wv_ref, sems, 1)]
     load_gain.wait()
     gain = flat_gain(gain_ref)
     tp = mod_ref.shape[0]
@@ -237,8 +231,8 @@
 
 def inside_kernel(
     normed_hbm, wq_hbm, wg_hbm, k_ref, v_ref, col_ref, line_ref, row_ref, column_ref,
-    q_ref, g_hbm, y_hbm,
-    normed_ref, wq_ref, wg_ref, g_ref, y_ref, sems,
+    q_ref, g_ref, y_ref,
+    normed_ref, wq_ref, wg_ref, sems,
 ):
     pairs = [(normed_hbm, normed_ref), (wq_hbm, wq_ref), (wg_hbm, wg_ref)]
     loads = [started(a, b, sems, i) for i, (a, b) in enumerate(pairs)]
@@ -254,13 +248,9 @@
         line_ref[1:2, :] - col_ref[:, 1:2],
     )
     weights = jnp.exp(gaps) * jnp.where(here == there, 2.0, 1.0)
-    y_ref[...] = dot((scores * weights).astype(bf16), v_ref[...])
-    stores = [started(y_ref, y_hbm, sems, 3)]
+    y_ref[...] = dot((scores * weights).astype(bf16), v_ref[...]).astype(bf16)
     loads[2].wait()
     g_ref[...] = dot(normed_ref[...], wg_ref[...]).astype(bf16)
-    stores.append(started(g_ref, g_hbm, sems, 4))
-    for copy in stores:
-        copy.wait()
 
 
 def scan_kernel(parts_ref, decay_ref, out_ref):
@@ -285,22 +275,20 @@
 
 
 def output_kernel(
-    part, y_hbm, g_hbm, q_ref, states_ref, col_ref, gain_ref, wo_ref, out_ref, y_ref, g_ref, sems
+    part, y_ref, g_ref, q_ref, states_ref, col_ref, gain_ref, wo_ref, out_ref
 ):
     half = out_ref.shape[0]
     own = slice(part * half, (part + 1) * half)
-    loads = [started(y_hbm.at[own], y_ref, sems, 0), started(g_hbm.at[own], g_ref, sems, 1)]
     queries = q_ref[own, :]
-    mixed = jnp.exp(col_ref[own, 2:3]) * dot_t(queries, states_ref[:, 0:DK]) + jnp.exp(
-        col_ref[own, 3:4]
-    ) * dot_t(queries, states_ref[:, DK:])
-    loads[0].wait()
-    mixed = mixed + y_ref[...]
+    mixed = (
+        y_ref[own, :].astype(f32)
+        + jnp.exp(col_ref[own, 2:3]) * dot_t(queries, states_ref[:, 0:DK])
+        + jnp.exp(col_ref[own, 3:4]) * dot_t(queries, states_ref[:, DK:])
+    )
     average = jnp.mean(mixed, axis=-1, keepdims=True)
     centred = mixed - average
     variance = jnp.mean(centred * centred, axis=-1, keepdims=True)
-    loads[1].wait()
-    gates = g_ref[...].astype(f32)
+    gates = g_ref[own, :].astype(f32)
     attended = (
         gates * jax.nn.sigmoid(gates) * (centred * lax.rsqrt(variance + epsilon))
         * flat_gain(gain_ref)
@@ -346,21 +334,27 @@
     columns = w_modulate.shape[1]
     sems = pltpu.SemaphoreType.DMA
     count, tp = lax.axis_size(SP), lax.axis_size(TP)
-    (packed,) = kernel_call(
-        prepare_kernel,
-        [("v", shaped(count, 16, 128))],
-        "hhh",
+    packed, decay_row, row_table, column_table = kernel_call(
+        functools.partial(prepare_kernel, lines),
+        [
+            ("v", shaped(count, 16, 128)),
+            ("v", shaped(1, rows, dtype=f32)),
+            ("v", shaped(x_size, 1, DK, dtype=f32)),
+            ("v", shaped(2 * lines, DK, dtype=f32)),
+        ],
+        "hhhhh",
         [
             pltpu.VMEM(w_modulate.shape, bf16),
             pltpu.VMEM(condition.shape, bf16),
-            pltpu.VMEM((1, rows), f32),
-            sems((3,)),
+            sems((5 + x_size,)),
         ],
         4,
         1000000,
         w_modulate,
         condition,
         log_decay.T,
+        jnp.asarray(rotary_tables(count * rows // GRID_W))[:, None],
+        jnp.asarray(rotary_tables(GRID_W)),
     )
     pieces = lax.all_to_all(packed, SP, 0, 0, tiled=True)
     spread, decays = kernel_call(
@@ -374,26 +368,18 @@
     )
     modulation = lax.all_to_all(spread, TP, 0, 0, tiled=True)
 
-    later, near, later_decay, _ = lax.optimization_barrier((latent, context, log_decay.T, packed))
+    later, near, _ = lax.optimization_barrier((latent, context, packed))
     own_rows = [later] + [lax.ppermute(later, "x", ring(x_size, d)) for d in range(1, x_size)]
     other_rows = [lax.ppermute(piece, "c", swap) for piece in own_rows]
     far = lax.ppermute(near, "y", [(0, 1), (1, 0), (2, 3), (3, 2)])
-    seq_rows = count * rows // GRID_W
-    col, line, row_table, column_table = kernel_call(
+    col, line = kernel_call(
         functools.partial(tables_kernel, lines, x_size),
-        [
-            ("v", shaped(rows, 8, dtype=f32)),
-            ("v", shaped(4, rows, dtype=f32)),
-            ("v", shaped(x_size, 1, DK, dtype=f32)),
-            ("v", shaped(2 * lines, DK, dtype=f32)),
-        ],
-        "hhh",
-        [pltpu.VMEM((1, rows), f32), sems((3 + x_size,))],
+        [("v", shaped(rows, 8, dtype=f32)), ("v", shaped(4, rows, dtype=f32))],
+        "v",
+        [],
         8,
         1000000,
-        later_decay,
-        jnp.asarray(rotary_tables(seq_rows))[:, None],
-        jnp.asarray(rotary_tables(GRID_W)),
+        decay_row,
     )
 
     ctx = 2 * context.shape[0]
@@ -436,17 +422,15 @@
         inside_kernel,
         [
             ("v", shaped(rows, DK)),
-            ("h", shaped(rows, DV)),
-            ("h", shaped(rows, DV, dtype=f32)),
+            ("v", shaped(rows, DV)),
+            ("v", shaped(rows, DV)),
         ],
         "hhhvvvvvv",
         [
             pltpu.VMEM((rows, width), bf16),
             pltpu.VMEM((width, DK), bf16),
             pltpu.VMEM((width, DV), bf16),
-            pltpu.VMEM((rows, DV), bf16),
-            pltpu.VMEM((rows, DV), f32),
-            sems((5,)),
+            sems((3,)),
         ],
         32,
         2 * rows * width * (DK + DV),
@@ -476,8 +460,8 @@
         (partial,) = kernel_call(
             functools.partial(output_kernel, part),
             [("v", shaped(half, width))],
-            "hhvvvvv",
-            [pltpu.VMEM((half, DV), f32), pltpu.VMEM((half, DV), bf16), sems((2,))],
+            "vvvvvvv",
+            [],
             32,
             2 * half * DV * width,
             inside,

time: 107 us -> 106 us (level)
  Pallas kernels: 16.6 us -> 12.8 us
  local copies, waits for them, and re-layouts: 0.04 us -> 1.89 us
    pallas_call x9, Pallas kernels: 16.6 us -> 12.8 us  [kernel_call(): pl.pallas_call(body, out_shape=tuple((pltpu.HBM(a.shape, a.dtype) if k ==...]
    unnamed x6 -> x14, local copies, waits for them, and re-layouts: 0.02 us -> 1.87 us
    all_to_all x1, waiting for transfers between devices: 2.97 us -> 4.37 us  [per_device(): modulation = lax.all_to_all(spread, TP, 0, 0, tiled=True)]
    all_to_all x1, waiting for transfers between devices: 9.71 us -> 8.58 us  [per_device(): states = lax.all_to_all(entering, YZ, 0, 0, tiled=True).reshape(DV, 2 * DK)]
  transfers between devices with their start and end apart: 15 -> 15, of which waited for: 5 -> 6; matrix products, arithmetic and copies ran while one was open for 0% -> 0% of each run, Pallas kernels for 8% -> 5%
where the time goes in v6:
time: 106 us; the launch traced here: 105 us
  starting transfers between devices  41.5 us (39%)
  blocking collectives  25.6 us (24%)
  waiting for transfers between devices  22.3 us (21%)
  Pallas kernels  12.8 us (12%)
  local copies, waits for them, and re-layouts  1.89 us (2%)
    all_to_all x1, blocking collectives, per_device(): lax.all_to_all(send.reshape(count, DV // count, lanes), YZ, 0, 0, tiled=T...  25.6 us
    pallas_call x9, Pallas kernels, kernel_call(): pl.pallas_call(body, out_shape=tuple((pltpu.HBM(a.shape, a.dtype) if k ==...  12.8 us
    all_to_all x1, starting transfers between devices, per_device(): pieces = lax.all_to_all(packed, SP, 0, 0, tiled=True)  12 us
    all_to_all x1, waiting for transfers between devices, per_device(): states = lax.all_to_all(entering, YZ, 0, 0, tiled=True).reshape(DV, 2 * DK)  8.58 us
    all_to_all x1, starting transfers between devices, per_device(): states = lax.all_to_all(entering, YZ, 0, 0, tiled=True).reshape(DV, 2 * DK)  7.73 us
    ppermute x3, waiting for transfers between devices, per_device(): arrived = lax.ppermute(tiles[d], 'x', ring(x_size, -d))  7.18 us
    ppermute x3, starting transfers between devices, per_device(): lax.ppermute(later, 'x', ring(x_size, d))  4.89 us
    ppermute x4, starting transfers between devices, per_device(): other_rows = [lax.ppermute(piece, 'c', swap) for piece in own_rows]  4.77 us
  transfers between devices with their start and end apart: 15, of which 6 were waited for; matrix products, arithmetic and copies ran while one was open for 0% of the time, Pallas kernels for 5%

profile of v6, /device:TPU:1, one launch (start us, length us, event | category | flops | bytes accessed | tf_op | source)
XLA Modules:
  0.0 105.1 jit_solution(14065343790190892139)
XLA Ops:
  0.0 1.8 %shard_map.136 = (bf16[32,16,128]{2,1,0:T(8,128)(2,1)}, f32[1,256]{1,0:T(1,128)S(1)}, f32[4,1,256]{2,1,0:T(1,128)S(1)}, f32[64,256]{1,0:T(8,128)S(1)}) custom-call(bf16[64,768]{1,0:T(8,128)(2,1)} %weights_hbm.1, bf16[2,2048]{1,0:T(2,128)(2,1)} %condition_hbm.1, f32[1,256]{1,0:T(1,128)} %bitcast.13, f32[128,1,256]{2,1,0:T(1,128)} %constant.9.row_hbm, ...), custom_call_target="tpu_custom_call" | custom-call | flops 1000000 | bytes 304128 | tf_op jit(solution)/shard_map/pallas_call | solution.py:35
  1.8 12.0 %all-to-all-start = ((bf16[32,16,128]{2,1,0:T(8,128)(2,1)}), bf16[32,16,128]{2,1,0:T(8,128)(2,1)S(1)}, u32[]{:S(2)}, u32[]{:S(2)}) async-start(bf16[32,16,128]{2,1,0:T(8,128)(2,1)} %get-tuple-element.26), calls=%async_computation | async-start | bytes 262144 | tf_op jit(solution)/shard_map/all_to_all | solution.py:359
  13.9 1.3 %collective-permute-start = (bf16[32,2048]{1,0:T(8,128)(2,1)}, bf16[32,2048]{1,0:T(8,128)(2,1)S(1)}, u32[]{:S(2)}, u32[]{:S(2)}) collective-permute-start(bf16[32,2048]{1,0:T(8,128)(2,1)} %refs_0_), channel_id=1, source_target_pairs={{0,2},{2,4},{4,6},{6,0},{1,3},{3,5},{5,7},{7,1},{8,10},{10,12},{12... | collective-permute-start | bytes 393224 | tf_op jit(solution)/shard_map/ppermute | solution.py:372
  15.2 2.5 %collective-permute-start.1 = (bf16[32,2048]{1,0:T(8,128)(2,1)}, bf16[32,2048]{1,0:T(8,128)(2,1)S(1)}, u32[]{:S(2)}, u32[]{:S(2)}) collective-permute-start(bf16[32,2048]{1,0:T(8,128)(2,1)} %refs_0_), channel_id=1, source_target_pairs={{0,4},{2,6},{4,0},{6,2},{1,5},{3,7},{5,1},{7,3},{8,12},{10,14},{12... | collective-permute-start | bytes 393224 | tf_op jit(solution)/shard_map/ppermute | solution.py:372
  17.6 1.2 %collective-permute-start.2 = (bf16[32,2048]{1,0:T(8,128)(2,1)}, bf16[32,2048]{1,0:T(8,128)(2,1)S(1)}, u32[]{:S(2)}, u32[]{:S(2)}) collective-permute-start(bf16[32,2048]{1,0:T(8,128)(2,1)} %refs_0_), channel_id=1, source_target_pairs={{0,6},{2,0},{4,2},{6,4},{1,7},{3,1},{5,3},{7,5},{8,14},{10,8},{12,... | collective-permute-start | bytes 393224 | tf_op jit(solution)/shard_map/ppermute | solution.py:372
  18.8 1.8 %collective-permute-start.3 = (bf16[32,2048]{1,0:T(8,128)(2,1)}, bf16[32,2048]{1,0:T(8,128)(2,1)S(1)}, u32[]{:S(2)}, u32[]{:S(2)}) collective-permute-start(bf16[32,2048]{1,0:T(8,128)(2,1)} %refs_0_), channel_id=1, source_target_pairs={{0,1},{1,0},{2,3},{3,2},{4,5},{5,4},{6,7},{7,6},{8,9},{9,8},{10,11... | collective-permute-start | bytes 393224 | tf_op jit(solution)/shard_map/ppermute | solution.py:373
  20.6 0.0 collective-permute-done.refs_1_
  20.6 1.2 %collective-permute-start.4 = (bf16[32,2048]{1,0:T(8,128)(2,1)S(1)}, bf16[32,2048]{1,0:T(8,128)(2,1)S(1)}, u32[]{:S(2)}, u32[]{:S(2)}) collective-permute-start(bf16[32,2048]{1,0:T(8,128)(2,1)S(1)} %collective-permute-done.refs_1_), channel_id=1, source_target_pairs={{0,1},{1,0},{2,3},{3,2},{4,5},{5,4},{6,7},{7,6},{8,9},{9,8},{10,11... | collective-permute-start | bytes 393224 | tf_op jit(solution)/shard_map/ppermute | solution.py:373
  21.7 1.5 %collective-permute-done.1.refs_2_ = bf16[32,2048]{1,0:T(8,128)(2,1)S(1)} collective-permute-done((bf16[32,2048]{1,0:T(8,128)(2,1)}, bf16[32,2048]{1,0:T(8,128)(2,1)S(1)}, u32[]{:S(2)}, u32[]{:S(2)}) %collective-permute-start.1) | collective-permute-done | bytes 131104 | tf_op jit(solution)/shard_map/ppermute | solution.py:372
  23.3 1.8 %collective-permute-start.5 = (bf16[32,2048]{1,0:T(8,128)(2,1)S(1)}, bf16[32,2048]{1,0:T(8,128)(2,1)S(1)}, u32[]{:S(2)}, u32[]{:S(2)}) collective-permute-start(bf16[32,2048]{1,0:T(8,128)(2,1)S(1)} %collective-permute-done.1.refs_2_), channel_id=1, source_target_pairs={{0,1},{1,0},{2,3},{3,2},{4,5},{5,4},{6,7},{7,6},{8,9},{9,8},{10,11... | collective-permute-start | bytes 393224 | tf_op jit(solution)/shard_map/ppermute | solution.py:373
  25.1 0.0 collective-permute-done.2.refs_3_
  25.1 0.0 collective-permute-start.6
  25.1 1.3 %collective-permute-start.7 = (bf16[16,2048]{1,0:T(8,128)(2,1)}, bf16[16,2048]{1,0:T(8,128)(2,1)S(1)}, u32[]{:S(2)}, u32[]{:S(2)}) collective-permute-start(bf16[16,2048]{1,0:T(8,128)(2,1)} %refs_8_), channel_id=1, source_target_pairs={{0,8},{8,0},{16,24},{24,16},{1,9},{9,1},{17,25},{25,17},{2,10},{10... | collective-permute-start | bytes 196616 | tf_op jit(solution)/shard_map/ppermute | solution.py:374
  26.4 0.0 all-to-all-done.pieces_ref
  26.4 0.7 shard_map.137
  27.0 4.2 %all-to-all-start.1 = ((f32[8,2,768]{2,1,0:T(2,128)}), f32[8,2,768]{2,1,0:T(2,128)S(1)}, u32[]{:S(2)}, u32[]{:S(2)}) async-start(f32[8,2,768]{2,1,0:T(2,128)} %get-tuple-element.27), calls=%async_computation.1 | async-start | bytes 98304 | tf_op jit(solution)/shard_map/all_to_all | solution.py:369
  31.2 0.4 shard_map.138
  31.6 0.0 collective-permute-done.7.refs_12_
  31.6 0.0 collective-permute-done.3.refs_4_
  31.6 0.0 collective-permute-done.4.refs_5_
  31.6 0.0 collective-permute-done.5.refs_6_
  31.6 0.0 collective-permute-done.6.refs_7_
  31.7 4.4 %all-to-all-done.1.refs_13_ = f32[8,2,768]{2,1,0:T(2,128)S(1)} async-done(((f32[8,2,768]{2,1,0:T(2,128)}), f32[8,2,768]{2,1,0:T(2,128)S(1)}, u32[]{:S(2)}, u32[]{:S(2)}) %all-to-all-start.1) | async-done | bytes 49184 | tf_op jit(solution)/shard_map/all_to_all | solution.py:369
  36.0 3.6 %shard_map.139 = (bf16[512,640]{1,0:T(8,128)(2,1)S(1)}, bf16[256,2048]{1,0:T(8,128)(2,1)}, bf16[256,256]{1,0:T(8,128)(2,1)S(1)}, bf16[256,512]{1,0:T(8,128)(2,1)S(1)}) custom-call(bf16[32,2048]{1,0:T(8,128)(2,1)} %refs_0_, bf16[32,2048]{1,0:T(8,128)(2,1)S(1)} %collective-permute-done.refs_1_, bf16[32,2048]{1,0:T(8,128)(2,1)S(1)} %collective-permute-done.1.refs_2_, ...), custom_call_target="tpu_custom_call" | custom-call | flops 905969664 | bytes 4460544 | tf_op jit(solution)/shard_map/pallas_call | solution.py:35
  39.6 0.0 copy-start.3
  39.6 25.6 %all_to_all.20.parts_ref = bf16[32,16,640]{2,1,0:T(8,128)(2,1)S(1)} all-to-all(bf16[32,16,640]{2,1,0:T(8,128)(2,1)S(1)} %bitcast.8), channel_id=1, replica_groups=mesh['z'=8,'y'=4,'x'=4,'c'=2] {'y','z'}, dimensions={0} | all-to-all | bytes 1310720 | tf_op jit(solution)/shard_map/all_to_all | solution.py:420
  65.3 0.0 copy-done.3
  65.3 1.0 shard_map.141
  66.2 7.7 %all-to-all-start.3 = ((bf16[32,16,512]{2,1,0:T(8,128)(2,1)}), bf16[32,16,512]{2,1,0:T(8,128)(2,1)S(1)}, u32[]{:S(2)}, u32[]{:S(2)}) async-start(bf16[32,16,512]{2,1,0:T(8,128)(2,1)} %shard_map.141), calls=%async_computation.3 | async-start | bytes 1048576 | tf_op jit(solution)/shard_map/all_to_all | solution.py:457
  74.0 0.0 copy-done.1
  74.0 0.0 copy-start.2
  74.0 0.9 copy-done.2
  74.9 0.9 copy-done.4
  75.8 3.5 %shard_map.140 = (bf16[256,256]{1,0:T(8,128)(2,1)S(1)}, bf16[256,512]{1,0:T(8,128)(2,1)S(1)}, bf16[256,512]{1,0:T(8,128)(2,1)S(1)}) custom-call(bf16[256,2048]{1,0:T(8,128)(2,1)} %get-tuple-element.35.normed_hbm, bf16[2048,256]{1,0:T(8,128)(2,1)} %wq_hbm.1, bf16[2048,512]{1,0:T(8,128)(2,1)} %wg_hbm.1, bf16[256,256]{1,0:T(8,128)(2,1)S(1)} %copy-done.4, ...), custom_call_target="tpu_custom_call" | custom-call | flops 805306368 | bytes 4669440 | tf_op jit(solution)/shard_map/pallas_call | solution.py:35
  79.4 8.6 %all-to-all-done.3 = bf16[32,16,512]{2,1,0:T(8,128)(2,1)S(1)} async-done(((bf16[32,16,512]{2,1,0:T(8,128)(2,1)}), bf16[32,16,512]{2,1,0:T(8,128)(2,1)S(1)}, u32[]{:S(2)}, u32[]{:S(2)}) %all-to-all-start.3) | async-done | bytes 524320 | tf_op jit(solution)/shard_map/all_to_all | solution.py:457
  88.0 0.9 shard_map.143
  88.9 0.0 copy-start.6
  88.9 4.3 %collective-permute-start.8 = (bf16[128,2048]{1,0:T(8,128)(2,1)S(1)}, bf16[128,2048]{1,0:T(8,128)(2,1)S(1)}, u32[]{:S(2)}, u32[]{:S(2)}) collective-permute-start(bf16[128,2048]{1,0:T(8,128)(2,1)S(1)} %shard_map.143), channel_id=1, source_target_pairs={{0,1},{1,0},{2,3},{3,2},{4,5},{5,4},{6,7},{7,6},{8,9},{9,8},{10,11... | collective-permute-start | bytes 1572872 | tf_op jit(solution)/shard_map/ppermute | solution.py:476
  93.2 0.9 shard_map.142.own_ref
  94.1 0.6 collective-permute-done.8.crossed_ref
  94.7 0.1 shard_map.144
  94.9 1.0 collective-permute-start.10
  95.8 0.6 collective-permute-start.11
  96.4 0.7 collective-permute-start.9
  97.2 2.4 %collective-permute-done.10 = bf16[32,2048]{1,0:T(8,128)(2,1)S(1)} collective-permute-done((bf16[32,2048]{1,0:T(8,128)(2,1)S(1)}, bf16[32,2048]{1,0:T(8,128)(2,1)S(1)}, u32[]{:S(2)}, u32[]{:S(2)}) %collective-permute-start.10) | collective-permute-done | bytes 131104 | tf_op jit(solution)/shard_map/ppermute | solution.py:489
  99.6 4.7 %collective-permute-done.11 = bf16[32,2048]{1,0:T(8,128)(2,1)S(1)} collective-permute-done((bf16[32,2048]{1,0:T(8,128)(2,1)S(1)}, bf16[32,2048]{1,0:T(8,128)(2,1)S(1)}, u32[]{:S(2)}, u32[]{:S(2)}) %collective-permute-start.11) | collective-permute-done | bytes 131104 | tf_op jit(solution)/shard_map/ppermute | solution.py:489
  104.4 0.0 collective-permute-done.9
  104.4 0.8 add_convert_fusion
  (9 shorter events, 0.0 us)
Async XLA Ops:
  1.8 24.5 %all-to-all-start = ((bf16[32,16,128]{2,1,0:T(8,128)(2,1)}), bf16[32,16,128]{2,1,0:T(8,128)(2,1)S(1)}, u32[]{:S(2)}, u32[]{:S(2)}) async-start(bf16[32,16,128]{2,1,0:T(8,128)(2,1)} %get-tuple-element.26), calls=%async_computation | async-start | bytes 262144 | tf_op jit(solution)/shard_map/all_to_all | solution.py:359
  13.9 6.7 %collective-permute-start = (bf16[32,2048]{1,0:T(8,128)(2,1)}, bf16[32,2048]{1,0:T(8,128)(2,1)S(1)}, u32[]{:S(2)}, u32[]{:S(2)}) collective-permute-start(bf16[32,2048]{1,0:T(8,128)(2,1)} %refs_0_), channel_id=1, source_target_pairs={{0,2},{2,4},{4,6},{6,0},{1,3},{3,5},{5,7},{7,1},{8,10},{10,12},{12... | collective-permute-start | bytes 393224 | tf_op jit(solution)/shard_map/ppermute | solution.py:372
  15.2 8.1 %collective-permute-start.1 = (bf16[32,2048]{1,0:T(8,128)(2,1)}, bf16[32,2048]{1,0:T(8,128)(2,1)S(1)}, u32[]{:S(2)}, u32[]{:S(2)}) collective-permute-start(bf16[32,2048]{1,0:T(8,128)(2,1)} %refs_0_), channel_id=1, source_target_pairs={{0,4},{2,6},{4,0},{6,2},{1,5},{3,7},{5,1},{7,3},{8,12},{10,14},{12... | collective-permute-start | bytes 393224 | tf_op jit(solution)/shard_map/ppermute | solution.py:372
  17.6 7.5 %collective-permute-start.2 = (bf16[32,2048]{1,0:T(8,128)(2,1)}, bf16[32,2048]{1,0:T(8,128)(2,1)S(1)}, u32[]{:S(2)}, u32[]{:S(2)}) collective-permute-start(bf16[32,2048]{1,0:T(8,128)(2,1)} %refs_0_), channel_id=1, source_target_pairs={{0,6},{2,0},{4,2},{6,4},{1,7},{3,1},{5,3},{7,5},{8,14},{10,8},{12,... | collective-permute-start | bytes 393224 | tf_op jit(solution)/shard_map/ppermute | solution.py:372
  18.8 12.9 %collective-permute-start.3 = (bf16[32,2048]{1,0:T(8,128)(2,1)}, bf16[32,2048]{1,0:T(8,128)(2,1)S(1)}, u32[]{:S(2)}, u32[]{:S(2)}) collective-permute-start(bf16[32,2048]{1,0:T(8,128)(2,1)} %refs_0_), channel_id=1, source_target_pairs={{0,1},{1,0},{2,3},{3,2},{4,5},{5,4},{6,7},{7,6},{8,9},{9,8},{10,11... | collective-permute-start | bytes 393224 | tf_op jit(solution)/shard_map/ppermute | solution.py:373
  20.6 11.1 %collective-permute-start.4 = (bf16[32,2048]{1,0:T(8,128)(2,1)S(1)}, bf16[32,2048]{1,0:T(8,128)(2,1)S(1)}, u32[]{:S(2)}, u32[]{:S(2)}) collective-permute-start(bf16[32,2048]{1,0:T(8,128)(2,1)S(1)} %collective-permute-done.refs_1_), channel_id=1, source_target_pairs={{0,1},{1,0},{2,3},{3,2},{4,5},{5,4},{6,7},{7,6},{8,9},{9,8},{10,11... | collective-permute-start | bytes 393224 | tf_op jit(solution)/shard_map/ppermute | solution.py:373
  23.3 8.4 %collective-permute-start.5 = (bf16[32,2048]{1,0:T(8,128)(2,1)S(1)}, bf16[32,2048]{1,0:T(8,128)(2,1)S(1)}, u32[]{:S(2)}, u32[]{:S(2)}) collective-permute-start(bf16[32,2048]{1,0:T(8,128)(2,1)S(1)} %collective-permute-done.1.refs_2_), channel_id=1, source_target_pairs={{0,1},{1,0},{2,3},{3,2},{4,5},{5,4},{6,7},{7,6},{8,9},{9,8},{10,11... | collective-permute-start | bytes 393224 | tf_op jit(solution)/shard_map/ppermute | solution.py:373
  25.1 6.6 %collective-permute-start.6 = (bf16[32,2048]{1,0:T(8,128)(2,1)S(1)}, bf16[32,2048]{1,0:T(8,128)(2,1)S(1)}, u32[]{:S(2)}, u32[]{:S(2)}) collective-permute-start(bf16[32,2048]{1,0:T(8,128)(2,1)S(1)} %collective-permute-done.2.refs_3_), channel_id=1, source_target_pairs={{0,1},{1,0},{2,3},{3,2},{4,5},{5,4},{6,7},{7,6},{8,9},{9,8},{10,11... | collective-permute-start | bytes 393224 | tf_op jit(solution)/shard_map/ppermute | solution.py:373
  25.1 6.5 %collective-permute-start.7 = (bf16[16,2048]{1,0:T(8,128)(2,1)}, bf16[16,2048]{1,0:T(8,128)(2,1)S(1)}, u32[]{:S(2)}, u32[]{:S(2)}) collective-permute-start(bf16[16,2048]{1,0:T(8,128)(2,1)} %refs_8_), channel_id=1, source_target_pairs={{0,8},{8,0},{16,24},{24,16},{1,9},{9,1},{17,25},{25,17},{2,10},{10... | collective-permute-start | bytes 196616 | tf_op jit(solution)/shard_map/ppermute | solution.py:374
  27.0 9.0 %all-to-all-start.1 = ((f32[8,2,768]{2,1,0:T(2,128)}), f32[8,2,768]{2,1,0:T(2,128)S(1)}, u32[]{:S(2)}, u32[]{:S(2)}) async-start(f32[8,2,768]{2,1,0:T(2,128)} %get-tuple-element.27), calls=%async_computation.1 | async-start | bytes 98304 | tf_op jit(solution)/shard_map/all_to_all | solution.py:369
  39.6 25.7 %copy-start.3 = (bf16[256,256]{1,0:T(8,128)(2,1)}, bf16[256,256]{1,0:T(8,128)(2,1)S(1)}, u32[]{:S(2)}) copy-start(bf16[256,256]{1,0:T(8,128)(2,1)S(1)} %get-tuple-element.36.k_ref) | copy-start | bytes 393220
  39.6 34.4 %copy-start.1 = (bf16[256,512]{1,0:T(8,128)(2,1)}, bf16[256,512]{1,0:T(8,128)(2,1)S(1)}, u32[]{:S(2)}) copy-start(bf16[256,512]{1,0:T(8,128)(2,1)S(1)} %get-tuple-element.37.v_ref) | copy-start | bytes 786436
  66.2 21.7 %all-to-all-start.3 = ((bf16[32,16,512]{2,1,0:T(8,128)(2,1)}), bf16[32,16,512]{2,1,0:T(8,128)(2,1)S(1)}, u32[]{:S(2)}, u32[]{:S(2)}) async-start(bf16[32,16,512]{2,1,0:T(8,128)(2,1)} %shard_map.141), calls=%async_computation.3 | async-start | bytes 1048576 | tf_op jit(solution)/shard_map/all_to_all | solution.py:457
  74.0 1.0 copy-start.2
  74.9 0.9 copy-start.4
  75.8 12.1 %copy-start = (bf16[512,2048]{1,0:T(8,128)(2,1)S(1)}, bf16[512,2048]{1,0:T(8,128)(2,1)}, u32[]{:S(2)}) copy-start(bf16[512,2048]{1,0:T(8,128)(2,1)} %wo_ref.3) | copy-start | bytes 6291460
  75.8 12.1 %copy-start.5 = (bf16[512]{0:T(512)(128)(2,1)S(1)}, bf16[512]{0:T(512)(128)(2,1)}, u32[]{:S(2)}) copy-start(bf16[512]{0:T(512)(128)(2,1)} %param.24) | copy-start | bytes 3076
  88.9 15.5 %copy-start.6 = (bf16[32,2048]{1,0:T(8,128)(2,1)S(1)}, bf16[32,2048]{1,0:T(8,128)(2,1)}, u32[]{:S(2)}) copy-start(bf16[32,2048]{1,0:T(8,128)(2,1)} %refs_0_) | copy-start | bytes 393220
  88.9 5.9 %collective-permute-start.8 = (bf16[128,2048]{1,0:T(8,128)(2,1)S(1)}, bf16[128,2048]{1,0:T(8,128)(2,1)S(1)}, u32[]{:S(2)}, u32[]{:S(2)}) collective-permute-start(bf16[128,2048]{1,0:T(8,128)(2,1)S(1)} %shard_map.143), channel_id=1, source_target_pairs={{0,1},{1,0},{2,3},{3,2},{4,5},{5,4},{6,7},{7,6},{8,9},{9,8},{10,11... | collective-permute-start | bytes 1572872 | tf_op jit(solution)/shard_map/ppermute | solution.py:476
  94.9 4.8 %collective-permute-start.10 = (bf16[32,2048]{1,0:T(8,128)(2,1)S(1)}, bf16[32,2048]{1,0:T(8,128)(2,1)S(1)}, u32[]{:S(2)}, u32[]{:S(2)}) collective-permute-start(bf16[32,2048]{1,0:T(8,128)(2,1)S(1)} %get-tuple-element.45), channel_id=1, source_target_pairs={{0,6},{2,0},{4,2},{6,4},{1,7},{3,1},{5,3},{7,5},{8,14},{10,8},{12,... | collective-permute-start | bytes 393224 | tf_op jit(solution)/shard_map/ppermute | solution.py:489
  95.8 8.5 %collective-permute-start.11 = (bf16[32,2048]{1,0:T(8,128)(2,1)S(1)}, bf16[32,2048]{1,0:T(8,128)(2,1)S(1)}, u32[]{:S(2)}, u32[]{:S(2)}) collective-permute-start(bf16[32,2048]{1,0:T(8,128)(2,1)S(1)} %get-tuple-element.46), channel_id=1, source_target_pairs={{0,2},{2,4},{4,6},{6,0},{1,3},{3,5},{5,7},{7,1},{8,10},{10,12},{12... | collective-permute-start | bytes 393224 | tf_op jit(solution)/shard_map/ppermute | solution.py:489
  96.4 8.0 %collective-permute-start.9 = (bf16[32,2048]{1,0:T(8,128)(2,1)S(1)}, bf16[32,2048]{1,0:T(8,128)(2,1)S(1)}, u32[]{:S(2)}, u32[]{:S(2)}) collective-permute-start(bf16[32,2048]{1,0:T(8,128)(2,1)S(1)} %get-tuple-element.44), channel_id=1, source_target_pairs={{0,4},{2,6},{4,0},{6,2},{1,5},{3,7},{5,1},{7,3},{8,12},{10,14},{12... | collective-permute-start | bytes 393224 | tf_op jit(solution)/shard_map/ppermute | solution.py:489

commit v7 on v6

--- a/solution.py
+++ b/solution.py
@@ -77,8 +77,8 @@
 
 
 def prepare_kernel(
-    lines, weights_hbm, condition_hbm, decay_hbm, row_hbm, column_hbm,
-    out_ref, decay_ref, row_ref, column_ref,
+    lines, weights_hbm, condition_hbm, decay_hbm, row_hbm, column_hbm, gain_hbm, wk_hbm, wv_hbm,
+    out_ref, decay_ref, row_ref, column_ref, gain_ref, wk_ref, wv_ref,
     weights_ref, condition_ref, sems,
 ):
     size, width = weights_hbm.shape[0], condition_hbm.shape[1]
@@ -97,6 +97,9 @@
     for d in range(chips):
         row = seq * chips + (chip - d + chips) % chips
         loads.append(started(row_hbm.at[row], row_ref.at[d], sems, 5 + d))
+    loads.append(started(gain_hbm, gain_ref, sems, 5 + chips))
+    loads.append(started(wk_hbm, wk_ref, sems, 6 + chips))
+    loads.append(started(wv_hbm.at[:, : wv_ref.shape[1]], wv_ref, sems, 7 + chips))
     loads[0].wait()
     values = condition_ref[...].astype(f32)
     values = jnp.concatenate([values] * 4, axis=0)
@@ -170,73 +173,94 @@
         out_ref[t] = jnp.concatenate(rows, axis=0)
     for r, piece in enumerate(pieces):
         decay = jnp.exp(jnp.sum(piece[2 * cuts :, :], axis=0, keepdims=True))
-        decay_ref[r : r + 1, :] = jnp.concatenate([decay, decay], axis=1)
+        decay_ref[r : r + 1, :] = decay
 
 
 def keys_kernel(*refs):
     pieces, refs = refs[:8], refs[8:]
     (
-        near_hbm, wk_hbm, wv_hbm, gain_hbm, far_ref, mod_ref, col_ref, line_ref, row_ref,
+        near_hbm, wv_hbm, wk_ref, low_ref, gain_ref, far_ref, mod_ref, col_ref, line_ref, row_ref,
         column_ref,
-        send_ref, normed_hbm, k_ref, v_ref,
-        own_ref, near_ref, gain_ref, wk_ref, wv_ref, normed_ref, sems,
+        send_ref, normed_hbm, k_hbm, v_hbm,
+        own_ref, near_ref, high_ref, normed_ref, k_ref, v_ref, sems,
     ) = refs
     lines, width = pieces[0].shape
     rows = 8 * lines
     near = near_ref.shape[0]
-    load_gain = started(gain_hbm, gain_ref, sems, 5)
-    own = [started(pieces[0], own_ref, sems, 7), started(near_hbm, near_ref, sems, 8)]
-    loads = [started(wk_hbm, wk_ref, sems, 0), started(wv_hbm, wv_ref, sems, 1)]
-    load_gain.wait()
+    own = [
+        started(pieces[0], own_ref, sems, 3),
+        started(near_hbm, near_ref, sems, 4),
+    ]
+    load = started(wv_hbm.at[:, low_ref.shape[1] :], high_ref, sems, 0)
     gain = flat_gain(gain_ref)
     tp = mod_ref.shape[0]
 
-    def modulated(values, which):
+    def line_of(which):
         line = jnp.concatenate([mod_ref[t, which : which + 1, :] for t in range(tp)], axis=1)
-        shift, scale = line[:, :width], line[:, width : 2 * width]
-        wide = values.astype(f32)
-        normal = wide * lax.rsqrt(jnp.mean(wide * wide, axis=-1, keepdims=True) + epsilon)
-        return (normal * gain * (1.0 + scale) + shift).astype(bf16)
+        return line[:, :width], gain * (1.0 + line[:, width : 2 * width])
+
+    lines_of = [line_of(which) for which in range(2)]
+
+    def modulate(source_ref, base, which):
+        shift, scale = lines_of[which]
+
+        def block(i, carry):
+            own = pl.ds(pl.multiple_of(i * 16, 16), 16)
+            wide = source_ref[own, :].astype(f32)
+            normal = wide * lax.rsqrt(jnp.mean(wide * wide, axis=-1, keepdims=True) + epsilon)
+            target = pl.ds(pl.multiple_of(base + i * 16, 16), 16)
+            normed_ref[target, :] = (normal * scale + shift).astype(bf16)
+            return carry
+
+        lax.fori_loop(0, source_ref.shape[0] // 16, block, 0)
 
     for i, piece in enumerate(pieces[1:]):
-        normed_ref[(i + 1) * lines : (i + 2) * lines, :] = modulated(piece[...], 0)
-    normed_ref[rows + near :, :] = modulated(far_ref[...], 1)
+        modulate(piece, (i + 1) * lines, 0)
+    modulate(far_ref, rows + near, 1)
     for copy in own:
         copy.wait()
-    normed_ref[0:lines, :] = modulated(own_ref[...], 0)
-    normed_ref[rows : rows + near, :] = modulated(near_ref[...], 1)
+    modulate(own_ref, 0, 0)
+    modulate(near_ref, rows, 1)
     stores = [started(normed_ref.at[0:rows], normed_hbm, sems, 2)]
-    loads[0].wait()
+    load.wait()
     keys = dot(normed_ref[...], wk_ref[...])
-    loads[1].wait()
-    values = dot(normed_ref[...], wv_ref[...]).astype(bf16)
-    v_ref[...] = values[:rows]
+    low = dot(normed_ref[...], low_ref[...]).astype(bf16)
+    high = dot(normed_ref[...], high_ref[...]).astype(bf16)
+    values = jnp.concatenate([low, high], axis=1)
     key_rows = (turn(keys[:rows], row_ref, column_ref) * DK ** (-0.5)).astype(bf16)
     ctx_keys = (keys[rows:] * DK ** (-0.5)).astype(bf16)
     k_ref[...] = key_rows
+    stores.append(started(k_ref, k_hbm, sems, 1))
     wide = key_rows.astype(f32)
     ahead = (wide * jnp.exp(col_ref[:, 0:1])).astype(bf16)
     behind = (wide * jnp.exp(col_ref[:, 1:2])).astype(bf16)
-    turned = values.T
-    send_ref[:, 0:DK] = dot(turned[:, :rows], ahead).astype(bf16)
-    send_ref[:, DK : 2 * DK] = dot(turned[:, :rows], behind).astype(bf16)
-    odd = line_ref[3:4, 0 : DK // 2] > 0.5
-    own_keys = jnp.where(
-        odd, ctx_keys[:, DK // 2 :].astype(f32), ctx_keys[:, : DK // 2].astype(f32)
+    turned = jnp.concatenate([ahead.T, behind.T], axis=0)
+    v_ref[...] = values[:rows]
+    stores.append(started(v_ref, v_hbm, sems, 5))
+    parts = dot(turned, values[:rows]).astype(bf16)
+    send_ref[:, 0:DV] = parts[:DK]
+    send_ref[:, DV : 2 * DV] = parts[DK:]
+    ctx_values = values[rows:]
+    odd = line_ref[3:4, 0 : DV // 2] > 0.5
+    own_values = jnp.where(
+        odd, ctx_values[:, DV // 2 :].astype(f32), ctx_values[:, : DV // 2].astype(f32)
     ).astype(bf16)
-    send_ref[:, 2 * DK :] = dot(turned[:, rows:], own_keys).astype(bf16)
+    send_ref[:, 2 * DV :] = dot(ctx_keys.T, own_values).astype(bf16)
     for copy in stores:
         copy.wait()
 
 
 def inside_kernel(
-    normed_hbm, wq_hbm, wg_hbm, k_ref, v_ref, col_ref, line_ref, row_ref, column_ref,
+    normed_hbm, wq_hbm, wg_hbm, k_hbm, v_hbm, col_ref, line_ref, row_ref, column_ref,
     q_ref, g_ref, y_ref,
-    normed_ref, wq_ref, wg_ref, sems,
+    normed_ref, wq_ref, wg_ref, k_ref, v_ref, sems,
 ):
-    pairs = [(normed_hbm, normed_ref), (wq_hbm, wq_ref), (wg_hbm, wg_ref)]
+    pairs = [
+        (normed_hbm, normed_ref), (wq_hbm, wq_ref), (k_hbm, k_ref), (v_hbm, v_ref),
+        (wg_hbm, wg_ref),
+    ]
     loads = [started(a, b, sems, i) for i, (a, b) in enumerate(pairs)]
-    for copy in loads[:2]:
+    for copy in loads[:4]:
         copy.wait()
     queries = turn(dot(normed_ref[...], wq_ref[...]), row_ref, column_ref).astype(bf16)
     q_ref[...] = queries
@@ -249,7 +273,7 @@
     )
     weights = jnp.exp(gaps) * jnp.where(here == there, 2.0, 1.0)
     y_ref[...] = dot((scores * weights).astype(bf16), v_ref[...]).astype(bf16)
-    loads[2].wait()
+    loads[4].wait()
     g_ref[...] = dot(normed_ref[...], wg_ref[...]).astype(bf16)
 
 
@@ -259,18 +283,19 @@
     spot = [(r % y_size) * z_size + r // y_size for r in range(count)]
     lifts = []
     for parity in range(2):
-        lift = parts_ref[spot[parity], :, 2 * DK :].astype(f32)
+        lift = parts_ref[spot[parity], :, 2 * DV :].astype(f32)
         for r in range(parity + 2, count, 2):
-            lift = lift + parts_ref[spot[r], :, 2 * DK :].astype(f32)
+            lift = lift + parts_ref[spot[r], :, 2 * DV :].astype(f32)
         lifts.append(lift)
     ahead = behind = jnp.concatenate(lifts, axis=1) * float(CTX_LIFT)
+    decays = [jnp.concatenate([decay_ref[r : r + 1, :]] * (DV // 128), axis=1) for r in range(count)]
     for r in range(count):
         s = count - 1 - r
-        out_ref[spot[r], :, 0:DK] = ahead.astype(bf16)
-        out_ref[spot[s], :, DK:] = behind.astype(bf16)
-        ahead = decay_ref[r : r + 1, :] * ahead + parts_ref[spot[r], :, 0:DK].astype(f32)
+        out_ref[spot[r], :, 0:DV] = ahead.astype(bf16)
+        out_ref[spot[s], :, DV:] = behind.astype(bf16)
+        ahead = decays[r] * ahead + parts_ref[spot[r], :, 0:DV].astype(f32)
         behind = (
-            decay_ref[s : s + 1, :] * behind + parts_ref[spot[s], :, DK : 2 * DK].astype(f32)
+            decays[s] * behind + parts_ref[spot[s], :, DV : 2 * DV].astype(f32)
         )
 
 
@@ -282,8 +307,8 @@
     queries = q_ref[own, :]
     mixed = (
         y_ref[own, :].astype(f32)
-        + jnp.exp(col_ref[own, 2:3]) * dot_t(queries, states_ref[:, 0:DK])
-        + jnp.exp(col_ref[own, 3:4]) * dot_t(queries, states_ref[:, DK:])
+        + jnp.exp(col_ref[own, 2:3]) * dot(queries, states_ref[:, 0:DV])
+        + jnp.exp(col_ref[own, 3:4]) * dot(queries, states_ref[:, DV:])
     )
     average = jnp.mean(mixed, axis=-1, keepdims=True)
     centred = mixed - average
@@ -334,32 +359,38 @@
     columns = w_modulate.shape[1]
     sems = pltpu.SemaphoreType.DMA
     count, tp = lax.axis_size(SP), lax.axis_size(TP)
-    packed, decay_row, row_table, column_table = kernel_call(
+    packed, decay_row, row_table, column_table, gain, early_key, early_value = kernel_call(
         functools.partial(prepare_kernel, lines),
         [
             ("v", shaped(count, 16, 128)),
             ("v", shaped(1, rows, dtype=f32)),
             ("v", shaped(x_size, 1, DK, dtype=f32)),
             ("v", shaped(2 * lines, DK, dtype=f32)),
+            ("v", shaped(width // 128, 128)),
+            ("v", shaped(width, DK)),
+            ("v", shaped(width, DV // 2)),
         ],
-        "hhhhh",
+        "hhhhhhhh",
         [
             pltpu.VMEM(w_modulate.shape, bf16),
             pltpu.VMEM(condition.shape, bf16),
-            sems((5 + x_size,)),
+            sems((8 + x_size,)),
         ],
-        4,
+        8,
         1000000,
         w_modulate,
         condition,
         log_decay.T,
         jnp.asarray(rotary_tables(count * rows // GRID_W))[:, None],
         jnp.asarray(rotary_tables(GRID_W)),
+        norm_gain.reshape(-1, 128),
+        w_key,
+        w_value,
     )
     pieces = lax.all_to_all(packed, SP, 0, 0, tiled=True)
     spread, decays = kernel_call(
         gather_kernel,
-        [("v", shaped(tp, 2, columns, dtype=f32)), ("v", shaped(count, DK, dtype=f32))],
+        [("v", shaped(tp, 2, columns, dtype=f32)), ("v", shaped(count, 128, dtype=f32))],
         "v",
         [],
         4,
@@ -383,33 +414,34 @@
     )
 
     ctx = 2 * context.shape[0]
-    lanes = 2 * DK + DK // 2
+    lanes = 2 * DV + DV // 2
     send, normed, key_rows, value_rows = kernel_call(
         keys_kernel,
         [
-            ("v", shaped(DV, lanes)),
+            ("v", shaped(DK, lanes)),
             ("h", shaped(rows, width)),
-            ("v", shaped(rows, DK)),
-            ("v", shaped(rows, DV)),
+            ("h", shaped(rows, DK)),
+            ("h", shaped(rows, DV)),
         ],
-        "hvvvvvvv" + "hhhhvvvvvv",
+        "hvvvvvvv" + "hhvvvvvvvvv",
         [
             pltpu.VMEM((lines, width), bf16),
             pltpu.VMEM(context.shape, bf16),
-            pltpu.VMEM((width // 128, 128), bf16),
-            pltpu.VMEM((width, DK), bf16),
-            pltpu.VMEM((width, DV), bf16),
+            pltpu.VMEM((width, DV // 2), bf16),
             pltpu.VMEM((rows + ctx, width), bf16),
-            sems((9,)),
+            pltpu.VMEM((rows, DK), bf16),
+            pltpu.VMEM((rows, DV), bf16),
+            sems((6,)),
         ],
         32,
         2 * (rows + ctx) * width * (DK + DV),
         *own_rows,
         *other_rows,
         near,
-        w_key,
         w_value,
-        norm_gain.reshape(-1, 128),
+        early_key,
+        early_value,
+        gain,
         far,
         modulation,
         col,
@@ -417,7 +449,7 @@
         row_table,
         column_table,
     )
-    parts = lax.all_to_all(send.reshape(count, DV // count, lanes), YZ, 0, 0, tiled=True)
+    parts = lax.all_to_all(send.reshape(count, DK // count, lanes), YZ, 0, 0, tiled=True)
     queries, gates, inside = kernel_call(
         inside_kernel,
         [
@@ -425,12 +457,14 @@
             ("v", shaped(rows, DV)),
             ("v", shaped(rows, DV)),
         ],
-        "hhhvvvvvv",
+        "hhhhhvvvv",
         [
             pltpu.VMEM((rows, width), bf16),
             pltpu.VMEM((width, DK), bf16),
             pltpu.VMEM((width, DV), bf16),
-            sems((3,)),
+            pltpu.VMEM((rows, DK), bf16),
+            pltpu.VMEM((rows, DV), bf16),
+            sems((5,)),
         ],
         32,
         2 * rows * width * (DK + DV),
@@ -446,7 +480,7 @@
     )
     (entering,) = kernel_call(
         scan_kernel,
-        [("v", shaped(count, DV // count, 2 * DK))],
+        [("v", shaped(count, DK // count, 2 * DV))],
         "vv",
         [],
         16,
@@ -454,7 +488,7 @@
         parts,
         decays,
     )
-    states = lax.all_to_all(entering, YZ, 0, 0, tiled=True).reshape(DV, 2 * DK)
+    states = lax.all_to_all(entering, YZ, 0, 0, tiled=True).reshape(DK, 2 * DV)
     partials = []
     for part in (1, 0):
         (partial,) = kernel_call(

time: 106 us -> 108 us (1.019)
  local copies, waits for them, and re-layouts: 1.89 us -> 0.03 us
  waiting for transfers between devices: 22.3 us -> 24.1 us
  Pallas kernels: 12.8 us -> 14 us
    unnamed x14 -> x4, local copies, waits for them, and re-layouts: 1.87 us -> 0.01 us
    all_to_all x1, waiting for transfers between devices: 8.58 us -> 10.3 us  [per_device(): states = lax.all_to_all(entering, YZ, 0, 0, tiled=True).reshape(DK, 2 * DV)]
    pallas_call x9, Pallas kernels: 12.8 us -> 14 us  [kernel_call(): pl.pallas_call(body, out_shape=tuple((pltpu.HBM(a.shape, a.dtype) if k ==...]
where the time goes in v7:
time: 108 us; the launch traced here: 107 us
  starting transfers between devices  41.5 us (38%)
  blocking collectives  25.6 us (24%)
  waiting for transfers between devices  24.1 us (22%)
  Pallas kernels  14 us (13%)
  other arithmetic  1.66 us (2%)
    all_to_all x1, blocking collectives, per_device(): lax.all_to_all(send.reshape(count, DK // count, lanes), YZ, 0, 0, tiled=T...  25.6 us
    pallas_call x9, Pallas kernels, kernel_call(): pl.pallas_call(body, out_shape=tuple((pltpu.HBM(a.shape, a.dtype) if k ==...  14 us
    all_to_all x1, starting transfers between devices, per_device(): pieces = lax.all_to_all(packed, SP, 0, 0, tiled=True)  12 us
    all_to_all x1, waiting for transfers between devices, per_device(): states = lax.all_to_all(entering, YZ, 0, 0, tiled=True).reshape(DK, 2 * DV)  10.3 us
    all_to_all x1, starting transfers between devices, per_device(): states = lax.all_to_all(entering, YZ, 0, 0, tiled=True).reshape(DK, 2 * DV)  7.73 us
    ppermute x3, waiting for transfers between devices, per_device(): arrived = lax.ppermute(tiles[d], 'x', ring(x_size, -d))  7.17 us
    ppermute x3, starting transfers between devices, per_device(): lax.ppermute(later, 'x', ring(x_size, d))  4.89 us
    ppermute x4, starting transfers between devices, per_device(): other_rows = [lax.ppermute(piece, 'c', swap) for piece in own_rows]  4.77 us
  transfers between devices with their start and end apart: 15, of which 6 were waited for; matrix products, arithmetic and copies ran while one was open for 0% of the time, Pallas kernels for 5%

profile of v7, /device:TPU:1, one launch (start us, length us, event | category | flops | bytes accessed | tf_op | source)
XLA Modules:
  0.0 107.2 jit_solution(4175976963880574808)
XLA Ops:
  0.0 2.5 %shard_map.136 = (bf16[32,16,128]{2,1,0:T(8,128)(2,1)}, f32[1,256]{1,0:T(1,128)S(1)}, f32[4,1,256]{2,1,0:T(1,128)S(1)}, f32[64,256]{1,0:T(8,128)S(1)}, bf16[16,1...) custom-call(bf16[64,768]{1,0:T(8,128)(2,1)} %weights_hbm.1, ...), custom_call_target="tpu_custom_call" | custom-call | flops 1000000 | bytes 3453952 | tf_op jit(solution)/shard_map/pallas_call | solution.py:35
  2.5 12.0 %all-to-all-start = ((bf16[32,16,128]{2,1,0:T(8,128)(2,1)}), bf16[32,16,128]{2,1,0:T(8,128)(2,1)S(1)}, u32[]{:S(2)}, u32[]{:S(2)}) async-start(bf16[32,16,128]{2,1,0:T(8,128)(2,1)} %get-tuple-element.29), calls=%async_computation | async-start | bytes 262144 | tf_op jit(solution)/shard_map/all_to_all | solution.py:390
  14.5 1.3 %collective-permute-start = (bf16[32,2048]{1,0:T(8,128)(2,1)}, bf16[32,2048]{1,0:T(8,128)(2,1)S(1)}, u32[]{:S(2)}, u32[]{:S(2)}) collective-permute-start(bf16[32,2048]{1,0:T(8,128)(2,1)} %refs_0_), channel_id=1, source_target_pairs={{0,2},{2,4},{4,6},{6,0},{1,3},{3,5},{5,7},{7,1},{8,10},{10,12},{12... | collective-permute-start | bytes 393224 | tf_op jit(solution)/shard_map/ppermute | solution.py:403
  15.8 2.5 %collective-permute-start.1 = (bf16[32,2048]{1,0:T(8,128)(2,1)}, bf16[32,2048]{1,0:T(8,128)(2,1)S(1)}, u32[]{:S(2)}, u32[]{:S(2)}) collective-permute-start(bf16[32,2048]{1,0:T(8,128)(2,1)} %refs_0_), channel_id=1, source_target_pairs={{0,4},{2,6},{4,0},{6,2},{1,5},{3,7},{5,1},{7,3},{8,12},{10,14},{12... | collective-permute-start | bytes 393224 | tf_op jit(solution)/shard_map/ppermute | solution.py:403
  18.3 1.2 %collective-permute-start.2 = (bf16[32,2048]{1,0:T(8,128)(2,1)}, bf16[32,2048]{1,0:T(8,128)(2,1)S(1)}, u32[]{:S(2)}, u32[]{:S(2)}) collective-permute-start(bf16[32,2048]{1,0:T(8,128)(2,1)} %refs_0_), channel_id=1, source_target_pairs={{0,6},{2,0},{4,2},{6,4},{1,7},{3,1},{5,3},{7,5},{8,14},{10,8},{12,... | collective-permute-start | bytes 393224 | tf_op jit(solution)/shard_map/ppermute | solution.py:403
  19.4 1.8 %collective-permute-start.3 = (bf16[32,2048]{1,0:T(8,128)(2,1)}, bf16[32,2048]{1,0:T(8,128)(2,1)S(1)}, u32[]{:S(2)}, u32[]{:S(2)}) collective-permute-start(bf16[32,2048]{1,0:T(8,128)(2,1)} %refs_0_), channel_id=1, source_target_pairs={{0,1},{1,0},{2,3},{3,2},{4,5},{5,4},{6,7},{7,6},{8,9},{9,8},{10,11... | collective-permute-start | bytes 393224 | tf_op jit(solution)/shard_map/ppermute | solution.py:404
  21.2 0.0 collective-permute-done.refs_1_
  21.2 1.2 %collective-permute-start.4 = (bf16[32,2048]{1,0:T(8,128)(2,1)S(1)}, bf16[32,2048]{1,0:T(8,128)(2,1)S(1)}, u32[]{:S(2)}, u32[]{:S(2)}) collective-permute-start(bf16[32,2048]{1,0:T(8,128)(2,1)S(1)} %collective-permute-done.refs_1_), channel_id=1, source_target_pairs={{0,1},{1,0},{2,3},{3,2},{4,5},{5,4},{6,7},{7,6},{8,9},{9,8},{10,11... | collective-permute-start | bytes 393224 | tf_op jit(solution)/shard_map/ppermute | solution.py:404
  22.4 1.5 %collective-permute-done.1.refs_2_ = bf16[32,2048]{1,0:T(8,128)(2,1)S(1)} collective-permute-done((bf16[32,2048]{1,0:T(8,128)(2,1)}, bf16[32,2048]{1,0:T(8,128)(2,1)S(1)}, u32[]{:S(2)}, u32[]{:S(2)}) %collective-permute-start.1) | collective-permute-done | bytes 131104 | tf_op jit(solution)/shard_map/ppermute | solution.py:403
  23.9 1.8 %collective-permute-start.5 = (bf16[32,2048]{1,0:T(8,128)(2,1)S(1)}, bf16[32,2048]{1,0:T(8,128)(2,1)S(1)}, u32[]{:S(2)}, u32[]{:S(2)}) collective-permute-start(bf16[32,2048]{1,0:T(8,128)(2,1)S(1)} %collective-permute-done.1.refs_2_), channel_id=1, source_target_pairs={{0,1},{1,0},{2,3},{3,2},{4,5},{5,4},{6,7},{7,6},{8,9},{9,8},{10,11... | collective-permute-start | bytes 393224 | tf_op jit(solution)/shard_map/ppermute | solution.py:404
  25.7 0.0 collective-permute-done.2.refs_3_
  25.7 0.0 collective-permute-start.6
  25.7 1.3 %collective-permute-start.7 = (bf16[16,2048]{1,0:T(8,128)(2,1)}, bf16[16,2048]{1,0:T(8,128)(2,1)S(1)}, u32[]{:S(2)}, u32[]{:S(2)}) collective-permute-start(bf16[16,2048]{1,0:T(8,128)(2,1)} %refs_8_), channel_id=1, source_target_pairs={{0,8},{8,0},{16,24},{24,16},{1,9},{9,1},{17,25},{25,17},{2,10},{10... | collective-permute-start | bytes 196616 | tf_op jit(solution)/shard_map/ppermute | solution.py:405
  27.0 0.0 all-to-all-done.pieces_ref
  27.0 0.7 shard_map.137
  27.7 4.2 %all-to-all-start.1 = ((f32[8,2,768]{2,1,0:T(2,128)}), f32[8,2,768]{2,1,0:T(2,128)S(1)}, u32[]{:S(2)}, u32[]{:S(2)}) async-start(f32[8,2,768]{2,1,0:T(2,128)} %get-tuple-element.30), calls=%async_computation.1 | async-start | bytes 98304 | tf_op jit(solution)/shard_map/all_to_all | solution.py:400
  31.9 0.4 shard_map.138
  32.3 0.0 collective-permute-done.7.refs_13_
  32.3 0.0 collective-permute-done.3.refs_4_
  32.3 0.0 collective-permute-done.4.refs_5_
  32.3 0.0 collective-permute-done.5.refs_6_
  32.3 0.0 collective-permute-done.6.refs_7_
  32.3 4.4 %all-to-all-done.1.refs_14_ = f32[8,2,768]{2,1,0:T(2,128)S(1)} async-done(((f32[8,2,768]{2,1,0:T(2,128)}), f32[8,2,768]{2,1,0:T(2,128)S(1)}, u32[]{:S(2)}, u32[]{:S(2)}) %all-to-all-start.1) | async-done | bytes 49184 | tf_op jit(solution)/shard_map/all_to_all | solution.py:400
  36.7 4.2 %shard_map.139 = (bf16[256,1280]{1,0:T(8,128)(2,1)S(1)}, bf16[256,2048]{1,0:T(8,128)(2,1)}, bf16[256,256]{1,0:T(8,128)(2,1)}, bf16[256,512]{1,0:T(8,128)(2,1)}) custom-call(bf16[32,2048]{1,0:T(8,128)(2,1)} %refs_0_, bf16[32,2048]{1,0:T(8,128)(2,1)S(1)} %collective-permute-done.refs_1_, bf16[32,2048]{1,0:T(8,128)(2,1)S(1)} %collective-permute-done.1.refs_2_, ...), custom_call_target="tpu_custom_call" | custom-call | flops 905969664 | bytes 5509120 | tf_op jit(solution)/shard_map/pallas_call | solution.py:35
  40.9 25.6 %all_to_all.20.parts_ref = bf16[32,8,1280]{2,1,0:T(8,128)(2,1)S(1)} all-to-all(bf16[32,8,1280]{2,1,0:T(8,128)(2,1)S(1)} %bitcast.8), channel_id=1, replica_groups=mesh['z'=8,'y'=4,'x'=4,'c'=2] {'y','z'}, dimensions={0} | all-to-all | bytes 1310720 | tf_op jit(solution)/shard_map/all_to_all | solution.py:452
  66.6 0.9 shard_map.141
  67.5 7.7 %all-to-all-start.3 = ((bf16[32,8,1024]{2,1,0:T(8,128)(2,1)}), bf16[32,8,1024]{2,1,0:T(8,128)(2,1)S(1)}, u32[]{:S(2)}, u32[]{:S(2)}) async-start(bf16[32,8,1024]{2,1,0:T(8,128)(2,1)} %shard_map.141), calls=%async_computation.3 | async-start | bytes 1048576 | tf_op jit(solution)/shard_map/all_to_all | solution.py:491
  75.2 0.0 copy-start
  75.2 0.0 copy-start.1
  75.3 3.6 %shard_map.140 = (bf16[256,256]{1,0:T(8,128)(2,1)S(1)}, bf16[256,512]{1,0:T(8,128)(2,1)S(1)}, bf16[256,512]{1,0:T(8,128)(2,1)S(1)}) custom-call(bf16[256,2048]{1,0:T(8,128)(2,1)} %get-tuple-element.41.normed_hbm, bf16[2048,256]{1,0:T(8,128)(2,1)} %wq_hbm.1, bf16[2048,512]{1,0:T(8,128)(2,1)} %wg_hbm.1, bf16[256,256]{1,0:T(8,128)(2,1)} %get-tuple-element.42.k_hbm, ...), custom_call_target="tpu_custom_call" | custom-call | flops 805306368 | bytes 4669440 | tf_op jit(solution)/shard_map/pallas_call | solution.py:35
  78.9 10.3 %all-to-all-done.3 = bf16[32,8,1024]{2,1,0:T(8,128)(2,1)S(1)} async-done(((bf16[32,8,1024]{2,1,0:T(8,128)(2,1)}), bf16[32,8,1024]{2,1,0:T(8,128)(2,1)S(1)}, u32[]{:S(2)}, u32[]{:S(2)}) %all-to-all-start.3) | async-done | bytes 524320 | tf_op jit(solution)/shard_map/all_to_all | solution.py:491
  89.2 0.0 copy-done
  89.2 0.0 copy-done.1
  89.2 0.8 shard_map.143
  90.0 4.3 %collective-permute-start.8 = (bf16[128,2048]{1,0:T(8,128)(2,1)S(1)}, bf16[128,2048]{1,0:T(8,128)(2,1)S(1)}, u32[]{:S(2)}, u32[]{:S(2)}) collective-permute-start(bf16[128,2048]{1,0:T(8,128)(2,1)S(1)} %shard_map.143), channel_id=1, source_target_pairs={{0,1},{1,0},{2,3},{3,2},{4,5},{5,4},{6,7},{7,6},{8,9},{9,8},{10,11... | collective-permute-start | bytes 1572872 | tf_op jit(solution)/shard_map/ppermute | solution.py:510
  94.4 0.8 shard_map.142.own_ref
  95.2 0.7 collective-permute-done.8.crossed_ref
  95.9 0.1 shard_map.144
  96.0 1.0 collective-permute-start.10
  97.0 0.6 collective-permute-start.11
  97.6 0.8 collective-permute-start.9
  98.4 2.4 %collective-permute-done.10 = bf16[32,2048]{1,0:T(8,128)(2,1)S(1)} collective-permute-done((bf16[32,2048]{1,0:T(8,128)(2,1)S(1)}, bf16[32,2048]{1,0:T(8,128)(2,1)S(1)}, u32[]{:S(2)}, u32[]{:S(2)}) %collective-permute-start.10) | collective-permute-done | bytes 131104 | tf_op jit(solution)/shard_map/ppermute | solution.py:523
  100.8 4.7 %collective-permute-done.11 = bf16[32,2048]{1,0:T(8,128)(2,1)S(1)} collective-permute-done((bf16[32,2048]{1,0:T(8,128)(2,1)S(1)}, bf16[32,2048]{1,0:T(8,128)(2,1)S(1)}, u32[]{:S(2)}, u32[]{:S(2)}) %collective-permute-start.11) | collective-permute-done | bytes 131104 | tf_op jit(solution)/shard_map/ppermute | solution.py:523
  105.5 0.0 collective-permute-done.9
  105.6 1.7 %add_convert_fusion = bf16[32,2048]{1,0:T(8,128)(2,1)} fusion(bf16[32,2048]{1,0:T(8,128)(2,1)S(1)} %collective-permute-done.11, bf16[32,2048]{1,0:T(8,128)(2,1)S(1)} %collective-permute-done.10, bf16[32,2048]{1,0:T(8,128)(2,1)S(1)} %collective-permute-done.9, bf16[32,2048]{1,0:T(8,128)(2,1)S(1)} %get-tuple-element.49, bf16[32,2048]{1,0:T(8,128)(2,1)} %refs_0_, ...), kind=kLoop, calls=%fused_computation | loop fusion | flops 720896 | bytes 794624 | tf_op jit(solution)/shard_map/convert_element_type | solution.py:526
  (2 shorter events, 0.0 us)
Async XLA Ops:
  2.5 24.5 %all-to-all-start = ((bf16[32,16,128]{2,1,0:T(8,128)(2,1)}), bf16[32,16,128]{2,1,0:T(8,128)(2,1)S(1)}, u32[]{:S(2)}, u32[]{:S(2)}) async-start(bf16[32,16,128]{2,1,0:T(8,128)(2,1)} %get-tuple-element.29), calls=%async_computation | async-start | bytes 262144 | tf_op jit(solution)/shard_map/all_to_all | solution.py:390
  14.5 6.7 %collective-permute-start = (bf16[32,2048]{1,0:T(8,128)(2,1)}, bf16[32,2048]{1,0:T(8,128)(2,1)S(1)}, u32[]{:S(2)}, u32[]{:S(2)}) collective-permute-start(bf16[32,2048]{1,0:T(8,128)(2,1)} %refs_0_), channel_id=1, source_target_pairs={{0,2},{2,4},{4,6},{6,0},{1,3},{3,5},{5,7},{7,1},{8,10},{10,12},{12... | collective-permute-start | bytes 393224 | tf_op jit(solution)/shard_map/ppermute | solution.py:403
  15.8 8.1 %collective-permute-start.1 = (bf16[32,2048]{1,0:T(8,128)(2,1)}, bf16[32,2048]{1,0:T(8,128)(2,1)S(1)}, u32[]{:S(2)}, u32[]{:S(2)}) collective-permute-start(bf16[32,2048]{1,0:T(8,128)(2,1)} %refs_0_), channel_id=1, source_target_pairs={{0,4},{2,6},{4,0},{6,2},{1,5},{3,7},{5,1},{7,3},{8,12},{10,14},{12... | collective-permute-start | bytes 393224 | tf_op jit(solution)/shard_map/ppermute | solution.py:403
  18.3 7.5 %collective-permute-start.2 = (bf16[32,2048]{1,0:T(8,128)(2,1)}, bf16[32,2048]{1,0:T(8,128)(2,1)S(1)}, u32[]{:S(2)}, u32[]{:S(2)}) collective-permute-start(bf16[32,2048]{1,0:T(8,128)(2,1)} %refs_0_), channel_id=1, source_target_pairs={{0,6},{2,0},{4,2},{6,4},{1,7},{3,1},{5,3},{7,5},{8,14},{10,8},{12,... | collective-permute-start | bytes 393224 | tf_op jit(solution)/shard_map/ppermute | solution.py:403
  19.4 12.9 %collective-permute-start.3 = (bf16[32,2048]{1,0:T(8,128)(2,1)}, bf16[32,2048]{1,0:T(8,128)(2,1)S(1)}, u32[]{:S(2)}, u32[]{:S(2)}) collective-permute-start(bf16[32,2048]{1,0:T(8,128)(2,1)} %refs_0_), channel_id=1, source_target_pairs={{0,1},{1,0},{2,3},{3,2},{4,5},{5,4},{6,7},{7,6},{8,9},{9,8},{10,11... | collective-permute-start | bytes 393224 | tf_op jit(solution)/shard_map/ppermute | solution.py:404
  21.2 11.1 %collective-permute-start.4 = (bf16[32,2048]{1,0:T(8,128)(2,1)S(1)}, bf16[32,2048]{1,0:T(8,128)(2,1)S(1)}, u32[]{:S(2)}, u32[]{:S(2)}) collective-permute-start(bf16[32,2048]{1,0:T(8,128)(2,1)S(1)} %collective-permute-done.refs_1_), channel_id=1, source_target_pairs={{0,1},{1,0},{2,3},{3,2},{4,5},{5,4},{6,7},{7,6},{8,9},{9,8},{10,11... | collective-permute-start | bytes 393224 | tf_op jit(solution)/shard_map/ppermute | solution.py:404
  23.9 8.4 %collective-permute-start.5 = (bf16[32,2048]{1,0:T(8,128)(2,1)S(1)}, bf16[32,2048]{1,0:T(8,128)(2,1)S(1)}, u32[]{:S(2)}, u32[]{:S(2)}) collective-permute-start(bf16[32,2048]{1,0:T(8,128)(2,1)S(1)} %collective-permute-done.1.refs_2_), channel_id=1, source_target_pairs={{0,1},{1,0},{2,3},{3,2},{4,5},{5,4},{6,7},{7,6},{8,9},{9,8},{10,11... | collective-permute-start | bytes 393224 | tf_op jit(solution)/shard_map/ppermute | solution.py:404
  25.7 6.6 %collective-permute-start.6 = (bf16[32,2048]{1,0:T(8,128)(2,1)S(1)}, bf16[32,2048]{1,0:T(8,128)(2,1)S(1)}, u32[]{:S(2)}, u32[]{:S(2)}) collective-permute-start(bf16[32,2048]{1,0:T(8,128)(2,1)S(1)} %collective-permute-done.2.refs_3_), channel_id=1, source_target_pairs={{0,1},{1,0},{2,3},{3,2},{4,5},{5,4},{6,7},{7,6},{8,9},{9,8},{10,11... | collective-permute-start | bytes 393224 | tf_op jit(solution)/shard_map/ppermute | solution.py:404
  25.7 6.5 %collective-permute-start.7 = (bf16[16,2048]{1,0:T(8,128)(2,1)}, bf16[16,2048]{1,0:T(8,128)(2,1)S(1)}, u32[]{:S(2)}, u32[]{:S(2)}) collective-permute-start(bf16[16,2048]{1,0:T(8,128)(2,1)} %refs_8_), channel_id=1, source_target_pairs={{0,8},{8,0},{16,24},{24,16},{1,9},{9,1},{17,25},{25,17},{2,10},{10... | collective-permute-start | bytes 196616 | tf_op jit(solution)/shard_map/ppermute | solution.py:405
  27.7 9.0 %all-to-all-start.1 = ((f32[8,2,768]{2,1,0:T(2,128)}), f32[8,2,768]{2,1,0:T(2,128)S(1)}, u32[]{:S(2)}, u32[]{:S(2)}) async-start(f32[8,2,768]{2,1,0:T(2,128)} %get-tuple-element.30), calls=%async_computation.1 | async-start | bytes 98304 | tf_op jit(solution)/shard_map/all_to_all | solution.py:400
  67.5 21.7 %all-to-all-start.3 = ((bf16[32,8,1024]{2,1,0:T(8,128)(2,1)}), bf16[32,8,1024]{2,1,0:T(8,128)(2,1)S(1)}, u32[]{:S(2)}, u32[]{:S(2)}) async-start(bf16[32,8,1024]{2,1,0:T(8,128)(2,1)} %shard_map.141), calls=%async_computation.3 | async-start | bytes 1048576 | tf_op jit(solution)/shard_map/all_to_all | solution.py:491
  75.2 14.0 %copy-start = (bf16[512,2048]{1,0:T(8,128)(2,1)S(1)}, bf16[512,2048]{1,0:T(8,128)(2,1)}, u32[]{:S(2)}) copy-start(bf16[512,2048]{1,0:T(8,128)(2,1)} %wo_ref.3) | copy-start | bytes 6291460
  75.2 14.0 %copy-start.1 = (bf16[512]{0:T(512)(128)(2,1)S(1)}, bf16[512]{0:T(512)(128)(2,1)}, u32[]{:S(2)}) copy-start(bf16[512]{0:T(512)(128)(2,1)} %param.24) | copy-start | bytes 3076
  90.0 5.9 %collective-permute-start.8 = (bf16[128,2048]{1,0:T(8,128)(2,1)S(1)}, bf16[128,2048]{1,0:T(8,128)(2,1)S(1)}, u32[]{:S(2)}, u32[]{:S(2)}) collective-permute-start(bf16[128,2048]{1,0:T(8,128)(2,1)S(1)} %shard_map.143), channel_id=1, source_target_pairs={{0,1},{1,0},{2,3},{3,2},{4,5},{5,4},{6,7},{7,6},{8,9},{9,8},{10,11... | collective-permute-start | bytes 1572872 | tf_op jit(solution)/shard_map/ppermute | solution.py:510
  96.0 4.8 %collective-permute-start.10 = (bf16[32,2048]{1,0:T(8,128)(2,1)S(1)}, bf16[32,2048]{1,0:T(8,128)(2,1)S(1)}, u32[]{:S(2)}, u32[]{:S(2)}) collective-permute-start(bf16[32,2048]{1,0:T(8,128)(2,1)S(1)} %get-tuple-element.51), channel_id=1, source_target_pairs={{0,6},{2,0},{4,2},{6,4},{1,7},{3,1},{5,3},{7,5},{8,14},{10,8},{12,... | collective-permute-start | bytes 393224 | tf_op jit(solution)/shard_map/ppermute | solution.py:523
  97.0 8.5 %collective-permute-start.11 = (bf16[32,2048]{1,0:T(8,128)(2,1)S(1)}, bf16[32,2048]{1,0:T(8,128)(2,1)S(1)}, u32[]{:S(2)}, u32[]{:S(2)}) collective-permute-start(bf16[32,2048]{1,0:T(8,128)(2,1)S(1)} %get-tuple-element.52), channel_id=1, source_target_pairs={{0,2},{2,4},{4,6},{6,0},{1,3},{3,5},{5,7},{7,1},{8,10},{10,12},{12... | collective-permute-start | bytes 393224 | tf_op jit(solution)/shard_map/ppermute | solution.py:523
  97.6 8.0 %collective-permute-start.9 = (bf16[32,2048]{1,0:T(8,128)(2,1)S(1)}, bf16[32,2048]{1,0:T(8,128)(2,1)S(1)}, u32[]{:S(2)}, u32[]{:S(2)}) collective-permute-start(bf16[32,2048]{1,0:T(8,128)(2,1)S(1)} %get-tuple-element.50), channel_id=1, source_target_pairs={{0,4},{2,6},{4,0},{6,2},{1,5},{3,7},{5,1},{7,3},{8,12},{10,14},{12... | collective-permute-start | bytes 393224 | tf_op jit(solution)/shard_map/ppermute | solution.py:523

commit v8 on v6

--- a/solution.py
+++ b/solution.py
@@ -77,8 +77,8 @@
 
 
 def prepare_kernel(
-    lines, weights_hbm, condition_hbm, decay_hbm, row_hbm, column_hbm,
-    out_ref, decay_ref, row_ref, column_ref,
+    lines, weights_hbm, condition_hbm, decay_hbm, row_hbm, column_hbm, gain_hbm,
+    out_ref, decay_ref, row_ref, column_ref, gain_ref,
     weights_ref, condition_ref, sems,
 ):
     size, width = weights_hbm.shape[0], condition_hbm.shape[1]
@@ -97,6 +97,7 @@
     for d in range(chips):
         row = seq * chips + (chip - d + chips) % chips
         loads.append(started(row_hbm.at[row], row_ref.at[d], sems, 5 + d))
+    loads.append(started(gain_hbm, gain_ref, sems, 5 + chips))
     loads[0].wait()
     values = condition_ref[...].astype(f32)
     values = jnp.concatenate([values] * 4, axis=0)
@@ -170,61 +171,68 @@
         out_ref[t] = jnp.concatenate(rows, axis=0)
     for r, piece in enumerate(pieces):
         decay = jnp.exp(jnp.sum(piece[2 * cuts :, :], axis=0, keepdims=True))
-        decay_ref[r : r + 1, :] = jnp.concatenate([decay, decay], axis=1)
+        decay_ref[r : r + 1, :] = decay
 
 
 def keys_kernel(*refs):
     pieces, refs = refs[:8], refs[8:]
     (
-        near_hbm, wk_hbm, wv_hbm, gain_hbm, far_ref, mod_ref, col_ref, line_ref, row_ref,
+        near_hbm, wk_hbm, wv_hbm, gain_ref, far_ref, mod_ref, col_ref, line_ref, row_ref,
         column_ref,
         send_ref, normed_hbm, k_ref, v_ref,
-        own_ref, near_ref, gain_ref, wk_ref, wv_ref, normed_ref, sems,
+        own_ref, near_ref, wk_ref, wv_ref, normed_ref, sems,
     ) = refs
     lines, width = pieces[0].shape
     rows = 8 * lines
     near = near_ref.shape[0]
-    load_gain = started(gain_hbm, gain_ref, sems, 5)
+    loads = [started(wk_hbm, wk_ref, sems, 0)]
     own = [started(pieces[0], own_ref, sems, 7), started(near_hbm, near_ref, sems, 8)]
-    loads = [started(wk_hbm, wk_ref, sems, 0), started(wv_hbm, wv_ref, sems, 1)]
-    load_gain.wait()
     gain = flat_gain(gain_ref)
     tp = mod_ref.shape[0]
 
+    def line_of(which):
+        line = jnp.concatenate([mod_ref[t, which : which + 1, :] for t in range(tp)], axis=1)
+        return line[:, :width], gain * (1.0 + line[:, width : 2 * width])
+
+    lines_of = [line_of(which) for which in range(2)]
+
     def modulated(values, which):
-        line = jnp.concatenate([mod_ref[t, which : which + 1, :] for t in range(tp)], axis=1)
-        shift, scale = line[:, :width], line[:, width : 2 * width]
+        shift, scale = lines_of[which]
         wide = values.astype(f32)
         normal = wide * lax.rsqrt(jnp.mean(wide * wide, axis=-1, keepdims=True) + epsilon)
-        return (normal * gain * (1.0 + scale) + shift).astype(bf16)
+        return (normal * scale + shift).astype(bf16)
 
     for i, piece in enumerate(pieces[1:]):
         normed_ref[(i + 1) * lines : (i + 2) * lines, :] = modulated(piece[...], 0)
+        if i == 2:
+            loads.append(started(wv_hbm, wv_ref, sems, 1))
     normed_ref[rows + near :, :] = modulated(far_ref[...], 1)
     for copy in own:
         copy.wait()
     normed_ref[0:lines, :] = modulated(own_ref[...], 0)
     normed_ref[rows : rows + near, :] = modulated(near_ref[...], 1)
-    stores = [started(normed_ref.at[0:rows], normed_hbm, sems, 2)]
     loads[0].wait()
     keys = dot(normed_ref[...], wk_ref[...])
-    loads[1].wait()
-    values = dot(normed_ref[...], wv_ref[...]).astype(bf16)
-    v_ref[...] = values[:rows]
     key_rows = (turn(keys[:rows], row_ref, column_ref) * DK ** (-0.5)).astype(bf16)
     ctx_keys = (keys[rows:] * DK ** (-0.5)).astype(bf16)
     k_ref[...] = key_rows
     wide = key_rows.astype(f32)
     ahead = (wide * jnp.exp(col_ref[:, 0:1])).astype(bf16)
     behind = (wide * jnp.exp(col_ref[:, 1:2])).astype(bf16)
-    turned = values.T
-    send_ref[:, 0:DK] = dot(turned[:, :rows], ahead).astype(bf16)
-    send_ref[:, DK : 2 * DK] = dot(turned[:, :rows], behind).astype(bf16)
-    odd = line_ref[3:4, 0 : DK // 2] > 0.5
-    own_keys = jnp.where(
-        odd, ctx_keys[:, DK // 2 :].astype(f32), ctx_keys[:, : DK // 2].astype(f32)
+    turned = jnp.concatenate([ahead.T, behind.T], axis=0)
+    loads[1].wait()
+    stores = [started(normed_ref.at[0:rows], normed_hbm, sems, 2)]
+    values = dot(normed_ref[...], wv_ref[...]).astype(bf16)
+    v_ref[...] = values[:rows]
+    parts = dot(turned, values[:rows]).astype(bf16)
+    send_ref[:, 0:DV] = parts[:DK]
+    send_ref[:, DV : 2 * DV] = parts[DK:]
+    ctx_values = values[rows:]
+    odd = line_ref[3:4, 0 : DV // 2] > 0.5
+    own_values = jnp.where(
+        odd, ctx_values[:, DV // 2 :].astype(f32), ctx_values[:, : DV // 2].astype(f32)
     ).astype(bf16)
-    send_ref[:, 2 * DK :] = dot(turned[:, rows:], own_keys).astype(bf16)
+    send_ref[:, 2 * DV :] = dot(ctx_keys.T, own_values).astype(bf16)
     for copy in stores:
         copy.wait()
 
@@ -259,18 +267,19 @@
     spot = [(r % y_size) * z_size + r // y_size for r in range(count)]
     lifts = []
     for parity in range(2):
-        lift = parts_ref[spot[parity], :, 2 * DK :].astype(f32)
+        lift = parts_ref[spot[parity], :, 2 * DV :].astype(f32)
         for r in range(parity + 2, count, 2):
-            lift = lift + parts_ref[spot[r], :, 2 * DK :].astype(f32)
+            lift = lift + parts_ref[spot[r], :, 2 * DV :].astype(f32)
         lifts.append(lift)
     ahead = behind = jnp.concatenate(lifts, axis=1) * float(CTX_LIFT)
+    decays = [jnp.concatenate([decay_ref[r : r + 1, :]] * (DV // 128), axis=1) for r in range(count)]
     for r in range(count):
         s = count - 1 - r
-        out_ref[spot[r], :, 0:DK] = ahead.astype(bf16)
-        out_ref[spot[s], :, DK:] = behind.astype(bf16)
-        ahead = decay_ref[r : r + 1, :] * ahead + parts_ref[spot[r], :, 0:DK].astype(f32)
+        out_ref[spot[r], :, 0:DV] = ahead.astype(bf16)
+        out_ref[spot[s], :, DV:] = behind.astype(bf16)
+        ahead = decays[r] * ahead + parts_ref[spot[r], :, 0:DV].astype(f32)
         behind = (
-            decay_ref[s : s + 1, :] * behind + parts_ref[spot[s], :, DK : 2 * DK].astype(f32)
+            decays[s] * behind + parts_ref[spot[s], :, DV : 2 * DV].astype(f32)
         )
 
 
@@ -282,8 +291,8 @@
     queries = q_ref[own, :]
     mixed = (
         y_ref[own, :].astype(f32)
-        + jnp.exp(col_ref[own, 2:3]) * dot_t(queries, states_ref[:, 0:DK])
-        + jnp.exp(col_ref[own, 3:4]) * dot_t(queries, states_ref[:, DK:])
+        + jnp.exp(col_ref[own, 2:3]) * dot(queries, states_ref[:, 0:DV])
+        + jnp.exp(col_ref[own, 3:4]) * dot(queries, states_ref[:, DV:])
     )
     average = jnp.mean(mixed, axis=-1, keepdims=True)
     centred = mixed - average
@@ -334,19 +343,20 @@
     columns = w_modulate.shape[1]
     sems = pltpu.SemaphoreType.DMA
     count, tp = lax.axis_size(SP), lax.axis_size(TP)
-    packed, decay_row, row_table, column_table = kernel_call(
+    packed, decay_row, row_table, column_table, gain = kernel_call(
         functools.partial(prepare_kernel, lines),
         [
             ("v", shaped(count, 16, 128)),
             ("v", shaped(1, rows, dtype=f32)),
             ("v", shaped(x_size, 1, DK, dtype=f32)),
             ("v", shaped(2 * lines, DK, dtype=f32)),
+            ("v", shaped(width // 128, 128)),
         ],
-        "hhhhh",
+        "hhhhhh",
         [
             pltpu.VMEM(w_modulate.shape, bf16),
             pltpu.VMEM(condition.shape, bf16),
-            sems((5 + x_size,)),
+            sems((6 + x_size,)),
         ],
         4,
         1000000,
@@ -355,11 +365,12 @@
         log_decay.T,
         jnp.asarray(rotary_tables(count * rows // GRID_W))[:, None],
         jnp.asarray(rotary_tables(GRID_W)),
+        norm_gain.reshape(-1, 128),
     )
     pieces = lax.all_to_all(packed, SP, 0, 0, tiled=True)
     spread, decays = kernel_call(
         gather_kernel,
-        [("v", shaped(tp, 2, columns, dtype=f32)), ("v", shaped(count, DK, dtype=f32))],
+        [("v", shaped(tp, 2, columns, dtype=f32)), ("v", shaped(count, 128, dtype=f32))],
         "v",
         [],
         4,
@@ -383,20 +394,19 @@
     )
 
     ctx = 2 * context.shape[0]
-    lanes = 2 * DK + DK // 2
+    lanes = 2 * DV + DV // 2
     send, normed, key_rows, value_rows = kernel_call(
         keys_kernel,
         [
-            ("v", shaped(DV, lanes)),
+            ("v", shaped(DK, lanes)),
             ("h", shaped(rows, width)),
             ("v", shaped(rows, DK)),
             ("v", shaped(rows, DV)),
         ],
-        "hvvvvvvv" + "hhhhvvvvvv",
+        "hvvvvvvv" + "hhhvvvvvvv",
         [
             pltpu.VMEM((lines, width), bf16),
             pltpu.VMEM(context.shape, bf16),
-            pltpu.VMEM((width // 128, 128), bf16),
             pltpu.VMEM((width, DK), bf16),
             pltpu.VMEM((width, DV), bf16),
             pltpu.VMEM((rows + ctx, width), bf16),
@@ -409,7 +419,7 @@
         near,
         w_key,
         w_value,
-        norm_gain.reshape(-1, 128),
+        gain,
         far,
         modulation,
         col,
@@ -417,7 +427,7 @@
         row_table,
         column_table,
     )
-    parts = lax.all_to_all(send.reshape(count, DV // count, lanes), YZ, 0, 0, tiled=True)
+    parts = lax.all_to_all(send.reshape(count, DK // count, lanes), YZ, 0, 0, tiled=True)
     queries, gates, inside = kernel_call(
         inside_kernel,
         [
@@ -446,7 +456,7 @@
     )
     (entering,) = kernel_call(
         scan_kernel,
-        [("v", shaped(count, DV // count, 2 * DK))],
+        [("v", shaped(count, DK // count, 2 * DV))],
         "vv",
         [],
         16,
@@ -454,7 +464,7 @@
         parts,
         decays,
     )
-    states = lax.all_to_all(entering, YZ, 0, 0, tiled=True).reshape(DV, 2 * DK)
+    states = lax.all_to_all(entering, YZ, 0, 0, tiled=True).reshape(DK, 2 * DV)
     partials = []
     for part in (1, 0):
         (partial,) = kernel_call(

time: 106 us -> 106 us (level)
  no operation moved by 1% of the time
where the time goes in v8:
time: 106 us; the launch traced here: 105 us
  starting transfers between devices  41.5 us (39%)
  blocking collectives  25.6 us (24%)
  waiting for transfers between devices  22.4 us (21%)
  Pallas kernels  12.7 us (12%)
  local copies, waits for them, and re-layouts  1.89 us (2%)
    all_to_all x1, blocking collectives, per_device(): lax.all_to_all(send.reshape(count, DK // count, lanes), YZ, 0, 0, tiled=T...  25.6 us
    pallas_call x9, Pallas kernels, kernel_call(): pl.pallas_call(body, out_shape=tuple((pltpu.HBM(a.shape, a.dtype) if k ==...  12.7 us
    all_to_all x1, starting transfers between devices, per_device(): pieces = lax.all_to_all(packed, SP, 0, 0, tiled=True)  12 us
    all_to_all x1, waiting for transfers between devices, per_device(): states = lax.all_to_all(entering, YZ, 0, 0, tiled=True).reshape(DK, 2 * DV)  8.58 us
    all_to_all x1, starting transfers between devices, per_device(): states = lax.all_to_all(entering, YZ, 0, 0, tiled=True).reshape(DK, 2 * DV)  7.73 us
    ppermute x3, waiting for transfers between devices, per_device(): arrived = lax.ppermute(tiles[d], 'x', ring(x_size, -d))  7.19 us
    ppermute x3, starting transfers between devices, per_device(): lax.ppermute(later, 'x', ring(x_size, d))  4.89 us
    ppermute x4, starting transfers between devices, per_device(): other_rows = [lax.ppermute(piece, 'c', swap) for piece in own_rows]  4.77 us
  transfers between devices with their start and end apart: 15, of which 6 were waited for; matrix products, arithmetic and copies ran while one was open for 0% of the time, Pallas kernels for 5%

profile of v8, /device:TPU:1, one launch (start us, length us, event | category | flops | bytes accessed | tf_op | source)
XLA Modules:
  0.0 105.1 jit_solution(15279617102262373159)
XLA Ops:
  0.0 1.8 %shard_map.136 = (bf16[32,16,128]{2,1,0:T(8,128)(2,1)}, f32[1,256]{1,0:T(1,128)S(1)}, f32[4,1,256]{2,1,0:T(1,128)S(1)}, f32[64,256]{1,0:T(8,128)S(1)}, bf16[16,128]{1,0:T(8,128)(2,1)S(1)}) custom-call(bf16[64,768]{1,0:T(8,128)(2,1)} %weights_hbm.1, bf16[2,2048]{1,0:T(2,128)(2,1)} %condition_hbm.1, f32[1,256]{1,0:T(1,128)} %bitcast.13, ...), custom_call_target="tpu_custom_call" | custom-call | flops 1000000 | bytes 308224 | tf_op jit(solution)/shard_map/pallas_call | solution.py:35
  1.8 12.0 %all-to-all-start = ((bf16[32,16,128]{2,1,0:T(8,128)(2,1)}), bf16[32,16,128]{2,1,0:T(8,128)(2,1)S(1)}, u32[]{:S(2)}, u32[]{:S(2)}) async-start(bf16[32,16,128]{2,1,0:T(8,128)(2,1)} %get-tuple-element.27), calls=%async_computation | async-start | bytes 262144 | tf_op jit(solution)/shard_map/all_to_all | solution.py:370
  13.9 1.3 %collective-permute-start = (bf16[32,2048]{1,0:T(8,128)(2,1)}, bf16[32,2048]{1,0:T(8,128)(2,1)S(1)}, u32[]{:S(2)}, u32[]{:S(2)}) collective-permute-start(bf16[32,2048]{1,0:T(8,128)(2,1)} %refs_0_), channel_id=1, source_target_pairs={{0,2},{2,4},{4,6},{6,0},{1,3},{3,5},{5,7},{7,1},{8,10},{10,12},{12... | collective-permute-start | bytes 393224 | tf_op jit(solution)/shard_map/ppermute | solution.py:383
  15.2 2.5 %collective-permute-start.1 = (bf16[32,2048]{1,0:T(8,128)(2,1)}, bf16[32,2048]{1,0:T(8,128)(2,1)S(1)}, u32[]{:S(2)}, u32[]{:S(2)}) collective-permute-start(bf16[32,2048]{1,0:T(8,128)(2,1)} %refs_0_), channel_id=1, source_target_pairs={{0,4},{2,6},{4,0},{6,2},{1,5},{3,7},{5,1},{7,3},{8,12},{10,14},{12... | collective-permute-start | bytes 393224 | tf_op jit(solution)/shard_map/ppermute | solution.py:383
  17.6 1.2 %collective-permute-start.2 = (bf16[32,2048]{1,0:T(8,128)(2,1)}, bf16[32,2048]{1,0:T(8,128)(2,1)S(1)}, u32[]{:S(2)}, u32[]{:S(2)}) collective-permute-start(bf16[32,2048]{1,0:T(8,128)(2,1)} %refs_0_), channel_id=1, source_target_pairs={{0,6},{2,0},{4,2},{6,4},{1,7},{3,1},{5,3},{7,5},{8,14},{10,8},{12,... | collective-permute-start | bytes 393224 | tf_op jit(solution)/shard_map/ppermute | solution.py:383
  18.8 1.8 %collective-permute-start.3 = (bf16[32,2048]{1,0:T(8,128)(2,1)}, bf16[32,2048]{1,0:T(8,128)(2,1)S(1)}, u32[]{:S(2)}, u32[]{:S(2)}) collective-permute-start(bf16[32,2048]{1,0:T(8,128)(2,1)} %refs_0_), channel_id=1, source_target_pairs={{0,1},{1,0},{2,3},{3,2},{4,5},{5,4},{6,7},{7,6},{8,9},{9,8},{10,11... | collective-permute-start | bytes 393224 | tf_op jit(solution)/shard_map/ppermute | solution.py:384
  20.6 0.0 collective-permute-done.refs_1_
  20.6 1.2 %collective-permute-start.4 = (bf16[32,2048]{1,0:T(8,128)(2,1)S(1)}, bf16[32,2048]{1,0:T(8,128)(2,1)S(1)}, u32[]{:S(2)}, u32[]{:S(2)}) collective-permute-start(bf16[32,2048]{1,0:T(8,128)(2,1)S(1)} %collective-permute-done.refs_1_), channel_id=1, source_target_pairs={{0,1},{1,0},{2,3},{3,2},{4,5},{5,4},{6,7},{7,6},{8,9},{9,8},{10,11... | collective-permute-start | bytes 393224 | tf_op jit(solution)/shard_map/ppermute | solution.py:384
  21.7 1.5 %collective-permute-done.1.refs_2_ = bf16[32,2048]{1,0:T(8,128)(2,1)S(1)} collective-permute-done((bf16[32,2048]{1,0:T(8,128)(2,1)}, bf16[32,2048]{1,0:T(8,128)(2,1)S(1)}, u32[]{:S(2)}, u32[]{:S(2)}) %collective-permute-start.1) | collective-permute-done | bytes 131104 | tf_op jit(solution)/shard_map/ppermute | solution.py:383
  23.3 1.8 %collective-permute-start.5 = (bf16[32,2048]{1,0:T(8,128)(2,1)S(1)}, bf16[32,2048]{1,0:T(8,128)(2,1)S(1)}, u32[]{:S(2)}, u32[]{:S(2)}) collective-permute-start(bf16[32,2048]{1,0:T(8,128)(2,1)S(1)} %collective-permute-done.1.refs_2_), channel_id=1, source_target_pairs={{0,1},{1,0},{2,3},{3,2},{4,5},{5,4},{6,7},{7,6},{8,9},{9,8},{10,11... | collective-permute-start | bytes 393224 | tf_op jit(solution)/shard_map/ppermute | solution.py:384
  25.1 0.0 collective-permute-done.2.refs_3_
  25.1 0.0 collective-permute-start.6
  25.1 1.3 %collective-permute-start.7 = (bf16[16,2048]{1,0:T(8,128)(2,1)}, bf16[16,2048]{1,0:T(8,128)(2,1)S(1)}, u32[]{:S(2)}, u32[]{:S(2)}) collective-permute-start(bf16[16,2048]{1,0:T(8,128)(2,1)} %refs_8_), channel_id=1, source_target_pairs={{0,8},{8,0},{16,24},{24,16},{1,9},{9,1},{17,25},{25,17},{2,10},{10... | collective-permute-start | bytes 196616 | tf_op jit(solution)/shard_map/ppermute | solution.py:385
  26.4 0.0 all-to-all-done.pieces_ref
  26.4 0.7 shard_map.137
  27.0 4.2 %all-to-all-start.1 = ((f32[8,2,768]{2,1,0:T(2,128)}), f32[8,2,768]{2,1,0:T(2,128)S(1)}, u32[]{:S(2)}, u32[]{:S(2)}) async-start(f32[8,2,768]{2,1,0:T(2,128)} %get-tuple-element.28), calls=%async_computation.1 | async-start | bytes 98304 | tf_op jit(solution)/shard_map/all_to_all | solution.py:380
  31.2 0.4 shard_map.138
  31.6 0.0 collective-permute-done.7.refs_12_
  31.6 0.0 collective-permute-done.3.refs_4_
  31.6 0.0 collective-permute-done.4.refs_5_
  31.6 0.0 collective-permute-done.5.refs_6_
  31.7 0.0 collective-permute-done.6.refs_7_
  31.7 4.4 %all-to-all-done.1.refs_13_ = f32[8,2,768]{2,1,0:T(2,128)S(1)} async-done(((f32[8,2,768]{2,1,0:T(2,128)}), f32[8,2,768]{2,1,0:T(2,128)S(1)}, u32[]{:S(2)}, u32[]{:S(2)}) %all-to-all-start.1) | async-done | bytes 49184 | tf_op jit(solution)/shard_map/all_to_all | solution.py:380
  36.0 3.6 %shard_map.139 = (bf16[256,1280]{1,0:T(8,128)(2,1)S(1)}, bf16[256,2048]{1,0:T(8,128)(2,1)}, bf16[256,256]{1,0:T(8,128)(2,1)S(1)}, bf16[256,512]{1,0:T(8,128)(2,1)S(1)}) custom-call(bf16[32,2048]{1,0:T(8,128)(2,1)} %refs_0_, bf16[32,2048]{1,0:T(8,128)(2,1)S(1)} %collective-permute-done.refs_1_, bf16[32,2048]{1,0:T(8,128)(2,1)S(1)} %collective-permute-done.1.refs_2_, ...), custom_call_target="tpu_custom_call" | custom-call | flops 905969664 | bytes 4460544 | tf_op jit(solution)/shard_map/pallas_call | solution.py:35
  39.7 0.0 copy-start.3
  39.7 0.0 copy-start.1
  39.7 25.6 %all_to_all.20.parts_ref = bf16[32,8,1280]{2,1,0:T(8,128)(2,1)S(1)} all-to-all(bf16[32,8,1280]{2,1,0:T(8,128)(2,1)S(1)} %bitcast.8), channel_id=1, replica_groups=mesh['z'=8,'y'=4,'x'=4,'c'=2] {'y','z'}, dimensions={0} | all-to-all | bytes 1310720 | tf_op jit(solution)/shard_map/all_to_all | solution.py:430
  65.3 0.0 copy-done.3
  65.3 1.0 shard_map.141
  66.3 7.7 %all-to-all-start.3 = ((bf16[32,8,1024]{2,1,0:T(8,128)(2,1)}), bf16[32,8,1024]{2,1,0:T(8,128)(2,1)S(1)}, u32[]{:S(2)}, u32[]{:S(2)}) async-start(bf16[32,8,1024]{2,1,0:T(8,128)(2,1)} %shard_map.141), calls=%async_computation.3 | async-start | bytes 1048576 | tf_op jit(solution)/shard_map/all_to_all | solution.py:467
  74.0 0.9 copy-done.2
  75.0 0.9 copy-done.4
  75.9 3.5 %shard_map.140 = (bf16[256,256]{1,0:T(8,128)(2,1)S(1)}, bf16[256,512]{1,0:T(8,128)(2,1)S(1)}, bf16[256,512]{1,0:T(8,128)(2,1)S(1)}) custom-call(bf16[256,2048]{1,0:T(8,128)(2,1)} %get-tuple-element.37.normed_hbm, bf16[2048,256]{1,0:T(8,128)(2,1)} %wq_hbm.1, bf16[2048,512]{1,0:T(8,128)(2,1)} %wg_hbm.1, bf16[256,256]{1,0:T(8,128)(2,1)S(1)} %copy-done.4, ...), custom_call_target="tpu_custom_call" | custom-call | flops 805306368 | bytes 4669440 | tf_op jit(solution)/shard_map/pallas_call | solution.py:35
  79.4 8.6 %all-to-all-done.3 = bf16[32,8,1024]{2,1,0:T(8,128)(2,1)S(1)} async-done(((bf16[32,8,1024]{2,1,0:T(8,128)(2,1)}), bf16[32,8,1024]{2,1,0:T(8,128)(2,1)S(1)}, u32[]{:S(2)}, u32[]{:S(2)}) %all-to-all-start.3) | async-done | bytes 524320 | tf_op jit(solution)/shard_map/all_to_all | solution.py:467
  88.0 0.8 shard_map.143
  88.8 0.0 copy-start.6
  88.8 4.3 %collective-permute-start.8 = (bf16[128,2048]{1,0:T(8,128)(2,1)S(1)}, bf16[128,2048]{1,0:T(8,128)(2,1)S(1)}, u32[]{:S(2)}, u32[]{:S(2)}) collective-permute-start(bf16[128,2048]{1,0:T(8,128)(2,1)S(1)} %shard_map.143), channel_id=1, source_target_pairs={{0,1},{1,0},{2,3},{3,2},{4,5},{5,4},{6,7},{7,6},{8,9},{9,8},{10,11... | collective-permute-start | bytes 1572872 | tf_op jit(solution)/shard_map/ppermute | solution.py:486
  93.2 0.8 shard_map.142.own_ref
  94.0 0.7 collective-permute-done.8.crossed_ref
  94.7 0.1 shard_map.144
  94.9 1.0 collective-permute-start.10
  95.8 0.6 collective-permute-start.11
  96.4 0.8 collective-permute-start.9
  97.2 2.4 %collective-permute-done.10 = bf16[32,2048]{1,0:T(8,128)(2,1)S(1)} collective-permute-done((bf16[32,2048]{1,0:T(8,128)(2,1)S(1)}, bf16[32,2048]{1,0:T(8,128)(2,1)S(1)}, u32[]{:S(2)}, u32[]{:S(2)}) %collective-permute-start.10) | collective-permute-done | bytes 131104 | tf_op jit(solution)/shard_map/ppermute | solution.py:499
  99.6 4.8 %collective-permute-done.11 = bf16[32,2048]{1,0:T(8,128)(2,1)S(1)} collective-permute-done((bf16[32,2048]{1,0:T(8,128)(2,1)S(1)}, bf16[32,2048]{1,0:T(8,128)(2,1)S(1)}, u32[]{:S(2)}, u32[]{:S(2)}) %collective-permute-start.11) | collective-permute-done | bytes 131104 | tf_op jit(solution)/shard_map/ppermute | solution.py:499
  104.4 0.0 collective-permute-done.9
  104.4 0.0 copy-done.6
  104.4 0.8 add_convert_fusion
  (9 shorter events, 0.0 us)
Async XLA Ops:
  1.8 24.5 %all-to-all-start = ((bf16[32,16,128]{2,1,0:T(8,128)(2,1)}), bf16[32,16,128]{2,1,0:T(8,128)(2,1)S(1)}, u32[]{:S(2)}, u32[]{:S(2)}) async-start(bf16[32,16,128]{2,1,0:T(8,128)(2,1)} %get-tuple-element.27), calls=%async_computation | async-start | bytes 262144 | tf_op jit(solution)/shard_map/all_to_all | solution.py:370
  13.9 6.7 %collective-permute-start = (bf16[32,2048]{1,0:T(8,128)(2,1)}, bf16[32,2048]{1,0:T(8,128)(2,1)S(1)}, u32[]{:S(2)}, u32[]{:S(2)}) collective-permute-start(bf16[32,2048]{1,0:T(8,128)(2,1)} %refs_0_), channel_id=1, source_target_pairs={{0,2},{2,4},{4,6},{6,0},{1,3},{3,5},{5,7},{7,1},{8,10},{10,12},{12... | collective-permute-start | bytes 393224 | tf_op jit(solution)/shard_map/ppermute | solution.py:383
  15.2 8.1 %collective-permute-start.1 = (bf16[32,2048]{1,0:T(8,128)(2,1)}, bf16[32,2048]{1,0:T(8,128)(2,1)S(1)}, u32[]{:S(2)}, u32[]{:S(2)}) collective-permute-start(bf16[32,2048]{1,0:T(8,128)(2,1)} %refs_0_), channel_id=1, source_target_pairs={{0,4},{2,6},{4,0},{6,2},{1,5},{3,7},{5,1},{7,3},{8,12},{10,14},{12... | collective-permute-start | bytes 393224 | tf_op jit(solution)/shard_map/ppermute | solution.py:383
  17.6 7.5 %collective-permute-start.2 = (bf16[32,2048]{1,0:T(8,128)(2,1)}, bf16[32,2048]{1,0:T(8,128)(2,1)S(1)}, u32[]{:S(2)}, u32[]{:S(2)}) collective-permute-start(bf16[32,2048]{1,0:T(8,128)(2,1)} %refs_0_), channel_id=1, source_target_pairs={{0,6},{2,0},{4,2},{6,4},{1,7},{3,1},{5,3},{7,5},{8,14},{10,8},{12,... | collective-permute-start | bytes 393224 | tf_op jit(solution)/shard_map/ppermute | solution.py:383
  18.8 12.9 %collective-permute-start.3 = (bf16[32,2048]{1,0:T(8,128)(2,1)}, bf16[32,2048]{1,0:T(8,128)(2,1)S(1)}, u32[]{:S(2)}, u32[]{:S(2)}) collective-permute-start(bf16[32,2048]{1,0:T(8,128)(2,1)} %refs_0_), channel_id=1, source_target_pairs={{0,1},{1,0},{2,3},{3,2},{4,5},{5,4},{6,7},{7,6},{8,9},{9,8},{10,11... | collective-permute-start | bytes 393224 | tf_op jit(solution)/shard_map/ppermute | solution.py:384
  20.6 11.1 %collective-permute-start.4 = (bf16[32,2048]{1,0:T(8,128)(2,1)S(1)}, bf16[32,2048]{1,0:T(8,128)(2,1)S(1)}, u32[]{:S(2)}, u32[]{:S(2)}) collective-permute-start(bf16[32,2048]{1,0:T(8,128)(2,1)S(1)} %collective-permute-done.refs_1_), channel_id=1, source_target_pairs={{0,1},{1,0},{2,3},{3,2},{4,5},{5,4},{6,7},{7,6},{8,9},{9,8},{10,11... | collective-permute-start | bytes 393224 | tf_op jit(solution)/shard_map/ppermute | solution.py:384
  23.3 8.4 %collective-permute-start.5 = (bf16[32,2048]{1,0:T(8,128)(2,1)S(1)}, bf16[32,2048]{1,0:T(8,128)(2,1)S(1)}, u32[]{:S(2)}, u32[]{:S(2)}) collective-permute-start(bf16[32,2048]{1,0:T(8,128)(2,1)S(1)} %collective-permute-done.1.refs_2_), channel_id=1, source_target_pairs={{0,1},{1,0},{2,3},{3,2},{4,5},{5,4},{6,7},{7,6},{8,9},{9,8},{10,11... | collective-permute-start | bytes 393224 | tf_op jit(solution)/shard_map/ppermute | solution.py:384
  25.1 6.6 %collective-permute-start.6 = (bf16[32,2048]{1,0:T(8,128)(2,1)S(1)}, bf16[32,2048]{1,0:T(8,128)(2,1)S(1)}, u32[]{:S(2)}, u32[]{:S(2)}) collective-permute-start(bf16[32,2048]{1,0:T(8,128)(2,1)S(1)} %collective-permute-done.2.refs_3_), channel_id=1, source_target_pairs={{0,1},{1,0},{2,3},{3,2},{4,5},{5,4},{6,7},{7,6},{8,9},{9,8},{10,11... | collective-permute-start | bytes 393224 | tf_op jit(solution)/shard_map/ppermute | solution.py:384
  25.1 6.5 %collective-permute-start.7 = (bf16[16,2048]{1,0:T(8,128)(2,1)}, bf16[16,2048]{1,0:T(8,128)(2,1)S(1)}, u32[]{:S(2)}, u32[]{:S(2)}) collective-permute-start(bf16[16,2048]{1,0:T(8,128)(2,1)} %refs_8_), channel_id=1, source_target_pairs={{0,8},{8,0},{16,24},{24,16},{1,9},{9,1},{17,25},{25,17},{2,10},{10... | collective-permute-start | bytes 196616 | tf_op jit(solution)/shard_map/ppermute | solution.py:385
  27.0 9.0 %all-to-all-start.1 = ((f32[8,2,768]{2,1,0:T(2,128)}), f32[8,2,768]{2,1,0:T(2,128)S(1)}, u32[]{:S(2)}, u32[]{:S(2)}) async-start(f32[8,2,768]{2,1,0:T(2,128)} %get-tuple-element.28), calls=%async_computation.1 | async-start | bytes 98304 | tf_op jit(solution)/shard_map/all_to_all | solution.py:380
  39.7 25.7 %copy-start.3 = (bf16[256,256]{1,0:T(8,128)(2,1)}, bf16[256,256]{1,0:T(8,128)(2,1)S(1)}, u32[]{:S(2)}) copy-start(bf16[256,256]{1,0:T(8,128)(2,1)S(1)} %get-tuple-element.38.k_ref) | copy-start | bytes 393220
  39.7 34.4 %copy-start.1 = (bf16[256,512]{1,0:T(8,128)(2,1)}, bf16[256,512]{1,0:T(8,128)(2,1)S(1)}, u32[]{:S(2)}) copy-start(bf16[256,512]{1,0:T(8,128)(2,1)S(1)} %get-tuple-element.39.v_ref) | copy-start | bytes 786436
  66.3 21.7 %all-to-all-start.3 = ((bf16[32,8,1024]{2,1,0:T(8,128)(2,1)}), bf16[32,8,1024]{2,1,0:T(8,128)(2,1)S(1)}, u32[]{:S(2)}, u32[]{:S(2)}) async-start(bf16[32,8,1024]{2,1,0:T(8,128)(2,1)} %shard_map.141), calls=%async_computation.3 | async-start | bytes 1048576 | tf_op jit(solution)/shard_map/all_to_all | solution.py:467
  74.0 1.0 copy-start.2
  75.0 0.9 copy-start.4
  75.9 12.1 %copy-start = (bf16[512,2048]{1,0:T(8,128)(2,1)S(1)}, bf16[512,2048]{1,0:T(8,128)(2,1)}, u32[]{:S(2)}) copy-start(bf16[512,2048]{1,0:T(8,128)(2,1)} %wo_ref.3) | copy-start | bytes 6291460
  75.9 12.1 %copy-start.5 = (bf16[512]{0:T(512)(128)(2,1)S(1)}, bf16[512]{0:T(512)(128)(2,1)}, u32[]{:S(2)}) copy-start(bf16[512]{0:T(512)(128)(2,1)} %param.24) | copy-start | bytes 3076
  88.8 15.5 %copy-start.6 = (bf16[32,2048]{1,0:T(8,128)(2,1)S(1)}, bf16[32,2048]{1,0:T(8,128)(2,1)}, u32[]{:S(2)}) copy-start(bf16[32,2048]{1,0:T(8,128)(2,1)} %refs_0_) | copy-start | bytes 393220
  88.8 5.9 %collective-permute-start.8 = (bf16[128,2048]{1,0:T(8,128)(2,1)S(1)}, bf16[128,2048]{1,0:T(8,128)(2,1)S(1)}, u32[]{:S(2)}, u32[]{:S(2)}) collective-permute-start(bf16[128,2048]{1,0:T(8,128)(2,1)S(1)} %shard_map.143), channel_id=1, source_target_pairs={{0,1},{1,0},{2,3},{3,2},{4,5},{5,4},{6,7},{7,6},{8,9},{9,8},{10,11... | collective-permute-start | bytes 1572872 | tf_op jit(solution)/shard_map/ppermute | solution.py:486
  94.9 4.8 %collective-permute-start.10 = (bf16[32,2048]{1,0:T(8,128)(2,1)S(1)}, bf16[32,2048]{1,0:T(8,128)(2,1)S(1)}, u32[]{:S(2)}, u32[]{:S(2)}) collective-permute-start(bf16[32,2048]{1,0:T(8,128)(2,1)S(1)} %get-tuple-element.47), channel_id=1, source_target_pairs={{0,6},{2,0},{4,2},{6,4},{1,7},{3,1},{5,3},{7,5},{8,14},{10,8},{12,... | collective-permute-start | bytes 393224 | tf_op jit(solution)/shard_map/ppermute | solution.py:499
  95.8 8.5 %collective-permute-start.11 = (bf16[32,2048]{1,0:T(8,128)(2,1)S(1)}, bf16[32,2048]{1,0:T(8,128)(2,1)S(1)}, u32[]{:S(2)}, u32[]{:S(2)}) collective-permute-start(bf16[32,2048]{1,0:T(8,128)(2,1)S(1)} %get-tuple-element.48), channel_id=1, source_target_pairs={{0,2},{2,4},{4,6},{6,0},{1,3},{3,5},{5,7},{7,1},{8,10},{10,12},{12... | collective-permute-start | bytes 393224 | tf_op jit(solution)/shard_map/ppermute | solution.py:499
  96.4 8.0 %collective-permute-start.9 = (bf16[32,2048]{1,0:T(8,128)(2,1)S(1)}, bf16[32,2048]{1,0:T(8,128)(2,1)S(1)}, u32[]{:S(2)}, u32[]{:S(2)}) collective-permute-start(bf16[32,2048]{1,0:T(8,128)(2,1)S(1)} %get-tuple-element.46), channel_id=1, source_target_pairs={{0,4},{2,6},{4,0},{6,2},{1,5},{3,7},{5,1},{7,3},{8,12},{10,14},{12... | collective-permute-start | bytes 393224 | tf_op jit(solution)/shard_map/ppermute | solution.py:499

commit v9 on v8

--- a/solution.py
+++ b/solution.py
@@ -52,6 +52,21 @@
 def flat_gain(gain_ref):
     wide = gain_ref[...].astype(f32)
     return jnp.concatenate([wide[i : i + 1, :] for i in range(wide.shape[0])], axis=1)
+
+
+class Split:
+    def __init__(self, source, target, sems, slot, cuts):
+        size = source.shape[0] // cuts
+        self.copies = [
+            started(
+                source.at[i * size : (i + 1) * size], target.at[i * size : (i + 1) * size], sems, slot + i
+            )
+            for i in range(cuts)
+        ]
+
+    def wait(self):
+        for copy in self.copies:
+            copy.wait()
 
 
 def dot(a, b):
@@ -185,7 +200,7 @@
     lines, width = pieces[0].shape
     rows = 8 * lines
     near = near_ref.shape[0]
-    loads = [started(wk_hbm, wk_ref, sems, 0)]
+    loads = [Split(wk_hbm, wk_ref, sems, 9, 8), Split(wv_hbm, wv_ref, sems, 17, 8)]
     own = [started(pieces[0], own_ref, sems, 7), started(near_hbm, near_ref, sems, 8)]
     gain = flat_gain(gain_ref)
     tp = mod_ref.shape[0]
@@ -204,8 +219,6 @@
 
     for i, piece in enumerate(pieces[1:]):
         normed_ref[(i + 1) * lines : (i + 2) * lines, :] = modulated(piece[...], 0)
-        if i == 2:
-            loads.append(started(wv_hbm, wv_ref, sems, 1))
     normed_ref[rows + near :, :] = modulated(far_ref[...], 1)
     for copy in own:
         copy.wait()
@@ -221,7 +234,7 @@
     behind = (wide * jnp.exp(col_ref[:, 1:2])).astype(bf16)
     turned = jnp.concatenate([ahead.T, behind.T], axis=0)
     loads[1].wait()
-    stores = [started(normed_ref.at[0:rows], normed_hbm, sems, 2)]
+    stores = [Split(normed_ref.at[0:rows], normed_hbm, sems, 0, 4)]
     values = dot(normed_ref[...], wv_ref[...]).astype(bf16)
     v_ref[...] = values[:rows]
     parts = dot(turned, values[:rows]).astype(bf16)
@@ -243,7 +256,7 @@
     normed_ref, wq_ref, wg_ref, sems,
 ):
     pairs = [(normed_hbm, normed_ref), (wq_hbm, wq_ref), (wg_hbm, wg_ref)]
-    loads = [started(a, b, sems, i) for i, (a, b) in enumerate(pairs)]
+    loads = [Split(a, b, sems, 8 * i, 8) for i, (a, b) in enumerate(pairs)]
     for copy in loads[:2]:
         copy.wait()
     queries = turn(dot(normed_ref[...], wq_ref[...]), row_ref, column_ref).astype(bf16)
@@ -410,7 +423,7 @@
             pltpu.VMEM((width, DK), bf16),
             pltpu.VMEM((width, DV), bf16),
             pltpu.VMEM((rows + ctx, width), bf16),
-            sems((9,)),
+            sems((25,)),
         ],
         32,
         2 * (rows + ctx) * width * (DK + DV),
@@ -440,7 +453,7 @@
             pltpu.VMEM((rows, width), bf16),
             pltpu.VMEM((width, DK), bf16),
             pltpu.VMEM((width, DV), bf16),
-            sems((3,)),
+            sems((24,)),
         ],
         32,
         2 * rows * width * (DK + DV),

time: 106 us -> 107 us (level)
  Pallas kernels: 12.7 us -> 13.9 us
    pallas_call x9, Pallas kernels: 12.7 us -> 13.9 us  [kernel_call(): pl.pallas_call(body, out_shape=tuple((pltpu.HBM(a.shape, a.dtype) if k ==...]
where the time goes in v9:
time: 107 us; the launch traced here: 106 us
  starting transfers between devices  41.5 us (39%)
  blocking collectives  25.6 us (24%)
  waiting for transfers between devices  22.2 us (21%)
  Pallas kernels  13.9 us (13%)
  local copies, waits for them, and re-layouts  1.89 us (2%)
    all_to_all x1, blocking collectives, per_device(): lax.all_to_all(send.reshape(count, DK // count, lanes), YZ, 0, 0, tiled=T...  25.6 us
    pallas_call x9, Pallas kernels, kernel_call(): pl.pallas_call(body, out_shape=tuple((pltpu.HBM(a.shape, a.dtype) if k ==...  13.9 us
    all_to_all x1, starting transfers between devices, per_device(): pieces = lax.all_to_all(packed, SP, 0, 0, tiled=True)  12 us
    all_to_all x1, waiting for transfers between devices, per_device(): states = lax.all_to_all(entering, YZ, 0, 0, tiled=True).reshape(DK, 2 * DV)  8.34 us
    all_to_all x1, starting transfers between devices, per_device(): states = lax.all_to_all(entering, YZ, 0, 0, tiled=True).reshape(DK, 2 * DV)  7.73 us
    ppermute x3, waiting for transfers between devices, per_device(): arrived = lax.ppermute(tiles[d], 'x', ring(x_size, -d))  7.17 us
    ppermute x3, starting transfers between devices, per_device(): lax.ppermute(later, 'x', ring(x_size, d))  4.89 us
    ppermute x4, starting transfers between devices, per_device(): other_rows = [lax.ppermute(piece, 'c', swap) for piece in own_rows]  4.77 us
  transfers between devices with their start and end apart: 15, of which 6 were waited for; matrix products, arithmetic and copies ran while one was open for 0% of the time, Pallas kernels for 5%

profile of v9, /device:TPU:1, one launch (start us, length us, event | category | flops | bytes accessed | tf_op | source)
XLA Modules:
  0.0 106.1 jit_solution(1384369050137615388)
XLA Ops:
  0.0 1.8 %shard_map.136 = (bf16[32,16,128]{2,1,0:T(8,128)(2,1)}, f32[1,256]{1,0:T(1,128)S(1)}, f32[4,1,256]{2,1,0:T(1,128)S(1)}, f32[64,256]{1,0:T(8,128)S(1)}, bf16[16,128]{1,0:T(8,128)(2,1)S(1)}) custom-call(bf16[64,768]{1,0:T(8,128)(2,1)} %weights_hbm.1, bf16[2,2048]{1,0:T(2,128)(2,1)} %condition_hbm.1, f32[1,256]{1,0:T(1,128)} %bitcast.13, ...), custom_call_target="tpu_custom_call" | custom-call | flops 1000000 | bytes 308224 | tf_op jit(solution)/shard_map/pallas_call | solution.py:35
  1.8 12.0 %all-to-all-start = ((bf16[32,16,128]{2,1,0:T(8,128)(2,1)}), bf16[32,16,128]{2,1,0:T(8,128)(2,1)S(1)}, u32[]{:S(2)}, u32[]{:S(2)}) async-start(bf16[32,16,128]{2,1,0:T(8,128)(2,1)} %get-tuple-element.27), calls=%async_computation | async-start | bytes 262144 | tf_op jit(solution)/shard_map/all_to_all | solution.py:383
  13.9 1.3 %collective-permute-start = (bf16[32,2048]{1,0:T(8,128)(2,1)}, bf16[32,2048]{1,0:T(8,128)(2,1)S(1)}, u32[]{:S(2)}, u32[]{:S(2)}) collective-permute-start(bf16[32,2048]{1,0:T(8,128)(2,1)} %refs_0_), channel_id=1, source_target_pairs={{0,2},{2,4},{4,6},{6,0},{1,3},{3,5},{5,7},{7,1},{8,10},{10,12},{12... | collective-permute-start | bytes 393224 | tf_op jit(solution)/shard_map/ppermute | solution.py:396
  15.2 2.5 %collective-permute-start.1 = (bf16[32,2048]{1,0:T(8,128)(2,1)}, bf16[32,2048]{1,0:T(8,128)(2,1)S(1)}, u32[]{:S(2)}, u32[]{:S(2)}) collective-permute-start(bf16[32,2048]{1,0:T(8,128)(2,1)} %refs_0_), channel_id=1, source_target_pairs={{0,4},{2,6},{4,0},{6,2},{1,5},{3,7},{5,1},{7,3},{8,12},{10,14},{12... | collective-permute-start | bytes 393224 | tf_op jit(solution)/shard_map/ppermute | solution.py:396
  17.6 1.2 %collective-permute-start.2 = (bf16[32,2048]{1,0:T(8,128)(2,1)}, bf16[32,2048]{1,0:T(8,128)(2,1)S(1)}, u32[]{:S(2)}, u32[]{:S(2)}) collective-permute-start(bf16[32,2048]{1,0:T(8,128)(2,1)} %refs_0_), channel_id=1, source_target_pairs={{0,6},{2,0},{4,2},{6,4},{1,7},{3,1},{5,3},{7,5},{8,14},{10,8},{12,... | collective-permute-start | bytes 393224 | tf_op jit(solution)/shard_map/ppermute | solution.py:396
  18.8 1.8 %collective-permute-start.3 = (bf16[32,2048]{1,0:T(8,128)(2,1)}, bf16[32,2048]{1,0:T(8,128)(2,1)S(1)}, u32[]{:S(2)}, u32[]{:S(2)}) collective-permute-start(bf16[32,2048]{1,0:T(8,128)(2,1)} %refs_0_), channel_id=1, source_target_pairs={{0,1},{1,0},{2,3},{3,2},{4,5},{5,4},{6,7},{7,6},{8,9},{9,8},{10,11... | collective-permute-start | bytes 393224 | tf_op jit(solution)/shard_map/ppermute | solution.py:397
  20.6 0.0 collective-permute-done.refs_1_
  20.6 1.2 %collective-permute-start.4 = (bf16[32,2048]{1,0:T(8,128)(2,1)S(1)}, bf16[32,2048]{1,0:T(8,128)(2,1)S(1)}, u32[]{:S(2)}, u32[]{:S(2)}) collective-permute-start(bf16[32,2048]{1,0:T(8,128)(2,1)S(1)} %collective-permute-done.refs_1_), channel_id=1, source_target_pairs={{0,1},{1,0},{2,3},{3,2},{4,5},{5,4},{6,7},{7,6},{8,9},{9,8},{10,11... | collective-permute-start | bytes 393224 | tf_op jit(solution)/shard_map/ppermute | solution.py:397
  21.7 1.5 %collective-permute-done.1.refs_2_ = bf16[32,2048]{1,0:T(8,128)(2,1)S(1)} collective-permute-done((bf16[32,2048]{1,0:T(8,128)(2,1)}, bf16[32,2048]{1,0:T(8,128)(2,1)S(1)}, u32[]{:S(2)}, u32[]{:S(2)}) %collective-permute-start.1) | collective-permute-done | bytes 131104 | tf_op jit(solution)/shard_map/ppermute | solution.py:396
  23.3 1.8 %collective-permute-start.5 = (bf16[32,2048]{1,0:T(8,128)(2,1)S(1)}, bf16[32,2048]{1,0:T(8,128)(2,1)S(1)}, u32[]{:S(2)}, u32[]{:S(2)}) collective-permute-start(bf16[32,2048]{1,0:T(8,128)(2,1)S(1)} %collective-permute-done.1.refs_2_), channel_id=1, source_target_pairs={{0,1},{1,0},{2,3},{3,2},{4,5},{5,4},{6,7},{7,6},{8,9},{9,8},{10,11... | collective-permute-start | bytes 393224 | tf_op jit(solution)/shard_map/ppermute | solution.py:397
  25.1 0.0 collective-permute-done.2.refs_3_
  25.1 0.0 collective-permute-start.6
  25.1 1.3 %collective-permute-start.7 = (bf16[16,2048]{1,0:T(8,128)(2,1)}, bf16[16,2048]{1,0:T(8,128)(2,1)S(1)}, u32[]{:S(2)}, u32[]{:S(2)}) collective-permute-start(bf16[16,2048]{1,0:T(8,128)(2,1)} %refs_8_), channel_id=1, source_target_pairs={{0,8},{8,0},{16,24},{24,16},{1,9},{9,1},{17,25},{25,17},{2,10},{10... | collective-permute-start | bytes 196616 | tf_op jit(solution)/shard_map/ppermute | solution.py:398
  26.4 0.0 all-to-all-done.pieces_ref
  26.4 0.7 shard_map.137
  27.0 4.2 %all-to-all-start.1 = ((f32[8,2,768]{2,1,0:T(2,128)}), f32[8,2,768]{2,1,0:T(2,128)S(1)}, u32[]{:S(2)}, u32[]{:S(2)}) async-start(f32[8,2,768]{2,1,0:T(2,128)} %get-tuple-element.28), calls=%async_computation.1 | async-start | bytes 98304 | tf_op jit(solution)/shard_map/all_to_all | solution.py:393
  31.2 0.4 shard_map.138
  31.6 0.0 collective-permute-done.7.refs_12_
  31.6 0.0 collective-permute-done.3.refs_4_
  31.6 0.0 collective-permute-done.4.refs_5_
  31.6 0.0 collective-permute-done.5.refs_6_
  31.7 0.0 collective-permute-done.6.refs_7_
  31.7 4.4 %all-to-all-done.1.refs_13_ = f32[8,2,768]{2,1,0:T(2,128)S(1)} async-done(((f32[8,2,768]{2,1,0:T(2,128)}), f32[8,2,768]{2,1,0:T(2,128)S(1)}, u32[]{:S(2)}, u32[]{:S(2)}) %all-to-all-start.1) | async-done | bytes 49184 | tf_op jit(solution)/shard_map/all_to_all | solution.py:393
  36.0 4.6 %shard_map.139 = (bf16[256,1280]{1,0:T(8,128)(2,1)S(1)}, bf16[256,2048]{1,0:T(8,128)(2,1)}, bf16[256,256]{1,0:T(8,128)(2,1)S(1)}, bf16[256,512]{1,0:T(8,128)(2,1)S(1)}) custom-call(bf16[32,2048]{1,0:T(8,128)(2,1)} %refs_0_, bf16[32,2048]{1,0:T(8,128)(2,1)S(1)} %collective-permute-done.refs_1_, bf16[32,2048]{1,0:T(8,128)(2,1)S(1)} %collective-permute-done.1.refs_2_, ...), custom_call_target="tpu_custom_call" | custom-call | flops 905969664 | bytes 4460544 | tf_op jit(solution)/shard_map/pallas_call | solution.py:35
  40.6 0.0 copy-start.3
  40.7 0.0 copy-start.1
  40.7 25.6 %all_to_all.20.parts_ref = bf16[32,8,1280]{2,1,0:T(8,128)(2,1)S(1)} all-to-all(bf16[32,8,1280]{2,1,0:T(8,128)(2,1)S(1)} %bitcast.8), channel_id=1, replica_groups=mesh['z'=8,'y'=4,'x'=4,'c'=2] {'y','z'}, dimensions={0} | all-to-all | bytes 1310720 | tf_op jit(solution)/shard_map/all_to_all | solution.py:443
  66.3 0.0 copy-done.3
  66.3 1.0 shard_map.141
  67.3 7.7 %all-to-all-start.3 = ((bf16[32,8,1024]{2,1,0:T(8,128)(2,1)}), bf16[32,8,1024]{2,1,0:T(8,128)(2,1)S(1)}, u32[]{:S(2)}, u32[]{:S(2)}) async-start(bf16[32,8,1024]{2,1,0:T(8,128)(2,1)} %shard_map.141), calls=%async_computation.3 | async-start | bytes 1048576 | tf_op jit(solution)/shard_map/all_to_all | solution.py:480
  75.0 0.9 copy-done.2
  76.0 0.9 copy-done.4
  76.9 3.8 %shard_map.140 = (bf16[256,256]{1,0:T(8,128)(2,1)S(1)}, bf16[256,512]{1,0:T(8,128)(2,1)S(1)}, bf16[256,512]{1,0:T(8,128)(2,1)S(1)}) custom-call(bf16[256,2048]{1,0:T(8,128)(2,1)} %get-tuple-element.37.normed_hbm, bf16[2048,256]{1,0:T(8,128)(2,1)} %wq_hbm.1, bf16[2048,512]{1,0:T(8,128)(2,1)} %wg_hbm.1, bf16[256,256]{1,0:T(8,128)(2,1)S(1)} %copy-done.4, ...), custom_call_target="tpu_custom_call" | custom-call | flops 805306368 | bytes 4669440 | tf_op jit(solution)/shard_map/pallas_call | solution.py:35
  80.7 8.3 %all-to-all-done.3 = bf16[32,8,1024]{2,1,0:T(8,128)(2,1)S(1)} async-done(((bf16[32,8,1024]{2,1,0:T(8,128)(2,1)}), bf16[32,8,1024]{2,1,0:T(8,128)(2,1)S(1)}, u32[]{:S(2)}, u32[]{:S(2)}) %all-to-all-start.3) | async-done | bytes 524320 | tf_op jit(solution)/shard_map/all_to_all | solution.py:480
  89.0 0.0 copy-done.5
  89.0 0.8 shard_map.143
  89.8 0.0 copy-start.6
  89.8 4.3 %collective-permute-start.8 = (bf16[128,2048]{1,0:T(8,128)(2,1)S(1)}, bf16[128,2048]{1,0:T(8,128)(2,1)S(1)}, u32[]{:S(2)}, u32[]{:S(2)}) collective-permute-start(bf16[128,2048]{1,0:T(8,128)(2,1)S(1)} %shard_map.143), channel_id=1, source_target_pairs={{0,1},{1,0},{2,3},{3,2},{4,5},{5,4},{6,7},{7,6},{8,9},{9,8},{10,11... | collective-permute-start | bytes 1572872 | tf_op jit(solution)/shard_map/ppermute | solution.py:499
  94.2 0.8 shard_map.142.own_ref
  95.0 0.7 collective-permute-done.8.crossed_ref
  95.7 0.1 shard_map.144
  95.8 1.0 collective-permute-start.10
  96.8 0.6 collective-permute-start.11
  97.4 0.8 collective-permute-start.9
  98.2 2.4 %collective-permute-done.10 = bf16[32,2048]{1,0:T(8,128)(2,1)S(1)} collective-permute-done((bf16[32,2048]{1,0:T(8,128)(2,1)S(1)}, bf16[32,2048]{1,0:T(8,128)(2,1)S(1)}, u32[]{:S(2)}, u32[]{:S(2)}) %collective-permute-start.10) | collective-permute-done | bytes 131104 | tf_op jit(solution)/shard_map/ppermute | solution.py:512
  100.6 4.7 %collective-permute-done.11 = bf16[32,2048]{1,0:T(8,128)(2,1)S(1)} collective-permute-done((bf16[32,2048]{1,0:T(8,128)(2,1)S(1)}, bf16[32,2048]{1,0:T(8,128)(2,1)S(1)}, u32[]{:S(2)}, u32[]{:S(2)}) %collective-permute-start.11) | collective-permute-done | bytes 131104 | tf_op jit(solution)/shard_map/ppermute | solution.py:512
  105.3 0.0 collective-permute-done.9
  105.3 0.8 add_convert_fusion
  (9 shorter events, 0.0 us)
Async XLA Ops:
  1.8 24.5 %all-to-all-start = ((bf16[32,16,128]{2,1,0:T(8,128)(2,1)}), bf16[32,16,128]{2,1,0:T(8,128)(2,1)S(1)}, u32[]{:S(2)}, u32[]{:S(2)}) async-start(bf16[32,16,128]{2,1,0:T(8,128)(2,1)} %get-tuple-element.27), calls=%async_computation | async-start | bytes 262144 | tf_op jit(solution)/shard_map/all_to_all | solution.py:383
  13.9 6.7 %collective-permute-start = (bf16[32,2048]{1,0:T(8,128)(2,1)}, bf16[32,2048]{1,0:T(8,128)(2,1)S(1)}, u32[]{:S(2)}, u32[]{:S(2)}) collective-permute-start(bf16[32,2048]{1,0:T(8,128)(2,1)} %refs_0_), channel_id=1, source_target_pairs={{0,2},{2,4},{4,6},{6,0},{1,3},{3,5},{5,7},{7,1},{8,10},{10,12},{12... | collective-permute-start | bytes 393224 | tf_op jit(solution)/shard_map/ppermute | solution.py:396
  15.2 8.1 %collective-permute-start.1 = (bf16[32,2048]{1,0:T(8,128)(2,1)}, bf16[32,2048]{1,0:T(8,128)(2,1)S(1)}, u32[]{:S(2)}, u32[]{:S(2)}) collective-permute-start(bf16[32,2048]{1,0:T(8,128)(2,1)} %refs_0_), channel_id=1, source_target_pairs={{0,4},{2,6},{4,0},{6,2},{1,5},{3,7},{5,1},{7,3},{8,12},{10,14},{12... | collective-permute-start | bytes 393224 | tf_op jit(solution)/shard_map/ppermute | solution.py:396
  17.6 7.5 %collective-permute-start.2 = (bf16[32,2048]{1,0:T(8,128)(2,1)}, bf16[32,2048]{1,0:T(8,128)(2,1)S(1)}, u32[]{:S(2)}, u32[]{:S(2)}) collective-permute-start(bf16[32,2048]{1,0:T(8,128)(2,1)} %refs_0_), channel_id=1, source_target_pairs={{0,6},{2,0},{4,2},{6,4},{1,7},{3,1},{5,3},{7,5},{8,14},{10,8},{12,... | collective-permute-start | bytes 393224 | tf_op jit(solution)/shard_map/ppermute | solution.py:396
  18.8 12.9 %collective-permute-start.3 = (bf16[32,2048]{1,0:T(8,128)(2,1)}, bf16[32,2048]{1,0:T(8,128)(2,1)S(1)}, u32[]{:S(2)}, u32[]{:S(2)}) collective-permute-start(bf16[32,2048]{1,0:T(8,128)(2,1)} %refs_0_), channel_id=1, source_target_pairs={{0,1},{1,0},{2,3},{3,2},{4,5},{5,4},{6,7},{7,6},{8,9},{9,8},{10,11... | collective-permute-start | bytes 393224 | tf_op jit(solution)/shard_map/ppermute | solution.py:397
  20.6 11.1 %collective-permute-start.4 = (bf16[32,2048]{1,0:T(8,128)(2,1)S(1)}, bf16[32,2048]{1,0:T(8,128)(2,1)S(1)}, u32[]{:S(2)}, u32[]{:S(2)}) collective-permute-start(bf16[32,2048]{1,0:T(8,128)(2,1)S(1)} %collective-permute-done.refs_1_), channel_id=1, source_target_pairs={{0,1},{1,0},{2,3},{3,2},{4,5},{5,4},{6,7},{7,6},{8,9},{9,8},{10,11... | collective-permute-start | bytes 393224 | tf_op jit(solution)/shard_map/ppermute | solution.py:397
  23.3 8.4 %collective-permute-start.5 = (bf16[32,2048]{1,0:T(8,128)(2,1)S(1)}, bf16[32,2048]{1,0:T(8,128)(2,1)S(1)}, u32[]{:S(2)}, u32[]{:S(2)}) collective-permute-start(bf16[32,2048]{1,0:T(8,128)(2,1)S(1)} %collective-permute-done.1.refs_2_), channel_id=1, source_target_pairs={{0,1},{1,0},{2,3},{3,2},{4,5},{5,4},{6,7},{7,6},{8,9},{9,8},{10,11... | collective-permute-start | bytes 393224 | tf_op jit(solution)/shard_map/ppermute | solution.py:397
  25.1 6.6 %collective-permute-start.6 = (bf16[32,2048]{1,0:T(8,128)(2,1)S(1)}, bf16[32,2048]{1,0:T(8,128)(2,1)S(1)}, u32[]{:S(2)}, u32[]{:S(2)}) collective-permute-start(bf16[32,2048]{1,0:T(8,128)(2,1)S(1)} %collective-permute-done.2.refs_3_), channel_id=1, source_target_pairs={{0,1},{1,0},{2,3},{3,2},{4,5},{5,4},{6,7},{7,6},{8,9},{9,8},{10,11... | collective-permute-start | bytes 393224 | tf_op jit(solution)/shard_map/ppermute | solution.py:397
  25.1 6.5 %collective-permute-start.7 = (bf16[16,2048]{1,0:T(8,128)(2,1)}, bf16[16,2048]{1,0:T(8,128)(2,1)S(1)}, u32[]{:S(2)}, u32[]{:S(2)}) collective-permute-start(bf16[16,2048]{1,0:T(8,128)(2,1)} %refs_8_), channel_id=1, source_target_pairs={{0,8},{8,0},{16,24},{24,16},{1,9},{9,1},{17,25},{25,17},{2,10},{10... | collective-permute-start | bytes 196616 | tf_op jit(solution)/shard_map/ppermute | solution.py:398
  27.0 9.0 %all-to-all-start.1 = ((f32[8,2,768]{2,1,0:T(2,128)}), f32[8,2,768]{2,1,0:T(2,128)S(1)}, u32[]{:S(2)}, u32[]{:S(2)}) async-start(f32[8,2,768]{2,1,0:T(2,128)} %get-tuple-element.28), calls=%async_computation.1 | async-start | bytes 98304 | tf_op jit(solution)/shard_map/all_to_all | solution.py:393
  40.6 25.7 %copy-start.3 = (bf16[256,256]{1,0:T(8,128)(2,1)}, bf16[256,256]{1,0:T(8,128)(2,1)S(1)}, u32[]{:S(2)}) copy-start(bf16[256,256]{1,0:T(8,128)(2,1)S(1)} %get-tuple-element.38.k_ref) | copy-start | bytes 393220
  40.7 34.4 %copy-start.1 = (bf16[256,512]{1,0:T(8,128)(2,1)}, bf16[256,512]{1,0:T(8,128)(2,1)S(1)}, u32[]{:S(2)}) copy-start(bf16[256,512]{1,0:T(8,128)(2,1)S(1)} %get-tuple-element.39.v_ref) | copy-start | bytes 786436
  67.3 21.7 %all-to-all-start.3 = ((bf16[32,8,1024]{2,1,0:T(8,128)(2,1)}), bf16[32,8,1024]{2,1,0:T(8,128)(2,1)S(1)}, u32[]{:S(2)}, u32[]{:S(2)}) async-start(bf16[32,8,1024]{2,1,0:T(8,128)(2,1)} %shard_map.141), calls=%async_computation.3 | async-start | bytes 1048576 | tf_op jit(solution)/shard_map/all_to_all | solution.py:480
  75.0 1.0 copy-start.2
  76.0 0.9 copy-start.4
  76.9 12.1 %copy-start = (bf16[512,2048]{1,0:T(8,128)(2,1)S(1)}, bf16[512,2048]{1,0:T(8,128)(2,1)}, u32[]{:S(2)}) copy-start(bf16[512,2048]{1,0:T(8,128)(2,1)} %wo_ref.3) | copy-start | bytes 6291460
  76.9 12.1 %copy-start.5 = (bf16[512]{0:T(512)(128)(2,1)S(1)}, bf16[512]{0:T(512)(128)(2,1)}, u32[]{:S(2)}) copy-start(bf16[512]{0:T(512)(128)(2,1)} %param.24) | copy-start | bytes 3076
  89.8 15.5 %copy-start.6 = (bf16[32,2048]{1,0:T(8,128)(2,1)S(1)}, bf16[32,2048]{1,0:T(8,128)(2,1)}, u32[]{:S(2)}) copy-start(bf16[32,2048]{1,0:T(8,128)(2,1)} %refs_0_) | copy-start | bytes 393220
  89.8 5.9 %collective-permute-start.8 = (bf16[128,2048]{1,0:T(8,128)(2,1)S(1)}, bf16[128,2048]{1,0:T(8,128)(2,1)S(1)}, u32[]{:S(2)}, u32[]{:S(2)}) collective-permute-start(bf16[128,2048]{1,0:T(8,128)(2,1)S(1)} %shard_map.143), channel_id=1, source_target_pairs={{0,1},{1,0},{2,3},{3,2},{4,5},{5,4},{6,7},{7,6},{8,9},{9,8},{10,11... | collective-permute-start | bytes 1572872 | tf_op jit(solution)/shard_map/ppermute | solution.py:499
  95.8 4.8 %collective-permute-start.10 = (bf16[32,2048]{1,0:T(8,128)(2,1)S(1)}, bf16[32,2048]{1,0:T(8,128)(2,1)S(1)}, u32[]{:S(2)}, u32[]{:S(2)}) collective-permute-start(bf16[32,2048]{1,0:T(8,128)(2,1)S(1)} %get-tuple-element.47), channel_id=1, source_target_pairs={{0,6},{2,0},{4,2},{6,4},{1,7},{3,1},{5,3},{7,5},{8,14},{10,8},{12,... | collective-permute-start | bytes 393224 | tf_op jit(solution)/shard_map/ppermute | solution.py:512
  96.8 8.5 %collective-permute-start.11 = (bf16[32,2048]{1,0:T(8,128)(2,1)S(1)}, bf16[32,2048]{1,0:T(8,128)(2,1)S(1)}, u32[]{:S(2)}, u32[]{:S(2)}) collective-permute-start(bf16[32,2048]{1,0:T(8,128)(2,1)S(1)} %get-tuple-element.48), channel_id=1, source_target_pairs={{0,2},{2,4},{4,6},{6,0},{1,3},{3,5},{5,7},{7,1},{8,10},{10,12},{12... | collective-permute-start | bytes 393224 | tf_op jit(solution)/shard_map/ppermute | solution.py:512
  97.4 8.0 %collective-permute-start.9 = (bf16[32,2048]{1,0:T(8,128)(2,1)S(1)}, bf16[32,2048]{1,0:T(8,128)(2,1)S(1)}, u32[]{:S(2)}, u32[]{:S(2)}) collective-permute-start(bf16[32,2048]{1,0:T(8,128)(2,1)S(1)} %get-tuple-element.46), channel_id=1, source_target_pairs={{0,4},{2,6},{4,0},{6,2},{1,5},{3,7},{5,1},{7,3},{8,12},{10,14},{12... | collective-permute-start | bytes 393224 | tf_op jit(solution)/shard_map/ppermute | solution.py:512

commit v10 on v7

--- a/solution.py
+++ b/solution.py
@@ -77,8 +77,8 @@
 
 
 def prepare_kernel(
-    lines, weights_hbm, condition_hbm, decay_hbm, row_hbm, column_hbm, gain_hbm, wk_hbm, wv_hbm,
-    out_ref, decay_ref, row_ref, column_ref, gain_ref, wk_ref, wv_ref,
+    lines, weights_hbm, condition_hbm, decay_hbm, row_hbm, column_hbm, gain_hbm,
+    out_ref, decay_ref, row_ref, column_ref, gain_ref,
     weights_ref, condition_ref, sems,
 ):
     size, width = weights_hbm.shape[0], condition_hbm.shape[1]
@@ -98,8 +98,6 @@
         row = seq * chips + (chip - d + chips) % chips
         loads.append(started(row_hbm.at[row], row_ref.at[d], sems, 5 + d))
     loads.append(started(gain_hbm, gain_ref, sems, 5 + chips))
-    loads.append(started(wk_hbm, wk_ref, sems, 6 + chips))
-    loads.append(started(wv_hbm.at[:, : wv_ref.shape[1]], wv_ref, sems, 7 + chips))
     loads[0].wait()
     values = condition_ref[...].astype(f32)
     values = jnp.concatenate([values] * 4, axis=0)
@@ -132,7 +130,13 @@
     return np.concatenate([np.cos(angles), np.sin(angles) * sign], axis=1)
 
 
-def tables_kernel(lines, chips, decay_ref, col_ref, line_ref):
+def tables_kernel(
+    lines, chips, wk_hbm, wv_hbm, decay_ref, col_ref, line_ref, wk_ref, wv_ref, sems
+):
+    loads = [
+        started(wk_hbm, wk_ref, sems, 0),
+        started(wv_hbm.at[:, : wv_ref.shape[1]], wv_ref, sems, 1),
+    ]
     rows = 2 * chips * lines
     chip, core = lax.axis_index("x"), lax.axis_index("c")
 
@@ -159,6 +163,8 @@
     line_ref[2:3, :] = place_line.astype(f32)
     odd = lax.axis_index("y") % 2
     line_ref[3:4, :] = jnp.full((1, rows), odd, jnp.int32).astype(f32)
+    for copy in loads:
+        copy.wait()
 
 
 def gather_kernel(pieces_ref, out_ref, decay_ref):
@@ -201,26 +207,19 @@
 
     lines_of = [line_of(which) for which in range(2)]
 
-    def modulate(source_ref, base, which):
+    def modulated(source, which):
         shift, scale = lines_of[which]
-
-        def block(i, carry):
-            own = pl.ds(pl.multiple_of(i * 16, 16), 16)
-            wide = source_ref[own, :].astype(f32)
-            normal = wide * lax.rsqrt(jnp.mean(wide * wide, axis=-1, keepdims=True) + epsilon)
-            target = pl.ds(pl.multiple_of(base + i * 16, 16), 16)
-            normed_ref[target, :] = (normal * scale + shift).astype(bf16)
-            return carry
-
-        lax.fori_loop(0, source_ref.shape[0] // 16, block, 0)
+        wide = source.astype(f32)
+        normal = wide * lax.rsqrt(jnp.mean(wide * wide, axis=-1, keepdims=True) + epsilon)
+        return (normal * scale + shift).astype(bf16)
 
     for i, piece in enumerate(pieces[1:]):
-        modulate(piece, (i + 1) * lines, 0)
-    modulate(far_ref, rows + near, 1)
+        normed_ref[(i + 1) * lines : (i + 2) * lines, :] = modulated(piece[...], 0)
+    normed_ref[rows + near :, :] = modulated(far_ref[...], 1)
     for copy in own:
         copy.wait()
-    modulate(own_ref, 0, 0)
-    modulate(near_ref, rows, 1)
+    normed_ref[0:lines, :] = modulated(own_ref[...], 0)
+    normed_ref[rows : rows + near, :] = modulated(near_ref[...], 1)
     stores = [started(normed_ref.at[0:rows], normed_hbm, sems, 2)]
     load.wait()
     keys = dot(normed_ref[...], wk_ref[...])
@@ -359,7 +358,7 @@
     columns = w_modulate.shape[1]
     sems = pltpu.SemaphoreType.DMA
     count, tp = lax.axis_size(SP), lax.axis_size(TP)
-    packed, decay_row, row_table, column_table, gain, early_key, early_value = kernel_call(
+    packed, decay_row, row_table, column_table, gain = kernel_call(
         functools.partial(prepare_kernel, lines),
         [
             ("v", shaped(count, 16, 128)),
@@ -367,14 +366,12 @@
             ("v", shaped(x_size, 1, DK, dtype=f32)),
             ("v", shaped(2 * lines, DK, dtype=f32)),
             ("v", shaped(width // 128, 128)),
-            ("v", shaped(width, DK)),
-            ("v", shaped(width, DV // 2)),
-        ],
-        "hhhhhhhh",
+        ],
+        "hhhhhh",
         [
             pltpu.VMEM(w_modulate.shape, bf16),
             pltpu.VMEM(condition.shape, bf16),
-            sems((8 + x_size,)),
+            sems((6 + x_size,)),
         ],
         8,
         1000000,
@@ -384,8 +381,6 @@
         jnp.asarray(rotary_tables(count * rows // GRID_W))[:, None],
         jnp.asarray(rotary_tables(GRID_W)),
         norm_gain.reshape(-1, 128),
-        w_key,
-        w_value,
     )
     pieces = lax.all_to_all(packed, SP, 0, 0, tiled=True)
     spread, decays = kernel_call(
@@ -403,13 +398,20 @@
     own_rows = [later] + [lax.ppermute(later, "x", ring(x_size, d)) for d in range(1, x_size)]
     other_rows = [lax.ppermute(piece, "c", swap) for piece in own_rows]
     far = lax.ppermute(near, "y", [(0, 1), (1, 0), (2, 3), (3, 2)])
-    col, line = kernel_call(
+    col, line, early_key, early_value = kernel_call(
         functools.partial(tables_kernel, lines, x_size),
-        [("v", shaped(rows, 8, dtype=f32)), ("v", shaped(4, rows, dtype=f32))],
-        "v",
-        [],
+        [
+            ("v", shaped(rows, 8, dtype=f32)),
+            ("v", shaped(4, rows, dtype=f32)),
+            ("v", shaped(width, DK)),
+            ("v", shaped(width, DV // 2)),
+        ],
+        "hhv",
+        [sems((2,))],
         8,
         1000000,
+        w_key,
+        w_value,
         decay_row,
     )
 

time: 108 us -> 106 us (0.981)
  waiting for transfers between devices: 24.1 us -> 22.9 us
    all_to_all x1, waiting for transfers between devices: 4.37 us -> 3.16 us  [per_device(): modulation = lax.all_to_all(spread, TP, 0, 0, tiled=True)]
  transfers between devices with their start and end apart: 15 -> 15, of which waited for: 6 -> 6; matrix products, arithmetic and copies ran while one was open for 0% -> 0% of each run, Pallas kernels for 5% -> 6%
where the time goes in v10:
time: 106 us; the launch traced here: 105 us
  starting transfers between devices  41.5 us (39%)
  blocking collectives  25.6 us (24%)
  waiting for transfers between devices  22.9 us (22%)
  Pallas kernels  13.8 us (13%)
    all_to_all x1, blocking collectives, per_device(): lax.all_to_all(send.reshape(count, DK // count, lanes), YZ, 0, 0, tiled=T...  25.6 us
    pallas_call x9, Pallas kernels, kernel_call(): pl.pallas_call(body, out_shape=tuple((pltpu.HBM(a.shape, a.dtype) if k ==...  13.8 us
    all_to_all x1, starting transfers between devices, per_device(): pieces = lax.all_to_all(packed, SP, 0, 0, tiled=True)  12 us
    all_to_all x1, waiting for transfers between devices, per_device(): states = lax.all_to_all(entering, YZ, 0, 0, tiled=True).reshape(DK, 2 * DV)  10.3 us
    all_to_all x1, starting transfers between devices, per_device(): states = lax.all_to_all(entering, YZ, 0, 0, tiled=True).reshape(DK, 2 * DV)  7.73 us
    ppermute x3, waiting for transfers between devices, per_device(): arrived = lax.ppermute(tiles[d], 'x', ring(x_size, -d))  7.17 us
    ppermute x3, starting transfers between devices, per_device(): lax.ppermute(later, 'x', ring(x_size, d))  4.89 us
    ppermute x4, starting transfers between devices, per_device(): other_rows = [lax.ppermute(piece, 'c', swap) for piece in own_rows]  4.77 us
  transfers between devices with their start and end apart: 15, of which 6 were waited for; matrix products, arithmetic and copies ran while one was open for 0% of the time, Pallas kernels for 6%

profile of v10, /device:TPU:1, one launch (start us, length us, event | category | flops | bytes accessed | tf_op | source)
XLA Modules:
  0.0 104.9 jit_solution(6868903087328947487)
XLA Ops:
  0.0 1.8 %shard_map.136 = (bf16[32,16,128]{2,1,0:T(8,128)(2,1)}, f32[1,256]{1,0:T(1,128)S(1)}, f32[4,1,256]{2,1,0:T(1,128)S(1)}, f32[64,256]{1,0:T(8,128)S(1)}, bf16[16,128]{1,0:T(8,128)(2,1)S(1)}) custom-call(bf16[64,768]{1,0:T(8,128)(2,1)} %weights_hbm.1, bf16[2,2048]{1,0:T(2,128)(2,1)} %condition_hbm.1, f32[1,256]{1,0:T(1,128)} %bitcast.13, ...), custom_call_target="tpu_custom_call" | custom-call | flops 1000000 | bytes 308224 | tf_op jit(solution)/shard_map/pallas_call | solution.py:35
  1.8 12.0 %all-to-all-start = ((bf16[32,16,128]{2,1,0:T(8,128)(2,1)}), bf16[32,16,128]{2,1,0:T(8,128)(2,1)S(1)}, u32[]{:S(2)}, u32[]{:S(2)}) async-start(bf16[32,16,128]{2,1,0:T(8,128)(2,1)} %get-tuple-element.29), calls=%async_computation | async-start | bytes 262144 | tf_op jit(solution)/shard_map/all_to_all | solution.py:385
  13.9 1.3 %collective-permute-start = (bf16[32,2048]{1,0:T(8,128)(2,1)}, bf16[32,2048]{1,0:T(8,128)(2,1)S(1)}, u32[]{:S(2)}, u32[]{:S(2)}) collective-permute-start(bf16[32,2048]{1,0:T(8,128)(2,1)} %refs_0_), channel_id=1, source_target_pairs={{0,2},{2,4},{4,6},{6,0},{1,3},{3,5},{5,7},{7,1},{8,10},{10,12},{12... | collective-permute-start | bytes 393224 | tf_op jit(solution)/shard_map/ppermute | solution.py:398
  15.2 2.5 %collective-permute-start.1 = (bf16[32,2048]{1,0:T(8,128)(2,1)}, bf16[32,2048]{1,0:T(8,128)(2,1)S(1)}, u32[]{:S(2)}, u32[]{:S(2)}) collective-permute-start(bf16[32,2048]{1,0:T(8,128)(2,1)} %refs_0_), channel_id=1, source_target_pairs={{0,4},{2,6},{4,0},{6,2},{1,5},{3,7},{5,1},{7,3},{8,12},{10,14},{12... | collective-permute-start | bytes 393224 | tf_op jit(solution)/shard_map/ppermute | solution.py:398
  17.6 1.2 %collective-permute-start.2 = (bf16[32,2048]{1,0:T(8,128)(2,1)}, bf16[32,2048]{1,0:T(8,128)(2,1)S(1)}, u32[]{:S(2)}, u32[]{:S(2)}) collective-permute-start(bf16[32,2048]{1,0:T(8,128)(2,1)} %refs_0_), channel_id=1, source_target_pairs={{0,6},{2,0},{4,2},{6,4},{1,7},{3,1},{5,3},{7,5},{8,14},{10,8},{12,... | collective-permute-start | bytes 393224 | tf_op jit(solution)/shard_map/ppermute | solution.py:398
  18.8 1.8 %collective-permute-start.3 = (bf16[32,2048]{1,0:T(8,128)(2,1)}, bf16[32,2048]{1,0:T(8,128)(2,1)S(1)}, u32[]{:S(2)}, u32[]{:S(2)}) collective-permute-start(bf16[32,2048]{1,0:T(8,128)(2,1)} %refs_0_), channel_id=1, source_target_pairs={{0,1},{1,0},{2,3},{3,2},{4,5},{5,4},{6,7},{7,6},{8,9},{9,8},{10,11... | collective-permute-start | bytes 393224 | tf_op jit(solution)/shard_map/ppermute | solution.py:399
  20.6 0.0 collective-permute-done.refs_1_
  20.6 1.2 %collective-permute-start.4 = (bf16[32,2048]{1,0:T(8,128)(2,1)S(1)}, bf16[32,2048]{1,0:T(8,128)(2,1)S(1)}, u32[]{:S(2)}, u32[]{:S(2)}) collective-permute-start(bf16[32,2048]{1,0:T(8,128)(2,1)S(1)} %collective-permute-done.refs_1_), channel_id=1, source_target_pairs={{0,1},{1,0},{2,3},{3,2},{4,5},{5,4},{6,7},{7,6},{8,9},{9,8},{10,11... | collective-permute-start | bytes 393224 | tf_op jit(solution)/shard_map/ppermute | solution.py:399
  21.7 1.5 %collective-permute-done.1.refs_2_ = bf16[32,2048]{1,0:T(8,128)(2,1)S(1)} collective-permute-done((bf16[32,2048]{1,0:T(8,128)(2,1)}, bf16[32,2048]{1,0:T(8,128)(2,1)S(1)}, u32[]{:S(2)}, u32[]{:S(2)}) %collective-permute-start.1) | collective-permute-done | bytes 131104 | tf_op jit(solution)/shard_map/ppermute | solution.py:398
  23.3 1.8 %collective-permute-start.5 = (bf16[32,2048]{1,0:T(8,128)(2,1)S(1)}, bf16[32,2048]{1,0:T(8,128)(2,1)S(1)}, u32[]{:S(2)}, u32[]{:S(2)}) collective-permute-start(bf16[32,2048]{1,0:T(8,128)(2,1)S(1)} %collective-permute-done.1.refs_2_), channel_id=1, source_target_pairs={{0,1},{1,0},{2,3},{3,2},{4,5},{5,4},{6,7},{7,6},{8,9},{9,8},{10,11... | collective-permute-start | bytes 393224 | tf_op jit(solution)/shard_map/ppermute | solution.py:399
  25.1 0.0 collective-permute-done.2.refs_3_
  25.1 0.0 collective-permute-start.6
  25.1 1.3 %collective-permute-start.7 = (bf16[16,2048]{1,0:T(8,128)(2,1)}, bf16[16,2048]{1,0:T(8,128)(2,1)S(1)}, u32[]{:S(2)}, u32[]{:S(2)}) collective-permute-start(bf16[16,2048]{1,0:T(8,128)(2,1)} %refs_8_), channel_id=1, source_target_pairs={{0,8},{8,0},{16,24},{24,16},{1,9},{9,1},{17,25},{25,17},{2,10},{10... | collective-permute-start | bytes 196616 | tf_op jit(solution)/shard_map/ppermute | solution.py:400
  26.4 0.0 all-to-all-done.pieces_ref
  26.4 0.7 shard_map.137
  27.0 4.2 %all-to-all-start.1 = ((f32[8,2,768]{2,1,0:T(2,128)}), f32[8,2,768]{2,1,0:T(2,128)S(1)}, u32[]{:S(2)}, u32[]{:S(2)}) async-start(f32[8,2,768]{2,1,0:T(2,128)} %get-tuple-element.30), calls=%async_computation.1 | async-start | bytes 98304 | tf_op jit(solution)/shard_map/all_to_all | solution.py:395
  31.2 1.6 %shard_map.138 = (f32[256,8]{1,0:T(8,128)S(1)}, f32[4,256]{1,0:T(4,128)S(1)}, bf16[2048,256]{1,0:T(8,128)(2,1)S(1)}, bf16[2048,256]{1,0:T(8,128)(2,1)S(1)}) custom-call(bf16[2048,256]{1,0:T(8,128)(2,1)} %wk_hbm.1, bf16[2048,512]{1,0:T(8,128)(2,1)} %refs_9_.1, f32[1,256]{1,0:T(1,128)S(1)} %get-tuple-element.33.decay_ref), custom_call_target="tpu_custom_call" | custom-call | flops 1000000 | bytes 3146752 | tf_op jit(solution)/shard_map/pallas_call | solution.py:35
  32.8 0.0 collective-permute-done.7.refs_13_
  32.8 0.0 collective-permute-done.3.refs_4_
  32.8 0.0 collective-permute-done.4.refs_5_
  32.8 0.0 collective-permute-done.5.refs_6_
  32.9 0.0 collective-permute-done.6.refs_7_
  32.9 3.2 %all-to-all-done.1.refs_14_ = f32[8,2,768]{2,1,0:T(2,128)S(1)} async-done(((f32[8,2,768]{2,1,0:T(2,128)}), f32[8,2,768]{2,1,0:T(2,128)S(1)}, u32[]{:S(2)}, u32[]{:S(2)}) %all-to-all-start.1) | async-done | bytes 49184 | tf_op jit(solution)/shard_map/all_to_all | solution.py:395
  36.0 3.5 %shard_map.139 = (bf16[256,1280]{1,0:T(8,128)(2,1)S(1)}, bf16[256,2048]{1,0:T(8,128)(2,1)}, bf16[256,256]{1,0:T(8,128)(2,1)}, bf16[256,512]{1,0:T(8,128)(2,1)}) custom-call(bf16[32,2048]{1,0:T(8,128)(2,1)} %refs_0_, bf16[32,2048]{1,0:T(8,128)(2,1)S(1)} %collective-permute-done.refs_1_, bf16[32,2048]{1,0:T(8,128)(2,1)S(1)} %collective-permute-done.1.refs_2_, ...), custom_call_target="tpu_custom_call" | custom-call | flops 905969664 | bytes 5509120 | tf_op jit(solution)/shard_map/pallas_call | solution.py:35
  39.5 25.6 %all_to_all.20.parts_ref = bf16[32,8,1280]{2,1,0:T(8,128)(2,1)S(1)} all-to-all(bf16[32,8,1280]{2,1,0:T(8,128)(2,1)S(1)} %bitcast.8), channel_id=1, replica_groups=mesh['z'=8,'y'=4,'x'=4,'c'=2] {'y','z'}, dimensions={0} | all-to-all | bytes 1310720 | tf_op jit(solution)/shard_map/all_to_all | solution.py:454
  65.1 1.0 shard_map.141
  66.1 7.7 %all-to-all-start.3 = ((bf16[32,8,1024]{2,1,0:T(8,128)(2,1)}), bf16[32,8,1024]{2,1,0:T(8,128)(2,1)S(1)}, u32[]{:S(2)}, u32[]{:S(2)}) async-start(bf16[32,8,1024]{2,1,0:T(8,128)(2,1)} %shard_map.141), calls=%async_computation.3 | async-start | bytes 1048576 | tf_op jit(solution)/shard_map/all_to_all | solution.py:493
  73.8 0.0 copy-start
  73.8 0.0 copy-start.1
  73.9 3.6 %shard_map.140 = (bf16[256,256]{1,0:T(8,128)(2,1)S(1)}, bf16[256,512]{1,0:T(8,128)(2,1)S(1)}, bf16[256,512]{1,0:T(8,128)(2,1)S(1)}) custom-call(bf16[256,2048]{1,0:T(8,128)(2,1)} %get-tuple-element.41.normed_hbm, bf16[2048,256]{1,0:T(8,128)(2,1)} %wq_hbm.1, bf16[2048,512]{1,0:T(8,128)(2,1)} %wg_hbm.1, bf16[256,256]{1,0:T(8,128)(2,1)} %get-tuple-element.42.k_hbm, ...), custom_call_target="tpu_custom_call" | custom-call | flops 805306368 | bytes 4669440 | tf_op jit(solution)/shard_map/pallas_call | solution.py:35
  77.5 10.3 %all-to-all-done.3 = bf16[32,8,1024]{2,1,0:T(8,128)(2,1)S(1)} async-done(((bf16[32,8,1024]{2,1,0:T(8,128)(2,1)}), bf16[32,8,1024]{2,1,0:T(8,128)(2,1)S(1)}, u32[]{:S(2)}, u32[]{:S(2)}) %all-to-all-start.3) | async-done | bytes 524320 | tf_op jit(solution)/shard_map/all_to_all | solution.py:493
  87.8 0.0 copy-done
  87.8 0.0 copy-done.1
  87.8 0.8 shard_map.143
  88.6 0.0 copy-start.2
  88.7 4.3 %collective-permute-start.8 = (bf16[128,2048]{1,0:T(8,128)(2,1)S(1)}, bf16[128,2048]{1,0:T(8,128)(2,1)S(1)}, u32[]{:S(2)}, u32[]{:S(2)}) collective-permute-start(bf16[128,2048]{1,0:T(8,128)(2,1)S(1)} %shard_map.143), channel_id=1, source_target_pairs={{0,1},{1,0},{2,3},{3,2},{4,5},{5,4},{6,7},{7,6},{8,9},{9,8},{10,11... | collective-permute-start | bytes 1572872 | tf_op jit(solution)/shard_map/ppermute | solution.py:512
  93.0 0.8 shard_map.142.own_ref
  93.8 0.7 collective-permute-done.8.crossed_ref
  94.5 0.1 shard_map.144
  94.7 1.0 collective-permute-start.10
  95.6 0.6 collective-permute-start.11
  96.2 0.8 collective-permute-start.9
  97.0 2.4 %collective-permute-done.10 = bf16[32,2048]{1,0:T(8,128)(2,1)S(1)} collective-permute-done((bf16[32,2048]{1,0:T(8,128)(2,1)S(1)}, bf16[32,2048]{1,0:T(8,128)(2,1)S(1)}, u32[]{:S(2)}, u32[]{:S(2)}) %collective-permute-start.10) | collective-permute-done | bytes 131104 | tf_op jit(solution)/shard_map/ppermute | solution.py:525
  99.4 4.7 %collective-permute-done.11 = bf16[32,2048]{1,0:T(8,128)(2,1)S(1)} collective-permute-done((bf16[32,2048]{1,0:T(8,128)(2,1)S(1)}, bf16[32,2048]{1,0:T(8,128)(2,1)S(1)}, u32[]{:S(2)}, u32[]{:S(2)}) %collective-permute-start.11) | collective-permute-done | bytes 131104 | tf_op jit(solution)/shard_map/ppermute | solution.py:525
  104.2 0.0 collective-permute-done.9
  104.2 0.0 copy-done.2
  104.2 0.8 add_convert_fusion
  (2 shorter events, 0.0 us)
Async XLA Ops:
  1.8 24.5 %all-to-all-start = ((bf16[32,16,128]{2,1,0:T(8,128)(2,1)}), bf16[32,16,128]{2,1,0:T(8,128)(2,1)S(1)}, u32[]{:S(2)}, u32[]{:S(2)}) async-start(bf16[32,16,128]{2,1,0:T(8,128)(2,1)} %get-tuple-element.29), calls=%async_computation | async-start | bytes 262144 | tf_op jit(solution)/shard_map/all_to_all | solution.py:385
  13.9 6.7 %collective-permute-start = (bf16[32,2048]{1,0:T(8,128)(2,1)}, bf16[32,2048]{1,0:T(8,128)(2,1)S(1)}, u32[]{:S(2)}, u32[]{:S(2)}) collective-permute-start(bf16[32,2048]{1,0:T(8,128)(2,1)} %refs_0_), channel_id=1, source_target_pairs={{0,2},{2,4},{4,6},{6,0},{1,3},{3,5},{5,7},{7,1},{8,10},{10,12},{12... | collective-permute-start | bytes 393224 | tf_op jit(solution)/shard_map/ppermute | solution.py:398
  15.2 8.1 %collective-permute-start.1 = (bf16[32,2048]{1,0:T(8,128)(2,1)}, bf16[32,2048]{1,0:T(8,128)(2,1)S(1)}, u32[]{:S(2)}, u32[]{:S(2)}) collective-permute-start(bf16[32,2048]{1,0:T(8,128)(2,1)} %refs_0_), channel_id=1, source_target_pairs={{0,4},{2,6},{4,0},{6,2},{1,5},{3,7},{5,1},{7,3},{8,12},{10,14},{12... | collective-permute-start | bytes 393224 | tf_op jit(solution)/shard_map/ppermute | solution.py:398
  17.6 7.5 %collective-permute-start.2 = (bf16[32,2048]{1,0:T(8,128)(2,1)}, bf16[32,2048]{1,0:T(8,128)(2,1)S(1)}, u32[]{:S(2)}, u32[]{:S(2)}) collective-permute-start(bf16[32,2048]{1,0:T(8,128)(2,1)} %refs_0_), channel_id=1, source_target_pairs={{0,6},{2,0},{4,2},{6,4},{1,7},{3,1},{5,3},{7,5},{8,14},{10,8},{12,... | collective-permute-start | bytes 393224 | tf_op jit(solution)/shard_map/ppermute | solution.py:398
  18.8 14.1 %collective-permute-start.3 = (bf16[32,2048]{1,0:T(8,128)(2,1)}, bf16[32,2048]{1,0:T(8,128)(2,1)S(1)}, u32[]{:S(2)}, u32[]{:S(2)}) collective-permute-start(bf16[32,2048]{1,0:T(8,128)(2,1)} %refs_0_), channel_id=1, source_target_pairs={{0,1},{1,0},{2,3},{3,2},{4,5},{5,4},{6,7},{7,6},{8,9},{9,8},{10,11... | collective-permute-start | bytes 393224 | tf_op jit(solution)/shard_map/ppermute | solution.py:399
  20.6 12.3 %collective-permute-start.4 = (bf16[32,2048]{1,0:T(8,128)(2,1)S(1)}, bf16[32,2048]{1,0:T(8,128)(2,1)S(1)}, u32[]{:S(2)}, u32[]{:S(2)}) collective-permute-start(bf16[32,2048]{1,0:T(8,128)(2,1)S(1)} %collective-permute-done.refs_1_), channel_id=1, source_target_pairs={{0,1},{1,0},{2,3},{3,2},{4,5},{5,4},{6,7},{7,6},{8,9},{9,8},{10,11... | collective-permute-start | bytes 393224 | tf_op jit(solution)/shard_map/ppermute | solution.py:399
  23.3 9.6 %collective-permute-start.5 = (bf16[32,2048]{1,0:T(8,128)(2,1)S(1)}, bf16[32,2048]{1,0:T(8,128)(2,1)S(1)}, u32[]{:S(2)}, u32[]{:S(2)}) collective-permute-start(bf16[32,2048]{1,0:T(8,128)(2,1)S(1)} %collective-permute-done.1.refs_2_), channel_id=1, source_target_pairs={{0,1},{1,0},{2,3},{3,2},{4,5},{5,4},{6,7},{7,6},{8,9},{9,8},{10,11... | collective-permute-start | bytes 393224 | tf_op jit(solution)/shard_map/ppermute | solution.py:399
  25.1 7.8 %collective-permute-start.6 = (bf16[32,2048]{1,0:T(8,128)(2,1)S(1)}, bf16[32,2048]{1,0:T(8,128)(2,1)S(1)}, u32[]{:S(2)}, u32[]{:S(2)}) collective-permute-start(bf16[32,2048]{1,0:T(8,128)(2,1)S(1)} %collective-permute-done.2.refs_3_), channel_id=1, source_target_pairs={{0,1},{1,0},{2,3},{3,2},{4,5},{5,4},{6,7},{7,6},{8,9},{9,8},{10,11... | collective-permute-start | bytes 393224 | tf_op jit(solution)/shard_map/ppermute | solution.py:399
  25.1 7.7 %collective-permute-start.7 = (bf16[16,2048]{1,0:T(8,128)(2,1)}, bf16[16,2048]{1,0:T(8,128)(2,1)S(1)}, u32[]{:S(2)}, u32[]{:S(2)}) collective-permute-start(bf16[16,2048]{1,0:T(8,128)(2,1)} %refs_8_), channel_id=1, source_target_pairs={{0,8},{8,0},{16,24},{24,16},{1,9},{9,1},{17,25},{25,17},{2,10},{10... | collective-permute-start | bytes 196616 | tf_op jit(solution)/shard_map/ppermute | solution.py:400
  27.0 9.0 %all-to-all-start.1 = ((f32[8,2,768]{2,1,0:T(2,128)}), f32[8,2,768]{2,1,0:T(2,128)S(1)}, u32[]{:S(2)}, u32[]{:S(2)}) async-start(f32[8,2,768]{2,1,0:T(2,128)} %get-tuple-element.30), calls=%async_computation.1 | async-start | bytes 98304 | tf_op jit(solution)/shard_map/all_to_all | solution.py:395
  66.1 21.7 %all-to-all-start.3 = ((bf16[32,8,1024]{2,1,0:T(8,128)(2,1)}), bf16[32,8,1024]{2,1,0:T(8,128)(2,1)S(1)}, u32[]{:S(2)}, u32[]{:S(2)}) async-start(bf16[32,8,1024]{2,1,0:T(8,128)(2,1)} %shard_map.141), calls=%async_computation.3 | async-start | bytes 1048576 | tf_op jit(solution)/shard_map/all_to_all | solution.py:493
  73.8 14.0 %copy-start = (bf16[512,2048]{1,0:T(8,128)(2,1)S(1)}, bf16[512,2048]{1,0:T(8,128)(2,1)}, u32[]{:S(2)}) copy-start(bf16[512,2048]{1,0:T(8,128)(2,1)} %wo_ref.3) | copy-start | bytes 6291460
  73.8 14.0 %copy-start.1 = (bf16[512]{0:T(512)(128)(2,1)S(1)}, bf16[512]{0:T(512)(128)(2,1)}, u32[]{:S(2)}) copy-start(bf16[512]{0:T(512)(128)(2,1)} %param.24) | copy-start | bytes 3076
  88.6 15.5 %copy-start.2 = (bf16[32,2048]{1,0:T(8,128)(2,1)S(1)}, bf16[32,2048]{1,0:T(8,128)(2,1)}, u32[]{:S(2)}) copy-start(bf16[32,2048]{1,0:T(8,128)(2,1)} %refs_0_) | copy-start | bytes 393220
  88.7 5.9 %collective-permute-start.8 = (bf16[128,2048]{1,0:T(8,128)(2,1)S(1)}, bf16[128,2048]{1,0:T(8,128)(2,1)S(1)}, u32[]{:S(2)}, u32[]{:S(2)}) collective-permute-start(bf16[128,2048]{1,0:T(8,128)(2,1)S(1)} %shard_map.143), channel_id=1, source_target_pairs={{0,1},{1,0},{2,3},{3,2},{4,5},{5,4},{6,7},{7,6},{8,9},{9,8},{10,11... | collective-permute-start | bytes 1572872 | tf_op jit(solution)/shard_map/ppermute | solution.py:512
  94.7 4.8 %collective-permute-start.10 = (bf16[32,2048]{1,0:T(8,128)(2,1)S(1)}, bf16[32,2048]{1,0:T(8,128)(2,1)S(1)}, u32[]{:S(2)}, u32[]{:S(2)}) collective-permute-start(bf16[32,2048]{1,0:T(8,128)(2,1)S(1)} %get-tuple-element.51), channel_id=1, source_target_pairs={{0,6},{2,0},{4,2},{6,4},{1,7},{3,1},{5,3},{7,5},{8,14},{10,8},{12,... | collective-permute-start | bytes 393224 | tf_op jit(solution)/shard_map/ppermute | solution.py:525
  95.6 8.5 %collective-permute-start.11 = (bf16[32,2048]{1,0:T(8,128)(2,1)S(1)}, bf16[32,2048]{1,0:T(8,128)(2,1)S(1)}, u32[]{:S(2)}, u32[]{:S(2)}) collective-permute-start(bf16[32,2048]{1,0:T(8,128)(2,1)S(1)} %get-tuple-element.52), channel_id=1, source_target_pairs={{0,2},{2,4},{4,6},{6,0},{1,3},{3,5},{5,7},{7,1},{8,10},{10,12},{12... | collective-permute-start | bytes 393224 | tf_op jit(solution)/shard_map/ppermute | solution.py:525
  96.2 8.0 %collective-permute-start.9 = (bf16[32,2048]{1,0:T(8,128)(2,1)S(1)}, bf16[32,2048]{1,0:T(8,128)(2,1)S(1)}, u32[]{:S(2)}, u32[]{:S(2)}) collective-permute-start(bf16[32,2048]{1,0:T(8,128)(2,1)S(1)} %get-tuple-element.50), channel_id=1, source_target_pairs={{0,4},{2,6},{4,0},{6,2},{1,5},{3,7},{5,1},{7,3},{8,12},{10,14},{12... | collective-permute-start | bytes 393224 | tf_op jit(solution)/shard_map/ppermute | solution.py:525

commit v11 on v10

--- a/solution.py
+++ b/solution.py
@@ -130,13 +130,8 @@
     return np.concatenate([np.cos(angles), np.sin(angles) * sign], axis=1)
 
 
-def tables_kernel(
-    lines, chips, wk_hbm, wv_hbm, decay_ref, col_ref, line_ref, wk_ref, wv_ref, sems
-):
-    loads = [
-        started(wk_hbm, wk_ref, sems, 0),
-        started(wv_hbm.at[:, : wv_ref.shape[1]], wv_ref, sems, 1),
-    ]
+def tables_kernel(lines, chips, wk_hbm, decay_ref, col_ref, line_ref, wk_ref, sems):
+    loads = [started(wk_hbm, wk_ref, sems, 0)]
     rows = 2 * chips * lines
     chip, core = lax.axis_index("x"), lax.axis_index("c")
 
@@ -185,10 +180,10 @@
 def keys_kernel(*refs):
     pieces, refs = refs[:8], refs[8:]
     (
-        near_hbm, wv_hbm, wk_ref, low_ref, gain_ref, far_ref, mod_ref, col_ref, line_ref, row_ref,
+        near_hbm, wv_hbm, wk_ref, gain_ref, far_ref, mod_ref, col_ref, line_ref, row_ref,
         column_ref,
-        send_ref, normed_hbm, k_hbm, v_hbm,
-        own_ref, near_ref, high_ref, normed_ref, k_ref, v_ref, sems,
+        send_ref, normed_hbm, k_ref, v_ref,
+        own_ref, near_ref, wv_ref, normed_ref, sems,
     ) = refs
     lines, width = pieces[0].shape
     rows = 8 * lines
@@ -197,7 +192,7 @@
         started(pieces[0], own_ref, sems, 3),
         started(near_hbm, near_ref, sems, 4),
     ]
-    load = started(wv_hbm.at[:, low_ref.shape[1] :], high_ref, sems, 0)
+    load = started(wv_hbm, wv_ref, sems, 0)
     gain = flat_gain(gain_ref)
     tp = mod_ref.shape[0]
 
@@ -221,21 +216,17 @@
     normed_ref[0:lines, :] = modulated(own_ref[...], 0)
     normed_ref[rows : rows + near, :] = modulated(near_ref[...], 1)
     stores = [started(normed_ref.at[0:rows], normed_hbm, sems, 2)]
-    load.wait()
     keys = dot(normed_ref[...], wk_ref[...])
-    low = dot(normed_ref[...], low_ref[...]).astype(bf16)
-    high = dot(normed_ref[...], high_ref[...]).astype(bf16)
-    values = jnp.concatenate([low, high], axis=1)
     key_rows = (turn(keys[:rows], row_ref, column_ref) * DK ** (-0.5)).astype(bf16)
     ctx_keys = (keys[rows:] * DK ** (-0.5)).astype(bf16)
     k_ref[...] = key_rows
-    stores.append(started(k_ref, k_hbm, sems, 1))
     wide = key_rows.astype(f32)
     ahead = (wide * jnp.exp(col_ref[:, 0:1])).astype(bf16)
     behind = (wide * jnp.exp(col_ref[:, 1:2])).astype(bf16)
     turned = jnp.concatenate([ahead.T, behind.T], axis=0)
+    load.wait()
+    values = dot(normed_ref[...], wv_ref[...]).astype(bf16)
     v_ref[...] = values[:rows]
-    stores.append(started(v_ref, v_hbm, sems, 5))
     parts = dot(turned, values[:rows]).astype(bf16)
     send_ref[:, 0:DV] = parts[:DK]
     send_ref[:, DV : 2 * DV] = parts[DK:]
@@ -398,20 +389,18 @@
     own_rows = [later] + [lax.ppermute(later, "x", ring(x_size, d)) for d in range(1, x_size)]
     other_rows = [lax.ppermute(piece, "c", swap) for piece in own_rows]
     far = lax.ppermute(near, "y", [(0, 1), (1, 0), (2, 3), (3, 2)])
-    col, line, early_key, early_value = kernel_call(
+    col, line, early_key = kernel_call(
         functools.partial(tables_kernel, lines, x_size),
         [
             ("v", shaped(rows, 8, dtype=f32)),
             ("v", shaped(4, rows, dtype=f32)),
             ("v", shaped(width, DK)),
-            ("v", shaped(width, DV // 2)),
-        ],
-        "hhv",
-        [sems((2,))],
+        ],
+        "hv",
+        [sems((1,))],
         8,
         1000000,
         w_key,
-        w_value,
         decay_row,
     )
 
@@ -422,18 +411,16 @@
         [
             ("v", shaped(DK, lanes)),
             ("h", shaped(rows, width)),
-            ("h", shaped(rows, DK)),
-            ("h", shaped(rows, DV)),
-        ],
-        "hvvvvvvv" + "hhvvvvvvvvv",
+            ("v", shaped(rows, DK)),
+            ("v", shaped(rows, DV)),
+        ],
+        "hvvvvvvv" + "hhvvvvvvvv",
         [
             pltpu.VMEM((lines, width), bf16),
             pltpu.VMEM(context.shape, bf16),
-            pltpu.VMEM((width, DV // 2), bf16),
+            pltpu.VMEM((width, DV), bf16),
             pltpu.VMEM((rows + ctx, width), bf16),
-            pltpu.VMEM((rows, DK), bf16),
-            pltpu.VMEM((rows, DV), bf16),
-            sems((6,)),
+            sems((5,)),
         ],
         32,
         2 * (rows + ctx) * width * (DK + DV),
@@ -442,7 +429,6 @@
         near,
         w_value,
         early_key,
-        early_value,
         gain,
         far,
         modulation,
@@ -521,7 +507,7 @@
         crossed,
     )
     projected = tiles[0].astype(f32)
-    for d in (2, 1, 3):
+    for d in (1, 3, 2):
         arrived = lax.ppermute(tiles[d], "x", ring(x_size, -d))
         projected = projected + arrived.astype(f32)
     gate = modulation[:, 0].reshape(-1)[2 * width :]

time: 106 us -> 105 us (level)
  transfers between devices with their start and end apart: 15 -> 15, of which waited for: 6 -> 7; matrix products, arithmetic and copies ran while one was open for 0% -> 0% of each run, Pallas kernels for 6% -> 6%
where the time goes in v11:
time: 105 us; the launch traced here: 104 us
  starting transfers between devices  42.1 us (40%)
  blocking collectives  25.6 us (24%)
  waiting for transfers between devices  22.3 us (21%)
  Pallas kernels  13.3 us (13%)
    all_to_all x1, blocking collectives, per_device(): lax.all_to_all(send.reshape(count, DK // count, lanes), YZ, 0, 0, tiled=T...  25.6 us
    pallas_call x9, Pallas kernels, kernel_call(): pl.pallas_call(body, out_shape=tuple((pltpu.HBM(a.shape, a.dtype) if k ==...  13.3 us
    all_to_all x1, starting transfers between devices, per_device(): pieces = lax.all_to_all(packed, SP, 0, 0, tiled=True)  12 us
    all_to_all x1, waiting for transfers between devices, per_device(): states = lax.all_to_all(entering, YZ, 0, 0, tiled=True).reshape(DK, 2 * DV)  10.3 us
    all_to_all x1, starting transfers between devices, per_device(): states = lax.all_to_all(entering, YZ, 0, 0, tiled=True).reshape(DK, 2 * DV)  7.73 us
    ppermute x3, waiting for transfers between devices, per_device(): arrived = lax.ppermute(tiles[d], 'x', ring(x_size, -d))  6.22 us
    ppermute x3, starting transfers between devices, per_device(): lax.ppermute(later, 'x', ring(x_size, d))  4.89 us
    ppermute x4, starting transfers between devices, per_device(): other_rows = [lax.ppermute(piece, 'c', swap) for piece in own_rows]  4.77 us
  transfers between devices with their start and end apart: 15, of which 7 were waited for; matrix products, arithmetic and copies ran while one was open for 0% of the time, Pallas kernels for 6%

profile of v11, /device:TPU:1, one launch (start us, length us, event | category | flops | bytes accessed | tf_op | source)
XLA Modules:
  0.0 104.4 jit_solution(18184538810477984716)
XLA Ops:
  0.0 1.8 %shard_map.136 = (bf16[32,16,128]{2,1,0:T(8,128)(2,1)}, f32[1,256]{1,0:T(1,128)S(1)}, f32[4,1,256]{2,1,0:T(1,128)S(1)}, f32[64,256]{1,0:T(8,128)S(1)}, bf16[16,128]{1,0:T(8,128)(2,1)S(1)}) custom-call(bf16[64,768]{1,0:T(8,128)(2,1)} %weights_hbm.1, bf16[2,2048]{1,0:T(2,128)(2,1)} %condition_hbm.1, f32[1,256]{1,0:T(1,128)} %bitcast.13, ...), custom_call_target="tpu_custom_call" | custom-call | flops 1000000 | bytes 308224 | tf_op jit(solution)/shard_map/pallas_call | solution.py:35
  1.8 12.0 %all-to-all-start = ((bf16[32,16,128]{2,1,0:T(8,128)(2,1)}), bf16[32,16,128]{2,1,0:T(8,128)(2,1)S(1)}, u32[]{:S(2)}, u32[]{:S(2)}) async-start(bf16[32,16,128]{2,1,0:T(8,128)(2,1)} %get-tuple-element.28), calls=%async_computation | async-start | bytes 262144 | tf_op jit(solution)/shard_map/all_to_all | solution.py:376
  13.9 1.3 %collective-permute-start = (bf16[32,2048]{1,0:T(8,128)(2,1)}, bf16[32,2048]{1,0:T(8,128)(2,1)S(1)}, u32[]{:S(2)}, u32[]{:S(2)}) collective-permute-start(bf16[32,2048]{1,0:T(8,128)(2,1)} %refs_0_), channel_id=1, source_target_pairs={{0,2},{2,4},{4,6},{6,0},{1,3},{3,5},{5,7},{7,1},{8,10},{10,12},{12... | collective-permute-start | bytes 393224 | tf_op jit(solution)/shard_map/ppermute | solution.py:389
  15.2 2.5 %collective-permute-start.1 = (bf16[32,2048]{1,0:T(8,128)(2,1)}, bf16[32,2048]{1,0:T(8,128)(2,1)S(1)}, u32[]{:S(2)}, u32[]{:S(2)}) collective-permute-start(bf16[32,2048]{1,0:T(8,128)(2,1)} %refs_0_), channel_id=1, source_target_pairs={{0,4},{2,6},{4,0},{6,2},{1,5},{3,7},{5,1},{7,3},{8,12},{10,14},{12... | collective-permute-start | bytes 393224 | tf_op jit(solution)/shard_map/ppermute | solution.py:389
  17.6 1.2 %collective-permute-start.2 = (bf16[32,2048]{1,0:T(8,128)(2,1)}, bf16[32,2048]{1,0:T(8,128)(2,1)S(1)}, u32[]{:S(2)}, u32[]{:S(2)}) collective-permute-start(bf16[32,2048]{1,0:T(8,128)(2,1)} %refs_0_), channel_id=1, source_target_pairs={{0,6},{2,0},{4,2},{6,4},{1,7},{3,1},{5,3},{7,5},{8,14},{10,8},{12,... | collective-permute-start | bytes 393224 | tf_op jit(solution)/shard_map/ppermute | solution.py:389
  18.8 1.8 %collective-permute-start.3 = (bf16[32,2048]{1,0:T(8,128)(2,1)}, bf16[32,2048]{1,0:T(8,128)(2,1)S(1)}, u32[]{:S(2)}, u32[]{:S(2)}) collective-permute-start(bf16[32,2048]{1,0:T(8,128)(2,1)} %refs_0_), channel_id=1, source_target_pairs={{0,1},{1,0},{2,3},{3,2},{4,5},{5,4},{6,7},{7,6},{8,9},{9,8},{10,11... | collective-permute-start | bytes 393224 | tf_op jit(solution)/shard_map/ppermute | solution.py:390
  20.6 0.0 collective-permute-done.refs_1_
  20.6 1.2 %collective-permute-start.4 = (bf16[32,2048]{1,0:T(8,128)(2,1)S(1)}, bf16[32,2048]{1,0:T(8,128)(2,1)S(1)}, u32[]{:S(2)}, u32[]{:S(2)}) collective-permute-start(bf16[32,2048]{1,0:T(8,128)(2,1)S(1)} %collective-permute-done.refs_1_), channel_id=1, source_target_pairs={{0,1},{1,0},{2,3},{3,2},{4,5},{5,4},{6,7},{7,6},{8,9},{9,8},{10,11... | collective-permute-start | bytes 393224 | tf_op jit(solution)/shard_map/ppermute | solution.py:390
  21.7 1.5 %collective-permute-done.1.refs_2_ = bf16[32,2048]{1,0:T(8,128)(2,1)S(1)} collective-permute-done((bf16[32,2048]{1,0:T(8,128)(2,1)}, bf16[32,2048]{1,0:T(8,128)(2,1)S(1)}, u32[]{:S(2)}, u32[]{:S(2)}) %collective-permute-start.1) | collective-permute-done | bytes 131104 | tf_op jit(solution)/shard_map/ppermute | solution.py:389
  23.3 1.8 %collective-permute-start.5 = (bf16[32,2048]{1,0:T(8,128)(2,1)S(1)}, bf16[32,2048]{1,0:T(8,128)(2,1)S(1)}, u32[]{:S(2)}, u32[]{:S(2)}) collective-permute-start(bf16[32,2048]{1,0:T(8,128)(2,1)S(1)} %collective-permute-done.1.refs_2_), channel_id=1, source_target_pairs={{0,1},{1,0},{2,3},{3,2},{4,5},{5,4},{6,7},{7,6},{8,9},{9,8},{10,11... | collective-permute-start | bytes 393224 | tf_op jit(solution)/shard_map/ppermute | solution.py:390
  25.1 0.0 collective-permute-done.2.refs_3_
  25.1 0.0 collective-permute-start.6
  25.1 1.3 %collective-permute-start.7 = (bf16[16,2048]{1,0:T(8,128)(2,1)}, bf16[16,2048]{1,0:T(8,128)(2,1)S(1)}, u32[]{:S(2)}, u32[]{:S(2)}) collective-permute-start(bf16[16,2048]{1,0:T(8,128)(2,1)} %refs_8_), channel_id=1, source_target_pairs={{0,8},{8,0},{16,24},{24,16},{1,9},{9,1},{17,25},{25,17},{2,10},{10... | collective-permute-start | bytes 196616 | tf_op jit(solution)/shard_map/ppermute | solution.py:391
  26.4 0.0 all-to-all-done.pieces_ref
  26.4 0.7 shard_map.137
  27.0 4.2 %all-to-all-start.1 = ((f32[8,2,768]{2,1,0:T(2,128)}), f32[8,2,768]{2,1,0:T(2,128)S(1)}, u32[]{:S(2)}, u32[]{:S(2)}) async-start(f32[8,2,768]{2,1,0:T(2,128)} %get-tuple-element.29), calls=%async_computation.1 | async-start | bytes 98304 | tf_op jit(solution)/shard_map/all_to_all | solution.py:386
  31.2 1.2 %shard_map.138 = (f32[256,8]{1,0:T(8,128)S(1)}, f32[4,256]{1,0:T(4,128)S(1)}, bf16[2048,256]{1,0:T(8,128)(2,1)S(1)}) custom-call(bf16[2048,256]{1,0:T(8,128)(2,1)} %wk_hbm.1, f32[1,256]{1,0:T(1,128)S(1)} %get-tuple-element.32.decay_ref), custom_call_target="tpu_custom_call" | custom-call | flops 1000000 | bytes 1049600 | tf_op jit(solution)/shard_map/pallas_call | solution.py:35
  32.5 0.0 collective-permute-done.7.refs_12_
  32.5 0.0 collective-permute-done.3.refs_4_
  32.5 0.0 collective-permute-done.4.refs_5_
  32.5 0.0 collective-permute-done.5.refs_6_
  32.5 0.0 collective-permute-done.6.refs_7_
  32.6 3.5 %all-to-all-done.1.refs_13_ = f32[8,2,768]{2,1,0:T(2,128)S(1)} async-done(((f32[8,2,768]{2,1,0:T(2,128)}), f32[8,2,768]{2,1,0:T(2,128)S(1)}, u32[]{:S(2)}, u32[]{:S(2)}) %all-to-all-start.1) | async-done | bytes 49184 | tf_op jit(solution)/shard_map/all_to_all | solution.py:386
  36.0 3.3 %shard_map.139 = (bf16[256,1280]{1,0:T(8,128)(2,1)S(1)}, bf16[256,2048]{1,0:T(8,128)(2,1)}, bf16[256,256]{1,0:T(8,128)(2,1)S(1)}, bf16[256,512]{1,0:T(8,128)(2,1)S(1)}) custom-call(bf16[32,2048]{1,0:T(8,128)(2,1)} %refs_0_, bf16[32,2048]{1,0:T(8,128)(2,1)S(1)} %collective-permute-done.refs_1_, bf16[32,2048]{1,0:T(8,128)(2,1)S(1)} %collective-permute-done.1.refs_2_, ...), custom_call_target="tpu_custom_call" | custom-call | flops 905969664 | bytes 4460544 | tf_op jit(solution)/shard_map/pallas_call | solution.py:35
  39.3 0.0 copy-start.2
  39.3 0.0 copy-start.1
  39.4 25.6 %all_to_all.20.parts_ref = bf16[32,8,1280]{2,1,0:T(8,128)(2,1)S(1)} all-to-all(bf16[32,8,1280]{2,1,0:T(8,128)(2,1)S(1)} %bitcast.8), channel_id=1, replica_groups=mesh['z'=8,'y'=4,'x'=4,'c'=2] {'y','z'}, dimensions={0} | all-to-all | bytes 1310720 | tf_op jit(solution)/shard_map/all_to_all | solution.py:440
  65.0 0.0 copy-done.2
  65.0 0.9 shard_map.141
  65.9 7.7 %all-to-all-start.3 = ((bf16[32,8,1024]{2,1,0:T(8,128)(2,1)}), bf16[32,8,1024]{2,1,0:T(8,128)(2,1)S(1)}, u32[]{:S(2)}, u32[]{:S(2)}) async-start(bf16[32,8,1024]{2,1,0:T(8,128)(2,1)} %shard_map.141), calls=%async_computation.3 | async-start | bytes 1048576 | tf_op jit(solution)/shard_map/all_to_all | solution.py:479
  73.7 0.0 copy-done.1
  73.7 0.0 copy-start
  73.7 0.0 copy-start.3
  73.7 3.6 %shard_map.140 = (bf16[256,256]{1,0:T(8,128)(2,1)S(1)}, bf16[256,512]{1,0:T(8,128)(2,1)S(1)}, bf16[256,512]{1,0:T(8,128)(2,1)S(1)}) custom-call(bf16[256,2048]{1,0:T(8,128)(2,1)} %get-tuple-element.39.normed_hbm, bf16[2048,256]{1,0:T(8,128)(2,1)} %wq_hbm.1, bf16[2048,512]{1,0:T(8,128)(2,1)} %wg_hbm.1, bf16[256,256]{1,0:T(8,128)(2,1)} %copy-done.2, ...), custom_call_target="tpu_custom_call" | custom-call | flops 805306368 | bytes 4669440 | tf_op jit(solution)/shard_map/pallas_call | solution.py:35
  77.3 10.3 %all-to-all-done.3 = bf16[32,8,1024]{2,1,0:T(8,128)(2,1)S(1)} async-done(((bf16[32,8,1024]{2,1,0:T(8,128)(2,1)}), bf16[32,8,1024]{2,1,0:T(8,128)(2,1)S(1)}, u32[]{:S(2)}, u32[]{:S(2)}) %all-to-all-start.3) | async-done | bytes 524320 | tf_op jit(solution)/shard_map/all_to_all | solution.py:479
  87.7 0.8 shard_map.143
  88.5 0.0 copy-start.4
  88.5 4.3 %collective-permute-start.8 = (bf16[128,2048]{1,0:T(8,128)(2,1)S(1)}, bf16[128,2048]{1,0:T(8,128)(2,1)S(1)}, u32[]{:S(2)}, u32[]{:S(2)}) collective-permute-start(bf16[128,2048]{1,0:T(8,128)(2,1)S(1)} %shard_map.143), channel_id=1, source_target_pairs={{0,1},{1,0},{2,3},{3,2},{4,5},{5,4},{6,7},{7,6},{8,9},{9,8},{10,11... | collective-permute-start | bytes 1572872 | tf_op jit(solution)/shard_map/ppermute | solution.py:498
  92.8 0.8 shard_map.142.own_ref
  93.6 0.7 collective-permute-done.8.crossed_ref
  94.4 0.1 shard_map.144
  94.5 0.4 collective-permute-start.10
  94.9 1.8 %collective-permute-start.11 = (bf16[32,2048]{1,0:T(8,128)(2,1)S(1)}, bf16[32,2048]{1,0:T(8,128)(2,1)S(1)}, u32[]{:S(2)}, u32[]{:S(2)}) collective-permute-start(bf16[32,2048]{1,0:T(8,128)(2,1)S(1)} %get-tuple-element.50), channel_id=1, source_target_pairs={{0,4},{2,6},{4,0},{6,2},{1,5},{3,7},{5,1},{7,3},{8,12},{10,14},{12... | collective-permute-start | bytes 393224 | tf_op jit(solution)/shard_map/ppermute | solution.py:511
  96.6 0.8 collective-permute-start.9
  97.4 3.6 %collective-permute-done.10 = bf16[32,2048]{1,0:T(8,128)(2,1)S(1)} collective-permute-done((bf16[32,2048]{1,0:T(8,128)(2,1)S(1)}, bf16[32,2048]{1,0:T(8,128)(2,1)S(1)}, u32[]{:S(2)}, u32[]{:S(2)}) %collective-permute-start.10) | collective-permute-done | bytes 131104 | tf_op jit(solution)/shard_map/ppermute | solution.py:511
  101.1 1.6 %collective-permute-done.11 = bf16[32,2048]{1,0:T(8,128)(2,1)S(1)} collective-permute-done((bf16[32,2048]{1,0:T(8,128)(2,1)S(1)}, bf16[32,2048]{1,0:T(8,128)(2,1)S(1)}, u32[]{:S(2)}, u32[]{:S(2)}) %collective-permute-start.11) | collective-permute-done | bytes 131104 | tf_op jit(solution)/shard_map/ppermute | solution.py:511
  102.7 0.9 collective-permute-done.9
  103.7 0.8 add_convert_fusion
  (5 shorter events, 0.0 us)
Async XLA Ops:
  1.8 24.5 %all-to-all-start = ((bf16[32,16,128]{2,1,0:T(8,128)(2,1)}), bf16[32,16,128]{2,1,0:T(8,128)(2,1)S(1)}, u32[]{:S(2)}, u32[]{:S(2)}) async-start(bf16[32,16,128]{2,1,0:T(8,128)(2,1)} %get-tuple-element.28), calls=%async_computation | async-start | bytes 262144 | tf_op jit(solution)/shard_map/all_to_all | solution.py:376
  13.9 6.7 %collective-permute-start = (bf16[32,2048]{1,0:T(8,128)(2,1)}, bf16[32,2048]{1,0:T(8,128)(2,1)S(1)}, u32[]{:S(2)}, u32[]{:S(2)}) collective-permute-start(bf16[32,2048]{1,0:T(8,128)(2,1)} %refs_0_), channel_id=1, source_target_pairs={{0,2},{2,4},{4,6},{6,0},{1,3},{3,5},{5,7},{7,1},{8,10},{10,12},{12... | collective-permute-start | bytes 393224 | tf_op jit(solution)/shard_map/ppermute | solution.py:389
  15.2 8.1 %collective-permute-start.1 = (bf16[32,2048]{1,0:T(8,128)(2,1)}, bf16[32,2048]{1,0:T(8,128)(2,1)S(1)}, u32[]{:S(2)}, u32[]{:S(2)}) collective-permute-start(bf16[32,2048]{1,0:T(8,128)(2,1)} %refs_0_), channel_id=1, source_target_pairs={{0,4},{2,6},{4,0},{6,2},{1,5},{3,7},{5,1},{7,3},{8,12},{10,14},{12... | collective-permute-start | bytes 393224 | tf_op jit(solution)/shard_map/ppermute | solution.py:389
  17.6 7.5 %collective-permute-start.2 = (bf16[32,2048]{1,0:T(8,128)(2,1)}, bf16[32,2048]{1,0:T(8,128)(2,1)S(1)}, u32[]{:S(2)}, u32[]{:S(2)}) collective-permute-start(bf16[32,2048]{1,0:T(8,128)(2,1)} %refs_0_), channel_id=1, source_target_pairs={{0,6},{2,0},{4,2},{6,4},{1,7},{3,1},{5,3},{7,5},{8,14},{10,8},{12,... | collective-permute-start | bytes 393224 | tf_op jit(solution)/shard_map/ppermute | solution.py:389
  18.8 13.8 %collective-permute-start.3 = (bf16[32,2048]{1,0:T(8,128)(2,1)}, bf16[32,2048]{1,0:T(8,128)(2,1)S(1)}, u32[]{:S(2)}, u32[]{:S(2)}) collective-permute-start(bf16[32,2048]{1,0:T(8,128)(2,1)} %refs_0_), channel_id=1, source_target_pairs={{0,1},{1,0},{2,3},{3,2},{4,5},{5,4},{6,7},{7,6},{8,9},{9,8},{10,11... | collective-permute-start | bytes 393224 | tf_op jit(solution)/shard_map/ppermute | solution.py:390
  20.6 12.0 %collective-permute-start.4 = (bf16[32,2048]{1,0:T(8,128)(2,1)S(1)}, bf16[32,2048]{1,0:T(8,128)(2,1)S(1)}, u32[]{:S(2)}, u32[]{:S(2)}) collective-permute-start(bf16[32,2048]{1,0:T(8,128)(2,1)S(1)} %collective-permute-done.refs_1_), channel_id=1, source_target_pairs={{0,1},{1,0},{2,3},{3,2},{4,5},{5,4},{6,7},{7,6},{8,9},{9,8},{10,11... | collective-permute-start | bytes 393224 | tf_op jit(solution)/shard_map/ppermute | solution.py:390
  23.3 9.3 %collective-permute-start.5 = (bf16[32,2048]{1,0:T(8,128)(2,1)S(1)}, bf16[32,2048]{1,0:T(8,128)(2,1)S(1)}, u32[]{:S(2)}, u32[]{:S(2)}) collective-permute-start(bf16[32,2048]{1,0:T(8,128)(2,1)S(1)} %collective-permute-done.1.refs_2_), channel_id=1, source_target_pairs={{0,1},{1,0},{2,3},{3,2},{4,5},{5,4},{6,7},{7,6},{8,9},{9,8},{10,11... | collective-permute-start | bytes 393224 | tf_op jit(solution)/shard_map/ppermute | solution.py:390
  25.1 7.5 %collective-permute-start.6 = (bf16[32,2048]{1,0:T(8,128)(2,1)S(1)}, bf16[32,2048]{1,0:T(8,128)(2,1)S(1)}, u32[]{:S(2)}, u32[]{:S(2)}) collective-permute-start(bf16[32,2048]{1,0:T(8,128)(2,1)S(1)} %collective-permute-done.2.refs_3_), channel_id=1, source_target_pairs={{0,1},{1,0},{2,3},{3,2},{4,5},{5,4},{6,7},{7,6},{8,9},{9,8},{10,11... | collective-permute-start | bytes 393224 | tf_op jit(solution)/shard_map/ppermute | solution.py:390
  25.1 7.4 %collective-permute-start.7 = (bf16[16,2048]{1,0:T(8,128)(2,1)}, bf16[16,2048]{1,0:T(8,128)(2,1)S(1)}, u32[]{:S(2)}, u32[]{:S(2)}) collective-permute-start(bf16[16,2048]{1,0:T(8,128)(2,1)} %refs_8_), channel_id=1, source_target_pairs={{0,8},{8,0},{16,24},{24,16},{1,9},{9,1},{17,25},{25,17},{2,10},{10... | collective-permute-start | bytes 196616 | tf_op jit(solution)/shard_map/ppermute | solution.py:391
  27.0 9.0 %all-to-all-start.1 = ((f32[8,2,768]{2,1,0:T(2,128)}), f32[8,2,768]{2,1,0:T(2,128)S(1)}, u32[]{:S(2)}, u32[]{:S(2)}) async-start(f32[8,2,768]{2,1,0:T(2,128)} %get-tuple-element.29), calls=%async_computation.1 | async-start | bytes 98304 | tf_op jit(solution)/shard_map/all_to_all | solution.py:386
  39.3 25.7 %copy-start.2 = (bf16[256,256]{1,0:T(8,128)(2,1)}, bf16[256,256]{1,0:T(8,128)(2,1)S(1)}, u32[]{:S(2)}) copy-start(bf16[256,256]{1,0:T(8,128)(2,1)S(1)} %get-tuple-element.40.k_hbm) | copy-start | bytes 393220
  39.3 34.3 %copy-start.1 = (bf16[256,512]{1,0:T(8,128)(2,1)}, bf16[256,512]{1,0:T(8,128)(2,1)S(1)}, u32[]{:S(2)}) copy-start(bf16[256,512]{1,0:T(8,128)(2,1)S(1)} %get-tuple-element.41.v_hbm) | copy-start | bytes 786436
  65.9 21.7 %all-to-all-start.3 = ((bf16[32,8,1024]{2,1,0:T(8,128)(2,1)}), bf16[32,8,1024]{2,1,0:T(8,128)(2,1)S(1)}, u32[]{:S(2)}, u32[]{:S(2)}) async-start(bf16[32,8,1024]{2,1,0:T(8,128)(2,1)} %shard_map.141), calls=%async_computation.3 | async-start | bytes 1048576 | tf_op jit(solution)/shard_map/all_to_all | solution.py:479
  73.7 14.0 %copy-start = (bf16[512,2048]{1,0:T(8,128)(2,1)S(1)}, bf16[512,2048]{1,0:T(8,128)(2,1)}, u32[]{:S(2)}) copy-start(bf16[512,2048]{1,0:T(8,128)(2,1)} %wo_ref.3) | copy-start | bytes 6291460
  73.7 14.0 %copy-start.3 = (bf16[512]{0:T(512)(128)(2,1)S(1)}, bf16[512]{0:T(512)(128)(2,1)}, u32[]{:S(2)}) copy-start(bf16[512]{0:T(512)(128)(2,1)} %param.24) | copy-start | bytes 3076
  88.5 15.2 %copy-start.4 = (bf16[32,2048]{1,0:T(8,128)(2,1)S(1)}, bf16[32,2048]{1,0:T(8,128)(2,1)}, u32[]{:S(2)}) copy-start(bf16[32,2048]{1,0:T(8,128)(2,1)} %refs_0_) | copy-start | bytes 393220
  88.5 5.9 %collective-permute-start.8 = (bf16[128,2048]{1,0:T(8,128)(2,1)S(1)}, bf16[128,2048]{1,0:T(8,128)(2,1)S(1)}, u32[]{:S(2)}, u32[]{:S(2)}) collective-permute-start(bf16[128,2048]{1,0:T(8,128)(2,1)S(1)} %shard_map.143), channel_id=1, source_target_pairs={{0,1},{1,0},{2,3},{3,2},{4,5},{5,4},{6,7},{7,6},{8,9},{9,8},{10,11... | collective-permute-start | bytes 1572872 | tf_op jit(solution)/shard_map/ppermute | solution.py:498
  94.5 6.6 %collective-permute-start.10 = (bf16[32,2048]{1,0:T(8,128)(2,1)S(1)}, bf16[32,2048]{1,0:T(8,128)(2,1)S(1)}, u32[]{:S(2)}, u32[]{:S(2)}) collective-permute-start(bf16[32,2048]{1,0:T(8,128)(2,1)S(1)} %get-tuple-element.49), channel_id=1, source_target_pairs={{0,2},{2,4},{4,6},{6,0},{1,3},{3,5},{5,7},{7,1},{8,10},{10,12},{12... | collective-permute-start | bytes 393224 | tf_op jit(solution)/shard_map/ppermute | solution.py:511
  94.9 7.9 %collective-permute-start.11 = (bf16[32,2048]{1,0:T(8,128)(2,1)S(1)}, bf16[32,2048]{1,0:T(8,128)(2,1)S(1)}, u32[]{:S(2)}, u32[]{:S(2)}) collective-permute-start(bf16[32,2048]{1,0:T(8,128)(2,1)S(1)} %get-tuple-element.50), channel_id=1, source_target_pairs={{0,4},{2,6},{4,0},{6,2},{1,5},{3,7},{5,1},{7,3},{8,12},{10,14},{12... | collective-permute-start | bytes 393224 | tf_op jit(solution)/shard_map/ppermute | solution.py:511
  96.6 7.0 %collective-permute-start.9 = (bf16[32,2048]{1,0:T(8,128)(2,1)S(1)}, bf16[32,2048]{1,0:T(8,128)(2,1)S(1)}, u32[]{:S(2)}, u32[]{:S(2)}) collective-permute-start(bf16[32,2048]{1,0:T(8,128)(2,1)S(1)} %get-tuple-element.48), channel_id=1, source_target_pairs={{0,6},{2,0},{4,2},{6,4},{1,7},{3,1},{5,3},{7,5},{8,14},{10,8},{12,... | collective-permute-start | bytes 393224 | tf_op jit(solution)/shard_map/ppermute | solution.py:511
